TPU v7x, 512 devices: a 8x2x16 block of a 8x8x16 slice. The times are simulated.
512 devices in a mesh: grp: 2 (over y), fs: 32 (over z, core), tp: 8 (over x).
Axes of the slice: x: 8, y: 2, z: 16, core: 2. Of those that a mesh axis runs over, the one named last changes fastest.
The devices are a block of a 8x8x16 slice.
Arguments:
- tokens: bfloat16 [24576, 2048], P(('grp', 'fs'), 'tp'), parts along dimension 0, may hold values from -6 to 6
- norm_gain: float32 [2048], P('fs'), may hold values from 0.1 to 1.9
- gate_weight: float32 [32, 2048, 1024], P(None, 'fs', 'tp'), may hold values from -0.125 to 0.125
- up_weight: float32 [32, 2048, 1024], P(None, 'fs', 'tp'), may hold values from -0.125 to 0.125
- down_weight: float32 [32, 1024, 2048], P(None, 'fs', 'tp'), may hold values from -0.1875 to 0.1875
- routes: int32 [24576, 2], P(('grp', 'fs')), parts along dimension 0, may hold values from 0 to 31, as said below
- route_weights: float32 [24576, 2], P(('grp', 'fs')), parts along dimension 0, may hold values from 0.2 to 1
Outputs:
- gate_serve: bfloat16 [64, 2048, 1024], P(('grp', 'fs'), None, 'tp'), parts along dimension 0
- up_serve: bfloat16 [64, 2048, 1024], P(('grp', 'fs'), None, 'tp'), parts along dimension 0
- down_serve: bfloat16 [64, 1024, 2048], P(('grp', 'fs'), None, 'tp'), parts along dimension 0
- mixture: bfloat16 [24576, 2048], P(('grp', 'fs'), 'tp'), parts along dimension 0
There are 2 independent parts, one for each index of `grp`. A program takes and returns all parts, laid end to end along the dimension named above; an argument that names none is the same for every part. Nothing has to cross between parts.
Inputs may be any that keep to these rules, and one draw needn't show every extreme that they name: `routes`: each row names two different experts of one group (expert e lies in group e // 8). In each aligned block of 384 rows no expert is named more than 36 times, and every expert of one group is named exactly 36 times.
All inputs are finite; a program needn't handle non-finite values.
Results may differ from a plain program's by a relative error of at most 0.0087.
Values may be sent and summed in bfloat16 or wider, within the bound.
No kernel may reach another device: no remote copies, remote signals or barrier semaphores. Data moves between devices by JAX's collectives and lax.ppermute only.
A program may use at most 64 MiB of HBM per device.

v0:
```python
import jax
import jax.numpy as jnp
from jax import lax
from jax.sharding import Mesh
from jax.sharding import PartitionSpec as P

CAP = 36
FS = ("fs_0", "fs_1")
GRP_FS = ("grp", "fs_0", "fs_1")


epsilon = 1e-06


def in_blocks(x, dim, length):
    before, after = (x.shape[:dim], x.shape[dim + 1 :])
    return jnp.moveaxis(x.reshape(*before, length, -1, *after), dim, 0)


def laid_out(blocks, dim):
    blocks = jnp.moveaxis(blocks, 0, dim)
    shape = blocks.shape
    return blocks.reshape(*shape[:dim], shape[dim] * shape[dim + 1], *shape[dim + 2 :])


def exchange_in_order(blocks, axes, order):
    shape = [lax.axis_size(a) for a in axes]
    blocks = blocks.reshape(*shape, *blocks.shape[1:])
    for k in order:
        blocks = lax.all_to_all(blocks, axes[k], split_axis=k, concat_axis=k, tiled=True)
    return blocks.reshape(-1, *blocks.shape[len(axes) :])


def exchange_by_chip(x, groups, order, split_dim, concat_dim):
    length = lax.axis_size(groups[0]) * lax.axis_size(groups[1])
    blocks = in_blocks(x, split_dim, length)
    return laid_out(exchange_in_order(blocks, groups, order), concat_dim)


def normalize(rows):
    values = rows.astype(jnp.float32)
    scale = lax.rsqrt(jnp.mean(values * values, axis=-1, keepdims=True) + epsilon)
    return (values * scale).astype(jnp.bfloat16)


def shards(tokens, norm_gain, gate_weight, up_weight, down_weight, routes, route_weights):
    experts = gate_weight.shape[0]
    n_shards = lax.axis_size(FS)
    local_experts = experts // n_shards
    tok_rows = tokens.shape[0]
    gate_low = (norm_gain[None, :, None] * gate_weight).astype(jnp.bfloat16)
    up_low = (norm_gain[None, :, None] * up_weight).astype(jnp.bfloat16)
    down_low = down_weight.astype(jnp.bfloat16)
    gate_serve, up_serve = (
        lax.all_to_all(gate_low, FS, split_axis=0, concat_axis=1, tiled=True),
        lax.all_to_all(up_low, FS, split_axis=0, concat_axis=1, tiled=True),
    )
    flat_routes = routes.reshape(-1)
    expert_ids = lax.iota(jnp.int32, experts)
    onehot = (flat_routes[:, None] == expert_ids[None, :]).astype(jnp.int32)
    position = jnp.sum((jnp.cumsum(onehot, axis=0) - 1) * onehot, axis=1)
    slot_index = (flat_routes * CAP + position).reshape(tok_rows, 2)
    slot_ids = lax.iota(jnp.int32, experts * CAP)
    select = jnp.any(slot_ids[:, None, None] == slot_index[None, :, :], axis=2).astype(jnp.bfloat16)
    outbound = jnp.dot(select, tokens, preferred_element_type=jnp.float32).astype(jnp.bfloat16)
    outbound = outbound.reshape(n_shards, local_experts, CAP, outbound.shape[1])
    arrived = lax.all_to_all(outbound, FS, split_axis=0, concat_axis=2, tiled=True)[0]
    expert_rows = normalize(lax.all_gather(arrived, "tp", axis=2, tiled=True))
    gate_part = jnp.einsum(
        "erd,edh->erh", expert_rows, gate_serve, preferred_element_type=jnp.float32
    )
    up_part = jnp.einsum("erd,edh->erh", expert_rows, up_serve, preferred_element_type=jnp.float32)
    hidden = (jax.nn.silu(gate_part) * up_part).astype(jnp.bfloat16)
    down_serve = lax.all_to_all(down_low, FS, split_axis=0, concat_axis=1, tiled=True)
    expert_out = jnp.einsum(
        "erk,ekd->erd",
        lax.all_gather(hidden, "tp", axis=2, tiled=True),
        down_serve,
        preferred_element_type=jnp.float32,
    ).astype(jnp.bfloat16)
    expert_out = expert_out.reshape(1, local_experts, hidden.shape[1], expert_out.shape[2])
    returned_rows = exchange_by_chip(expert_out, ("fs_0", "fs_1"), (1, 0), 2, 0)
    returned_rows = returned_rows.reshape(experts * CAP, returned_rows.shape[3])
    picked = returned_rows[slot_index]
    mixture = jnp.sum(route_weights[:, :, None] * picked.astype(jnp.float32), axis=1).astype(
        jnp.bfloat16
    )
    return (gate_serve, up_serve, down_serve, mixture)


def solution(mesh):
    split = Mesh(
        mesh.devices.reshape(mesh.shape["grp"], 16, 2, mesh.shape["tp"]),
        ("grp", "fs_0", "fs_1", "tp"),
    )
    placed = (
        P(GRP_FS, "tp"),
        P(FS),
        P(None, FS, "tp"),
        P(None, FS, "tp"),
        P(None, FS, "tp"),
        P(GRP_FS, None),
        P(GRP_FS, None),
    )
    return jax.shard_map(
        shards,
        mesh=split,
        in_specs=placed,
        out_specs=(
            P(GRP_FS, None, "tp"),
            P(GRP_FS, None, "tp"),
            P(GRP_FS, None, "tp"),
            P(GRP_FS, "tp"),
        ),
        check_vma=False,
    )
```

profile of v0, /device:TPU:66, one launch (start us, length us, event | category | flops | bytes accessed | tf_op | source)
XLA Modules:
  0.0 293.5 jit_solution(14518242084303444602)
XLA Ops:
  7.2 0.1 all-gather.4.cloned.1.call-start
  7.3 0.9 copy.41
  8.2 0.1 eq.43
  8.3 0.1 eq.39
  8.5 1.7 reduce-window.6
  10.3 0.3 slice_reduce_fusion
  10.5 0.1 fusion.9
  10.7 0.2 reduce_sum.30
  10.8 0.1 copy.44
  10.9 0.7 compare_select_fusion
  11.6 0.8 fusion.3
  12.4 0.5 convolution_convert_fusion.1
  12.9 0.1 reshape.99
  13.0 82.9 %all_to_all.55 = bf16[32,1,36,256]{3,2,1,0:T(8,128)(2,1)S(1)} all-to-all(bf16[32,1,36,256]{3,2,1,0:T(8,128)(2,1)S(1)} %bitcast.35), channel_id=1, replica_groups=mesh['grp'=2,'fs_0'=16,'fs_1'=2,'tp'=8] {'fs_0','fs_1'}, dimensions={0} | all-to-all | bytes 1179648 | tf_op jit(solution)/shard_map/all_to_all | solution.py:67
  95.9 0.9 squeeze.3
  96.9 0.1 all-gather.4.cloned.1.call-update
  96.9 2.3 multiply_convert_fusion
  99.2 37.1 %all_to_all.56 = bf16[32,64,128]{2,1,0:T(8,128)(2,1)S(1)} all-to-all(bf16[32,64,128]{2,1,0:T(8,128)(2,1)S(1)} %get-tuple-element.7), channel_id=1, replica_groups=mesh['grp'=2,'fs_0'=16,'fs_1'=2,'tp'=8] {'fs_0','fs_1'}, dimensions={0} | all-to-all | bytes 1048576 | tf_op jit(solution)/shard_map/all_to_all | solution.py:55
  136.3 4.8 %all-to-all-start.1 = ((bf16[32,64,128]{2,1,0:T(8,128)(2,1)}), bf16[32,64,128]{2,1,0:T(8,128)(2,1)S(1)}, u32[]{:S(2)}, u32[]{:S(2)}) async-start(bf16[32,64,128]{2,1,0:T(8,128)(2,1)} %get-tuple-element.6), calls=%async_computation.1 | async-start | bytes 1048576 | tf_op jit(solution)/shard_map/all_to_all | solution.py:56
  141.1 0.1 all-gather.6.cloned.1.call-start
  141.2 22.0 %all-gather.4.cloned.1.call-done = bf16[1,1152,2048]{2,1,0:T(8,128)(2,1)} async-done(((bf16[1,1152,256]{2,1,0:T(8,128)(2,1)}), bf16[1,1152,2048]{2,1,0:T(8,128)(2,1)}) %all-gather.4.cloned.1.call-update) | async-done | bytes 4718608 | tf_op jit(solution)/shard_map/all_gather | solution.py:68
  163.2 3.5 %fusion = f32[1152]{0:T(1024)S(1)} fusion(bf16[1,1152,2048]{2,1,0:T(8,128)(2,1)} %all-gather.4.cloned.1.call-done), kind=kLoop, calls=%fused_computation.3 | loop fusion | flops 7076736 | bytes 4723200 | tf_op jit(solution)/shard_map/reduce_sum | solution.py:42
  166.7 0.3 copy-done.1
  167.0 1.5 fusion.6
  168.5 5.8 %all-to-all-done.1 = bf16[32,64,128]{2,1,0:T(8,128)(2,1)S(1)} async-done(((bf16[32,64,128]{2,1,0:T(8,128)(2,1)}), bf16[32,64,128]{2,1,0:T(8,128)(2,1)S(1)}, u32[]{:S(2)}, u32[]{:S(2)}) %all-to-all-start.1) | async-done | bytes 524320 | tf_op jit(solution)/shard_map/all_to_all | solution.py:56
  174.3 4.6 %fusion.4 = bf16[1152,128]{1,0:T(8,128)(2,1)} fusion(bf16[2048,128]{1,0:T(8,128)(2,1)S(1)} %bitcast.38, bf16[1,1152,2048]{2,1,0:T(8,128)(2,1)} %all-gather.4.cloned.1.call-done, f32[1152]{0:T(1024)S(1)} %add_rsqrt_fusion, f32[1152,128]{1,0:T(8,128)S(1)} %fusion.6), kind=kOutput, calls=%fused_computation.11 | convolution fusion | flops 611942400 | bytes 6132224 | tf_op jit(solution)/shard_map/erd,edh->erh/dot_general | solution.py:72
  178.9 0.1 all-gather.6.cloned.1.call-update
  179.0 0.1 convert_element_type.42
  179.0 38.7 %all_to_all.57 = bf16[32,32,256]{2,1,0:T(8,128)(2,1)S(1)} all-to-all(bf16[32,32,256]{2,1,0:T(8,128)(2,1)S(1)} %convert_element_type.42), channel_id=1, replica_groups=mesh['grp'=2,'fs_0'=16,'fs_1'=2,'tp'=8] {'fs_0','fs_1'}, dimensions={0} | all-to-all | bytes 1048576 | tf_op jit(solution)/shard_map/all_to_all | solution.py:74
  217.8 9.2 %all-gather.6.cloned.1.call-done = bf16[1152,1024]{1,0:T(8,128)(2,1)} async-done(((bf16[1152,128]{1,0:T(8,128)(2,1)}), bf16[1152,1024]{1,0:T(8,128)(2,1)}) %all-gather.6.cloned.1.call-update) | async-done | bytes 2359312 | tf_op jit(solution)/shard_map/all_gather | solution.py:77
  226.9 2.4 convolution_convert_fusion
  229.4 0.1 reshape_transpose_reshape_reshape.3
  229.5 0.2 copy.46
  229.7 4.2 %all_to_all.58 = bf16[16,2,1,1,36,256]{5,0,4,3,2,1:T(8,128)(2,1)S(1)} all-to-all(bf16[16,2,1,1,36,256]{5,0,4,3,2,1:T(8,128)(2,1)S(1)} %copy.46), channel_id=1, replica_groups=mesh['grp'=2,'fs_0'=16,'fs_1'=2,'tp'=8] {'fs_1'}, dimensions={1} | all-to-all | bytes 1179648 | tf_op jit(solution)/shard_map/all_to_all | solution.py:30
  233.9 1.4 copy.47
  235.3 13.1 %all-to-all-start.5 = ((bf16[16,2,1,1,36,256]{5,1,4,3,2,0:T(2,128)(2,1)}), bf16[16,2,1,1,36,256]{5,1,4,3,2,0:T(2,128)(2,1)S(1)}, u32[]{:S(2)}, u32[]{:S(2)}) async-start(bf16[16,2,1,1,36,256]{5,1,4,3,2,0:T(2,128)(2,1)} %copy.47), calls=%async_computation.5 | async-start | bytes 1179648 | tf_op jit(solution)/shard_map/all_to_all | solution.py:30
  248.4 0.1 copy.49
  248.6 0.1 reshape.107
  248.7 0.1 copy.40
  248.9 30.4 %all-to-all-done.5 = bf16[16,2,1,1,36,256]{5,1,4,3,2,0:T(2,128)(2,1)S(1)} async-done(((bf16[16,2,1,1,36,256]{5,1,4,3,2,0:T(2,128)(2,1)}), bf16[16,2,1,1,36,256]{5,1,4,3,2,0:T(2,128)(2,1)S(1)}, u32[]{:S(2)}, u32[]{:S(2)}) %all-to-all-start.5) | async-done | bytes 589856 | tf_op jit(solution)/shard_map/all_to_all | solution.py:30
  279.3 0.1 copy.48
  279.3 0.1 reshape_reshape_reshape.3
  279.5 2.7 gather_fusion
  282.1 0.4 reshape.117
  282.5 1.7 multiply_reduce_fusion
  284.2 0.8 copy.55
  285.0 0.8 copy.56
  285.8 0.8 copy.57
  (15 shorter events, 0.1 us)
Async XLA Ops:
  7.2 5.2 %copy-start = (bf16[384,256]{1,0:T(8,128)(2,1)S(1)}, bf16[384,256]{1,0:T(8,128)(2,1)}, u32[]{:S(2)}) copy-start(bf16[384,256]{1,0:T(8,128)(2,1)} %param.7) | copy-start | bytes 589828
  7.2 89.7 %copy-start.3 = (f32[32,64,128]{2,1,0:T(8,128)S(1)}, f32[32,64,128]{2,1,0:T(8,128)}, u32[]{:S(2)}) copy-start(f32[32,64,128]{2,1,0:T(8,128)} %param.10) | copy-start | bytes 3145732
  7.2 89.7 %copy-start.5 = (f32[64]{0:T(128)S(1)}, f32[64]{0:T(128)}, u32[]{:S(2)}) copy-start(f32[64]{0:T(128)} %param.8) | copy-start | bytes 772
  7.2 156.0 %all-gather.4.cloned.1.call-start = ((), (), s32[]{:S(2)}) async-start(), calls=%async_computation.6 | async-start | bytes 5308416 | tf_op jit(solution)/shard_map/all_gather | solution.py:68
  136.3 38.0 %all-to-all-start.1 = ((bf16[32,64,128]{2,1,0:T(8,128)(2,1)}), bf16[32,64,128]{2,1,0:T(8,128)(2,1)S(1)}, u32[]{:S(2)}, u32[]{:S(2)}) async-start(bf16[32,64,128]{2,1,0:T(8,128)(2,1)} %get-tuple-element.6), calls=%async_computation.1 | async-start | bytes 1048576 | tf_op jit(solution)/shard_map/all_to_all | solution.py:56
  141.1 85.8 %all-gather.6.cloned.1.call-start = ((), (), s32[]{:S(2)}) async-start(), calls=%async_computation.7 | async-start | bytes 2654208 | tf_op jit(solution)/shard_map/all_gather | solution.py:77
  163.2 3.8 %copy-start.1 = (bf16[1,1152,2048]{2,1,0:T(8,128)(2,1)S(1)}, bf16[1,1152,2048]{2,1,0:T(8,128)(2,1)}, u32[]{:S(2)}) copy-start(bf16[1,1152,2048]{2,1,0:T(8,128)(2,1)} %all-gather.4.cloned.1.call-done) | copy-start | bytes 14155780
  174.3 4.7 %copy-start.2 = (f32[32,32,256]{2,1,0:T(8,128)S(1)}, f32[32,32,256]{2,1,0:T(8,128)}, u32[]{:S(2)}) copy-start(f32[32,32,256]{2,1,0:T(8,128)} %param.11) | copy-start | bytes 3145732
  229.4 19.4 %copy-start.4 = (f32[384,2]{0,1:T(2,128)S(1)}, f32[384,2]{0,1:T(2,128)}, u32[]{:S(2)}) copy-start(f32[384,2]{0,1:T(2,128)} %param.13) | copy-start | bytes 9220
  235.3 43.9 %all-to-all-start.5 = ((bf16[16,2,1,1,36,256]{5,1,4,3,2,0:T(2,128)(2,1)}), bf16[16,2,1,1,36,256]{5,1,4,3,2,0:T(2,128)(2,1)S(1)}, u32[]{:S(2)}, u32[]{:S(2)}) async-start(bf16[16,2,1,1,36,256]{5,1,4,3,2,0:T(2,128)(2,1)} %copy.47), calls=%async_computation.5 | async-start | bytes 1179648 | tf_op jit(solution)/shard_map/all_to_all | solution.py:30
Sparse Core Ops, SparseCore 0:
  97.0 66.1 all-gather.3
  179.1 47.8 all-gather.5
where the time goes:
time: 294 us; the launch traced here: 293 us
  blocking collectives  163 us (55%)
  waiting for transfers between devices  67.5 us (23%)
  starting transfers between devices  18 us (6%)
  between operations  14.3 us (5%)
  other arithmetic  10.9 us (4%)
  local copies, waits for them, and re-layouts  10.8 us (4%)
  matrix products  8.96 us (3%)
    all_to_all x1, blocking collectives, shards(): lax.all_to_all(outbound, FS, split_axis=0, concat_axis=2, tiled=True)[0]  82.9 us
    all_to_all x1, blocking collectives, shards(): lax.all_to_all(down_low, FS, split_axis=0, concat_axis=1, tiled=True)  38.7 us
    all_to_all x1, blocking collectives, shards(): lax.all_to_all(gate_low, FS, split_axis=0, concat_axis=1, tiled=True)  37.1 us
    all_to_all x1, waiting for transfers between devices, exchange_in_order(): lax.all_to_all(blocks, axes[k], split_axis=k, concat_axis=k, tiled=True)  30.4 us
    all_gather x1, waiting for transfers between devices, shards(): expert_rows = normalize(lax.all_gather(arrived, 'tp', axis=2, tiled=True))  22 us
    all_to_all x1, starting transfers between devices, exchange_in_order(): lax.all_to_all(blocks, axes[k], split_axis=k, concat_axis=k, tiled=True)  13.1 us
    all_gather x1, waiting for transfers between devices, shards(): lax.all_gather(hidden, 'tp', axis=2, tiled=True)  9.16 us
  transfers between devices with their start and end apart: 4, of which 4 were waited for; matrix products, arithmetic and copies ran while one was open for 3% of the time, Pallas kernels for 0%

commit v1 on v0

v1 whole, which is shorter than its diff:
```python
import jax
import jax.numpy as jnp
from jax import lax
from jax.experimental import pallas as pl
from jax.experimental.pallas import tpu as pltpu
from jax.sharding import PartitionSpec as P


CAP = 36
MAIN = 32
SLAB = 72
HALF = 128
BF16 = jnp.bfloat16
F32 = jnp.float32
epsilon = 1e-06


def route_kernel(routes, tokens, outbound, rows):
    experts = outbound.shape[0] // SLAB
    n_tok = tokens.shape[0]
    first, second = routes[0:1, :], routes[1:2, :]
    ids = lax.broadcasted_iota(jnp.int32, (experts, n_tok), 0)
    hit0 = (ids == first).astype(F32)
    hit1 = (ids == second).astype(F32)
    before = (
        lax.broadcasted_iota(jnp.int32, (n_tok, n_tok), 0)
        < lax.broadcasted_iota(jnp.int32, (n_tok, n_tok), 1)
    ).astype(F32).astype(BF16)
    count0 = jnp.dot(hit0.astype(BF16), before, preferred_element_type=F32)
    count1 = jnp.dot(hit1.astype(BF16), before, preferred_element_type=F32)
    count1 = count1 + jnp.sum(hit0, axis=1, keepdims=True)
    slot0 = jnp.sum(hit0 * count0, axis=0, keepdims=True).astype(jnp.int32)
    slot1 = jnp.sum(hit1 * count1, axis=0, keepdims=True).astype(jnp.int32)
    low0 = first * SLAB + jnp.where(slot0 < MAIN, slot0, slot0 + MAIN)
    low1 = second * SLAB + jnp.where(slot1 < MAIN, slot1, slot1 + MAIN)
    high0 = low0 + jnp.where(slot0 < MAIN, MAIN, CAP - MAIN)
    high1 = low1 + jnp.where(slot1 < MAIN, MAIN, CAP - MAIN)
    rows[...] = jnp.concatenate([low0, low1, high0, high1, low0, low1, high0, high1], axis=0)
    part = 8 * SLAB
    left, right = tokens[:, :HALF], tokens[:, HALF:]
    for g in range(experts // 8):
        ids = lax.broadcasted_iota(jnp.int32, (part, n_tok), 0) + g * part
        low = jnp.logical_or(ids == low0, ids == low1).astype(F32).astype(BF16)
        high = jnp.logical_or(ids == high0, ids == high1).astype(F32).astype(BF16)
        out = jnp.dot(low, left, preferred_element_type=F32)
        out = out + jnp.dot(high, right, preferred_element_type=F32)
        outbound[g * part : (g + 1) * part, :] = out.astype(BF16)


def tile_row(shape):
    return lax.broadcasted_iota(jnp.int32, shape, len(shape) - 2)


def ffn_kernel(me, *refs):
    half_a, half_b, weights = refs[0:9], refs[9:18], refs[18]
    hidden, gate_out, up_out = refs[19:22]
    i = pl.program_id(0)
    n_tp = 8
    offsets = (0, -1, 1, -2, 2, -3, 3, 4)
    pairs = 8 * MAIN
    acc = jnp.zeros((pairs, 2 * HALF), F32)
    rest0 = jnp.zeros((64, 2 * HALF), F32)
    rest1 = jnp.zeros((64, 2 * HALF), F32)
    square = jnp.zeros((pairs, HALF), F32)
    square_rest = jnp.zeros((64, HALF), F32)
    for n, offset in enumerate(offsets):
        if n < 7:
            x = jnp.where(i < 2, half_a[n][...], half_b[n][...])
        else:
            x = jnp.where(
                i < 2,
                jnp.where(i == 0, half_a[7][...], half_a[8][...]),
                jnp.where(i == 2, half_b[7][...], half_b[8][...]),
            )
        x = x.reshape(8, SLAB, HALF)
        left = x[:, :MAIN].reshape(pairs, HALF)
        right = x[:, MAIN : 2 * MAIN].reshape(pairs, HALF)
        rest = x[:, 2 * MAIN :].reshape(64, HALF)
        source = (me[0] + offset + n_tp) % n_tp
        w = weights[pl.ds(pl.multiple_of(source * 256, 256), 256), :]
        both = jnp.concatenate([left, right], axis=1)
        acc = acc + jnp.dot(both, w, preferred_element_type=F32)
        rest0 = rest0 + jnp.dot(rest, w[:HALF], preferred_element_type=F32)
        rest1 = rest1 + jnp.dot(rest, w[HALF:], preferred_element_type=F32)
        l32, r32, s32 = left.astype(F32), right.astype(F32), rest.astype(F32)
        square = square + (l32 * l32 + r32 * r32)
        square_rest = square_rest + s32 * s32
    features = weights.shape[0]

    def activate(part, total):
        scale = lax.rsqrt(total * (1.0 / features) + epsilon)
        gate = part[:, :HALF] * scale
        up = part[:, HALF:] * scale
        return gate / (1.0 + jnp.exp(-gate)) * up

    main = activate(acc, jnp.sum(square, axis=1, keepdims=True))
    low = tile_row((8, 8, 2 * HALF)) < CAP - MAIN
    part = jnp.where(low, rest0.reshape(8, 8, 2 * HALF), rest1.reshape(8, 8, 2 * HALF))
    part = (part + pltpu.roll(part, 4, 1)).reshape(64, 2 * HALF)
    total = jnp.broadcast_to(jnp.sum(square_rest, axis=1, keepdims=True), (64, HALF)).reshape(8, 8, HALF)
    total = (total + pltpu.roll(total, 4, 1)).reshape(64, HALF)
    extra = activate(part, total).reshape(4, 2, 8, HALF)
    extra = jnp.where(tile_row((4, 8, HALF)) < CAP - MAIN, extra[:, 0], extra[:, 1]).reshape(32, HALF)
    hidden[0:pairs, :] = main.astype(BF16)
    hidden[pairs:, :] = extra.astype(BF16)
    share = gate_out.shape[0]
    w = weights[pl.ds(pl.multiple_of(i * share, share), share), :]
    gate_out[...] = w[:, :HALF]
    up_out[...] = w[:, HALF:]


def down_kernel(me, *refs):
    chunks, weights, out, down_out = refs[0:9], refs[9], refs[10], refs[11]
    i = pl.program_id(0)
    n_tp = 8
    offsets = (0, -1, 1, -2, 2, -3, 3, 4)
    pairs = 8 * MAIN
    acc = jnp.zeros((pairs + 32, 2 * HALF), F32)
    for n, offset in enumerate(offsets):
        h = chunks[n][...] if n < 7 else jnp.where(i < 2, chunks[7][...], chunks[8][...])
        source = (me[0] + offset + n_tp) % n_tp
        w = weights[pl.ds(pl.multiple_of(source * HALF, HALF), HALF), :]
        acc = acc + jnp.dot(h, w, preferred_element_type=F32)
    left = acc[:pairs, :HALF].reshape(8, MAIN, HALF)
    right = acc[:pairs, HALF:].reshape(8, MAIN, HALF)
    rest_l = acc[pairs:, :HALF].reshape(4, 8, HALF)
    rest_r = acc[pairs:, HALF:].reshape(4, 8, HALF)
    low = tile_row((4, 8, HALF)) < CAP - MAIN
    even = jnp.where(low, rest_l, pltpu.roll(rest_r, 4, 1))
    odd = jnp.where(low, pltpu.roll(rest_l, 4, 1), rest_r)
    rest = jnp.stack([even, odd], axis=1).reshape(8, 8, HALF)
    out[:, 0:MAIN, :] = left.astype(BF16)
    out[:, MAIN : 2 * MAIN, :] = right.astype(BF16)
    out[:, 2 * MAIN :, :] = rest.astype(BF16)
    share = down_out.shape[0]
    down_out[...] = weights[pl.ds(pl.multiple_of(i * share, share), share), :]


def combine_kernel(rows, gains, returned, mixture):
    n_tok = rows.shape[0]
    slots = returned.shape[0]
    ids = lax.broadcasted_iota(jnp.int32, (n_tok, slots), 1)

    def pick(n):
        onehot = (ids == rows[:, n : n + 1]).astype(F32).astype(BF16)
        return jnp.dot(onehot, returned[...], preferred_element_type=F32)

    gain0, gain1 = gains[:, 0:1], gains[:, 1:2]
    mixture[:, :HALF] = (gain0 * pick(0) + gain1 * pick(1)).astype(BF16)
    mixture[:, HALF:] = (gain0 * pick(2) + gain1 * pick(3)).astype(BF16)


def all_to_all(x):
    return lax.all_to_all(x, "fs", split_axis=0, concat_axis=0, tiled=True)


def ring(x):
    n = lax.axis_size("tp")

    def step(v, side):
        shift = 1 if side == "r" else -1
        return lax.ppermute(v, "tp", [(d, (d + shift) % n) for d in range(n)])

    half = x.shape[0] // 2
    r1, l1 = step(x, "r"), step(x, "l")
    r2, l2 = step(r1, "r"), step(l1, "l")
    r3, l3 = step(r2, "r"), step(l2, "l")
    r4, l4 = step(r3[:half], "r"), step(l3[half:], "l")
    return (x, r1, l1, r2, l2, r3, l3, r4, l4)


def mixture_of_experts(tokens, norm_gain, gate_weight, up_weight, down_weight, routes, route_weights):
    experts, _, cols = gate_weight.shape
    n_tok = tokens.shape[0]
    features = tokens.shape[1] * lax.axis_size("tp")
    me = lax.axis_index("tp").reshape(1).astype(jnp.int32)
    smem = pl.BlockSpec(memory_space=pltpu.SMEM)
    outbound, rows = pl.pallas_call(
        route_kernel,
        out_shape=(
            jax.ShapeDtypeStruct((experts * SLAB, HALF), BF16),
            jax.ShapeDtypeStruct((8, n_tok), jnp.int32),
        ),
        name="route",
    )(routes.T, tokens)
    arrived = all_to_all(outbound.reshape(experts, SLAB, HALF)).reshape(experts * SLAB, HALF)
    gain = norm_gain[None, :, None]
    both_low = jnp.concatenate([gain * gate_weight, gain * up_weight], axis=2).astype(BF16)
    both_serve = all_to_all(both_low).reshape(features, 2 * cols)
    cut = experts * SLAB // 2
    halves = ring(arrived[:cut]) + ring(arrived[cut:])
    quarter = cut // 2

    def spec_a(n):
        if n < 7:
            return pl.BlockSpec((quarter, HALF), lambda i: (jnp.minimum(i, 1), 0))
        return pl.BlockSpec((quarter, HALF), lambda i: (0, 0))

    def spec_b(n):
        if n < 7:
            return pl.BlockSpec((quarter, HALF), lambda i: (jnp.maximum(i - 2, 0), 0))
        return pl.BlockSpec((quarter, HALF), lambda i: (0, 0))

    row_share = experts * CAP // 4
    hidden, gate_serve, up_serve = pl.pallas_call(
        ffn_kernel,
        grid=(4,),
        in_specs=[smem]
        + [spec_a(n) for n in range(9)]
        + [spec_b(n) for n in range(9)]
        + [pl.BlockSpec((features, 2 * cols), lambda i: (0, 0))],
        out_specs=(
            pl.BlockSpec((row_share, cols), lambda i: (i, 0)),
            pl.BlockSpec((features // 4, cols), lambda i: (i, 0)),
            pl.BlockSpec((features // 4, cols), lambda i: (i, 0)),
        ),
        out_shape=(
            jax.ShapeDtypeStruct((experts * CAP, cols), BF16),
            jax.ShapeDtypeStruct((features, cols), BF16),
            jax.ShapeDtypeStruct((features, cols), BF16),
        ),
        name="ffn",
    )(me, *halves, both_serve)
    down_low = down_weight.astype(BF16)
    down_cols = down_low.shape[2]
    down_both = all_to_all(down_low).reshape(-1, down_cols)
    inner = down_both.shape[0]
    chunks = ring(hidden)

    def spec_h(n):
        if n < 7:
            return pl.BlockSpec((row_share, cols), lambda i: (i, 0))
        if n == 7:
            return pl.BlockSpec((row_share, cols), lambda i: (jnp.minimum(i, 1), 0))
        return pl.BlockSpec((row_share, cols), lambda i: (jnp.maximum(i - 2, 0), 0))

    expert_out, down_serve = pl.pallas_call(
        down_kernel,
        grid=(4,),
        in_specs=[smem]
        + [spec_h(n) for n in range(9)]
        + [pl.BlockSpec((inner, down_cols), lambda i: (0, 0))],
        out_specs=(
            pl.BlockSpec((experts // 4, SLAB, HALF), lambda i: (i, 0, 0)),
            pl.BlockSpec((inner // 4, down_cols), lambda i: (i, 0)),
        ),
        out_shape=(
            jax.ShapeDtypeStruct((experts, SLAB, HALF), BF16),
            jax.ShapeDtypeStruct((inner, down_cols), BF16),
        ),
        name="down",
    )(me, *chunks, down_both)
    returned = all_to_all(expert_out).reshape(experts * SLAB, HALF)
    mixture = pl.pallas_call(
        combine_kernel,
        out_shape=jax.ShapeDtypeStruct(tokens.shape, BF16),
        name="combine",
    )(rows.T, route_weights, returned)
    return (gate_serve[None], up_serve[None], down_serve[None], mixture)


def solution(mesh):
    block = ("grp", "fs")
    return jax.shard_map(
        mixture_of_experts,
        mesh=mesh,
        in_specs=(
            P(block, "tp"),
            P("fs"),
            P(None, "fs", "tp"),
            P(None, "fs", "tp"),
            P(None, "fs", "tp"),
            P(block, None),
            P(block, None),
        ),
        out_specs=(
            P(block, None, "tp"),
            P(block, None, "tp"),
            P(block, None, "tp"),
            P(block, "tp"),
        ),
        check_vma=False,
    )
```

time: 294 us -> 311 us (1.058)
  the two profiles are of different devices: /device:TPU:66 before, /device:TPU:71 now
where the time goes in v1:
time: 311 us; the launch traced here: 310 us
  starting transfers between devices  148 us (48%)
  waiting for transfers between devices  132 us (42%)
  Pallas kernels  18.9 us (6%)
  local copies, waits for them, and re-layouts  6.15 us (2%)
  other arithmetic  3.55 us (1%)
    all_to_all x4, waiting for transfers between devices, all_to_all(): return lax.all_to_all(x, 'fs', split_axis=0, concat_axis=0, tiled=True)  109 us
    all_to_all x4, starting transfers between devices, all_to_all(): return lax.all_to_all(x, 'fs', split_axis=0, concat_axis=0, tiled=True)  74 us
    ppermute x24, starting transfers between devices, step(): return lax.ppermute(v, 'tp', [(d, (d + shift) % n) for d in range(n)])  73.8 us
    ppermute x24, waiting for transfers between devices, step(): return lax.ppermute(v, 'tp', [(d, (d + shift) % n) for d in range(n)])  22.7 us
    pallas_call x1, Pallas kernels, mixture_of_experts(): pl.pallas_call(ffn_kernel, grid=(4,), in_specs=[smem] + [spec_a(n) for n...  6.48 us
  transfers between devices with their start and end apart: 28, of which 11 were waited for; matrix products, arithmetic and copies ran while one was open for 3% of the time, Pallas kernels for 2%

profile of v1, /device:TPU:71, one launch (start us, length us, event | category | flops | bytes accessed | tf_op | source)
XLA Modules:
  0.0 309.7 jit_solution(12852418402902859520)
XLA Ops:
  0.7 3.6 %route.1 = (bf16[2304,128]{1,0:T(8,128)(2,1)}, s32[8,384]{1,0:T(8,128)}) custom-call(s32[2,384]{1,0:T(2,128)} %bitcast.23, bf16[384,256]{1,0:T(8,128)(2,1)} %tokens.1), custom_call_target="tpu_custom_call" | custom-call | tf_op jit(solution)/shard_map/route/pallas_call | solution.py:178
  4.2 44.4 %all-to-all-start = ((bf16[32,72,128]{2,1,0:T(8,128)(2,1)}), bf16[32,72,128]{2,1,0:T(8,128)(2,1)S(1)}, u32[]{:S(2)}, u32[]{:S(2)}) async-start(bf16[32,72,128]{2,1,0:T(8,128)(2,1)} %bitcast.22), calls=%async_computation | async-start | bytes 1179648 | tf_op jit(solution)/shard_map/all_to_all | solution.py:154
  48.6 1.5 multiply_convert_fusion.1
  50.2 1.1 pad_maximum_fusion
  51.3 33.4 %all-to-all-done = bf16[32,72,128]{2,1,0:T(8,128)(2,1)S(1)} async-done(((bf16[32,72,128]{2,1,0:T(8,128)(2,1)}), bf16[32,72,128]{2,1,0:T(8,128)(2,1)S(1)}, u32[]{:S(2)}, u32[]{:S(2)}) %all-to-all-start) | async-done | bytes 589856 | tf_op jit(solution)/shard_map/all_to_all | solution.py:154
  84.7 4.3 %all-to-all-start.1 = ((bf16[32,64,256]{2,1,0:T(8,128)(2,1)}), bf16[32,64,256]{2,1,0:T(8,128)(2,1)S(1)}, u32[]{:S(2)}, u32[]{:S(2)}) async-start(bf16[32,64,256]{2,1,0:T(8,128)(2,1)} %pad_maximum_fusion), calls=%async_computation.1 | async-start | bytes 2097152 | tf_op jit(solution)/shard_map/all_to_all | solution.py:154
  89.1 4.6 %collective-permute-start.8 = (bf16[1152,128]{1,0:T(8,128)(2,1)S(1)}, bf16[1152,128]{1,0:T(8,128)(2,1)S(1)}, u32[]{:S(2)}, u32[]{:S(2)}) collective-permute-start(bf16[1152,128]{1,0:T(8,128)(2,1)S(1)} %bitcast.15), channel_id=1, source_target_pairs={{0,1},{1,2},{2,3},{3,4},{4,5},{5,6},{6,7},{7,0},{8,9},{9,10},{10,1... | collective-permute-start | bytes 884744 | tf_op jit(solution)/shard_map/ppermute | solution.py:162
  93.8 2.0 collective-permute-start.9
  95.7 4.6 %collective-permute-start = (bf16[1152,128]{1,0:T(8,128)(2,1)S(1)}, bf16[1152,128]{1,0:T(8,128)(2,1)S(1)}, u32[]{:S(2)}, u32[]{:S(2)}) collective-permute-start(bf16[1152,128]{1,0:T(8,128)(2,1)S(1)} %bitcast.18), channel_id=1, source_target_pairs={{0,1},{1,2},{2,3},{3,4},{4,5},{5,6},{6,7},{7,0},{8,9},{9,10},{10,1... | collective-permute-start | bytes 884744 | tf_op jit(solution)/shard_map/ppermute | solution.py:162
  100.3 2.0 collective-permute-start.1
  102.3 0.9 convert_element_type.4
  103.2 41.5 %all-to-all-done.1 = bf16[32,64,256]{2,1,0:T(8,128)(2,1)S(1)} async-done(((bf16[32,64,256]{2,1,0:T(8,128)(2,1)}), bf16[32,64,256]{2,1,0:T(8,128)(2,1)S(1)}, u32[]{:S(2)}, u32[]{:S(2)}) %all-to-all-start.1) | async-done | bytes 1048608 | tf_op jit(solution)/shard_map/all_to_all | solution.py:154
  144.6 4.9 %all-to-all-start.2 = ((bf16[32,32,256]{2,1,0:T(8,128)(2,1)}), bf16[32,32,256]{2,1,0:T(8,128)(2,1)S(1)}, u32[]{:S(2)}, u32[]{:S(2)}) async-start(bf16[32,32,256]{2,1,0:T(8,128)(2,1)} %convert_element_type.4), calls=%async_computation.2 | async-start | bytes 1048576 | tf_op jit(solution)/shard_map/all_to_all | solution.py:154
  149.6 4.5 %collective-permute-start.10 = (bf16[1152,128]{1,0:T(8,128)(2,1)S(1)}, bf16[1152,128]{1,0:T(8,128)(2,1)S(1)}, u32[]{:S(2)}, u32[]{:S(2)}) collective-permute-start(bf16[1152,128]{1,0:T(8,128)(2,1)S(1)} %collective-permute-done.8.refs_10_), channel_id=1, source_target_pairs={{0,1},{1,2},{2,3},{3,4},{4,5},{5,6},{6,7},{7,0},{8,9},{9,10},{10,1... | collective-permute-start | bytes 884744 | tf_op jit(solution)/shard_map/ppermute | solution.py:162
  154.1 2.0 collective-permute-start.11
  156.1 4.6 %collective-permute-start.2 = (bf16[1152,128]{1,0:T(8,128)(2,1)S(1)}, bf16[1152,128]{1,0:T(8,128)(2,1)S(1)}, u32[]{:S(2)}, u32[]{:S(2)}) collective-permute-start(bf16[1152,128]{1,0:T(8,128)(2,1)S(1)} %collective-permute-done.refs_1_), channel_id=1, source_target_pairs={{0,1},{1,2},{2,3},{3,4},{4,5},{5,6},{6,7},{7,0},{8,9},{9,10},{10,1... | collective-permute-start | bytes 884744 | tf_op jit(solution)/shard_map/ppermute | solution.py:162
  160.7 2.0 collective-permute-start.3
  162.7 4.6 %collective-permute-start.12 = (bf16[1152,128]{1,0:T(8,128)(2,1)S(1)}, bf16[1152,128]{1,0:T(8,128)(2,1)S(1)}, u32[]{:S(2)}, u32[]{:S(2)}) collective-permute-start(bf16[1152,128]{1,0:T(8,128)(2,1)S(1)} %collective-permute-done.10.refs_12_), channel_id=1, source_target_pairs={{0,1},{1,2},{2,3},{3,4},{4,5},{5,6},{6,7},{7,0},{8,9},{9,10},{10,1... | collective-permute-start | bytes 884744 | tf_op jit(solution)/shard_map/ppermute | solution.py:162
  167.3 2.0 collective-permute-start.13
  169.3 4.6 %collective-permute-start.4 = (bf16[1152,128]{1,0:T(8,128)(2,1)S(1)}, bf16[1152,128]{1,0:T(8,128)(2,1)S(1)}, u32[]{:S(2)}, u32[]{:S(2)}) collective-permute-start(bf16[1152,128]{1,0:T(8,128)(2,1)S(1)} %collective-permute-done.2.refs_3_), channel_id=1, source_target_pairs={{0,1},{1,2},{2,3},{3,4},{4,5},{5,6},{6,7},{7,0},{8,9},{9,10},{10,1... | collective-permute-start | bytes 884744 | tf_op jit(solution)/shard_map/ppermute | solution.py:162
  174.0 2.0 collective-permute-start.5
  176.7 4.6 %collective-permute-start.14 = (bf16[576,128]{1,0:T(8,128)(2,1)}, bf16[576,128]{1,0:T(8,128)(2,1)S(1)}, u32[]{:S(2)}, u32[]{:S(2)}) collective-permute-start(bf16[576,128]{1,0:T(8,128)(2,1)} %slice.44), channel_id=1, source_target_pairs={{0,1},{1,2},{2,3},{3,4},{4,5},{5,6},{6,7},{7,0},{8,9},{9,10},{10,1... | collective-permute-start | bytes 442376 | tf_op jit(solution)/shard_map/ppermute | solution.py:162
  182.0 1.9 collective-permute-start.15
  184.7 4.6 %collective-permute-start.6 = (bf16[576,128]{1,0:T(8,128)(2,1)}, bf16[576,128]{1,0:T(8,128)(2,1)}, u32[]{:S(2)}, u32[]{:S(2)}) collective-permute-start(bf16[576,128]{1,0:T(8,128)(2,1)} %slice.41), channel_id=1, source_target_pairs={{0,1},{1,2},{2,3},{3,4},{4,5},{5,6},{6,7},{7,0},{8,9},{9,10},{10,1... | collective-permute-start | bytes 442376 | tf_op jit(solution)/shard_map/ppermute | solution.py:162
  189.3 0.7 slice.42
  190.0 1.9 collective-permute-start.7
  192.1 5.4 %collective-permute-done.7.refs_8_ = bf16[576,128]{1,0:T(8,128)(2,1)} collective-permute-done((bf16[576,128]{1,0:T(8,128)(2,1)}, bf16[576,128]{1,0:T(8,128)(2,1)}, u32[]{:S(2)}, u32[]{:S(2)}) %collective-permute-start.7) | collective-permute-done | bytes 147488 | tf_op jit(solution)/shard_map/ppermute | solution.py:162
  197.5 6.5 %ffn.1 = (bf16[1152,128]{1,0:T(8,128)(2,1)}, bf16[2048,128]{1,0:T(8,128)(2,1)}, bf16[2048,128]{1,0:T(8,128)(2,1)}) custom-call(s32[1]{0:T(128)} %bitcast.me, bf16[1152,128]{1,0:T(8,128)(2,1)} %bitcast.20, bf16[1152,128]{1,0:T(8,128)(2,1)} %copy-done.15, bf16[1152,128]{1,0:T(8,128)(2,1)} %copy-done.16, bf16[1152,128]{1,0:T(8,128)(2,1)} %copy-done.19, ...), custom_call_target="tpu_custom_call" | custom-call | tf_op jit(solution)/shard_map/ffn/pallas_call | solution.py:205
  204.0 2.0 collective-permute-start.16
  206.0 3.4 %collective-permute-start.17 = (bf16[1152,128]{1,0:T(8,128)(2,1)}, bf16[1152,128]{1,0:T(8,128)(2,1)S(1)}, u32[]{:S(2)}, u32[]{:S(2)}) collective-permute-start(bf16[1152,128]{1,0:T(8,128)(2,1)} %get-tuple-element.14.refs_0_), channel_id=1, source_target_pairs={{0,7},{1,0},{2,1},{3,2},{4,3},{5,4},{6,5},{7,6},{8,15},{9,8},{10,9... | collective-permute-start | bytes 884744 | tf_op jit(solution)/shard_map/ppermute | solution.py:162
  209.4 2.3 collective-permute-done.16.refs_1_
  211.7 3.1 %collective-permute-start.18 = (bf16[1152,128]{1,0:T(8,128)(2,1)S(1)}, bf16[1152,128]{1,0:T(8,128)(2,1)S(1)}, u32[]{:S(2)}, u32[]{:S(2)}) collective-permute-start(bf16[1152,128]{1,0:T(8,128)(2,1)S(1)} %collective-permute-done.16.refs_1_), channel_id=1, source_target_pairs={{0,1},{1,2},{2,3},{3,4},{4,5},{5,6},{6,7},{7,0},{8,9},{9,10},{10,1... | collective-permute-start | bytes 884744 | tf_op jit(solution)/shard_map/ppermute | solution.py:162
  214.9 2.5 collective-permute-start.19
  217.4 3.5 %collective-permute-done.18.refs_3_ = bf16[1152,128]{1,0:T(8,128)(2,1)S(1)} collective-permute-done((bf16[1152,128]{1,0:T(8,128)(2,1)S(1)}, bf16[1152,128]{1,0:T(8,128)(2,1)S(1)}, u32[]{:S(2)}, u32[]{:S(2)}) %collective-permute-start.18) | collective-permute-done | bytes 294944 | tf_op jit(solution)/shard_map/ppermute | solution.py:162
  220.9 2.7 collective-permute-start.20
  223.8 2.7 collective-permute-start.21
  226.5 4.4 %collective-permute-done.20.refs_5_ = bf16[1152,128]{1,0:T(8,128)(2,1)S(1)} collective-permute-done((bf16[1152,128]{1,0:T(8,128)(2,1)S(1)}, bf16[1152,128]{1,0:T(8,128)(2,1)S(1)}, u32[]{:S(2)}, u32[]{:S(2)}) %collective-permute-start.20) | collective-permute-done | bytes 294944 | tf_op jit(solution)/shard_map/ppermute | solution.py:162
  231.0 2.6 collective-permute-start.22
  233.8 2.5 collective-permute-start.23
  236.4 2.4 collective-permute-done.22.refs_7_
  238.7 4.1 %collective-permute-done.23.refs_8_ = bf16[576,128]{1,0:T(8,128)(2,1)S(1)} collective-permute-done((bf16[576,128]{1,0:T(8,128)(2,1)S(1)}, bf16[576,128]{1,0:T(8,128)(2,1)S(1)}, u32[]{:S(2)}, u32[]{:S(2)}) %collective-permute-start.23) | collective-permute-done | bytes 147488 | tf_op jit(solution)/shard_map/ppermute | solution.py:162
  243.5 4.8 %down.1 = (bf16[32,72,128]{2,1,0:T(8,128)(2,1)}, bf16[1024,256]{1,0:T(8,128)(2,1)}) custom-call(s32[1]{0:T(128)} %bitcast.me, bf16[1152,128]{1,0:T(8,128)(2,1)} %get-tuple-element.14.refs_0_, bf16[1152,128]{1,0:T(8,128)(2,1)} %copy-done.21, bf16[1152,128]{1,0:T(8,128)(2,1)} %copy-done.22, bf16[1152,128]{1,0:T(8,128)(2,1)} %copy-done.23, ...), custom_call_target="tpu_custom_call" | custom-call | tf_op jit(solution)/shard_map/down/pallas_call | solution.py:237
  248.4 20.4 %all-to-all-start.3 = ((bf16[32,72,128]{2,1,0:T(8,128)(2,1)}), bf16[32,72,128]{2,1,0:T(8,128)(2,1)S(1)}, u32[]{:S(2)}, u32[]{:S(2)}) async-start(bf16[32,72,128]{2,1,0:T(8,128)(2,1)} %get-tuple-element.17), calls=%async_computation.3 | async-start | bytes 1179648 | tf_op jit(solution)/shard_map/all_to_all | solution.py:154
  268.8 0.8 copy.11
  269.6 0.8 copy.12.gains
  270.4 34.4 %all-to-all-done.3 = bf16[32,72,128]{2,1,0:T(8,128)(2,1)S(1)} async-done(((bf16[32,72,128]{2,1,0:T(8,128)(2,1)}), bf16[32,72,128]{2,1,0:T(8,128)(2,1)S(1)}, u32[]{:S(2)}, u32[]{:S(2)}) %all-to-all-start.3) | async-done | bytes 589856 | tf_op jit(solution)/shard_map/all_to_all | solution.py:154
  304.9 0.8 copy-done.1
  305.7 4.0 %combine.1 = bf16[384,256]{1,0:T(8,128)(2,1)} custom-call(s32[384,8]{1,0:T(8,128)} %bitcast.21, f32[384,2]{1,0:T(8,128)} %copy.12.gains, bf16[2304,128]{1,0:T(8,128)(2,1)} %bitcast.13), custom_call_target="tpu_custom_call" | custom-call | tf_op jit(solution)/shard_map/combine/pallas_call | solution.py:254
  (86 shorter events, 3.5 us)
Async XLA Ops:
  0.6 48.0 %copy-start.30 = (f32[64]{0:T(128)S(1)}, f32[64]{0:T(128)}, u32[]{:S(2)}) copy-start(f32[64]{0:T(128)} %param.8) | copy-start | bytes 772
  0.6 48.0 %copy-start.6 = (f32[32,64,128]{2,1,0:T(8,128)S(1)}, f32[32,64,128]{2,1,0:T(8,128)}, u32[]{:S(2)}) copy-start(f32[32,64,128]{2,1,0:T(8,128)} %param.9) | copy-start | bytes 3145732
  4.2 80.5 %all-to-all-start = ((bf16[32,72,128]{2,1,0:T(8,128)(2,1)}), bf16[32,72,128]{2,1,0:T(8,128)(2,1)S(1)}, u32[]{:S(2)}, u32[]{:S(2)}) async-start(bf16[32,72,128]{2,1,0:T(8,128)(2,1)} %bitcast.22), calls=%async_computation | async-start | bytes 1179648 | tf_op jit(solution)/shard_map/all_to_all | solution.py:154
  84.7 59.9 %all-to-all-start.1 = ((bf16[32,64,256]{2,1,0:T(8,128)(2,1)}), bf16[32,64,256]{2,1,0:T(8,128)(2,1)S(1)}, u32[]{:S(2)}, u32[]{:S(2)}) async-start(bf16[32,64,256]{2,1,0:T(8,128)(2,1)} %pad_maximum_fusion), calls=%async_computation.1 | async-start | bytes 2097152 | tf_op jit(solution)/shard_map/all_to_all | solution.py:154
  89.0 13.3 %copy-start.5 = (f32[32,32,256]{2,1,0:T(8,128)S(1)}, f32[32,32,256]{2,1,0:T(8,128)}, u32[]{:S(2)}) copy-start(f32[32,32,256]{2,1,0:T(8,128)} %param.11) | copy-start | bytes 3145732
  89.1 55.5 %copy-start.3 = (bf16[16,72,128]{2,1,0:T(8,128)(2,1)}, bf16[16,72,128]{2,1,0:T(8,128)(2,1)S(1)}, u32[]{:S(2)}) copy-start(bf16[16,72,128]{2,1,0:T(8,128)(2,1)S(1)} %get-tuple-element.18) | copy-start | bytes 884740
  89.1 55.5 %copy-start.4 = (bf16[16,72,128]{2,1,0:T(8,128)(2,1)}, bf16[16,72,128]{2,1,0:T(8,128)(2,1)S(1)}, u32[]{:S(2)}) copy-start(bf16[16,72,128]{2,1,0:T(8,128)(2,1)S(1)} %get-tuple-element.19) | copy-start | bytes 884740
  89.1 60.4 %collective-permute-start.8 = (bf16[1152,128]{1,0:T(8,128)(2,1)S(1)}, bf16[1152,128]{1,0:T(8,128)(2,1)S(1)}, u32[]{:S(2)}, u32[]{:S(2)}) collective-permute-start(bf16[1152,128]{1,0:T(8,128)(2,1)S(1)} %bitcast.15), channel_id=1, source_target_pairs={{0,1},{1,2},{2,3},{3,4},{4,5},{5,6},{6,7},{7,0},{8,9},{9,10},{10,1... | collective-permute-start | bytes 884744 | tf_op jit(solution)/shard_map/ppermute | solution.py:162
  93.8 60.3 %collective-permute-start.9 = (bf16[1152,128]{1,0:T(8,128)(2,1)S(1)}, bf16[1152,128]{1,0:T(8,128)(2,1)S(1)}, u32[]{:S(2)}, u32[]{:S(2)}) collective-permute-start(bf16[1152,128]{1,0:T(8,128)(2,1)S(1)} %bitcast.16), channel_id=1, source_target_pairs={{0,7},{1,0},{2,1},{3,2},{4,3},{5,4},{6,5},{7,6},{8,15},{9,8},{10,9... | collective-permute-start | bytes 884744 | tf_op jit(solution)/shard_map/ppermute | solution.py:162
  95.7 60.4 %collective-permute-start = (bf16[1152,128]{1,0:T(8,128)(2,1)S(1)}, bf16[1152,128]{1,0:T(8,128)(2,1)S(1)}, u32[]{:S(2)}, u32[]{:S(2)}) collective-permute-start(bf16[1152,128]{1,0:T(8,128)(2,1)S(1)} %bitcast.18), channel_id=1, source_target_pairs={{0,1},{1,2},{2,3},{3,4},{4,5},{5,6},{6,7},{7,0},{8,9},{9,10},{10,1... | collective-permute-start | bytes 884744 | tf_op jit(solution)/shard_map/ppermute | solution.py:162
  100.3 60.4 %collective-permute-start.1 = (bf16[1152,128]{1,0:T(8,128)(2,1)S(1)}, bf16[1152,128]{1,0:T(8,128)(2,1)S(1)}, u32[]{:S(2)}, u32[]{:S(2)}) collective-permute-start(bf16[1152,128]{1,0:T(8,128)(2,1)S(1)} %bitcast.19), channel_id=1, source_target_pairs={{0,7},{1,0},{2,1},{3,2},{4,3},{5,4},{6,5},{7,6},{8,15},{9,8},{10,9... | collective-permute-start | bytes 884744 | tf_op jit(solution)/shard_map/ppermute | solution.py:162
  144.6 45.4 %copy-start = (bf16[32,64,256]{2,1,0:T(8,128)(2,1)}, bf16[32,64,256]{2,1,0:T(8,128)(2,1)S(1)}, u32[]{:S(2)}) copy-start(bf16[32,64,256]{2,1,0:T(8,128)(2,1)S(1)} %all-to-all-done.1) | copy-start | bytes 3145732
  144.6 91.7 %all-to-all-start.2 = ((bf16[32,32,256]{2,1,0:T(8,128)(2,1)}), bf16[32,32,256]{2,1,0:T(8,128)(2,1)S(1)}, u32[]{:S(2)}, u32[]{:S(2)}) async-start(bf16[32,32,256]{2,1,0:T(8,128)(2,1)} %convert_element_type.4), calls=%async_computation.2 | async-start | bytes 1048576 | tf_op jit(solution)/shard_map/all_to_all | solution.py:154
  149.6 47.9 %copy-start.13 = (bf16[1152,128]{1,0:T(8,128)(2,1)}, bf16[1152,128]{1,0:T(8,128)(2,1)S(1)}, u32[]{:S(2)}) copy-start(bf16[1152,128]{1,0:T(8,128)(2,1)S(1)} %collective-permute-done.8.refs_10_) | copy-start | bytes 884740
  149.6 13.1 %collective-permute-start.10 = (bf16[1152,128]{1,0:T(8,128)(2,1)S(1)}, bf16[1152,128]{1,0:T(8,128)(2,1)S(1)}, u32[]{:S(2)}, u32[]{:S(2)}) collective-permute-start(bf16[1152,128]{1,0:T(8,128)(2,1)S(1)} %collective-permute-done.8.refs_10_), channel_id=1, source_target_pairs={{0,1},{1,2},{2,3},{3,4},{4,5},{5,6},{6,7},{7,0},{8,9},{9,10},{10,1... | collective-permute-start | bytes 884744 | tf_op jit(solution)/shard_map/ppermute | solution.py:162
  154.1 43.4 %copy-start.14 = (bf16[1152,128]{1,0:T(8,128)(2,1)}, bf16[1152,128]{1,0:T(8,128)(2,1)S(1)}, u32[]{:S(2)}) copy-start(bf16[1152,128]{1,0:T(8,128)(2,1)S(1)} %collective-permute-done.9.refs_11_) | copy-start | bytes 884740
  154.1 13.2 %collective-permute-start.11 = (bf16[1152,128]{1,0:T(8,128)(2,1)S(1)}, bf16[1152,128]{1,0:T(8,128)(2,1)S(1)}, u32[]{:S(2)}, u32[]{:S(2)}) collective-permute-start(bf16[1152,128]{1,0:T(8,128)(2,1)S(1)} %collective-permute-done.9.refs_11_), channel_id=1, source_target_pairs={{0,7},{1,0},{2,1},{3,2},{4,3},{5,4},{6,5},{7,6},{8,15},{9,8},{10,9... | collective-permute-start | bytes 884744 | tf_op jit(solution)/shard_map/ppermute | solution.py:162
  156.1 13.2 %collective-permute-start.2 = (bf16[1152,128]{1,0:T(8,128)(2,1)S(1)}, bf16[1152,128]{1,0:T(8,128)(2,1)S(1)}, u32[]{:S(2)}, u32[]{:S(2)}) collective-permute-start(bf16[1152,128]{1,0:T(8,128)(2,1)S(1)} %collective-permute-done.refs_1_), channel_id=1, source_target_pairs={{0,1},{1,2},{2,3},{3,4},{4,5},{5,6},{6,7},{7,0},{8,9},{9,10},{10,1... | collective-permute-start | bytes 884744 | tf_op jit(solution)/shard_map/ppermute | solution.py:162
  160.7 13.2 %collective-permute-start.3 = (bf16[1152,128]{1,0:T(8,128)(2,1)S(1)}, bf16[1152,128]{1,0:T(8,128)(2,1)S(1)}, u32[]{:S(2)}, u32[]{:S(2)}) collective-permute-start(bf16[1152,128]{1,0:T(8,128)(2,1)S(1)} %collective-permute-done.1.refs_2_), channel_id=1, source_target_pairs={{0,7},{1,0},{2,1},{3,2},{4,3},{5,4},{6,5},{7,6},{8,15},{9,8},{10,9... | collective-permute-start | bytes 884744 | tf_op jit(solution)/shard_map/ppermute | solution.py:162
  162.7 13.2 %collective-permute-start.12 = (bf16[1152,128]{1,0:T(8,128)(2,1)S(1)}, bf16[1152,128]{1,0:T(8,128)(2,1)S(1)}, u32[]{:S(2)}, u32[]{:S(2)}) collective-permute-start(bf16[1152,128]{1,0:T(8,128)(2,1)S(1)} %collective-permute-done.10.refs_12_), channel_id=1, source_target_pairs={{0,1},{1,2},{2,3},{3,4},{4,5},{5,6},{6,7},{7,0},{8,9},{9,10},{10,1... | collective-permute-start | bytes 884744 | tf_op jit(solution)/shard_map/ppermute | solution.py:162
  167.3 24.7 %copy-start.18 = (bf16[1152,128]{1,0:T(8,128)(2,1)}, bf16[1152,128]{1,0:T(8,128)(2,1)S(1)}, u32[]{:S(2)}) copy-start(bf16[1152,128]{1,0:T(8,128)(2,1)S(1)} %collective-permute-done.11.refs_13_) | copy-start | bytes 884740
  167.3 13.9 %collective-permute-start.13 = (bf16[1152,128]{1,0:T(8,128)(2,1)S(1)}, bf16[1152,128]{1,0:T(8,128)(2,1)S(1)}, u32[]{:S(2)}, u32[]{:S(2)}) collective-permute-start(bf16[1152,128]{1,0:T(8,128)(2,1)S(1)} %collective-permute-done.11.refs_13_), channel_id=1, source_target_pairs={{0,7},{1,0},{2,1},{3,2},{4,3},{5,4},{6,5},{7,6},{8,15},{9,8},{10,9... | collective-permute-start | bytes 884744 | tf_op jit(solution)/shard_map/ppermute | solution.py:162
  169.3 22.7 %copy-start.19 = (bf16[1152,128]{1,0:T(8,128)(2,1)}, bf16[1152,128]{1,0:T(8,128)(2,1)S(1)}, u32[]{:S(2)}) copy-start(bf16[1152,128]{1,0:T(8,128)(2,1)S(1)} %collective-permute-done.2.refs_3_) | copy-start | bytes 884740
  169.3 14.6 %collective-permute-start.4 = (bf16[1152,128]{1,0:T(8,128)(2,1)S(1)}, bf16[1152,128]{1,0:T(8,128)(2,1)S(1)}, u32[]{:S(2)}, u32[]{:S(2)}) collective-permute-start(bf16[1152,128]{1,0:T(8,128)(2,1)S(1)} %collective-permute-done.2.refs_3_), channel_id=1, source_target_pairs={{0,1},{1,2},{2,3},{3,4},{4,5},{5,6},{6,7},{7,0},{8,9},{9,10},{10,1... | collective-permute-start | bytes 884744 | tf_op jit(solution)/shard_map/ppermute | solution.py:162
  174.0 18.1 %copy-start.20 = (bf16[1152,128]{1,0:T(8,128)(2,1)}, bf16[1152,128]{1,0:T(8,128)(2,1)S(1)}, u32[]{:S(2)}) copy-start(bf16[1152,128]{1,0:T(8,128)(2,1)S(1)} %collective-permute-done.3.refs_4_) | copy-start | bytes 884740
  174.0 15.3 %collective-permute-start.5 = (bf16[1152,128]{1,0:T(8,128)(2,1)S(1)}, bf16[1152,128]{1,0:T(8,128)(2,1)S(1)}, u32[]{:S(2)}, u32[]{:S(2)}) collective-permute-start(bf16[1152,128]{1,0:T(8,128)(2,1)S(1)} %collective-permute-done.3.refs_4_), channel_id=1, source_target_pairs={{0,7},{1,0},{2,1},{3,2},{4,3},{5,4},{6,5},{7,6},{8,15},{9,8},{10,9... | collective-permute-start | bytes 884744 | tf_op jit(solution)/shard_map/ppermute | solution.py:162
  175.9 21.5 %copy-start.7 = (bf16[1152,128]{1,0:T(8,128)(2,1)}, bf16[1152,128]{1,0:T(8,128)(2,1)S(1)}, u32[]{:S(2)}) copy-start(bf16[1152,128]{1,0:T(8,128)(2,1)S(1)} %collective-permute-done.12.refs_14_) | copy-start | bytes 884740
  176.7 15.4 %collective-permute-start.14 = (bf16[576,128]{1,0:T(8,128)(2,1)}, bf16[576,128]{1,0:T(8,128)(2,1)S(1)}, u32[]{:S(2)}, u32[]{:S(2)}) collective-permute-start(bf16[576,128]{1,0:T(8,128)(2,1)} %slice.44), channel_id=1, source_target_pairs={{0,1},{1,2},{2,3},{3,4},{4,5},{5,6},{6,7},{7,0},{8,9},{9,10},{10,1... | collective-permute-start | bytes 442376 | tf_op jit(solution)/shard_map/ppermute | solution.py:162
  181.3 16.2 %copy-start.8 = (bf16[1152,128]{1,0:T(8,128)(2,1)}, bf16[1152,128]{1,0:T(8,128)(2,1)S(1)}, u32[]{:S(2)}) copy-start(bf16[1152,128]{1,0:T(8,128)(2,1)S(1)} %collective-permute-done.13.refs_15_) | copy-start | bytes 884740
  182.0 10.1 %collective-permute-start.15 = (bf16[576,128]{1,0:T(8,128)(2,1)}, bf16[576,128]{1,0:T(8,128)(2,1)}, u32[]{:S(2)}, u32[]{:S(2)}) collective-permute-start(bf16[576,128]{1,0:T(8,128)(2,1)} %slice.45), channel_id=1, source_target_pairs={{0,7},{1,0},{2,1},{3,2},{4,3},{5,4},{6,5},{7,6},{8,15},{9,8},{10,9... | collective-permute-start | bytes 442376 | tf_op jit(solution)/shard_map/ppermute | solution.py:162
  184.0 13.5 %copy-start.9 = (bf16[1152,128]{1,0:T(8,128)(2,1)}, bf16[1152,128]{1,0:T(8,128)(2,1)S(1)}, u32[]{:S(2)}) copy-start(bf16[1152,128]{1,0:T(8,128)(2,1)S(1)} %collective-permute-done.4.refs_5_) | copy-start | bytes 884740
  184.7 7.4 %collective-permute-start.6 = (bf16[576,128]{1,0:T(8,128)(2,1)}, bf16[576,128]{1,0:T(8,128)(2,1)}, u32[]{:S(2)}, u32[]{:S(2)}) collective-permute-start(bf16[576,128]{1,0:T(8,128)(2,1)} %slice.41), channel_id=1, source_target_pairs={{0,1},{1,2},{2,3},{3,4},{4,5},{5,6},{6,7},{7,0},{8,9},{9,10},{10,1... | collective-permute-start | bytes 442376 | tf_op jit(solution)/shard_map/ppermute | solution.py:162
  190.0 7.4 %collective-permute-start.7 = (bf16[576,128]{1,0:T(8,128)(2,1)}, bf16[576,128]{1,0:T(8,128)(2,1)}, u32[]{:S(2)}, u32[]{:S(2)}) collective-permute-start(bf16[576,128]{1,0:T(8,128)(2,1)} %slice.42), channel_id=1, source_target_pairs={{0,7},{1,0},{2,1},{3,2},{4,3},{5,4},{6,5},{7,6},{8,15},{9,8},{10,9... | collective-permute-start | bytes 442376 | tf_op jit(solution)/shard_map/ppermute | solution.py:162
  204.0 7.7 %collective-permute-start.16 = (bf16[1152,128]{1,0:T(8,128)(2,1)}, bf16[1152,128]{1,0:T(8,128)(2,1)S(1)}, u32[]{:S(2)}, u32[]{:S(2)}) collective-permute-start(bf16[1152,128]{1,0:T(8,128)(2,1)} %get-tuple-element.14.refs_0_), channel_id=1, source_target_pairs={{0,1},{1,2},{2,3},{3,4},{4,5},{5,6},{6,7},{7,0},{8,9},{9,10},{10,1... | collective-permute-start | bytes 884744 | tf_op jit(solution)/shard_map/ppermute | solution.py:162
  206.0 8.9 %collective-permute-start.17 = (bf16[1152,128]{1,0:T(8,128)(2,1)}, bf16[1152,128]{1,0:T(8,128)(2,1)S(1)}, u32[]{:S(2)}, u32[]{:S(2)}) collective-permute-start(bf16[1152,128]{1,0:T(8,128)(2,1)} %get-tuple-element.14.refs_0_), channel_id=1, source_target_pairs={{0,7},{1,0},{2,1},{3,2},{4,3},{5,4},{6,5},{7,6},{8,15},{9,8},{10,9... | collective-permute-start | bytes 884744 | tf_op jit(solution)/shard_map/ppermute | solution.py:162
  211.7 31.1 %copy-start.21 = (bf16[1152,128]{1,0:T(8,128)(2,1)}, bf16[1152,128]{1,0:T(8,128)(2,1)S(1)}, u32[]{:S(2)}) copy-start(bf16[1152,128]{1,0:T(8,128)(2,1)S(1)} %collective-permute-done.16.refs_1_) | copy-start | bytes 884740
  211.7 9.2 %collective-permute-start.18 = (bf16[1152,128]{1,0:T(8,128)(2,1)S(1)}, bf16[1152,128]{1,0:T(8,128)(2,1)S(1)}, u32[]{:S(2)}, u32[]{:S(2)}) collective-permute-start(bf16[1152,128]{1,0:T(8,128)(2,1)S(1)} %collective-permute-done.16.refs_1_), channel_id=1, source_target_pairs={{0,1},{1,2},{2,3},{3,4},{4,5},{5,6},{6,7},{7,0},{8,9},{9,10},{10,1... | collective-permute-start | bytes 884744 | tf_op jit(solution)/shard_map/ppermute | solution.py:162
  214.9 28.0 %copy-start.22 = (bf16[1152,128]{1,0:T(8,128)(2,1)}, bf16[1152,128]{1,0:T(8,128)(2,1)S(1)}, u32[]{:S(2)}) copy-start(bf16[1152,128]{1,0:T(8,128)(2,1)S(1)} %collective-permute-done.17.refs_2_) | copy-start | bytes 884740
  214.9 8.9 %collective-permute-start.19 = (bf16[1152,128]{1,0:T(8,128)(2,1)S(1)}, bf16[1152,128]{1,0:T(8,128)(2,1)S(1)}, u32[]{:S(2)}, u32[]{:S(2)}) collective-permute-start(bf16[1152,128]{1,0:T(8,128)(2,1)S(1)} %collective-permute-done.17.refs_2_), channel_id=1, source_target_pairs={{0,7},{1,0},{2,1},{3,2},{4,3},{5,4},{6,5},{7,6},{8,15},{9,8},{10,9... | collective-permute-start | bytes 884744 | tf_op jit(solution)/shard_map/ppermute | solution.py:162
  220.9 22.0 %copy-start.23 = (bf16[1152,128]{1,0:T(8,128)(2,1)}, bf16[1152,128]{1,0:T(8,128)(2,1)S(1)}, u32[]{:S(2)}) copy-start(bf16[1152,128]{1,0:T(8,128)(2,1)S(1)} %collective-permute-done.18.refs_3_) | copy-start | bytes 884740
  220.9 10.0 %collective-permute-start.20 = (bf16[1152,128]{1,0:T(8,128)(2,1)S(1)}, bf16[1152,128]{1,0:T(8,128)(2,1)S(1)}, u32[]{:S(2)}, u32[]{:S(2)}) collective-permute-start(bf16[1152,128]{1,0:T(8,128)(2,1)S(1)} %collective-permute-done.18.refs_3_), channel_id=1, source_target_pairs={{0,1},{1,2},{2,3},{3,4},{4,5},{5,6},{6,7},{7,0},{8,9},{9,10},{10,1... | collective-permute-start | bytes 884744 | tf_op jit(solution)/shard_map/ppermute | solution.py:162
  223.8 19.1 %copy-start.24 = (bf16[1152,128]{1,0:T(8,128)(2,1)}, bf16[1152,128]{1,0:T(8,128)(2,1)S(1)}, u32[]{:S(2)}) copy-start(bf16[1152,128]{1,0:T(8,128)(2,1)S(1)} %collective-permute-done.19.refs_4_) | copy-start | bytes 884740
  223.8 10.1 %collective-permute-start.21 = (bf16[1152,128]{1,0:T(8,128)(2,1)S(1)}, bf16[1152,128]{1,0:T(8,128)(2,1)S(1)}, u32[]{:S(2)}, u32[]{:S(2)}) collective-permute-start(bf16[1152,128]{1,0:T(8,128)(2,1)S(1)} %collective-permute-done.19.refs_4_), channel_id=1, source_target_pairs={{0,7},{1,0},{2,1},{3,2},{4,3},{5,4},{6,5},{7,6},{8,15},{9,8},{10,9... | collective-permute-start | bytes 884744 | tf_op jit(solution)/shard_map/ppermute | solution.py:162
  231.0 7.8 %collective-permute-start.22 = (bf16[576,128]{1,0:T(8,128)(2,1)S(1)}, bf16[576,128]{1,0:T(8,128)(2,1)S(1)}, u32[]{:S(2)}, u32[]{:S(2)}) collective-permute-start(bf16[576,128]{1,0:T(8,128)(2,1)S(1)} %slice.46), channel_id=1, source_target_pairs={{0,1},{1,2},{2,3},{3,4},{4,5},{5,6},{6,7},{7,0},{8,9},{9,10},{10,1... | collective-permute-start | bytes 442376 | tf_op jit(solution)/shard_map/ppermute | solution.py:162
  233.8 9.0 %collective-permute-start.23 = (bf16[576,128]{1,0:T(8,128)(2,1)S(1)}, bf16[576,128]{1,0:T(8,128)(2,1)S(1)}, u32[]{:S(2)}, u32[]{:S(2)}) collective-permute-start(bf16[576,128]{1,0:T(8,128)(2,1)S(1)} %slice.47), channel_id=1, source_target_pairs={{0,7},{1,0},{2,1},{3,2},{4,3},{5,4},{6,5},{7,6},{8,15},{9,8},{10,9... | collective-permute-start | bytes 442376 | tf_op jit(solution)/shard_map/ppermute | solution.py:162
  248.4 20.4 %copy-start.28 = (s32[8,384]{1,0:T(8,128)S(1)}, s32[8,384]{1,0:T(8,128)}, u32[]{:S(2)}) copy-start(s32[8,384]{1,0:T(8,128)} %get-tuple-element.16) | copy-start | bytes 36868
  248.4 21.2 %copy-start.29 = (f32[384,2]{0,1:T(2,128)S(1)}, f32[384,2]{0,1:T(2,128)}, u32[]{:S(2)}) copy-start(f32[384,2]{0,1:T(2,128)} %param.13) | copy-start | bytes 9220
  248.4 56.5 %all-to-all-start.3 = ((bf16[32,72,128]{2,1,0:T(8,128)(2,1)}), bf16[32,72,128]{2,1,0:T(8,128)(2,1)S(1)}, u32[]{:S(2)}, u32[]{:S(2)}) async-start(bf16[32,72,128]{2,1,0:T(8,128)(2,1)} %get-tuple-element.17), calls=%async_computation.3 | async-start | bytes 1179648 | tf_op jit(solution)/shard_map/all_to_all | solution.py:154
  (11 other events, 84.6 us)

commit v2 on v0

v2 whole, which is shorter than its diff:
```python
import jax
import jax.numpy as jnp
from jax import lax
from jax.experimental import pallas as pl
from jax.experimental.pallas import tpu as pltpu
from jax.sharding import PartitionSpec as P


CAP = 36
MAIN = 32
SLAB = 72
HALF = 128
BF16 = jnp.bfloat16
F32 = jnp.float32
epsilon = 1e-06


def tile_row(shape):
    return lax.broadcasted_iota(jnp.int32, shape, len(shape) - 2)


def from_slabs(x):
    x = x.reshape(8, SLAB, HALF)
    left = x[:, :MAIN].reshape(8 * MAIN, HALF)
    right = x[:, MAIN : 2 * MAIN].reshape(8 * MAIN, HALF)
    rest = x[:, 2 * MAIN :].astype(F32).reshape(4, 2, 8, HALF)
    even, odd = rest[:, 0], rest[:, 1]
    low = tile_row((4, 8, HALF)) < CAP - MAIN
    rest_l = jnp.where(low, even, pltpu.roll(odd, 4, 1)).reshape(32, HALF).astype(BF16)
    rest_r = jnp.where(low, pltpu.roll(even, 4, 1), odd).reshape(32, HALF).astype(BF16)
    return jnp.concatenate([left, rest_l], axis=0), jnp.concatenate([right, rest_r], axis=0)


def to_slabs(rows, out, first):
    pairs = 8 * MAIN
    rest_l = rows[pairs:, :HALF].reshape(4, 8, HALF)
    rest_r = rows[pairs:, HALF:].reshape(4, 8, HALF)
    low = tile_row((4, 8, HALF)) < CAP - MAIN
    even = jnp.where(low, rest_l, pltpu.roll(rest_r, 4, 1))
    odd = jnp.where(low, pltpu.roll(rest_l, 4, 1), rest_r)
    rest = jnp.stack([even, odd], axis=1).reshape(8, 8, HALF)
    out[first : first + 8, 0:MAIN, :] = rows[:pairs, :HALF].reshape(8, MAIN, HALF).astype(BF16)
    out[first : first + 8, MAIN : 2 * MAIN, :] = rows[:pairs, HALF:].reshape(8, MAIN, HALF).astype(BF16)
    out[first : first + 8, 2 * MAIN :, :] = rest.astype(BF16)


def route_kernel(routes, tokens, outbound, rows):
    experts = outbound.shape[0]
    n_tok = tokens.shape[0]
    first, second = routes[0:1, :], routes[1:2, :]
    ids = lax.broadcasted_iota(jnp.int32, (experts, n_tok), 0)
    hit0 = (ids == first).astype(F32)
    hit1 = (ids == second).astype(F32)
    before = (
        lax.broadcasted_iota(jnp.int32, (n_tok, n_tok), 0)
        < lax.broadcasted_iota(jnp.int32, (n_tok, n_tok), 1)
    ).astype(F32).astype(BF16)
    count0 = jnp.dot(hit0.astype(BF16), before, preferred_element_type=F32)
    count1 = jnp.dot(hit1.astype(BF16), before, preferred_element_type=F32)
    count1 = count1 + jnp.sum(hit0, axis=1, keepdims=True)

    def row_of(expert, hit, count):
        slot = jnp.sum(hit * count, axis=0, keepdims=True).astype(jnp.int32)
        base = jnp.right_shift(expert, 3) * (8 * CAP)
        within = jnp.bitwise_and(expert, 7)
        main = within * MAIN + slot
        rest = 8 * MAIN + within * (CAP - MAIN) + (slot - MAIN)
        return base + jnp.where(slot < MAIN, main, rest)

    row0, row1 = row_of(first, hit0, count0), row_of(second, hit1, count1)
    rows[...] = jnp.concatenate([row0, row1] * 4, axis=0)
    part = 8 * CAP
    for g in range(experts // 8):
        ids = lax.broadcasted_iota(jnp.int32, (part, n_tok), 0) + g * part
        select = jnp.logical_or(ids == row0, ids == row1).astype(F32).astype(BF16)
        out = jnp.dot(select, tokens[...], preferred_element_type=F32)
        to_slabs(out, outbound, 8 * g)


def offsets_of(me):
    n_tp = 8
    return [(me + offset + n_tp) % n_tp for offset in (0, -1, 1, -2, 2, -3, 3, 4)]


def ffn_kernel(me, *refs):
    halves, weights, hidden = (refs[0:8], refs[8:16]), refs[16], refs[17]
    sources = offsets_of(me[0])
    features = weights.shape[0]
    part, slabs = 8 * CAP, 8 * SLAB
    for g in range(4):
        acc = jnp.zeros((part, 2 * HALF), F32)
        square = jnp.zeros((part, HALF), F32)
        for source, chunk in zip(sources, halves[g // 2]):
            left, right = from_slabs(chunk[(g % 2) * slabs : (g % 2 + 1) * slabs, :])
            w = weights[pl.ds(pl.multiple_of(source * 256, 256), 256), :]
            both = jnp.concatenate([left, right], axis=1)
            acc = acc + jnp.dot(both, w, preferred_element_type=F32)
            l32, r32 = left.astype(F32), right.astype(F32)
            square = square + (l32 * l32 + r32 * r32)
        total = jnp.sum(square, axis=1, keepdims=True)
        scale = lax.rsqrt(total * (1.0 / features) + epsilon)
        gate = acc[:, :HALF] * scale
        up = acc[:, HALF:] * scale
        value = gate / (1.0 + jnp.exp(-gate)) * up
        hidden[g * part : (g + 1) * part, :] = value.astype(BF16)


def down_kernel(me, *refs):
    chunks, weights, out = refs[0:8], refs[8], refs[9]
    sources = offsets_of(me[0])
    part = 8 * CAP
    pairs = ((0, 7), (1, 2), (3, 4), (5, 6))

    def rows_of(source):
        return weights[pl.ds(pl.multiple_of(source * HALF, HALF), HALF), :]

    for g in range(4):
        acc = jnp.zeros((part, 2 * HALF), F32)
        for m, n in pairs:
            h = jnp.concatenate([chunks[k][g * part : (g + 1) * part, :] for k in (m, n)], axis=1)
            w = jnp.concatenate([rows_of(sources[m]), rows_of(sources[n])], axis=0)
            acc = acc + jnp.dot(h, w, preferred_element_type=F32)
        to_slabs(acc, out, 8 * g)


def combine_kernel(rows, gains, returned, mixture):
    n_tok = rows.shape[0]
    slabs, part = 8 * SLAB, 8 * CAP
    sums = [jnp.zeros((n_tok, 2 * HALF), F32) for _ in range(2)]
    for g in range(returned.shape[0] // slabs):
        left, right = from_slabs(returned[g * slabs : (g + 1) * slabs, :])
        both = jnp.concatenate([left, right], axis=1)
        ids = lax.broadcasted_iota(jnp.int32, (n_tok, part), 1) + g * part
        for k in range(2):
            onehot = (ids == rows[:, k : k + 1]).astype(F32).astype(BF16)
            sums[k] = sums[k] + jnp.dot(onehot, both, preferred_element_type=F32)
    mixture[...] = (gains[:, 0:1] * sums[0] + gains[:, 1:2] * sums[1]).astype(BF16)


LIMIT = pltpu.CompilerParams(vmem_limit_bytes=16 * 1024 * 1024)


def in_vmem(*arrays):
    return [pltpu.with_memory_space_constraint(x, pltpu.VMEM) for x in arrays]


def all_to_all(x):
    return lax.all_to_all(x, "fs", split_axis=0, concat_axis=0, tiled=True)


def ring(x, last):
    n = lax.axis_size("tp")

    def step(v, side):
        shift = 1 if side == "r" else -1
        return lax.ppermute(v, "tp", [(d, (d + shift) % n) for d in range(n)])

    r1, l1 = step(x, "r"), step(x, "l")
    r2, l2 = step(r1, "r"), step(l1, "l")
    r3, l3 = step(r2, "r"), step(l2, "l")
    x4 = step(r3, "r") if last == "r" else step(l3, "l")
    return (x, r1, l1, r2, l2, r3, l3, x4)


def mixture_of_experts(tokens, norm_gain, gate_weight, up_weight, down_weight, routes, route_weights):
    experts, _, cols = gate_weight.shape
    n_tok = tokens.shape[0]
    me = lax.axis_index("tp").reshape(1).astype(jnp.int32)
    smem = pl.BlockSpec(memory_space=pltpu.SMEM)
    vmem = pl.BlockSpec(memory_space=pltpu.VMEM)
    slabs = (experts, SLAB, HALF)
    outbound, rows = pl.pallas_call(
        route_kernel,
        in_specs=[vmem, vmem],
        out_specs=(vmem, vmem),
        out_shape=(pltpu.VMEM(slabs, BF16), pltpu.VMEM((8, n_tok), jnp.int32)),
        name="route",
        compiler_params=LIMIT,
    )(*in_vmem(routes.T, tokens))
    arrived = all_to_all(outbound).reshape(experts * SLAB, HALF)
    gain = norm_gain[None, :, None]
    both_low = jnp.concatenate([gain * gate_weight, gain * up_weight], axis=2).astype(BF16)
    both_serve = all_to_all(both_low).reshape(-1, 2 * cols)
    cut = experts * SLAB // 2
    halves = ring(arrived[:cut], "r") + ring(arrived[cut:], "l")
    hidden = pl.pallas_call(
        ffn_kernel,
        in_specs=[smem] + [vmem] * 17,
        out_specs=vmem,
        out_shape=pltpu.VMEM((experts * CAP, cols), BF16),
        name="ffn",
        compiler_params=LIMIT,
    )(me, *in_vmem(*halves, both_serve))
    down_low = down_weight.astype(BF16)
    down_serve = all_to_all(down_low).reshape(-1, down_low.shape[2])
    expert_out = pl.pallas_call(
        down_kernel,
        in_specs=[smem] + [vmem] * 9,
        out_specs=vmem,
        out_shape=pltpu.VMEM(slabs, BF16),
        name="down",
        compiler_params=LIMIT,
    )(me, *in_vmem(*ring(hidden, "r"), down_serve))
    returned = all_to_all(expert_out).reshape(experts * SLAB, HALF)
    mixture = pl.pallas_call(
        combine_kernel,
        in_specs=[vmem] * 3,
        out_specs=vmem,
        out_shape=jax.ShapeDtypeStruct(tokens.shape, BF16),
        name="combine",
        compiler_params=LIMIT,
    )(*in_vmem(rows.T, route_weights, returned))
    gate_serve, up_serve = both_serve[None, :, :cols], both_serve[None, :, cols:]
    return (gate_serve, up_serve, down_serve[None], mixture)


def solution(mesh):
    block = ("grp", "fs")
    return jax.shard_map(
        mixture_of_experts,
        mesh=mesh,
        in_specs=(
            P(block, "tp"),
            P("fs"),
            P(None, "fs", "tp"),
            P(None, "fs", "tp"),
            P(None, "fs", "tp"),
            P(block, None),
            P(block, None),
        ),
        out_specs=(
            P(block, None, "tp"),
            P(block, None, "tp"),
            P(block, None, "tp"),
            P(block, "tp"),
        ),
        check_vma=False,
    )
```

time: 294 us -> 288 us (0.980)
  the two profiles are of different devices: /device:TPU:66 before, /device:TPU:65 now
where the time goes in v2:
time: 288 us; the launch traced here: 287 us
  starting transfers between devices  141 us (49%)
  waiting for transfers between devices  124 us (43%)
  Pallas kernels  9.28 us (3%)
  local copies, waits for them, and re-layouts  7.11 us (2%)
  other arithmetic  3.9 us (1%)
    all_to_all x4, waiting for transfers between devices, all_to_all(): return lax.all_to_all(x, 'fs', split_axis=0, concat_axis=0, tiled=True)  103 us
    all_to_all x4, starting transfers between devices, all_to_all(): return lax.all_to_all(x, 'fs', split_axis=0, concat_axis=0, tiled=True)  75.6 us
    ppermute x21, starting transfers between devices, step(): return lax.ppermute(v, 'tp', [(d, (d + shift) % n) for d in range(n)])  65.8 us
    ppermute x21, waiting for transfers between devices, step(): return lax.ppermute(v, 'tp', [(d, (d + shift) % n) for d in range(n)])  20.7 us
    unnamed x20, local copies, waits for them, and re-layouts  5.9 us
  transfers between devices with their start and end apart: 25, of which 10 were waited for; matrix products, arithmetic and copies ran while one was open for 2% of the time, Pallas kernels for 1%

profile of v2, /device:TPU:65, one launch (start us, length us, event | category | flops | bytes accessed | tf_op | source)
XLA Modules:
  0.0 286.9 jit_solution(516308661981297876)
XLA Ops:
  0.7 0.9 copy-done.4
  2.3 1.5 route.1
  3.8 45.2 %all-to-all-start.2 = ((bf16[32,72,128]{2,1,0:T(8,128)(2,1)}), bf16[32,72,128]{2,1,0:T(8,128)(2,1)S(1)}, u32[]{:S(2)}, u32[]{:S(2)}) async-start(bf16[32,72,128]{2,1,0:T(8,128)(2,1)} %get-tuple-element.7), calls=%async_computation.2 | async-start | bytes 1179648 | tf_op jit(solution)/shard_map/all_to_all | solution.py:148
  49.0 1.9 multiply_convert_fusion.1
  50.9 1.1 pad_maximum_fusion
  52.1 33.1 %all-to-all-done.2 = bf16[32,72,128]{2,1,0:T(8,128)(2,1)S(1)} async-done(((bf16[32,72,128]{2,1,0:T(8,128)(2,1)}), bf16[32,72,128]{2,1,0:T(8,128)(2,1)S(1)}, u32[]{:S(2)}, u32[]{:S(2)}) %all-to-all-start.2) | async-done | bytes 589856 | tf_op jit(solution)/shard_map/all_to_all | solution.py:148
  85.2 4.6 %all-to-all-start = ((bf16[32,64,256]{2,1,0:T(8,128)(2,1)}), bf16[32,64,256]{2,1,0:T(8,128)(2,1)S(1)}, u32[]{:S(2)}, u32[]{:S(2)}) async-start(bf16[32,64,256]{2,1,0:T(8,128)(2,1)} %pad_maximum_fusion), calls=%async_computation | async-start | bytes 2097152 | tf_op jit(solution)/shard_map/all_to_all | solution.py:148
  89.9 5.2 %collective-permute-start.8 = (bf16[1152,128]{1,0:T(8,128)(2,1)S(1)}, bf16[1152,128]{1,0:T(8,128)(2,1)S(1)}, u32[]{:S(2)}, u32[]{:S(2)}) collective-permute-start(bf16[1152,128]{1,0:T(8,128)(2,1)S(1)} %bitcast.18), channel_id=1, source_target_pairs={{0,7},{1,0},{2,1},{3,2},{4,3},{5,4},{6,5},{7,6},{8,15},{9,8},{10,9... | collective-permute-start | bytes 884744 | tf_op jit(solution)/shard_map/ppermute | solution.py:156
  95.1 2.0 collective-permute-start
  97.1 2.0 collective-permute-start.7
  99.0 4.6 %collective-permute-start.1 = (bf16[1152,128]{1,0:T(8,128)(2,1)S(1)}, bf16[1152,128]{1,0:T(8,128)(2,1)S(1)}, u32[]{:S(2)}, u32[]{:S(2)}) collective-permute-start(bf16[1152,128]{1,0:T(8,128)(2,1)S(1)} %bitcast.22), channel_id=1, source_target_pairs={{0,7},{1,0},{2,1},{3,2},{4,3},{5,4},{6,5},{7,6},{8,15},{9,8},{10,9... | collective-permute-start | bytes 884744 | tf_op jit(solution)/shard_map/ppermute | solution.py:156
  103.6 3.4 %collective-permute-start.10 = (bf16[1152,128]{1,0:T(8,128)(2,1)S(1)}, bf16[1152,128]{1,0:T(8,128)(2,1)}, u32[]{:S(2)}, u32[]{:S(2)}) collective-permute-start(bf16[1152,128]{1,0:T(8,128)(2,1)S(1)} %collective-permute-done.8.refs_10_), channel_id=1, source_target_pairs={{0,7},{1,0},{2,1},{3,2},{4,3},{5,4},{6,5},{7,6},{8,15},{9,8},{10,9... | collective-permute-start | bytes 884744 | tf_op jit(solution)/shard_map/ppermute | solution.py:156
  107.0 2.0 collective-permute-start.2
  109.0 0.9 convert_element_type.4
  109.9 35.6 %all-to-all-done = bf16[32,64,256]{2,1,0:T(8,128)(2,1)S(1)} async-done(((bf16[32,64,256]{2,1,0:T(8,128)(2,1)}), bf16[32,64,256]{2,1,0:T(8,128)(2,1)S(1)}, u32[]{:S(2)}, u32[]{:S(2)}) %all-to-all-start) | async-done | bytes 1048608 | tf_op jit(solution)/shard_map/all_to_all | solution.py:148
  145.5 4.9 %all-to-all-start.1 = ((bf16[32,32,256]{2,1,0:T(8,128)(2,1)}), bf16[32,32,256]{2,1,0:T(8,128)(2,1)S(1)}, u32[]{:S(2)}, u32[]{:S(2)}) async-start(bf16[32,32,256]{2,1,0:T(8,128)(2,1)} %convert_element_type.4), calls=%async_computation.1 | async-start | bytes 1048576 | tf_op jit(solution)/shard_map/all_to_all | solution.py:148
  150.4 2.8 collective-permute-start.9
  153.2 4.1 %collective-permute-start.3 = (bf16[1152,128]{1,0:T(8,128)(2,1)S(1)}, bf16[1152,128]{1,0:T(8,128)(2,1)}, u32[]{:S(2)}, u32[]{:S(2)}) collective-permute-start(bf16[1152,128]{1,0:T(8,128)(2,1)S(1)} %collective-permute-done.1.refs_2_), channel_id=1, source_target_pairs={{0,7},{1,0},{2,1},{3,2},{4,3},{5,4},{6,5},{7,6},{8,15},{9,8},{10,9... | collective-permute-start | bytes 884744 | tf_op jit(solution)/shard_map/ppermute | solution.py:156
  158.1 3.4 %collective-permute-start.12 = (bf16[1152,128]{1,0:T(8,128)(2,1)}, bf16[1152,128]{1,0:T(8,128)(2,1)}, u32[]{:S(2)}, u32[]{:S(2)}) collective-permute-start(bf16[1152,128]{1,0:T(8,128)(2,1)} %collective-permute-done.10.refs_12_), channel_id=1, source_target_pairs={{0,7},{1,0},{2,1},{3,2},{4,3},{5,4},{6,5},{7,6},{8,15},{9,8},{10,9... | collective-permute-start | bytes 884744 | tf_op jit(solution)/shard_map/ppermute | solution.py:156
  161.5 2.0 collective-permute-start.4
  163.5 2.0 collective-permute-start.11
  165.5 4.6 %collective-permute-start.5 = (bf16[1152,128]{1,0:T(8,128)(2,1)}, bf16[1152,128]{1,0:T(8,128)(2,1)S(1)}, u32[]{:S(2)}, u32[]{:S(2)}) collective-permute-start(bf16[1152,128]{1,0:T(8,128)(2,1)} %collective-permute-done.3.refs_4_), channel_id=1, source_target_pairs={{0,7},{1,0},{2,1},{3,2},{4,3},{5,4},{6,5},{7,6},{8,15},{9,8},{10,9... | collective-permute-start | bytes 884744 | tf_op jit(solution)/shard_map/ppermute | solution.py:156
  170.1 4.4 %collective-permute-start.13 = (bf16[1152,128]{1,0:T(8,128)(2,1)}, bf16[1152,128]{1,0:T(8,128)(2,1)}, u32[]{:S(2)}, u32[]{:S(2)}) collective-permute-start(bf16[1152,128]{1,0:T(8,128)(2,1)} %collective-permute-done.12.refs_14_), channel_id=1, source_target_pairs={{0,7},{1,0},{2,1},{3,2},{4,3},{5,4},{6,5},{7,6},{8,15},{9,8},{10,9... | collective-permute-start | bytes 884744 | tf_op jit(solution)/shard_map/ppermute | solution.py:156
  174.5 2.0 collective-permute-start.6
  176.5 1.5 collective-permute-done.11.refs_13_
  178.0 0.7 copy-done.2
  178.7 2.9 %collective-permute-done.13.refs_15_ = bf16[1152,128]{1,0:T(8,128)(2,1)} collective-permute-done((bf16[1152,128]{1,0:T(8,128)(2,1)}, bf16[1152,128]{1,0:T(8,128)(2,1)}, u32[]{:S(2)}, u32[]{:S(2)}) %collective-permute-start.13) | collective-permute-done | bytes 294944 | tf_op jit(solution)/shard_map/ppermute | solution.py:156
  181.6 2.7 collective-permute-done.6.refs_7_
  184.3 1.0 copy-done.1
  185.3 1.0 copy-done.3
  186.2 3.3 %ffn.1.refs_0_ = bf16[1152,128]{1,0:T(8,128)(2,1)S(1)} custom-call(s32[1]{0:T(128)} %bitcast.6.me, bf16[1152,128]{1,0:T(8,128)(2,1)S(1)} %bitcast.23, bf16[1152,128]{1,0:T(8,128)(2,1)S(1)} %collective-permute-done.refs_1_, bf16[1152,128]{1,0:T(8,128)(2,1)S(1)} %copy-done.1, bf16[1152,128]{1,0:T(8,128)(2,1)} %collective-permute-done.2.refs_3_, ...), custom_call_target="tpu_custom_call" | custom-call | tf_op jit(solution)/shard_map/ffn/pallas_call | solution.py:186
  189.6 2.0 collective-permute-start.14
  191.5 4.6 %collective-permute-start.15 = (bf16[1152,128]{1,0:T(8,128)(2,1)S(1)}, bf16[1152,128]{1,0:T(8,128)(2,1)S(1)}, u32[]{:S(2)}, u32[]{:S(2)}) collective-permute-start(bf16[1152,128]{1,0:T(8,128)(2,1)S(1)} %ffn.1.refs_0_), channel_id=1, source_target_pairs={{0,7},{1,0},{2,1},{3,2},{4,3},{5,4},{6,5},{7,6},{8,15},{9,8},{10,9... | collective-permute-start | bytes 884744 | tf_op jit(solution)/shard_map/ppermute | solution.py:156
  196.1 2.1 collective-permute-done.14.refs_1_
  198.3 1.9 collective-permute-start.16
  200.2 4.6 %collective-permute-start.17 = (bf16[1152,128]{1,0:T(8,128)(2,1)S(1)}, bf16[1152,128]{1,0:T(8,128)(2,1)S(1)}, u32[]{:S(2)}, u32[]{:S(2)}) collective-permute-start(bf16[1152,128]{1,0:T(8,128)(2,1)S(1)} %collective-permute-done.15.refs_2_), channel_id=1, source_target_pairs={{0,7},{1,0},{2,1},{3,2},{4,3},{5,4},{6,5},{7,6},{8,15},{9,8},{10,9... | collective-permute-start | bytes 884744 | tf_op jit(solution)/shard_map/ppermute | solution.py:156
  204.8 2.1 collective-permute-done.16.refs_3_
  207.0 1.9 collective-permute-start.18
  208.9 4.6 %collective-permute-start.19 = (bf16[1152,128]{1,0:T(8,128)(2,1)S(1)}, bf16[1152,128]{1,0:T(8,128)(2,1)}, u32[]{:S(2)}, u32[]{:S(2)}) collective-permute-start(bf16[1152,128]{1,0:T(8,128)(2,1)S(1)} %collective-permute-done.17.refs_4_), channel_id=1, source_target_pairs={{0,7},{1,0},{2,1},{3,2},{4,3},{5,4},{6,5},{7,6},{8,15},{9,8},{10,9... | collective-permute-start | bytes 884744 | tf_op jit(solution)/shard_map/ppermute | solution.py:156
  213.5 2.1 collective-permute-done.18.refs_5_
  215.7 1.9 collective-permute-start.20
  217.6 7.1 %collective-permute-done.20.refs_7_ = bf16[1152,128]{1,0:T(8,128)(2,1)} collective-permute-done((bf16[1152,128]{1,0:T(8,128)(2,1)S(1)}, bf16[1152,128]{1,0:T(8,128)(2,1)}, u32[]{:S(2)}, u32[]{:S(2)}) %collective-permute-start.20) | collective-permute-done | bytes 294944 | tf_op jit(solution)/shard_map/ppermute | solution.py:156
  224.8 2.7 down.1
  227.4 20.8 %all-to-all-start.3 = ((bf16[32,72,128]{2,1,0:T(8,128)(2,1)}), bf16[32,72,128]{2,1,0:T(8,128)(2,1)S(1)}, u32[]{:S(2)}, u32[]{:S(2)}) async-start(bf16[32,72,128]{2,1,0:T(8,128)(2,1)} %down.1), calls=%async_computation.3 | async-start | bytes 1179648 | tf_op jit(solution)/shard_map/all_to_all | solution.py:148
  248.5 1.0 slice_bitcast_fusion
  249.6 34.8 %all-to-all-done.3 = bf16[32,72,128]{2,1,0:T(8,128)(2,1)S(1)} async-done(((bf16[32,72,128]{2,1,0:T(8,128)(2,1)}), bf16[32,72,128]{2,1,0:T(8,128)(2,1)S(1)}, u32[]{:S(2)}, u32[]{:S(2)}) %all-to-all-start.3) | async-done | bytes 589856 | tf_op jit(solution)/shard_map/all_to_all | solution.py:148
  284.3 1.7 combine.1
  286.1 0.8 copy.14
  (32 shorter events, 1.8 us)
Async XLA Ops:
  0.6 48.4 %copy-start.8 = (f32[64]{0:T(128)S(1)}, f32[64]{0:T(128)}, u32[]{:S(2)}) copy-start(f32[64]{0:T(128)} %param.8) | copy-start | bytes 772
  0.6 0.9 copy-start.4
  1.6 0.7 copy-start.5
  3.8 81.4 %all-to-all-start.2 = ((bf16[32,72,128]{2,1,0:T(8,128)(2,1)}), bf16[32,72,128]{2,1,0:T(8,128)(2,1)S(1)}, u32[]{:S(2)}, u32[]{:S(2)}) async-start(bf16[32,72,128]{2,1,0:T(8,128)(2,1)} %get-tuple-element.7), calls=%async_computation.2 | async-start | bytes 1179648 | tf_op jit(solution)/shard_map/all_to_all | solution.py:148
  85.2 60.3 %all-to-all-start = ((bf16[32,64,256]{2,1,0:T(8,128)(2,1)}), bf16[32,64,256]{2,1,0:T(8,128)(2,1)S(1)}, u32[]{:S(2)}, u32[]{:S(2)}) async-start(bf16[32,64,256]{2,1,0:T(8,128)(2,1)} %pad_maximum_fusion), calls=%async_computation | async-start | bytes 2097152 | tf_op jit(solution)/shard_map/all_to_all | solution.py:148
  89.8 19.2 %copy-start.6 = (f32[32,32,256]{2,1,0:T(8,128)S(1)}, f32[32,32,256]{2,1,0:T(8,128)}, u32[]{:S(2)}) copy-start(f32[32,32,256]{2,1,0:T(8,128)} %param.11) | copy-start | bytes 3145732
  89.9 13.7 %collective-permute-start.8 = (bf16[1152,128]{1,0:T(8,128)(2,1)S(1)}, bf16[1152,128]{1,0:T(8,128)(2,1)S(1)}, u32[]{:S(2)}, u32[]{:S(2)}) collective-permute-start(bf16[1152,128]{1,0:T(8,128)(2,1)S(1)} %bitcast.18), channel_id=1, source_target_pairs={{0,7},{1,0},{2,1},{3,2},{4,3},{5,4},{6,5},{7,6},{8,15},{9,8},{10,9... | collective-permute-start | bytes 884744 | tf_op jit(solution)/shard_map/ppermute | solution.py:156
  95.1 11.9 %collective-permute-start = (bf16[1152,128]{1,0:T(8,128)(2,1)S(1)}, bf16[1152,128]{1,0:T(8,128)(2,1)S(1)}, u32[]{:S(2)}, u32[]{:S(2)}) collective-permute-start(bf16[1152,128]{1,0:T(8,128)(2,1)S(1)} %bitcast.21), channel_id=1, source_target_pairs={{0,1},{1,2},{2,3},{3,4},{4,5},{5,6},{6,7},{7,0},{8,9},{9,10},{10,1... | collective-permute-start | bytes 884744 | tf_op jit(solution)/shard_map/ppermute | solution.py:156
  97.1 53.3 %collective-permute-start.7 = (bf16[1152,128]{1,0:T(8,128)(2,1)S(1)}, bf16[1152,128]{1,0:T(8,128)(2,1)S(1)}, u32[]{:S(2)}, u32[]{:S(2)}) collective-permute-start(bf16[1152,128]{1,0:T(8,128)(2,1)S(1)} %bitcast.19), channel_id=1, source_target_pairs={{0,1},{1,2},{2,3},{3,4},{4,5},{5,6},{6,7},{7,0},{8,9},{9,10},{10,1... | collective-permute-start | bytes 884744 | tf_op jit(solution)/shard_map/ppermute | solution.py:156
  99.0 54.2 %collective-permute-start.1 = (bf16[1152,128]{1,0:T(8,128)(2,1)S(1)}, bf16[1152,128]{1,0:T(8,128)(2,1)S(1)}, u32[]{:S(2)}, u32[]{:S(2)}) collective-permute-start(bf16[1152,128]{1,0:T(8,128)(2,1)S(1)} %bitcast.22), channel_id=1, source_target_pairs={{0,7},{1,0},{2,1},{3,2},{4,3},{5,4},{6,5},{7,6},{8,15},{9,8},{10,9... | collective-permute-start | bytes 884744 | tf_op jit(solution)/shard_map/ppermute | solution.py:156
  103.6 54.5 %collective-permute-start.10 = (bf16[1152,128]{1,0:T(8,128)(2,1)S(1)}, bf16[1152,128]{1,0:T(8,128)(2,1)}, u32[]{:S(2)}, u32[]{:S(2)}) collective-permute-start(bf16[1152,128]{1,0:T(8,128)(2,1)S(1)} %collective-permute-done.8.refs_10_), channel_id=1, source_target_pairs={{0,7},{1,0},{2,1},{3,2},{4,3},{5,4},{6,5},{7,6},{8,15},{9,8},{10,9... | collective-permute-start | bytes 884744 | tf_op jit(solution)/shard_map/ppermute | solution.py:156
  107.0 54.5 %collective-permute-start.2 = (bf16[1152,128]{1,0:T(8,128)(2,1)S(1)}, bf16[1152,128]{1,0:T(8,128)(2,1)}, u32[]{:S(2)}, u32[]{:S(2)}) collective-permute-start(bf16[1152,128]{1,0:T(8,128)(2,1)S(1)} %collective-permute-done.refs_1_), channel_id=1, source_target_pairs={{0,1},{1,2},{2,3},{3,4},{4,5},{5,6},{6,7},{7,0},{8,9},{9,10},{10,1... | collective-permute-start | bytes 884744 | tf_op jit(solution)/shard_map/ppermute | solution.py:156
  145.5 72.2 %all-to-all-start.1 = ((bf16[32,32,256]{2,1,0:T(8,128)(2,1)}), bf16[32,32,256]{2,1,0:T(8,128)(2,1)S(1)}, u32[]{:S(2)}, u32[]{:S(2)}) async-start(bf16[32,32,256]{2,1,0:T(8,128)(2,1)} %convert_element_type.4), calls=%async_computation.1 | async-start | bytes 1048576 | tf_op jit(solution)/shard_map/all_to_all | solution.py:148
  150.4 13.1 %collective-permute-start.9 = (bf16[1152,128]{1,0:T(8,128)(2,1)S(1)}, bf16[1152,128]{1,0:T(8,128)(2,1)}, u32[]{:S(2)}, u32[]{:S(2)}) collective-permute-start(bf16[1152,128]{1,0:T(8,128)(2,1)S(1)} %collective-permute-done.7.refs_9_), channel_id=1, source_target_pairs={{0,1},{1,2},{2,3},{3,4},{4,5},{5,6},{6,7},{7,0},{8,9},{9,10},{10,1... | collective-permute-start | bytes 884744 | tf_op jit(solution)/shard_map/ppermute | solution.py:156
  153.2 12.2 %collective-permute-start.3 = (bf16[1152,128]{1,0:T(8,128)(2,1)S(1)}, bf16[1152,128]{1,0:T(8,128)(2,1)}, u32[]{:S(2)}, u32[]{:S(2)}) collective-permute-start(bf16[1152,128]{1,0:T(8,128)(2,1)S(1)} %collective-permute-done.1.refs_2_), channel_id=1, source_target_pairs={{0,7},{1,0},{2,1},{3,2},{4,3},{5,4},{6,5},{7,6},{8,15},{9,8},{10,9... | collective-permute-start | bytes 884744 | tf_op jit(solution)/shard_map/ppermute | solution.py:156
  157.4 0.7 copy-start
  158.1 12.0 %collective-permute-start.12 = (bf16[1152,128]{1,0:T(8,128)(2,1)}, bf16[1152,128]{1,0:T(8,128)(2,1)}, u32[]{:S(2)}, u32[]{:S(2)}) collective-permute-start(bf16[1152,128]{1,0:T(8,128)(2,1)} %collective-permute-done.10.refs_12_), channel_id=1, source_target_pairs={{0,7},{1,0},{2,1},{3,2},{4,3},{5,4},{6,5},{7,6},{8,15},{9,8},{10,9... | collective-permute-start | bytes 884744 | tf_op jit(solution)/shard_map/ppermute | solution.py:156
  161.5 13.0 %collective-permute-start.4 = (bf16[1152,128]{1,0:T(8,128)(2,1)}, bf16[1152,128]{1,0:T(8,128)(2,1)}, u32[]{:S(2)}, u32[]{:S(2)}) collective-permute-start(bf16[1152,128]{1,0:T(8,128)(2,1)} %collective-permute-done.2.refs_3_), channel_id=1, source_target_pairs={{0,1},{1,2},{2,3},{3,4},{4,5},{5,6},{6,7},{7,0},{8,9},{9,10},{10,1... | collective-permute-start | bytes 884744 | tf_op jit(solution)/shard_map/ppermute | solution.py:156
  163.5 14.5 %collective-permute-start.11 = (bf16[1152,128]{1,0:T(8,128)(2,1)}, bf16[1152,128]{1,0:T(8,128)(2,1)}, u32[]{:S(2)}, u32[]{:S(2)}) collective-permute-start(bf16[1152,128]{1,0:T(8,128)(2,1)} %collective-permute-done.9.refs_11_), channel_id=1, source_target_pairs={{0,1},{1,2},{2,3},{3,4},{4,5},{5,6},{6,7},{7,0},{8,9},{9,10},{10,1... | collective-permute-start | bytes 884744 | tf_op jit(solution)/shard_map/ppermute | solution.py:156
  165.5 12.5 %collective-permute-start.5 = (bf16[1152,128]{1,0:T(8,128)(2,1)}, bf16[1152,128]{1,0:T(8,128)(2,1)S(1)}, u32[]{:S(2)}, u32[]{:S(2)}) collective-permute-start(bf16[1152,128]{1,0:T(8,128)(2,1)} %collective-permute-done.3.refs_4_), channel_id=1, source_target_pairs={{0,7},{1,0},{2,1},{3,2},{4,3},{5,4},{6,5},{7,6},{8,15},{9,8},{10,9... | collective-permute-start | bytes 884744 | tf_op jit(solution)/shard_map/ppermute | solution.py:156
  170.1 11.5 %collective-permute-start.13 = (bf16[1152,128]{1,0:T(8,128)(2,1)}, bf16[1152,128]{1,0:T(8,128)(2,1)}, u32[]{:S(2)}, u32[]{:S(2)}) collective-permute-start(bf16[1152,128]{1,0:T(8,128)(2,1)} %collective-permute-done.12.refs_14_), channel_id=1, source_target_pairs={{0,7},{1,0},{2,1},{3,2},{4,3},{5,4},{6,5},{7,6},{8,15},{9,8},{10,9... | collective-permute-start | bytes 884744 | tf_op jit(solution)/shard_map/ppermute | solution.py:156
  174.5 9.8 %collective-permute-start.6 = (bf16[1152,128]{1,0:T(8,128)(2,1)}, bf16[1152,128]{1,0:T(8,128)(2,1)}, u32[]{:S(2)}, u32[]{:S(2)}) collective-permute-start(bf16[1152,128]{1,0:T(8,128)(2,1)} %collective-permute-done.4.refs_5_), channel_id=1, source_target_pairs={{0,1},{1,2},{2,3},{3,4},{4,5},{5,6},{6,7},{7,0},{8,9},{9,10},{10,1... | collective-permute-start | bytes 884744 | tf_op jit(solution)/shard_map/ppermute | solution.py:156
  178.0 0.7 copy-start.2
  184.3 1.0 copy-start.1
  185.3 1.0 copy-start.3
  189.6 8.7 %collective-permute-start.14 = (bf16[1152,128]{1,0:T(8,128)(2,1)S(1)}, bf16[1152,128]{1,0:T(8,128)(2,1)S(1)}, u32[]{:S(2)}, u32[]{:S(2)}) collective-permute-start(bf16[1152,128]{1,0:T(8,128)(2,1)S(1)} %ffn.1.refs_0_), channel_id=1, source_target_pairs={{0,1},{1,2},{2,3},{3,4},{4,5},{5,6},{6,7},{7,0},{8,9},{9,10},{10,1... | collective-permute-start | bytes 884744 | tf_op jit(solution)/shard_map/ppermute | solution.py:156
  191.5 8.7 %collective-permute-start.15 = (bf16[1152,128]{1,0:T(8,128)(2,1)S(1)}, bf16[1152,128]{1,0:T(8,128)(2,1)S(1)}, u32[]{:S(2)}, u32[]{:S(2)}) collective-permute-start(bf16[1152,128]{1,0:T(8,128)(2,1)S(1)} %ffn.1.refs_0_), channel_id=1, source_target_pairs={{0,7},{1,0},{2,1},{3,2},{4,3},{5,4},{6,5},{7,6},{8,15},{9,8},{10,9... | collective-permute-start | bytes 884744 | tf_op jit(solution)/shard_map/ppermute | solution.py:156
  198.3 8.7 %collective-permute-start.16 = (bf16[1152,128]{1,0:T(8,128)(2,1)S(1)}, bf16[1152,128]{1,0:T(8,128)(2,1)S(1)}, u32[]{:S(2)}, u32[]{:S(2)}) collective-permute-start(bf16[1152,128]{1,0:T(8,128)(2,1)S(1)} %collective-permute-done.14.refs_1_), channel_id=1, source_target_pairs={{0,1},{1,2},{2,3},{3,4},{4,5},{5,6},{6,7},{7,0},{8,9},{9,10},{10,1... | collective-permute-start | bytes 884744 | tf_op jit(solution)/shard_map/ppermute | solution.py:156
  200.2 8.7 %collective-permute-start.17 = (bf16[1152,128]{1,0:T(8,128)(2,1)S(1)}, bf16[1152,128]{1,0:T(8,128)(2,1)S(1)}, u32[]{:S(2)}, u32[]{:S(2)}) collective-permute-start(bf16[1152,128]{1,0:T(8,128)(2,1)S(1)} %collective-permute-done.15.refs_2_), channel_id=1, source_target_pairs={{0,7},{1,0},{2,1},{3,2},{4,3},{5,4},{6,5},{7,6},{8,15},{9,8},{10,9... | collective-permute-start | bytes 884744 | tf_op jit(solution)/shard_map/ppermute | solution.py:156
  207.0 8.7 %collective-permute-start.18 = (bf16[1152,128]{1,0:T(8,128)(2,1)S(1)}, bf16[1152,128]{1,0:T(8,128)(2,1)S(1)}, u32[]{:S(2)}, u32[]{:S(2)}) collective-permute-start(bf16[1152,128]{1,0:T(8,128)(2,1)S(1)} %collective-permute-done.16.refs_3_), channel_id=1, source_target_pairs={{0,1},{1,2},{2,3},{3,4},{4,5},{5,6},{6,7},{7,0},{8,9},{9,10},{10,1... | collective-permute-start | bytes 884744 | tf_op jit(solution)/shard_map/ppermute | solution.py:156
  208.9 8.7 %collective-permute-start.19 = (bf16[1152,128]{1,0:T(8,128)(2,1)S(1)}, bf16[1152,128]{1,0:T(8,128)(2,1)}, u32[]{:S(2)}, u32[]{:S(2)}) collective-permute-start(bf16[1152,128]{1,0:T(8,128)(2,1)S(1)} %collective-permute-done.17.refs_4_), channel_id=1, source_target_pairs={{0,7},{1,0},{2,1},{3,2},{4,3},{5,4},{6,5},{7,6},{8,15},{9,8},{10,9... | collective-permute-start | bytes 884744 | tf_op jit(solution)/shard_map/ppermute | solution.py:156
  215.7 9.1 %collective-permute-start.20 = (bf16[1152,128]{1,0:T(8,128)(2,1)S(1)}, bf16[1152,128]{1,0:T(8,128)(2,1)}, u32[]{:S(2)}, u32[]{:S(2)}) collective-permute-start(bf16[1152,128]{1,0:T(8,128)(2,1)S(1)} %collective-permute-done.18.refs_5_), channel_id=1, source_target_pairs={{0,1},{1,2},{2,3},{3,4},{4,5},{5,6},{6,7},{7,0},{8,9},{9,10},{10,1... | collective-permute-start | bytes 884744 | tf_op jit(solution)/shard_map/ppermute | solution.py:156
  227.4 21.0 %copy-start.7 = (f32[384,2]{0,1:T(2,128)S(1)}, f32[384,2]{0,1:T(2,128)}, u32[]{:S(2)}) copy-start(f32[384,2]{0,1:T(2,128)} %param.13) | copy-start | bytes 9220
  227.4 56.9 %all-to-all-start.3 = ((bf16[32,72,128]{2,1,0:T(8,128)(2,1)}), bf16[32,72,128]{2,1,0:T(8,128)(2,1)S(1)}, u32[]{:S(2)}, u32[]{:S(2)}) async-start(bf16[32,72,128]{2,1,0:T(8,128)(2,1)} %down.1), calls=%async_computation.3 | async-start | bytes 1179648 | tf_op jit(solution)/shard_map/all_to_all | solution.py:148

commit v3 on v2

--- a/solution.py
+++ b/solution.py
@@ -82,17 +82,46 @@
     return [(me + offset + n_tp) % n_tp for offset in (0, -1, 1, -2, 2, -3, 3, 4)]
 
 
+def join_pieces(mine, pieces, serve):
+    count, rows = len(pieces), pieces[0].shape[1]
+    for n, piece in enumerate(pieces):
+        place = (mine + n) % count
+        serve[:, pl.ds(pl.multiple_of(place * rows, rows), rows), :] = piece[...]
+
+
 def ffn_kernel(me, *refs):
-    halves, weights, hidden = (refs[0:8], refs[8:16]), refs[16], refs[17]
+    chunks, pieces = refs[0:16], refs[16:-5]
+    hidden, serve, held, chunk_done, piece_done = refs[-5:]
     sources = offsets_of(me[0])
-    features = weights.shape[0]
+    features = serve.shape[0] * serve.shape[1]
+    count, rows = len(pieces), pieces[0].shape[1]
+    spread = 2 * HALF // serve.shape[1]
     part, slabs = 8 * CAP, 8 * SLAB
+
+    def fetch_piece(n):
+        place = (me[1] + n) % count
+        target = serve.at[:, pl.ds(pl.multiple_of(place * rows, rows), rows), :]
+        return pltpu.make_async_copy(pieces[n], target, piece_done.at[n])
+
+    def fetch(g, k):
+        n = 8 * (g // 2) + k
+        span = pl.ds((g % 2) * slabs, slabs)
+        return pltpu.make_async_copy(chunks[n].at[span, :], held.at[g, k], chunk_done.at[g, k])
+
+    for n in range(count):
+        fetch_piece(n).start()
+    for g in range(4):
+        for k in range(8):
+            fetch(g, k).start()
+    for n in range(count):
+        fetch_piece(n).wait()
     for g in range(4):
         acc = jnp.zeros((part, 2 * HALF), F32)
         square = jnp.zeros((part, HALF), F32)
-        for source, chunk in zip(sources, halves[g // 2]):
-            left, right = from_slabs(chunk[(g % 2) * slabs : (g % 2 + 1) * slabs, :])
-            w = weights[pl.ds(pl.multiple_of(source * 256, 256), 256), :]
+        for k, source in enumerate(sources):
+            fetch(g, k).wait()
+            left, right = from_slabs(held[g, k])
+            w = serve[pl.ds(source * spread, spread)].reshape(2 * HALF, 2 * HALF)
             both = jnp.concatenate([left, right], axis=1)
             acc = acc + jnp.dot(both, w, preferred_element_type=F32)
             l32, r32 = left.astype(F32), right.astype(F32)
@@ -106,13 +135,17 @@
 
 
 def down_kernel(me, *refs):
-    chunks, weights, out = refs[0:8], refs[8], refs[9]
+    chunks, pieces, out, serve_out, serve, done = refs[0:8], refs[8:-4], *refs[-4:]
     sources = offsets_of(me[0])
+    join_pieces(me[1], pieces, serve)
+    copy = pltpu.make_async_copy(serve, serve_out, done)
+    copy.start()
+    spread = HALF // serve.shape[1]
     part = 8 * CAP
     pairs = ((0, 7), (1, 2), (3, 4), (5, 6))
 
     def rows_of(source):
-        return weights[pl.ds(pl.multiple_of(source * HALF, HALF), HALF), :]
+        return serve[pl.ds(source * spread, spread)].reshape(HALF, 2 * HALF)
 
     for g in range(4):
         acc = jnp.zeros((part, 2 * HALF), F32)
@@ -121,6 +154,7 @@
             w = jnp.concatenate([rows_of(sources[m]), rows_of(sources[n])], axis=0)
             acc = acc + jnp.dot(h, w, preferred_element_type=F32)
         to_slabs(acc, out, 8 * g)
+    copy.wait()
 
 
 def combine_kernel(rows, gains, returned, mixture):
@@ -144,6 +178,10 @@
     return [pltpu.with_memory_space_constraint(x, pltpu.VMEM) for x in arrays]
 
 
+def in_hbm(*arrays):
+    return [pltpu.with_memory_space_constraint(x, pltpu.HBM) for x in arrays]
+
+
 def all_to_all(x):
     return lax.all_to_all(x, "fs", split_axis=0, concat_axis=0, tiled=True)
 
@@ -163,9 +201,13 @@
 
 
 def mixture_of_experts(tokens, norm_gain, gate_weight, up_weight, down_weight, routes, route_weights):
-    experts, _, cols = gate_weight.shape
+    experts, rows_in, cols = gate_weight.shape
+    rows_down, down_cols = down_weight.shape[1:]
     n_tok = tokens.shape[0]
-    me = lax.axis_index("tp").reshape(1).astype(jnp.int32)
+    groups = lax.axis_size("grp")
+    count = 2 if groups % 2 == 0 else 1
+    mine = lax.axis_index("grp") % count
+    me = jnp.stack([lax.axis_index("tp"), mine]).astype(jnp.int32)
     smem = pl.BlockSpec(memory_space=pltpu.SMEM)
     vmem = pl.BlockSpec(memory_space=pltpu.VMEM)
     slabs = (experts, SLAB, HALF)
@@ -176,31 +218,57 @@
         out_shape=(pltpu.VMEM(slabs, BF16), pltpu.VMEM((8, n_tok), jnp.int32)),
         name="route",
         compiler_params=LIMIT,
-    )(*in_vmem(routes.T, tokens))
+    )(routes.T, tokens)
     arrived = all_to_all(outbound).reshape(experts * SLAB, HALF)
-    gain = norm_gain[None, :, None]
-    both_low = jnp.concatenate([gain * gate_weight, gain * up_weight], axis=2).astype(BF16)
-    both_serve = all_to_all(both_low).reshape(-1, 2 * cols)
+
+    def piece(x, axis):
+        size = x.shape[axis] // count
+        return lax.dynamic_slice_in_dim(x, mine * size, size, axis)
+
+    def swapped(x):
+        if count == 1:
+            return [x]
+        return [x, lax.ppermute(x, "grp", [(g, g ^ 1) for g in range(groups)])]
+
+    gain = piece(norm_gain, 0)[None, :, None]
+    both_low = jnp.concatenate([gain * piece(gate_weight, 1), gain * piece(up_weight, 1)], axis=2)
+    weights_low = jnp.concatenate([both_low, piece(down_weight, 1)], axis=1).astype(BF16)
+    arrived_weights = all_to_all(weights_low)
+    both_pieces = swapped(arrived_weights[:, : rows_in // count])
+    down_pieces = swapped(arrived_weights[:, rows_in // count :])
     cut = experts * SLAB // 2
     halves = ring(arrived[:cut], "r") + ring(arrived[cut:], "l")
-    hidden = pl.pallas_call(
+    hidden, both_serve = pl.pallas_call(
         ffn_kernel,
-        in_specs=[smem] + [vmem] * 17,
-        out_specs=vmem,
-        out_shape=pltpu.VMEM((experts * CAP, cols), BF16),
+        in_specs=[smem] + [pl.BlockSpec(memory_space=pl.ANY)] * (16 + count),
+        out_specs=(vmem, vmem),
+        out_shape=(
+            pltpu.VMEM((experts * CAP, cols), BF16),
+            pltpu.VMEM((experts, rows_in, 2 * cols), BF16),
+        ),
+        scratch_shapes=[
+            pltpu.VMEM((4, 8, 8 * SLAB, HALF), BF16),
+            pltpu.SemaphoreType.DMA((4, 8)),
+            pltpu.SemaphoreType.DMA((count,)),
+        ],
         name="ffn",
         compiler_params=LIMIT,
-    )(me, *in_vmem(*halves, both_serve))
-    down_low = down_weight.astype(BF16)
-    down_serve = all_to_all(down_low).reshape(-1, down_low.shape[2])
-    expert_out = pl.pallas_call(
+    )(me, *in_hbm(*halves, *both_pieces))
+    expert_out, down_serve = pl.pallas_call(
         down_kernel,
-        in_specs=[smem] + [vmem] * 9,
-        out_specs=vmem,
-        out_shape=pltpu.VMEM(slabs, BF16),
+        in_specs=[smem] + [vmem] * (8 + count),
+        out_specs=(vmem, pl.BlockSpec(memory_space=pl.ANY)),
+        out_shape=(
+            pltpu.VMEM(slabs, BF16),
+            jax.ShapeDtypeStruct((experts, rows_down, down_cols), BF16),
+        ),
+        scratch_shapes=[
+            pltpu.VMEM((experts, rows_down, down_cols), BF16),
+            pltpu.SemaphoreType.DMA,
+        ],
         name="down",
         compiler_params=LIMIT,
-    )(me, *in_vmem(*ring(hidden, "r"), down_serve))
+    )(me, *in_vmem(*ring(hidden, "r"), *down_pieces))
     returned = all_to_all(expert_out).reshape(experts * SLAB, HALF)
     mixture = pl.pallas_call(
         combine_kernel,
@@ -210,8 +278,9 @@
         name="combine",
         compiler_params=LIMIT,
     )(*in_vmem(rows.T, route_weights, returned))
-    gate_serve, up_serve = both_serve[None, :, :cols], both_serve[None, :, cols:]
-    return (gate_serve, up_serve, down_serve[None], mixture)
+    both_serve = both_serve.reshape(1, -1, 2 * cols)
+    gate_serve, up_serve = both_serve[:, :, :cols], both_serve[:, :, cols:]
+    return (gate_serve, up_serve, down_serve.reshape(1, -1, down_cols), mixture)
 
 
 def solution(mesh):

time: 288 us -> 259 us (0.90)
  waiting for transfers between devices: 124 us -> 101 us
  starting transfers between devices: 141 us -> 135 us
  Pallas kernels: 9.28 us -> 13.8 us
    all_to_all x4 -> x3, waiting for transfers between devices: 103 us -> 79.2 us  [all_to_all(): return lax.all_to_all(x, 'fs', split_axis=0, concat_axis=0, tiled=True)]
    all_to_all x4 -> x3, starting transfers between devices: 75.6 us -> 64 us  [all_to_all(): return lax.all_to_all(x, 'fs', split_axis=0, concat_axis=0, tiled=True)]
    ppermute x0 -> x2, starting transfers between devices: none -> 6.61 us  [swapped(): return [x, lax.ppermute(x, 'grp', [(g, g ^ 1) for g in range(groups)])]]
    pallas_call x2, Pallas kernels: 6 us -> 10.5 us  [the longest x1 7.72 us: mixture_of_experts(): pl.pallas_call(ffn_kernel, in_specs=[smem] + [pl.BlockSpec(memory_space=p...]
    ppermute x0 -> x2, waiting for transfers between devices: none -> 4.52 us  [swapped(): return [x, lax.ppermute(x, 'grp', [(g, g ^ 1) for g in range(groups)])]]
    unnamed x20 -> x25, local copies, waits for them, and re-layouts: 5.9 us -> 1.89 us
  transfers between devices with their start and end apart: 25 -> 26, of which waited for: 10 -> 12; matrix products, arithmetic and copies ran while one was open for 2% -> 2% of each run, Pallas kernels for 1% -> 0%
where the time goes in v3:
time: 259 us; the launch traced here: 258 us
  starting transfers between devices  135 us (52%)
  waiting for transfers between devices  101 us (39%)
  Pallas kernels  13.8 us (5%)
  local copies, waits for them, and re-layouts  4.24 us (2%)
    all_to_all x3, waiting for transfers between devices, all_to_all(): return lax.all_to_all(x, 'fs', split_axis=0, concat_axis=0, tiled=True)  79.2 us
    ppermute x21, starting transfers between devices, step(): return lax.ppermute(v, 'tp', [(d, (d + shift) % n) for d in range(n)])  64.6 us
    all_to_all x3, starting transfers between devices, all_to_all(): return lax.all_to_all(x, 'fs', split_axis=0, concat_axis=0, tiled=True)  64 us
    ppermute x21, waiting for transfers between devices, step(): return lax.ppermute(v, 'tp', [(d, (d + shift) % n) for d in range(n)])  17.8 us
    pallas_call x1, Pallas kernels, mixture_of_experts(): pl.pallas_call(ffn_kernel, in_specs=[smem] + [pl.BlockSpec(memory_space=p...  7.72 us
    ppermute x2, starting transfers between devices, swapped(): return [x, lax.ppermute(x, 'grp', [(g, g ^ 1) for g in range(groups)])]  6.61 us
  transfers between devices with their start and end apart: 26, of which 12 were waited for; matrix products, arithmetic and copies ran while one was open for 2% of the time, Pallas kernels for 0%

profile of v3, /device:TPU:65, one launch (start us, length us, event | category | flops | bytes accessed | tf_op | source)
XLA Modules:
  0.0 258.2 jit_solution(16293036446995864632)
XLA Ops:
  0.7 1.0 copy-done.1
  1.7 0.7 copy-done.2
  2.4 1.5 route.1
  3.9 45.2 %all-to-all-start = ((bf16[32,72,128]{2,1,0:T(8,128)(2,1)}), bf16[32,72,128]{2,1,0:T(8,128)(2,1)S(1)}, u32[]{:S(2)}, u32[]{:S(2)}) async-start(bf16[32,72,128]{2,1,0:T(8,128)(2,1)} %get-tuple-element.10), calls=%async_computation | async-start | bytes 1179648 | tf_op jit(solution)/shard_map/all_to_all | solution.py:186
  49.3 1.3 multiply_convert_fusion.1
  50.6 1.0 pad_maximum_fusion
  51.5 33.8 %all-to-all-done = bf16[32,72,128]{2,1,0:T(8,128)(2,1)S(1)} async-done(((bf16[32,72,128]{2,1,0:T(8,128)(2,1)}), bf16[32,72,128]{2,1,0:T(8,128)(2,1)S(1)}, u32[]{:S(2)}, u32[]{:S(2)}) %all-to-all-start) | async-done | bytes 589856 | tf_op jit(solution)/shard_map/all_to_all | solution.py:186
  85.3 4.6 %all-to-all-start.1 = ((bf16[32,48,256]{2,1,0:T(8,128)(2,1)}), bf16[32,48,256]{2,1,0:T(8,128)(2,1)S(1)}, u32[]{:S(2)}, u32[]{:S(2)}) async-start(bf16[32,48,256]{2,1,0:T(8,128)(2,1)} %pad_maximum_fusion), calls=%async_computation.1 | async-start | bytes 1572864 | tf_op jit(solution)/shard_map/all_to_all | solution.py:186
  90.0 5.0 %collective-permute-start.8 = (bf16[1152,128]{1,0:T(8,128)(2,1)S(1)}, bf16[1152,128]{1,0:T(8,128)(2,1)S(1)}, u32[]{:S(2)}, u32[]{:S(2)}) collective-permute-start(bf16[1152,128]{1,0:T(8,128)(2,1)S(1)} %bitcast.13), channel_id=1, source_target_pairs={{0,7},{1,0},{2,1},{3,2},{4,3},{5,4},{6,5},{7,6},{8,15},{9,8},{10,9... | collective-permute-start | bytes 884744 | tf_op jit(solution)/shard_map/ppermute | solution.py:194
  95.1 2.0 collective-permute-start
  97.0 2.0 collective-permute-start.7
  99.0 4.6 %collective-permute-start.1 = (bf16[1152,128]{1,0:T(8,128)(2,1)S(1)}, bf16[1152,128]{1,0:T(8,128)(2,1)}, u32[]{:S(2)}, u32[]{:S(2)}) collective-permute-start(bf16[1152,128]{1,0:T(8,128)(2,1)S(1)} %bitcast.17), channel_id=1, source_target_pairs={{0,7},{1,0},{2,1},{3,2},{4,3},{5,4},{6,5},{7,6},{8,15},{9,8},{10,9... | collective-permute-start | bytes 884744 | tf_op jit(solution)/shard_map/ppermute | solution.py:194
  103.6 3.4 %collective-permute-start.10 = (bf16[1152,128]{1,0:T(8,128)(2,1)S(1)}, bf16[1152,128]{1,0:T(8,128)(2,1)}, u32[]{:S(2)}, u32[]{:S(2)}) collective-permute-start(bf16[1152,128]{1,0:T(8,128)(2,1)S(1)} %collective-permute-done.8.refs_10_), channel_id=1, source_target_pairs={{0,7},{1,0},{2,1},{3,2},{4,3},{5,4},{6,5},{7,6},{8,15},{9,8},{10,9... | collective-permute-start | bytes 884744 | tf_op jit(solution)/shard_map/ppermute | solution.py:194
  107.0 2.0 collective-permute-start.2
  109.0 2.9 %collective-permute-done.7.refs_9_ = bf16[1152,128]{1,0:T(8,128)(2,1)} collective-permute-done((bf16[1152,128]{1,0:T(8,128)(2,1)S(1)}, bf16[1152,128]{1,0:T(8,128)(2,1)}, u32[]{:S(2)}, u32[]{:S(2)}) %collective-permute-start.7) | collective-permute-done | bytes 294944 | tf_op jit(solution)/shard_map/ppermute | solution.py:194
  111.9 1.9 collective-permute-start.9
  113.8 4.6 %collective-permute-start.3 = (bf16[1152,128]{1,0:T(8,128)(2,1)}, bf16[1152,128]{1,0:T(8,128)(2,1)}, u32[]{:S(2)}, u32[]{:S(2)}) collective-permute-start(bf16[1152,128]{1,0:T(8,128)(2,1)} %collective-permute-done.1.refs_2_), channel_id=1, source_target_pairs={{0,7},{1,0},{2,1},{3,2},{4,3},{5,4},{6,5},{7,6},{8,15},{9,8},{10,9... | collective-permute-start | bytes 884744 | tf_op jit(solution)/shard_map/ppermute | solution.py:194
  118.5 2.0 collective-permute-start.12
  120.4 3.4 %collective-permute-start.4 = (bf16[1152,128]{1,0:T(8,128)(2,1)}, bf16[1152,128]{1,0:T(8,128)(2,1)}, u32[]{:S(2)}, u32[]{:S(2)}) collective-permute-start(bf16[1152,128]{1,0:T(8,128)(2,1)} %collective-permute-done.2.refs_3_), channel_id=1, source_target_pairs={{0,1},{1,2},{2,3},{3,4},{4,5},{5,6},{6,7},{7,0},{8,9},{9,10},{10,1... | collective-permute-start | bytes 884744 | tf_op jit(solution)/shard_map/ppermute | solution.py:194
  123.8 10.6 %all-to-all-done.1 = bf16[32,48,256]{2,1,0:T(8,128)(2,1)S(1)} async-done(((bf16[32,48,256]{2,1,0:T(8,128)(2,1)}), bf16[32,48,256]{2,1,0:T(8,128)(2,1)S(1)}, u32[]{:S(2)}, u32[]{:S(2)}) %all-to-all-start.1) | async-done | bytes 786464 | tf_op jit(solution)/shard_map/all_to_all | solution.py:186
  134.5 4.0 %collective-permute-start.14 = (bf16[32,32,256]{2,1,0:T(8,128)(2,1)S(1)}, bf16[32,32,256]{2,1,0:T(8,128)(2,1)}, u32[]{:S(2)}, u32[]{:S(2)}) collective-permute-start(bf16[32,32,256]{2,1,0:T(8,128)(2,1)S(1)} %slice.34.refs_16_), channel_id=1, source_target_pairs={{0,256},{256,0},{1,257},{257,1},{2,258},{258,2},{3,259},{259,3},{4... | collective-permute-start | bytes 1572872 | tf_op jit(solution)/shard_map/ppermute | solution.py:231
  138.5 3.3 %collective-permute-start.11 = (bf16[1152,128]{1,0:T(8,128)(2,1)}, bf16[1152,128]{1,0:T(8,128)(2,1)}, u32[]{:S(2)}, u32[]{:S(2)}) collective-permute-start(bf16[1152,128]{1,0:T(8,128)(2,1)} %collective-permute-done.9.refs_11_), channel_id=1, source_target_pairs={{0,1},{1,2},{2,3},{3,4},{4,5},{5,6},{6,7},{7,0},{8,9},{9,10},{10,1... | collective-permute-start | bytes 884744 | tf_op jit(solution)/shard_map/ppermute | solution.py:194
  141.8 4.1 %collective-permute-start.5 = (bf16[1152,128]{1,0:T(8,128)(2,1)}, bf16[1152,128]{1,0:T(8,128)(2,1)}, u32[]{:S(2)}, u32[]{:S(2)}) collective-permute-start(bf16[1152,128]{1,0:T(8,128)(2,1)} %collective-permute-done.3.refs_4_), channel_id=1, source_target_pairs={{0,7},{1,0},{2,1},{3,2},{4,3},{5,4},{6,5},{7,6},{8,15},{9,8},{10,9... | collective-permute-start | bytes 884744 | tf_op jit(solution)/shard_map/ppermute | solution.py:194
  146.0 3.4 %collective-permute-start.13 = (bf16[1152,128]{1,0:T(8,128)(2,1)}, bf16[1152,128]{1,0:T(8,128)(2,1)}, u32[]{:S(2)}, u32[]{:S(2)}) collective-permute-start(bf16[1152,128]{1,0:T(8,128)(2,1)} %collective-permute-done.12.refs_14_), channel_id=1, source_target_pairs={{0,7},{1,0},{2,1},{3,2},{4,3},{5,4},{6,5},{7,6},{8,15},{9,8},{10,9... | collective-permute-start | bytes 884744 | tf_op jit(solution)/shard_map/ppermute | solution.py:194
  149.4 2.0 collective-permute-start.6
  151.5 6.3 %collective-permute-done.13.refs_15_ = bf16[1152,128]{1,0:T(8,128)(2,1)} collective-permute-done((bf16[1152,128]{1,0:T(8,128)(2,1)}, bf16[1152,128]{1,0:T(8,128)(2,1)}, u32[]{:S(2)}, u32[]{:S(2)}) %collective-permute-start.13) | collective-permute-done | bytes 294944 | tf_op jit(solution)/shard_map/ppermute | solution.py:194
  157.8 1.6 collective-permute-done.6.refs_7_
  159.5 7.7 %ffn.1 = (bf16[1152,128]{1,0:T(8,128)(2,1)S(1)}, bf16[32,64,256]{2,1,0:T(8,128)(2,1)S(1)}) custom-call(s32[2]{0:T(128)S(1)} %pad_add_fusion.me, bf16[1152,128]{1,0:T(8,128)(2,1)} %bitcast.18, bf16[1152,128]{1,0:T(8,128)(2,1)} %copy-done.8, bf16[1152,128]{1,0:T(8,128)(2,1)} %collective-permute-done.1.refs_2_, ...), custom_call_target="tpu_custom_call" | custom-call | tf_op jit(solution)/shard_map/ffn/pallas_call | solution.py:241
  167.2 2.0 collective-permute-start.15
  169.1 4.6 %collective-permute-start.16 = (bf16[1152,128]{1,0:T(8,128)(2,1)S(1)}, bf16[1152,128]{1,0:T(8,128)(2,1)S(1)}, u32[]{:S(2)}, u32[]{:S(2)}) collective-permute-start(bf16[1152,128]{1,0:T(8,128)(2,1)S(1)} %get-tuple-element.12.refs_0_), channel_id=1, source_target_pairs={{0,7},{1,0},{2,1},{3,2},{4,3},{5,4},{6,5},{7,6},{8,15},{9,8},{10,9... | collective-permute-start | bytes 884744 | tf_op jit(solution)/shard_map/ppermute | solution.py:194
  173.7 2.1 collective-permute-done.15.refs_1_
  175.9 1.9 collective-permute-start.17
  177.8 0.3 collective-permute-done.16.refs_2_
  178.2 4.3 %collective-permute-start.18 = (bf16[1152,128]{1,0:T(8,128)(2,1)S(1)}, bf16[1152,128]{1,0:T(8,128)(2,1)S(1)}, u32[]{:S(2)}, u32[]{:S(2)}) collective-permute-start(bf16[1152,128]{1,0:T(8,128)(2,1)S(1)} %collective-permute-done.16.refs_2_), channel_id=1, source_target_pairs={{0,7},{1,0},{2,1},{3,2},{4,3},{5,4},{6,5},{7,6},{8,15},{9,8},{10,9... | collective-permute-start | bytes 884744 | tf_op jit(solution)/shard_map/ppermute | solution.py:194
  182.5 2.1 collective-permute-done.17.refs_3_
  184.6 1.9 collective-permute-start.19
  186.5 0.2 collective-permute-done.18.refs_4_
  186.7 4.4 %collective-permute-start.20 = (bf16[1152,128]{1,0:T(8,128)(2,1)S(1)}, bf16[1152,128]{1,0:T(8,128)(2,1)S(1)}, u32[]{:S(2)}, u32[]{:S(2)}) collective-permute-start(bf16[1152,128]{1,0:T(8,128)(2,1)S(1)} %collective-permute-done.18.refs_4_), channel_id=1, source_target_pairs={{0,7},{1,0},{2,1},{3,2},{4,3},{5,4},{6,5},{7,6},{8,15},{9,8},{10,9... | collective-permute-start | bytes 884744 | tf_op jit(solution)/shard_map/ppermute | solution.py:194
  191.2 2.1 collective-permute-done.19.refs_5_
  193.3 1.9 collective-permute-start.21
  195.2 1.0 slice.37.refs_8_
  196.2 2.6 %collective-permute-start.22 = (bf16[32,16,256]{2,1,0:T(8,128)(2,1)S(1)}, bf16[32,16,256]{2,1,0:T(8,128)(2,1)S(1)}, u32[]{:S(2)}, u32[]{:S(2)}) collective-permute-start(bf16[32,16,256]{2,1,0:T(8,128)(2,1)S(1)} %slice.37.refs_8_), channel_id=1, source_target_pairs={{0,256},{256,0},{1,257},{257,1},{2,258},{258,2},{3,259},{259,3},{4... | collective-permute-start | bytes 786440 | tf_op jit(solution)/shard_map/ppermute | solution.py:231
  198.8 4.5 %collective-permute-done.22.refs_9_ = bf16[32,16,256]{2,1,0:T(8,128)(2,1)S(1)} collective-permute-done((bf16[32,16,256]{2,1,0:T(8,128)(2,1)S(1)}, bf16[32,16,256]{2,1,0:T(8,128)(2,1)S(1)}, u32[]{:S(2)}, u32[]{:S(2)}) %collective-permute-start.22) | collective-permute-done | bytes 262176 | tf_op jit(solution)/shard_map/ppermute | solution.py:231
  203.4 2.8 %down.1 = (bf16[32,72,128]{2,1,0:T(8,128)(2,1)}, bf16[32,32,256]{2,1,0:T(8,128)(2,1)}) custom-call(s32[2]{0:T(128)S(1)} %pad_add_fusion.me, bf16[1152,128]{1,0:T(8,128)(2,1)S(1)} %get-tuple-element.12.refs_0_, bf16[1152,128]{1,0:T(8,128)(2,1)S(1)} %collective-permute-done.15.refs_1_, bf16[1152,128]{1,0:T(8,128)(2,1)S(1)} %collective-permute-done.16.refs_2_, ...), custom_call_target="tpu_custom_call" | custom-call | tf_op jit(solution)/shard_map/down/pallas_call | solution.py:257
  206.2 14.2 %all-to-all-start.2 = ((bf16[32,72,128]{2,1,0:T(8,128)(2,1)}), bf16[32,72,128]{2,1,0:T(8,128)(2,1)S(1)}, u32[]{:S(2)}, u32[]{:S(2)}) async-start(bf16[32,72,128]{2,1,0:T(8,128)(2,1)} %get-tuple-element.15), calls=%async_computation.2 | async-start | bytes 1179648 | tf_op jit(solution)/shard_map/all_to_all | solution.py:186
  220.6 1.0 fusion
  221.7 34.8 %all-to-all-done.2 = bf16[32,72,128]{2,1,0:T(8,128)(2,1)S(1)} async-done(((bf16[32,72,128]{2,1,0:T(8,128)(2,1)}), bf16[32,72,128]{2,1,0:T(8,128)(2,1)S(1)}, u32[]{:S(2)}, u32[]{:S(2)}) %all-to-all-start.2) | async-done | bytes 589856 | tf_op jit(solution)/shard_map/all_to_all | solution.py:186
  256.4 1.7 combine.1
  (43 shorter events, 0.6 us)
Async XLA Ops:
  0.6 48.6 %copy-start = (f32[32,32,256]{2,1,0:T(8,128)S(1)}, f32[32,32,256]{2,1,0:T(8,128)}, u32[]{:S(2)}) copy-start(f32[32,32,256]{2,1,0:T(8,128)} %param.11) | copy-start | bytes 3145732
  0.6 48.5 %copy-start.11 = (f32[64]{0:T(128)S(1)}, f32[64]{0:T(128)}, u32[]{:S(2)}) copy-start(f32[64]{0:T(128)} %param.8) | copy-start | bytes 772
  0.7 1.0 copy-start.1
  1.7 0.7 copy-start.2
  2.4 46.9 %copy-start.9 = (f32[32,64,128]{2,1,0:T(8,128)S(1)}, f32[32,64,128]{2,1,0:T(8,128)}, u32[]{:S(2)}) copy-start(f32[32,64,128]{2,1,0:T(8,128)} %param.9) | copy-start | bytes 3145732
  3.9 81.4 %all-to-all-start = ((bf16[32,72,128]{2,1,0:T(8,128)(2,1)}), bf16[32,72,128]{2,1,0:T(8,128)(2,1)S(1)}, u32[]{:S(2)}, u32[]{:S(2)}) async-start(bf16[32,72,128]{2,1,0:T(8,128)(2,1)} %get-tuple-element.10), calls=%async_computation | async-start | bytes 1179648 | tf_op jit(solution)/shard_map/all_to_all | solution.py:186
  85.3 49.1 %all-to-all-start.1 = ((bf16[32,48,256]{2,1,0:T(8,128)(2,1)}), bf16[32,48,256]{2,1,0:T(8,128)(2,1)S(1)}, u32[]{:S(2)}, u32[]{:S(2)}) async-start(bf16[32,48,256]{2,1,0:T(8,128)(2,1)} %pad_maximum_fusion), calls=%async_computation.1 | async-start | bytes 1572864 | tf_op jit(solution)/shard_map/all_to_all | solution.py:186
  90.0 30.4 %copy-start.6 = (bf16[16,72,128]{2,1,0:T(8,128)(2,1)}, bf16[16,72,128]{2,1,0:T(8,128)(2,1)S(1)}, u32[]{:S(2)}) copy-start(bf16[16,72,128]{2,1,0:T(8,128)(2,1)S(1)} %get-tuple-element.19) | copy-start | bytes 884740
  90.0 69.4 %copy-start.5 = (bf16[16,72,128]{2,1,0:T(8,128)(2,1)}, bf16[16,72,128]{2,1,0:T(8,128)(2,1)S(1)}, u32[]{:S(2)}) copy-start(bf16[16,72,128]{2,1,0:T(8,128)(2,1)S(1)} %get-tuple-element.18) | copy-start | bytes 884740
  90.0 13.6 %collective-permute-start.8 = (bf16[1152,128]{1,0:T(8,128)(2,1)S(1)}, bf16[1152,128]{1,0:T(8,128)(2,1)S(1)}, u32[]{:S(2)}, u32[]{:S(2)}) collective-permute-start(bf16[1152,128]{1,0:T(8,128)(2,1)S(1)} %bitcast.13), channel_id=1, source_target_pairs={{0,7},{1,0},{2,1},{3,2},{4,3},{5,4},{6,5},{7,6},{8,15},{9,8},{10,9... | collective-permute-start | bytes 884744 | tf_op jit(solution)/shard_map/ppermute | solution.py:194
  95.1 12.0 %collective-permute-start = (bf16[1152,128]{1,0:T(8,128)(2,1)S(1)}, bf16[1152,128]{1,0:T(8,128)(2,1)S(1)}, u32[]{:S(2)}, u32[]{:S(2)}) collective-permute-start(bf16[1152,128]{1,0:T(8,128)(2,1)S(1)} %bitcast.16), channel_id=1, source_target_pairs={{0,1},{1,2},{2,3},{3,4},{4,5},{5,6},{6,7},{7,0},{8,9},{9,10},{10,1... | collective-permute-start | bytes 884744 | tf_op jit(solution)/shard_map/ppermute | solution.py:194
  97.0 14.9 %collective-permute-start.7 = (bf16[1152,128]{1,0:T(8,128)(2,1)S(1)}, bf16[1152,128]{1,0:T(8,128)(2,1)}, u32[]{:S(2)}, u32[]{:S(2)}) collective-permute-start(bf16[1152,128]{1,0:T(8,128)(2,1)S(1)} %bitcast.14), channel_id=1, source_target_pairs={{0,1},{1,2},{2,3},{3,4},{4,5},{5,6},{6,7},{7,0},{8,9},{9,10},{10,1... | collective-permute-start | bytes 884744 | tf_op jit(solution)/shard_map/ppermute | solution.py:194
  99.0 14.9 %collective-permute-start.1 = (bf16[1152,128]{1,0:T(8,128)(2,1)S(1)}, bf16[1152,128]{1,0:T(8,128)(2,1)}, u32[]{:S(2)}, u32[]{:S(2)}) collective-permute-start(bf16[1152,128]{1,0:T(8,128)(2,1)S(1)} %bitcast.17), channel_id=1, source_target_pairs={{0,7},{1,0},{2,1},{3,2},{4,3},{5,4},{6,5},{7,6},{8,15},{9,8},{10,9... | collective-permute-start | bytes 884744 | tf_op jit(solution)/shard_map/ppermute | solution.py:194
  103.6 55.8 %copy-start.7 = (bf16[1152,128]{1,0:T(8,128)(2,1)}, bf16[1152,128]{1,0:T(8,128)(2,1)S(1)}, u32[]{:S(2)}) copy-start(bf16[1152,128]{1,0:T(8,128)(2,1)S(1)} %collective-permute-done.8.refs_10_) | copy-start | bytes 884740
  103.6 14.8 %collective-permute-start.10 = (bf16[1152,128]{1,0:T(8,128)(2,1)S(1)}, bf16[1152,128]{1,0:T(8,128)(2,1)}, u32[]{:S(2)}, u32[]{:S(2)}) collective-permute-start(bf16[1152,128]{1,0:T(8,128)(2,1)S(1)} %collective-permute-done.8.refs_10_), channel_id=1, source_target_pairs={{0,7},{1,0},{2,1},{3,2},{4,3},{5,4},{6,5},{7,6},{8,15},{9,8},{10,9... | collective-permute-start | bytes 884744 | tf_op jit(solution)/shard_map/ppermute | solution.py:194
  107.0 52.4 %copy-start.8 = (bf16[1152,128]{1,0:T(8,128)(2,1)}, bf16[1152,128]{1,0:T(8,128)(2,1)S(1)}, u32[]{:S(2)}) copy-start(bf16[1152,128]{1,0:T(8,128)(2,1)S(1)} %collective-permute-done.refs_1_) | copy-start | bytes 884740
  107.0 13.4 %collective-permute-start.2 = (bf16[1152,128]{1,0:T(8,128)(2,1)S(1)}, bf16[1152,128]{1,0:T(8,128)(2,1)}, u32[]{:S(2)}, u32[]{:S(2)}) collective-permute-start(bf16[1152,128]{1,0:T(8,128)(2,1)S(1)} %collective-permute-done.refs_1_), channel_id=1, source_target_pairs={{0,1},{1,2},{2,3},{3,4},{4,5},{5,6},{6,7},{7,0},{8,9},{9,10},{10,1... | collective-permute-start | bytes 884744 | tf_op jit(solution)/shard_map/ppermute | solution.py:194
  111.9 26.7 %collective-permute-start.9 = (bf16[1152,128]{1,0:T(8,128)(2,1)}, bf16[1152,128]{1,0:T(8,128)(2,1)}, u32[]{:S(2)}, u32[]{:S(2)}) collective-permute-start(bf16[1152,128]{1,0:T(8,128)(2,1)} %collective-permute-done.7.refs_9_), channel_id=1, source_target_pairs={{0,1},{1,2},{2,3},{3,4},{4,5},{5,6},{6,7},{7,0},{8,9},{9,10},{10,1... | collective-permute-start | bytes 884744 | tf_op jit(solution)/shard_map/ppermute | solution.py:194
  113.8 28.0 %collective-permute-start.3 = (bf16[1152,128]{1,0:T(8,128)(2,1)}, bf16[1152,128]{1,0:T(8,128)(2,1)}, u32[]{:S(2)}, u32[]{:S(2)}) collective-permute-start(bf16[1152,128]{1,0:T(8,128)(2,1)} %collective-permute-done.1.refs_2_), channel_id=1, source_target_pairs={{0,7},{1,0},{2,1},{3,2},{4,3},{5,4},{6,5},{7,6},{8,15},{9,8},{10,9... | collective-permute-start | bytes 884744 | tf_op jit(solution)/shard_map/ppermute | solution.py:194
  118.5 27.5 %collective-permute-start.12 = (bf16[1152,128]{1,0:T(8,128)(2,1)}, bf16[1152,128]{1,0:T(8,128)(2,1)}, u32[]{:S(2)}, u32[]{:S(2)}) collective-permute-start(bf16[1152,128]{1,0:T(8,128)(2,1)} %collective-permute-done.10.refs_12_), channel_id=1, source_target_pairs={{0,7},{1,0},{2,1},{3,2},{4,3},{5,4},{6,5},{7,6},{8,15},{9,8},{10,9... | collective-permute-start | bytes 884744 | tf_op jit(solution)/shard_map/ppermute | solution.py:194
  120.4 29.0 %collective-permute-start.4 = (bf16[1152,128]{1,0:T(8,128)(2,1)}, bf16[1152,128]{1,0:T(8,128)(2,1)}, u32[]{:S(2)}, u32[]{:S(2)}) collective-permute-start(bf16[1152,128]{1,0:T(8,128)(2,1)} %collective-permute-done.2.refs_3_), channel_id=1, source_target_pairs={{0,1},{1,2},{2,3},{3,4},{4,5},{5,6},{6,7},{7,0},{8,9},{9,10},{10,1... | collective-permute-start | bytes 884744 | tf_op jit(solution)/shard_map/ppermute | solution.py:194
  134.5 16.9 %copy-start.3 = (bf16[32,48,256]{2,1,0:T(8,128)(2,1)}, bf16[32,48,256]{2,1,0:T(8,128)(2,1)S(1)}, u32[]{:S(2)}) copy-start(bf16[32,48,256]{2,1,0:T(8,128)(2,1)S(1)} %all-to-all-done.1) | copy-start | bytes 2359300
  134.5 24.9 %copy-start.4 = (bf16[32,32,256]{2,1,0:T(8,128)(2,1)}, bf16[32,32,256]{2,1,0:T(8,128)(2,1)S(1)}, u32[]{:S(2)}) copy-start(bf16[32,32,256]{2,1,0:T(8,128)(2,1)S(1)} %slice.34.refs_16_) | copy-start | bytes 1572868
  134.5 24.9 %collective-permute-start.14 = (bf16[32,32,256]{2,1,0:T(8,128)(2,1)S(1)}, bf16[32,32,256]{2,1,0:T(8,128)(2,1)}, u32[]{:S(2)}, u32[]{:S(2)}) collective-permute-start(bf16[32,32,256]{2,1,0:T(8,128)(2,1)S(1)} %slice.34.refs_16_), channel_id=1, source_target_pairs={{0,256},{256,0},{1,257},{257,1},{2,258},{258,2},{3,259},{259,3},{4... | collective-permute-start | bytes 1572872 | tf_op jit(solution)/shard_map/ppermute | solution.py:231
  138.5 12.9 %collective-permute-start.11 = (bf16[1152,128]{1,0:T(8,128)(2,1)}, bf16[1152,128]{1,0:T(8,128)(2,1)}, u32[]{:S(2)}, u32[]{:S(2)}) collective-permute-start(bf16[1152,128]{1,0:T(8,128)(2,1)} %collective-permute-done.9.refs_11_), channel_id=1, source_target_pairs={{0,1},{1,2},{2,3},{3,4},{4,5},{5,6},{6,7},{7,0},{8,9},{9,10},{10,1... | collective-permute-start | bytes 884744 | tf_op jit(solution)/shard_map/ppermute | solution.py:194
  141.8 9.6 %collective-permute-start.5 = (bf16[1152,128]{1,0:T(8,128)(2,1)}, bf16[1152,128]{1,0:T(8,128)(2,1)}, u32[]{:S(2)}, u32[]{:S(2)}) collective-permute-start(bf16[1152,128]{1,0:T(8,128)(2,1)} %collective-permute-done.3.refs_4_), channel_id=1, source_target_pairs={{0,7},{1,0},{2,1},{3,2},{4,3},{5,4},{6,5},{7,6},{8,15},{9,8},{10,9... | collective-permute-start | bytes 884744 | tf_op jit(solution)/shard_map/ppermute | solution.py:194
  146.0 11.8 %collective-permute-start.13 = (bf16[1152,128]{1,0:T(8,128)(2,1)}, bf16[1152,128]{1,0:T(8,128)(2,1)}, u32[]{:S(2)}, u32[]{:S(2)}) collective-permute-start(bf16[1152,128]{1,0:T(8,128)(2,1)} %collective-permute-done.12.refs_14_), channel_id=1, source_target_pairs={{0,7},{1,0},{2,1},{3,2},{4,3},{5,4},{6,5},{7,6},{8,15},{9,8},{10,9... | collective-permute-start | bytes 884744 | tf_op jit(solution)/shard_map/ppermute | solution.py:194
  149.4 10.0 %collective-permute-start.6 = (bf16[1152,128]{1,0:T(8,128)(2,1)}, bf16[1152,128]{1,0:T(8,128)(2,1)}, u32[]{:S(2)}, u32[]{:S(2)}) collective-permute-start(bf16[1152,128]{1,0:T(8,128)(2,1)} %collective-permute-done.4.refs_5_), channel_id=1, source_target_pairs={{0,1},{1,2},{2,3},{3,4},{4,5},{5,6},{6,7},{7,0},{8,9},{9,10},{10,1... | collective-permute-start | bytes 884744 | tf_op jit(solution)/shard_map/ppermute | solution.py:194
  167.2 8.7 %collective-permute-start.15 = (bf16[1152,128]{1,0:T(8,128)(2,1)S(1)}, bf16[1152,128]{1,0:T(8,128)(2,1)S(1)}, u32[]{:S(2)}, u32[]{:S(2)}) collective-permute-start(bf16[1152,128]{1,0:T(8,128)(2,1)S(1)} %get-tuple-element.12.refs_0_), channel_id=1, source_target_pairs={{0,1},{1,2},{2,3},{3,4},{4,5},{5,6},{6,7},{7,0},{8,9},{9,10},{10,1... | collective-permute-start | bytes 884744 | tf_op jit(solution)/shard_map/ppermute | solution.py:194
  169.1 9.0 %collective-permute-start.16 = (bf16[1152,128]{1,0:T(8,128)(2,1)S(1)}, bf16[1152,128]{1,0:T(8,128)(2,1)S(1)}, u32[]{:S(2)}, u32[]{:S(2)}) collective-permute-start(bf16[1152,128]{1,0:T(8,128)(2,1)S(1)} %get-tuple-element.12.refs_0_), channel_id=1, source_target_pairs={{0,7},{1,0},{2,1},{3,2},{4,3},{5,4},{6,5},{7,6},{8,15},{9,8},{10,9... | collective-permute-start | bytes 884744 | tf_op jit(solution)/shard_map/ppermute | solution.py:194
  175.9 8.7 %collective-permute-start.17 = (bf16[1152,128]{1,0:T(8,128)(2,1)S(1)}, bf16[1152,128]{1,0:T(8,128)(2,1)S(1)}, u32[]{:S(2)}, u32[]{:S(2)}) collective-permute-start(bf16[1152,128]{1,0:T(8,128)(2,1)S(1)} %collective-permute-done.15.refs_1_), channel_id=1, source_target_pairs={{0,1},{1,2},{2,3},{3,4},{4,5},{5,6},{6,7},{7,0},{8,9},{9,10},{10,1... | collective-permute-start | bytes 884744 | tf_op jit(solution)/shard_map/ppermute | solution.py:194
  178.2 8.6 %collective-permute-start.18 = (bf16[1152,128]{1,0:T(8,128)(2,1)S(1)}, bf16[1152,128]{1,0:T(8,128)(2,1)S(1)}, u32[]{:S(2)}, u32[]{:S(2)}) collective-permute-start(bf16[1152,128]{1,0:T(8,128)(2,1)S(1)} %collective-permute-done.16.refs_2_), channel_id=1, source_target_pairs={{0,7},{1,0},{2,1},{3,2},{4,3},{5,4},{6,5},{7,6},{8,15},{9,8},{10,9... | collective-permute-start | bytes 884744 | tf_op jit(solution)/shard_map/ppermute | solution.py:194
  184.6 8.7 %collective-permute-start.19 = (bf16[1152,128]{1,0:T(8,128)(2,1)S(1)}, bf16[1152,128]{1,0:T(8,128)(2,1)S(1)}, u32[]{:S(2)}, u32[]{:S(2)}) collective-permute-start(bf16[1152,128]{1,0:T(8,128)(2,1)S(1)} %collective-permute-done.17.refs_3_), channel_id=1, source_target_pairs={{0,1},{1,2},{2,3},{3,4},{4,5},{5,6},{6,7},{7,0},{8,9},{9,10},{10,1... | collective-permute-start | bytes 884744 | tf_op jit(solution)/shard_map/ppermute | solution.py:194
  186.7 16.6 %collective-permute-start.20 = (bf16[1152,128]{1,0:T(8,128)(2,1)S(1)}, bf16[1152,128]{1,0:T(8,128)(2,1)S(1)}, u32[]{:S(2)}, u32[]{:S(2)}) collective-permute-start(bf16[1152,128]{1,0:T(8,128)(2,1)S(1)} %collective-permute-done.18.refs_4_), channel_id=1, source_target_pairs={{0,7},{1,0},{2,1},{3,2},{4,3},{5,4},{6,5},{7,6},{8,15},{9,8},{10,9... | collective-permute-start | bytes 884744 | tf_op jit(solution)/shard_map/ppermute | solution.py:194
  193.3 10.1 %collective-permute-start.21 = (bf16[1152,128]{1,0:T(8,128)(2,1)S(1)}, bf16[1152,128]{1,0:T(8,128)(2,1)S(1)}, u32[]{:S(2)}, u32[]{:S(2)}) collective-permute-start(bf16[1152,128]{1,0:T(8,128)(2,1)S(1)} %collective-permute-done.19.refs_5_), channel_id=1, source_target_pairs={{0,1},{1,2},{2,3},{3,4},{4,5},{5,6},{6,7},{7,0},{8,9},{9,10},{10,1... | collective-permute-start | bytes 884744 | tf_op jit(solution)/shard_map/ppermute | solution.py:194
  196.2 7.1 %collective-permute-start.22 = (bf16[32,16,256]{2,1,0:T(8,128)(2,1)S(1)}, bf16[32,16,256]{2,1,0:T(8,128)(2,1)S(1)}, u32[]{:S(2)}, u32[]{:S(2)}) collective-permute-start(bf16[32,16,256]{2,1,0:T(8,128)(2,1)S(1)} %slice.37.refs_8_), channel_id=1, source_target_pairs={{0,256},{256,0},{1,257},{257,1},{2,258},{258,2},{3,259},{259,3},{4... | collective-permute-start | bytes 786440 | tf_op jit(solution)/shard_map/ppermute | solution.py:231
  206.2 14.3 %copy-start.10 = (f32[384,2]{0,1:T(2,128)S(1)}, f32[384,2]{0,1:T(2,128)}, u32[]{:S(2)}) copy-start(f32[384,2]{0,1:T(2,128)} %param.13) | copy-start | bytes 9220
  206.2 50.3 %all-to-all-start.2 = ((bf16[32,72,128]{2,1,0:T(8,128)(2,1)}), bf16[32,72,128]{2,1,0:T(8,128)(2,1)S(1)}, u32[]{:S(2)}, u32[]{:S(2)}) async-start(bf16[32,72,128]{2,1,0:T(8,128)(2,1)} %get-tuple-element.15), calls=%async_computation.2 | async-start | bytes 1179648 | tf_op jit(solution)/shard_map/all_to_all | solution.py:186

commit v4 on v3

--- a/solution.py
+++ b/solution.py
@@ -44,9 +44,14 @@
     out[first : first + 8, 2 * MAIN :, :] = rest.astype(BF16)
 
 
-def route_kernel(routes, tokens, outbound, rows):
+def route_kernel(routes_in, tokens_in, outbound, rows, routes, tokens, done):
     experts = outbound.shape[0]
     n_tok = tokens.shape[0]
+    fetch_routes = pltpu.make_async_copy(routes_in, routes, done.at[0])
+    fetch_tokens = pltpu.make_async_copy(tokens_in, tokens, done.at[1])
+    fetch_routes.start()
+    fetch_tokens.start()
+    fetch_routes.wait()
     first, second = routes[0:1, :], routes[1:2, :]
     ids = lax.broadcasted_iota(jnp.int32, (experts, n_tok), 0)
     hit0 = (ids == first).astype(F32)
@@ -70,6 +75,7 @@
     row0, row1 = row_of(first, hit0, count0), row_of(second, hit1, count1)
     rows[...] = jnp.concatenate([row0, row1] * 4, axis=0)
     part = 8 * CAP
+    fetch_tokens.wait()
     for g in range(experts // 8):
         ids = lax.broadcasted_iota(jnp.int32, (part, n_tok), 0) + g * part
         select = jnp.logical_or(ids == row0, ids == row1).astype(F32).astype(BF16)
@@ -90,37 +96,34 @@
 
 
 def ffn_kernel(me, *refs):
-    chunks, pieces = refs[0:16], refs[16:-5]
-    hidden, serve, held, chunk_done, piece_done = refs[-5:]
-    sources = offsets_of(me[0])
+    whole, middle, late, pieces = refs[0:3], (refs[3:5], refs[5:7]), (refs[7:10], refs[10:13]), refs[13:-4]
+    hidden, serve, held, done = refs[-4:]
+    own, r1, l1, r2, l2, r3, l3, x4 = offsets_of(me[0])
     features = serve.shape[0] * serve.shape[1]
-    count, rows = len(pieces), pieces[0].shape[1]
     spread = 2 * HALF // serve.shape[1]
     part, slabs = 8 * CAP, 8 * SLAB
 
-    def fetch_piece(n):
-        place = (me[1] + n) % count
-        target = serve.at[:, pl.ds(pl.multiple_of(place * rows, rows), rows), :]
-        return pltpu.make_async_copy(pieces[n], target, piece_done.at[n])
-
     def fetch(g, k):
-        n = 8 * (g // 2) + k
-        span = pl.ds((g % 2) * slabs, slabs)
-        return pltpu.make_async_copy(chunks[n].at[span, :], held.at[g, k], chunk_done.at[g, k])
-
-    for n in range(count):
-        fetch_piece(n).start()
+        if k < 3:
+            source = whole[k].at[pl.ds(g * slabs, slabs), :]
+        else:
+            source = middle[g // 2][k - 3].at[pl.ds((g % 2) * slabs, slabs), :]
+        return pltpu.make_async_copy(source, held.at[g, k], done.at[g, k])
+
     for g in range(4):
-        for k in range(8):
+        for k in range(5):
             fetch(g, k).start()
-    for n in range(count):
-        fetch_piece(n).wait()
+    join_pieces(me[1], pieces, serve)
     for g in range(4):
         acc = jnp.zeros((part, 2 * HALF), F32)
         square = jnp.zeros((part, HALF), F32)
-        for k, source in enumerate(sources):
-            fetch(g, k).wait()
-            left, right = from_slabs(held[g, k])
+        for k, source in enumerate((r3, l3, x4, own, r1, l1, r2, l2)):
+            if k < 3:
+                x = late[g // 2][k][(g % 2) * slabs : (g % 2 + 1) * slabs, :]
+            else:
+                fetch(g, k - 3).wait()
+                x = held[g, k - 3]
+            left, right = from_slabs(x)
             w = serve[pl.ds(source * spread, spread)].reshape(2 * HALF, 2 * HALF)
             both = jnp.concatenate([left, right], axis=1)
             acc = acc + jnp.dot(both, w, preferred_element_type=F32)
@@ -135,11 +138,9 @@
 
 
 def down_kernel(me, *refs):
-    chunks, pieces, out, serve_out, serve, done = refs[0:8], refs[8:-4], *refs[-4:]
+    chunks, pieces, out, serve = refs[0:8], refs[8:-2], *refs[-2:]
     sources = offsets_of(me[0])
     join_pieces(me[1], pieces, serve)
-    copy = pltpu.make_async_copy(serve, serve_out, done)
-    copy.start()
     spread = HALF // serve.shape[1]
     part = 8 * CAP
     pairs = ((0, 7), (1, 2), (3, 4), (5, 6))
@@ -154,7 +155,6 @@
             w = jnp.concatenate([rows_of(sources[m]), rows_of(sources[n])], axis=0)
             acc = acc + jnp.dot(h, w, preferred_element_type=F32)
         to_slabs(acc, out, 8 * g)
-    copy.wait()
 
 
 def combine_kernel(rows, gains, returned, mixture):
@@ -186,18 +186,29 @@
     return lax.all_to_all(x, "fs", split_axis=0, concat_axis=0, tiled=True)
 
 
-def ring(x, last):
+def step(x, shift):
     n = lax.axis_size("tp")
-
-    def step(v, side):
-        shift = 1 if side == "r" else -1
-        return lax.ppermute(v, "tp", [(d, (d + shift) % n) for d in range(n)])
-
-    r1, l1 = step(x, "r"), step(x, "l")
-    r2, l2 = step(r1, "r"), step(l1, "l")
-    r3, l3 = step(r2, "r"), step(l2, "l")
-    x4 = step(r3, "r") if last == "r" else step(l3, "l")
-    return (x, r1, l1, r2, l2, r3, l3, x4)
+    return lax.ppermute(x, "tp", [(d, (d + shift) % n) for d in range(n)])
+
+
+def ring(x):
+    r1, l1 = step(x, 1), step(x, -1)
+    r2, l2 = step(r1, 1), step(l1, -1)
+    r3, l3 = step(r2, 1), step(l2, -1)
+    return (x, r1, l1, r2, l2, r3, l3, step(r3, 1))
+
+
+def token_ring(x):
+    cut = x.shape[0] // 2
+    r1, l1 = step(x, 1), step(x, -1)
+    middle, late = [], []
+    for span, end in ((slice(0, cut), "r"), (slice(cut, None), "l")):
+        r2, l2 = step(r1[span], 1), step(l1[span], -1)
+        r3, l3 = step(r2, 1), step(l2, -1)
+        x4 = step(r3, 1) if end == "r" else step(l3, -1)
+        middle += [r2, l2]
+        late += [r3, l3, x4]
+    return (x, r1, l1), middle, late
 
 
 def mixture_of_experts(tokens, norm_gain, gate_weight, up_weight, down_weight, routes, route_weights):
@@ -210,15 +221,21 @@
     me = jnp.stack([lax.axis_index("tp"), mine]).astype(jnp.int32)
     smem = pl.BlockSpec(memory_space=pltpu.SMEM)
     vmem = pl.BlockSpec(memory_space=pltpu.VMEM)
+    anywhere = pl.BlockSpec(memory_space=pl.ANY)
     slabs = (experts, SLAB, HALF)
     outbound, rows = pl.pallas_call(
         route_kernel,
-        in_specs=[vmem, vmem],
+        in_specs=[anywhere, anywhere],
         out_specs=(vmem, vmem),
+        scratch_shapes=[
+            pltpu.VMEM((2, n_tok), jnp.int32),
+            pltpu.VMEM(tokens.shape, BF16),
+            pltpu.SemaphoreType.DMA((2,)),
+        ],
         out_shape=(pltpu.VMEM(slabs, BF16), pltpu.VMEM((8, n_tok), jnp.int32)),
         name="route",
         compiler_params=LIMIT,
-    )(routes.T, tokens)
+    )(*in_hbm(routes.T, tokens))
     arrived = all_to_all(outbound).reshape(experts * SLAB, HALF)
 
     def piece(x, axis):
@@ -236,39 +253,29 @@
     arrived_weights = all_to_all(weights_low)
     both_pieces = swapped(arrived_weights[:, : rows_in // count])
     down_pieces = swapped(arrived_weights[:, rows_in // count :])
-    cut = experts * SLAB // 2
-    halves = ring(arrived[:cut], "r") + ring(arrived[cut:], "l")
-    hidden, both_serve = pl.pallas_call(
+    whole, middle, late = token_ring(arrived)
+    hidden = pl.pallas_call(
         ffn_kernel,
-        in_specs=[smem] + [pl.BlockSpec(memory_space=pl.ANY)] * (16 + count),
-        out_specs=(vmem, vmem),
-        out_shape=(
-            pltpu.VMEM((experts * CAP, cols), BF16),
+        in_specs=[smem] + [anywhere] * 7 + [vmem] * (6 + count),
+        out_specs=vmem,
+        out_shape=pltpu.VMEM((experts * CAP, cols), BF16),
+        scratch_shapes=[
             pltpu.VMEM((experts, rows_in, 2 * cols), BF16),
-        ),
-        scratch_shapes=[
-            pltpu.VMEM((4, 8, 8 * SLAB, HALF), BF16),
-            pltpu.SemaphoreType.DMA((4, 8)),
-            pltpu.SemaphoreType.DMA((count,)),
+            pltpu.VMEM((4, 5, 8 * SLAB, HALF), BF16),
+            pltpu.SemaphoreType.DMA((4, 5)),
         ],
         name="ffn",
         compiler_params=LIMIT,
-    )(me, *in_hbm(*halves, *both_pieces))
-    expert_out, down_serve = pl.pallas_call(
+    )(me, *in_hbm(*whole, *middle), *in_vmem(*late, *both_pieces))
+    expert_out = pl.pallas_call(
         down_kernel,
         in_specs=[smem] + [vmem] * (8 + count),
-        out_specs=(vmem, pl.BlockSpec(memory_space=pl.ANY)),
-        out_shape=(
-            pltpu.VMEM(slabs, BF16),
-            jax.ShapeDtypeStruct((experts, rows_down, down_cols), BF16),
-        ),
-        scratch_shapes=[
-            pltpu.VMEM((experts, rows_down, down_cols), BF16),
-            pltpu.SemaphoreType.DMA,
-        ],
+        out_specs=vmem,
+        out_shape=pltpu.VMEM(slabs, BF16),
+        scratch_shapes=[pltpu.VMEM((experts, rows_down, down_cols), BF16)],
         name="down",
         compiler_params=LIMIT,
-    )(me, *in_vmem(*ring(hidden, "r"), *down_pieces))
+    )(me, *in_vmem(*ring(hidden), *down_pieces))
     returned = all_to_all(expert_out).reshape(experts * SLAB, HALF)
     mixture = pl.pallas_call(
         combine_kernel,
@@ -278,9 +285,17 @@
         name="combine",
         compiler_params=LIMIT,
     )(*in_vmem(rows.T, route_weights, returned))
-    both_serve = both_serve.reshape(1, -1, 2 * cols)
-    gate_serve, up_serve = both_serve[:, :, :cols], both_serve[:, :, cols:]
-    return (gate_serve, up_serve, down_serve.reshape(1, -1, down_cols), mixture)
+
+    def assembled(pieces):
+        if count == 1:
+            return pieces[0].reshape(1, -1, pieces[0].shape[2])
+        own, other = pieces
+        both = jnp.where(mine == 0, own, other), jnp.where(mine == 0, other, own)
+        return jnp.concatenate(both, axis=1).reshape(1, -1, own.shape[2])
+
+    gate_serve = assembled([x[:, :, :cols] for x in both_pieces])
+    up_serve = assembled([x[:, :, cols:] for x in both_pieces])
+    return (gate_serve, up_serve, assembled(down_pieces), mixture)
 
 
 def solution(mesh):

time: 259 us -> 259 us (level)
  the two profiles are of different devices: /device:TPU:65 before, /device:TPU:69 now
where the time goes in v4:
time: 259 us; the launch traced here: 258 us
  starting transfers between devices  132 us (51%)
  waiting for transfers between devices  104 us (40%)
  Pallas kernels  11.5 us (4%)
  other arithmetic  6.42 us (2%)
  local copies, waits for them, and re-layouts  3.29 us (1%)
    all_to_all x3, waiting for transfers between devices, all_to_all(): return lax.all_to_all(x, 'fs', split_axis=0, concat_axis=0, tiled=True)  73.7 us
    all_to_all x3, starting transfers between devices, all_to_all(): return lax.all_to_all(x, 'fs', split_axis=0, concat_axis=0, tiled=True)  67.6 us
    ppermute x19, starting transfers between devices, step(): return lax.ppermute(x, 'tp', [(d, (d + shift) % n) for d in range(n)])  57.6 us
    ppermute x19, waiting for transfers between devices, step(): return lax.ppermute(x, 'tp', [(d, (d + shift) % n) for d in range(n)])  25.2 us
    ppermute x2, starting transfers between devices, swapped(): return [x, lax.ppermute(x, 'grp', [(g, g ^ 1) for g in range(groups)])]  6.94 us
  transfers between devices with their start and end apart: 24, of which 13 were waited for; matrix products, arithmetic and copies ran while one was open for 4% of the time, Pallas kernels for 0%

profile of v4, /device:TPU:69, one launch (start us, length us, event | category | flops | bytes accessed | tf_op | source)
XLA Modules:
  0.0 258.2 jit_solution(6052518035129704797)
XLA Ops:
  0.7 2.5 route.1
  3.1 44.4 %all-to-all-start.1 = ((bf16[32,72,128]{2,1,0:T(8,128)(2,1)}), bf16[32,72,128]{2,1,0:T(8,128)(2,1)S(1)}, u32[]{:S(2)}, u32[]{:S(2)}) async-start(bf16[32,72,128]{2,1,0:T(8,128)(2,1)} %get-tuple-element.7), calls=%async_computation.1 | async-start | bytes 1179648 | tf_op jit(solution)/shard_map/all_to_all | solution.py:186
  47.7 1.3 multiply_convert_fusion.1
  48.9 1.0 pad_maximum_fusion
  49.9 33.7 %all-to-all-done.1 = bf16[32,72,128]{2,1,0:T(8,128)(2,1)S(1)} async-done(((bf16[32,72,128]{2,1,0:T(8,128)(2,1)}), bf16[32,72,128]{2,1,0:T(8,128)(2,1)S(1)}, u32[]{:S(2)}, u32[]{:S(2)}) %all-to-all-start.1) | async-done | bytes 589856 | tf_op jit(solution)/shard_map/all_to_all | solution.py:186
  83.6 4.9 %all-to-all-start = ((bf16[32,48,256]{2,1,0:T(8,128)(2,1)}), bf16[32,48,256]{2,1,0:T(8,128)(2,1)}, u32[]{:S(2)}, u32[]{:S(2)}) async-start(bf16[32,48,256]{2,1,0:T(8,128)(2,1)} %pad_maximum_fusion), calls=%async_computation | async-start | bytes 1572864 | tf_op jit(solution)/shard_map/all_to_all | solution.py:186
  88.5 3.3 %collective-permute-start.2 = (bf16[2304,128]{1,0:T(8,128)(2,1)S(1)}, bf16[2304,128]{1,0:T(8,128)(2,1)S(1)}, u32[]{:S(2)}, u32[]{:S(2)}) collective-permute-start(bf16[2304,128]{1,0:T(8,128)(2,1)S(1)} %bitcast.11), channel_id=1, source_target_pairs={{0,1},{1,2},{2,3},{3,4},{4,5},{5,6},{6,7},{7,0},{8,9},{9,10},{10,1... | collective-permute-start | bytes 1769480 | tf_op jit(solution)/shard_map/ppermute | solution.py:191
  91.8 2.1 collective-permute-start.3
  93.9 10.5 %collective-permute-done.2.refs_1_ = bf16[2304,128]{1,0:T(8,128)(2,1)S(1)} collective-permute-done((bf16[2304,128]{1,0:T(8,128)(2,1)S(1)}, bf16[2304,128]{1,0:T(8,128)(2,1)S(1)}, u32[]{:S(2)}, u32[]{:S(2)}) %collective-permute-start.2) | collective-permute-done | bytes 589856 | tf_op jit(solution)/shard_map/ppermute | solution.py:191
  104.5 3.5 %collective-permute-start.4 = (bf16[1152,128]{1,0:T(8,128)(2,1)S(1)}, bf16[1152,128]{1,0:T(8,128)(2,1)}, u32[]{:S(2)}, u32[]{:S(2)}) collective-permute-start(bf16[1152,128]{1,0:T(8,128)(2,1)S(1)} %get-tuple-element.17), channel_id=1, source_target_pairs={{0,1},{1,2},{2,3},{3,4},{4,5},{5,6},{6,7},{7,0},{8,9},{9,10},{10,1... | collective-permute-start | bytes 884744 | tf_op jit(solution)/shard_map/ppermute | solution.py:191
  108.7 0.8 fusion
  109.5 1.9 collective-permute-start.7
  111.5 4.8 %collective-permute-start.6 = (bf16[1152,128]{1,0:T(8,128)(2,1)S(1)}, bf16[1152,128]{1,0:T(8,128)(2,1)}, u32[]{:S(2)}, u32[]{:S(2)}) collective-permute-start(bf16[1152,128]{1,0:T(8,128)(2,1)S(1)} %get-tuple-element.16), channel_id=1, source_target_pairs={{0,1},{1,2},{2,3},{3,4},{4,5},{5,6},{6,7},{7,0},{8,9},{9,10},{10,1... | collective-permute-start | bytes 884744 | tf_op jit(solution)/shard_map/ppermute | solution.py:191
  116.3 2.0 collective-permute-start.5
  118.3 4.6 %collective-permute-start.8 = (bf16[1152,128]{1,0:T(8,128)(2,1)}, bf16[1152,128]{1,0:T(8,128)(2,1)S(1)}, u32[]{:S(2)}, u32[]{:S(2)}) collective-permute-start(bf16[1152,128]{1,0:T(8,128)(2,1)} %collective-permute-done.4.refs_3_), channel_id=1, source_target_pairs={{0,1},{1,2},{2,3},{3,4},{4,5},{5,6},{6,7},{7,0},{8,9},{9,10},{10,1... | collective-permute-start | bytes 884744 | tf_op jit(solution)/shard_map/ppermute | solution.py:191
  122.9 2.0 collective-permute-start.12
  124.8 8.3 %all-to-all-done = bf16[32,48,256]{2,1,0:T(8,128)(2,1)} async-done(((bf16[32,48,256]{2,1,0:T(8,128)(2,1)}), bf16[32,48,256]{2,1,0:T(8,128)(2,1)}, u32[]{:S(2)}, u32[]{:S(2)}) %all-to-all-start) | async-done | bytes 786464 | tf_op jit(solution)/shard_map/all_to_all | solution.py:186
  133.2 1.1 slice.43.refs_13_
  134.2 4.4 %collective-permute-start = (bf16[32,32,256]{2,1,0:T(8,128)(2,1)S(1)}, bf16[32,32,256]{2,1,0:T(8,128)(2,1)S(1)}, u32[]{:S(2)}, u32[]{:S(2)}) collective-permute-start(bf16[32,32,256]{2,1,0:T(8,128)(2,1)S(1)} %slice.43.refs_13_), channel_id=1, source_target_pairs={{0,256},{256,0},{1,257},{257,1},{2,258},{258,2},{3,259},{259,3},{4... | collective-permute-start | bytes 1572872 | tf_op jit(solution)/shard_map/ppermute | solution.py:248
  138.7 3.3 %collective-permute-start.11 = (bf16[1152,128]{1,0:T(8,128)(2,1)}, bf16[1152,128]{1,0:T(8,128)(2,1)S(1)}, u32[]{:S(2)}, u32[]{:S(2)}) collective-permute-start(bf16[1152,128]{1,0:T(8,128)(2,1)} %collective-permute-done.6.refs_5_), channel_id=1, source_target_pairs={{0,1},{1,2},{2,3},{3,4},{4,5},{5,6},{6,7},{7,0},{8,9},{9,10},{10,1... | collective-permute-start | bytes 884744 | tf_op jit(solution)/shard_map/ppermute | solution.py:191
  142.0 2.1 collective-permute-start.9
  144.1 4.4 %collective-permute-start.10 = (bf16[1152,128]{1,0:T(8,128)(2,1)S(1)}, bf16[1152,128]{1,0:T(8,128)(2,1)}, u32[]{:S(2)}, u32[]{:S(2)}) collective-permute-start(bf16[1152,128]{1,0:T(8,128)(2,1)S(1)} %collective-permute-done.8.refs_7_), channel_id=1, source_target_pairs={{0,1},{1,2},{2,3},{3,4},{4,5},{5,6},{6,7},{7,0},{8,9},{9,10},{10,1... | collective-permute-start | bytes 884744 | tf_op jit(solution)/shard_map/ppermute | solution.py:191
  148.5 2.0 collective-permute-start.13
  150.5 2.2 collective-permute-done.9.refs_8_
  152.7 2.4 collective-permute-done.10.refs_9_
  155.1 3.4 %collective-permute-done.13.refs_12_ = bf16[1152,128]{1,0:T(8,128)(2,1)} collective-permute-done((bf16[1152,128]{1,0:T(8,128)(2,1)S(1)}, bf16[1152,128]{1,0:T(8,128)(2,1)}, u32[]{:S(2)}, u32[]{:S(2)}) %collective-permute-start.13) | collective-permute-done | bytes 294944 | tf_op jit(solution)/shard_map/ppermute | solution.py:191
  158.5 5.1 %ffn.1.refs_0_ = bf16[1152,128]{1,0:T(8,128)(2,1)S(1)} custom-call(s32[2]{0:T(128)S(1)} %pad_add_fusion.me, bf16[2304,128]{1,0:T(8,128)(2,1)} %bitcast.13, bf16[2304,128]{1,0:T(8,128)(2,1)} %copy-done.2, bf16[2304,128]{1,0:T(8,128)(2,1)} %copy-done.3, bf16[1152,128]{1,0:T(8,128)(2,1)} %collective-permute-done.4.refs_3_, ...), custom_call_target="tpu_custom_call" | custom-call | tf_op jit(solution)/shard_map/ffn/pallas_call | solution.py:257
  163.7 4.3 %collective-permute-start.14 = (bf16[1152,128]{1,0:T(8,128)(2,1)S(1)}, bf16[1152,128]{1,0:T(8,128)(2,1)S(1)}, u32[]{:S(2)}, u32[]{:S(2)}) collective-permute-start(bf16[1152,128]{1,0:T(8,128)(2,1)S(1)} %ffn.1.refs_0_), channel_id=1, source_target_pairs={{0,1},{1,2},{2,3},{3,4},{4,5},{5,6},{6,7},{7,0},{8,9},{9,10},{10,1... | collective-permute-start | bytes 884744 | tf_op jit(solution)/shard_map/ppermute | solution.py:191
  168.0 2.0 collective-permute-start.15
  170.0 1.7 collective-permute-done.14.refs_1_
  171.6 3.8 %collective-permute-start.16 = (bf16[1152,128]{1,0:T(8,128)(2,1)S(1)}, bf16[1152,128]{1,0:T(8,128)(2,1)S(1)}, u32[]{:S(2)}, u32[]{:S(2)}) collective-permute-start(bf16[1152,128]{1,0:T(8,128)(2,1)S(1)} %collective-permute-done.14.refs_1_), channel_id=1, source_target_pairs={{0,1},{1,2},{2,3},{3,4},{4,5},{5,6},{6,7},{7,0},{8,9},{9,10},{10,1... | collective-permute-start | bytes 884744 | tf_op jit(solution)/shard_map/ppermute | solution.py:191
  175.5 1.9 collective-permute-start.17
  177.5 2.0 collective-permute-done.16.refs_3_
  179.4 3.6 %collective-permute-start.18 = (bf16[1152,128]{1,0:T(8,128)(2,1)S(1)}, bf16[1152,128]{1,0:T(8,128)(2,1)S(1)}, u32[]{:S(2)}, u32[]{:S(2)}) collective-permute-start(bf16[1152,128]{1,0:T(8,128)(2,1)S(1)} %collective-permute-done.16.refs_3_), channel_id=1, source_target_pairs={{0,1},{1,2},{2,3},{3,4},{4,5},{5,6},{6,7},{7,0},{8,9},{9,10},{10,1... | collective-permute-start | bytes 884744 | tf_op jit(solution)/shard_map/ppermute | solution.py:191
  183.4 1.9 collective-permute-start.19
  185.4 1.8 collective-permute-done.18.refs_5_
  187.2 4.2 %collective-permute-start.20 = (bf16[1152,128]{1,0:T(8,128)(2,1)S(1)}, bf16[1152,128]{1,0:T(8,128)(2,1)S(1)}, u32[]{:S(2)}, u32[]{:S(2)}) collective-permute-start(bf16[1152,128]{1,0:T(8,128)(2,1)S(1)} %collective-permute-done.18.refs_5_), channel_id=1, source_target_pairs={{0,1},{1,2},{2,3},{3,4},{4,5},{5,6},{6,7},{7,0},{8,9},{9,10},{10,1... | collective-permute-start | bytes 884744 | tf_op jit(solution)/shard_map/ppermute | solution.py:191
  191.4 1.0 slice.47.refs_8_
  192.4 2.5 collective-permute-start.1
  194.9 4.9 %collective-permute-done.1.refs_9_ = bf16[32,16,256]{2,1,0:T(8,128)(2,1)S(1)} collective-permute-done((bf16[32,16,256]{2,1,0:T(8,128)(2,1)S(1)}, bf16[32,16,256]{2,1,0:T(8,128)(2,1)S(1)}, u32[]{:S(2)}, u32[]{:S(2)}) %collective-permute-start.1) | collective-permute-done | bytes 262176 | tf_op jit(solution)/shard_map/ppermute | solution.py:248
  199.8 2.2 down.1
  202.0 18.4 %all-to-all-start.2 = ((bf16[32,72,128]{2,1,0:T(8,128)(2,1)}), bf16[32,72,128]{2,1,0:T(8,128)(2,1)S(1)}, u32[]{:S(2)}, u32[]{:S(2)}) async-start(bf16[32,72,128]{2,1,0:T(8,128)(2,1)} %down.1), calls=%async_computation.2 | async-start | bytes 1179648 | tf_op jit(solution)/shard_map/all_to_all | solution.py:186
  220.7 1.0 broadcast_select_fusion.1
  221.7 0.9 pad_maximum_fusion.3
  222.5 1.1 broadcast_select_fusion.3
  223.6 1.1 pad_maximum_fusion.1
  224.8 31.7 %all-to-all-done.2 = bf16[32,72,128]{2,1,0:T(8,128)(2,1)S(1)} async-done(((bf16[32,72,128]{2,1,0:T(8,128)(2,1)}), bf16[32,72,128]{2,1,0:T(8,128)(2,1)S(1)}, u32[]{:S(2)}, u32[]{:S(2)}) %all-to-all-start.2) | async-done | bytes 589856 | tf_op jit(solution)/shard_map/all_to_all | solution.py:186
  256.4 1.7 combine.1
  (33 shorter events, 1.7 us)
Async XLA Ops:
  0.6 47.0 %copy-start = (f32[32,32,256]{2,1,0:T(8,128)S(1)}, f32[32,32,256]{2,1,0:T(8,128)}, u32[]{:S(2)}) copy-start(f32[32,32,256]{2,1,0:T(8,128)} %param.11) | copy-start | bytes 3145732
  0.6 46.9 %copy-start.6 = (f32[64]{0:T(128)S(1)}, f32[64]{0:T(128)}, u32[]{:S(2)}) copy-start(f32[64]{0:T(128)} %param.8) | copy-start | bytes 772
  0.7 47.0 %copy-start.4 = (f32[32,64,128]{2,1,0:T(8,128)S(1)}, f32[32,64,128]{2,1,0:T(8,128)}, u32[]{:S(2)}) copy-start(f32[32,64,128]{2,1,0:T(8,128)} %param.9) | copy-start | bytes 3145732
  3.1 80.5 %all-to-all-start.1 = ((bf16[32,72,128]{2,1,0:T(8,128)(2,1)}), bf16[32,72,128]{2,1,0:T(8,128)(2,1)S(1)}, u32[]{:S(2)}, u32[]{:S(2)}) async-start(bf16[32,72,128]{2,1,0:T(8,128)(2,1)} %get-tuple-element.7), calls=%async_computation.1 | async-start | bytes 1179648 | tf_op jit(solution)/shard_map/all_to_all | solution.py:186
  83.6 20.9 %copy-start.1 = (bf16[32,72,128]{2,1,0:T(8,128)(2,1)}, bf16[32,72,128]{2,1,0:T(8,128)(2,1)S(1)}, u32[]{:S(2)}) copy-start(bf16[32,72,128]{2,1,0:T(8,128)(2,1)S(1)} %all-to-all-done.1) | copy-start | bytes 1769476
  83.6 49.5 %all-to-all-start = ((bf16[32,48,256]{2,1,0:T(8,128)(2,1)}), bf16[32,48,256]{2,1,0:T(8,128)(2,1)}, u32[]{:S(2)}, u32[]{:S(2)}) async-start(bf16[32,48,256]{2,1,0:T(8,128)(2,1)} %pad_maximum_fusion), calls=%async_computation | async-start | bytes 1572864 | tf_op jit(solution)/shard_map/all_to_all | solution.py:186
  88.5 15.9 %collective-permute-start.2 = (bf16[2304,128]{1,0:T(8,128)(2,1)S(1)}, bf16[2304,128]{1,0:T(8,128)(2,1)S(1)}, u32[]{:S(2)}, u32[]{:S(2)}) collective-permute-start(bf16[2304,128]{1,0:T(8,128)(2,1)S(1)} %bitcast.11), channel_id=1, source_target_pairs={{0,1},{1,2},{2,3},{3,4},{4,5},{5,6},{6,7},{7,0},{8,9},{9,10},{10,1... | collective-permute-start | bytes 1769480 | tf_op jit(solution)/shard_map/ppermute | solution.py:191
  91.8 16.9 %collective-permute-start.3 = (bf16[2304,128]{1,0:T(8,128)(2,1)S(1)}, bf16[2304,128]{1,0:T(8,128)(2,1)S(1)}, u32[]{:S(2)}, u32[]{:S(2)}) collective-permute-start(bf16[2304,128]{1,0:T(8,128)(2,1)S(1)} %bitcast.12), channel_id=1, source_target_pairs={{0,7},{1,0},{2,1},{3,2},{4,3},{5,4},{6,5},{7,6},{8,15},{9,8},{10,9... | collective-permute-start | bytes 1769480 | tf_op jit(solution)/shard_map/ppermute | solution.py:191
  104.4 5.1 %copy-start.2 = (bf16[2304,128]{1,0:T(8,128)(2,1)}, bf16[2304,128]{1,0:T(8,128)(2,1)S(1)}, u32[]{:S(2)}) copy-start(bf16[2304,128]{1,0:T(8,128)(2,1)S(1)} %collective-permute-done.2.refs_1_) | copy-start | bytes 1769476
  104.5 13.8 %collective-permute-start.4 = (bf16[1152,128]{1,0:T(8,128)(2,1)S(1)}, bf16[1152,128]{1,0:T(8,128)(2,1)}, u32[]{:S(2)}, u32[]{:S(2)}) collective-permute-start(bf16[1152,128]{1,0:T(8,128)(2,1)S(1)} %get-tuple-element.17), channel_id=1, source_target_pairs={{0,1},{1,2},{2,3},{3,4},{4,5},{5,6},{6,7},{7,0},{8,9},{9,10},{10,1... | collective-permute-start | bytes 884744 | tf_op jit(solution)/shard_map/ppermute | solution.py:191
  108.7 9.5 %copy-start.3 = (bf16[2304,128]{1,0:T(8,128)(2,1)}, bf16[2304,128]{1,0:T(8,128)(2,1)S(1)}, u32[]{:S(2)}) copy-start(bf16[2304,128]{1,0:T(8,128)(2,1)S(1)} %collective-permute-done.3.refs_2_) | copy-start | bytes 1769476
  109.5 13.4 %collective-permute-start.7 = (bf16[1152,128]{1,0:T(8,128)(2,1)S(1)}, bf16[1152,128]{1,0:T(8,128)(2,1)}, u32[]{:S(2)}, u32[]{:S(2)}) collective-permute-start(bf16[1152,128]{1,0:T(8,128)(2,1)S(1)} %get-tuple-element.14), channel_id=1, source_target_pairs={{0,7},{1,0},{2,1},{3,2},{4,3},{5,4},{6,5},{7,6},{8,15},{9,8},{10,9... | collective-permute-start | bytes 884744 | tf_op jit(solution)/shard_map/ppermute | solution.py:191
  111.5 27.2 %collective-permute-start.6 = (bf16[1152,128]{1,0:T(8,128)(2,1)S(1)}, bf16[1152,128]{1,0:T(8,128)(2,1)}, u32[]{:S(2)}, u32[]{:S(2)}) collective-permute-start(bf16[1152,128]{1,0:T(8,128)(2,1)S(1)} %get-tuple-element.16), channel_id=1, source_target_pairs={{0,1},{1,2},{2,3},{3,4},{4,5},{5,6},{6,7},{7,0},{8,9},{9,10},{10,1... | collective-permute-start | bytes 884744 | tf_op jit(solution)/shard_map/ppermute | solution.py:191
  116.3 25.7 %collective-permute-start.5 = (bf16[1152,128]{1,0:T(8,128)(2,1)}, bf16[1152,128]{1,0:T(8,128)(2,1)}, u32[]{:S(2)}, u32[]{:S(2)}) collective-permute-start(bf16[1152,128]{1,0:T(8,128)(2,1)} %get-tuple-element.15), channel_id=1, source_target_pairs={{0,7},{1,0},{2,1},{3,2},{4,3},{5,4},{6,5},{7,6},{8,15},{9,8},{10,9... | collective-permute-start | bytes 884744 | tf_op jit(solution)/shard_map/ppermute | solution.py:191
  118.3 25.8 %collective-permute-start.8 = (bf16[1152,128]{1,0:T(8,128)(2,1)}, bf16[1152,128]{1,0:T(8,128)(2,1)S(1)}, u32[]{:S(2)}, u32[]{:S(2)}) collective-permute-start(bf16[1152,128]{1,0:T(8,128)(2,1)} %collective-permute-done.4.refs_3_), channel_id=1, source_target_pairs={{0,1},{1,2},{2,3},{3,4},{4,5},{5,6},{6,7},{7,0},{8,9},{9,10},{10,1... | collective-permute-start | bytes 884744 | tf_op jit(solution)/shard_map/ppermute | solution.py:191
  122.9 25.6 %collective-permute-start.12 = (bf16[1152,128]{1,0:T(8,128)(2,1)}, bf16[1152,128]{1,0:T(8,128)(2,1)S(1)}, u32[]{:S(2)}, u32[]{:S(2)}) collective-permute-start(bf16[1152,128]{1,0:T(8,128)(2,1)} %collective-permute-done.7.refs_6_), channel_id=1, source_target_pairs={{0,7},{1,0},{2,1},{3,2},{4,3},{5,4},{6,5},{7,6},{8,15},{9,8},{10,9... | collective-permute-start | bytes 884744 | tf_op jit(solution)/shard_map/ppermute | solution.py:191
  134.2 18.5 %collective-permute-start = (bf16[32,32,256]{2,1,0:T(8,128)(2,1)S(1)}, bf16[32,32,256]{2,1,0:T(8,128)(2,1)S(1)}, u32[]{:S(2)}, u32[]{:S(2)}) collective-permute-start(bf16[32,32,256]{2,1,0:T(8,128)(2,1)S(1)} %slice.43.refs_13_), channel_id=1, source_target_pairs={{0,256},{256,0},{1,257},{257,1},{2,258},{258,2},{3,259},{259,3},{4... | collective-permute-start | bytes 1572872 | tf_op jit(solution)/shard_map/ppermute | solution.py:248
  138.7 11.8 %collective-permute-start.11 = (bf16[1152,128]{1,0:T(8,128)(2,1)}, bf16[1152,128]{1,0:T(8,128)(2,1)S(1)}, u32[]{:S(2)}, u32[]{:S(2)}) collective-permute-start(bf16[1152,128]{1,0:T(8,128)(2,1)} %collective-permute-done.6.refs_5_), channel_id=1, source_target_pairs={{0,1},{1,2},{2,3},{3,4},{4,5},{5,6},{6,7},{7,0},{8,9},{9,10},{10,1... | collective-permute-start | bytes 884744 | tf_op jit(solution)/shard_map/ppermute | solution.py:191
  142.0 10.7 %collective-permute-start.9 = (bf16[1152,128]{1,0:T(8,128)(2,1)}, bf16[1152,128]{1,0:T(8,128)(2,1)S(1)}, u32[]{:S(2)}, u32[]{:S(2)}) collective-permute-start(bf16[1152,128]{1,0:T(8,128)(2,1)} %collective-permute-done.5.refs_4_), channel_id=1, source_target_pairs={{0,7},{1,0},{2,1},{3,2},{4,3},{5,4},{6,5},{7,6},{8,15},{9,8},{10,9... | collective-permute-start | bytes 884744 | tf_op jit(solution)/shard_map/ppermute | solution.py:191
  144.1 11.1 %collective-permute-start.10 = (bf16[1152,128]{1,0:T(8,128)(2,1)S(1)}, bf16[1152,128]{1,0:T(8,128)(2,1)}, u32[]{:S(2)}, u32[]{:S(2)}) collective-permute-start(bf16[1152,128]{1,0:T(8,128)(2,1)S(1)} %collective-permute-done.8.refs_7_), channel_id=1, source_target_pairs={{0,1},{1,2},{2,3},{3,4},{4,5},{5,6},{6,7},{7,0},{8,9},{9,10},{10,1... | collective-permute-start | bytes 884744 | tf_op jit(solution)/shard_map/ppermute | solution.py:191
  148.5 10.1 %collective-permute-start.13 = (bf16[1152,128]{1,0:T(8,128)(2,1)S(1)}, bf16[1152,128]{1,0:T(8,128)(2,1)}, u32[]{:S(2)}, u32[]{:S(2)}) collective-permute-start(bf16[1152,128]{1,0:T(8,128)(2,1)S(1)} %collective-permute-done.12.refs_11_), channel_id=1, source_target_pairs={{0,7},{1,0},{2,1},{3,2},{4,3},{5,4},{6,5},{7,6},{8,15},{9,8},{10,9... | collective-permute-start | bytes 884744 | tf_op jit(solution)/shard_map/ppermute | solution.py:191
  163.7 8.0 %collective-permute-start.14 = (bf16[1152,128]{1,0:T(8,128)(2,1)S(1)}, bf16[1152,128]{1,0:T(8,128)(2,1)S(1)}, u32[]{:S(2)}, u32[]{:S(2)}) collective-permute-start(bf16[1152,128]{1,0:T(8,128)(2,1)S(1)} %ffn.1.refs_0_), channel_id=1, source_target_pairs={{0,1},{1,2},{2,3},{3,4},{4,5},{5,6},{6,7},{7,0},{8,9},{9,10},{10,1... | collective-permute-start | bytes 884744 | tf_op jit(solution)/shard_map/ppermute | solution.py:191
  168.0 7.5 %collective-permute-start.15 = (bf16[1152,128]{1,0:T(8,128)(2,1)S(1)}, bf16[1152,128]{1,0:T(8,128)(2,1)S(1)}, u32[]{:S(2)}, u32[]{:S(2)}) collective-permute-start(bf16[1152,128]{1,0:T(8,128)(2,1)S(1)} %ffn.1.refs_0_), channel_id=1, source_target_pairs={{0,7},{1,0},{2,1},{3,2},{4,3},{5,4},{6,5},{7,6},{8,15},{9,8},{10,9... | collective-permute-start | bytes 884744 | tf_op jit(solution)/shard_map/ppermute | solution.py:191
  171.6 7.8 %collective-permute-start.16 = (bf16[1152,128]{1,0:T(8,128)(2,1)S(1)}, bf16[1152,128]{1,0:T(8,128)(2,1)S(1)}, u32[]{:S(2)}, u32[]{:S(2)}) collective-permute-start(bf16[1152,128]{1,0:T(8,128)(2,1)S(1)} %collective-permute-done.14.refs_1_), channel_id=1, source_target_pairs={{0,1},{1,2},{2,3},{3,4},{4,5},{5,6},{6,7},{7,0},{8,9},{9,10},{10,1... | collective-permute-start | bytes 884744 | tf_op jit(solution)/shard_map/ppermute | solution.py:191
  175.5 8.0 %collective-permute-start.17 = (bf16[1152,128]{1,0:T(8,128)(2,1)S(1)}, bf16[1152,128]{1,0:T(8,128)(2,1)S(1)}, u32[]{:S(2)}, u32[]{:S(2)}) collective-permute-start(bf16[1152,128]{1,0:T(8,128)(2,1)S(1)} %collective-permute-done.15.refs_2_), channel_id=1, source_target_pairs={{0,7},{1,0},{2,1},{3,2},{4,3},{5,4},{6,5},{7,6},{8,15},{9,8},{10,9... | collective-permute-start | bytes 884744 | tf_op jit(solution)/shard_map/ppermute | solution.py:191
  179.4 7.8 %collective-permute-start.18 = (bf16[1152,128]{1,0:T(8,128)(2,1)S(1)}, bf16[1152,128]{1,0:T(8,128)(2,1)S(1)}, u32[]{:S(2)}, u32[]{:S(2)}) collective-permute-start(bf16[1152,128]{1,0:T(8,128)(2,1)S(1)} %collective-permute-done.16.refs_3_), channel_id=1, source_target_pairs={{0,1},{1,2},{2,3},{3,4},{4,5},{5,6},{6,7},{7,0},{8,9},{9,10},{10,1... | collective-permute-start | bytes 884744 | tf_op jit(solution)/shard_map/ppermute | solution.py:191
  183.4 16.4 %collective-permute-start.19 = (bf16[1152,128]{1,0:T(8,128)(2,1)S(1)}, bf16[1152,128]{1,0:T(8,128)(2,1)S(1)}, u32[]{:S(2)}, u32[]{:S(2)}) collective-permute-start(bf16[1152,128]{1,0:T(8,128)(2,1)S(1)} %collective-permute-done.17.refs_4_), channel_id=1, source_target_pairs={{0,7},{1,0},{2,1},{3,2},{4,3},{5,4},{6,5},{7,6},{8,15},{9,8},{10,9... | collective-permute-start | bytes 884744 | tf_op jit(solution)/shard_map/ppermute | solution.py:191
  187.2 12.6 %collective-permute-start.20 = (bf16[1152,128]{1,0:T(8,128)(2,1)S(1)}, bf16[1152,128]{1,0:T(8,128)(2,1)S(1)}, u32[]{:S(2)}, u32[]{:S(2)}) collective-permute-start(bf16[1152,128]{1,0:T(8,128)(2,1)S(1)} %collective-permute-done.18.refs_5_), channel_id=1, source_target_pairs={{0,1},{1,2},{2,3},{3,4},{4,5},{5,6},{6,7},{7,0},{8,9},{9,10},{10,1... | collective-permute-start | bytes 884744 | tf_op jit(solution)/shard_map/ppermute | solution.py:191
  192.4 7.4 %collective-permute-start.1 = (bf16[32,16,256]{2,1,0:T(8,128)(2,1)S(1)}, bf16[32,16,256]{2,1,0:T(8,128)(2,1)S(1)}, u32[]{:S(2)}, u32[]{:S(2)}) collective-permute-start(bf16[32,16,256]{2,1,0:T(8,128)(2,1)S(1)} %slice.47.refs_8_), channel_id=1, source_target_pairs={{0,256},{256,0},{1,257},{257,1},{2,258},{258,2},{3,259},{259,3},{4... | collective-permute-start | bytes 786440 | tf_op jit(solution)/shard_map/ppermute | solution.py:248
  202.0 18.5 %copy-start.5 = (f32[384,2]{0,1:T(2,128)S(1)}, f32[384,2]{0,1:T(2,128)}, u32[]{:S(2)}) copy-start(f32[384,2]{0,1:T(2,128)} %param.13) | copy-start | bytes 9220
  202.0 54.4 %all-to-all-start.2 = ((bf16[32,72,128]{2,1,0:T(8,128)(2,1)}), bf16[32,72,128]{2,1,0:T(8,128)(2,1)S(1)}, u32[]{:S(2)}, u32[]{:S(2)}) async-start(bf16[32,72,128]{2,1,0:T(8,128)(2,1)} %down.1), calls=%async_computation.2 | async-start | bytes 1179648 | tf_op jit(solution)/shard_map/all_to_all | solution.py:186

commit v5 on v4

--- a/solution.py
+++ b/solution.py
@@ -7,6 +7,7 @@
 
 
 CAP = 36
+FETCHED = (0,)
 MAIN = 32
 SLAB = 72
 HALF = 128
@@ -96,35 +97,33 @@
 
 
 def ffn_kernel(me, *refs):
-    whole, middle, late, pieces = refs[0:3], (refs[3:5], refs[5:7]), (refs[7:10], refs[10:13]), refs[13:-4]
+    chunks, pieces = (refs[0:8], refs[8:16]), refs[16:-4]
     hidden, serve, held, done = refs[-4:]
-    own, r1, l1, r2, l2, r3, l3, x4 = offsets_of(me[0])
+    sources = offsets_of(me[0])
     features = serve.shape[0] * serve.shape[1]
     spread = 2 * HALF // serve.shape[1]
     part, slabs = 8 * CAP, 8 * SLAB
 
-    def fetch(g, k):
-        if k < 3:
-            source = whole[k].at[pl.ds(g * slabs, slabs), :]
-        else:
-            source = middle[g // 2][k - 3].at[pl.ds((g % 2) * slabs, slabs), :]
-        return pltpu.make_async_copy(source, held.at[g, k], done.at[g, k])
+    def fetch(g, n):
+        source = chunks[g // 2][FETCHED[n]].at[pl.ds((g % 2) * slabs, slabs), :]
+        return pltpu.make_async_copy(source, held.at[g, n], done.at[g, n])
 
     for g in range(4):
-        for k in range(5):
-            fetch(g, k).start()
+        for n in range(len(FETCHED)):
+            fetch(g, n).start()
     join_pieces(me[1], pieces, serve)
+    order = [k for k in range(8) if k not in FETCHED] + list(FETCHED)
     for g in range(4):
         acc = jnp.zeros((part, 2 * HALF), F32)
         square = jnp.zeros((part, HALF), F32)
-        for k, source in enumerate((r3, l3, x4, own, r1, l1, r2, l2)):
-            if k < 3:
-                x = late[g // 2][k][(g % 2) * slabs : (g % 2 + 1) * slabs, :]
+        for k in order:
+            if k in FETCHED:
+                fetch(g, FETCHED.index(k)).wait()
+                x = held[g, FETCHED.index(k)]
             else:
-                fetch(g, k - 3).wait()
-                x = held[g, k - 3]
+                x = chunks[g // 2][k][(g % 2) * slabs : (g % 2 + 1) * slabs, :]
             left, right = from_slabs(x)
-            w = serve[pl.ds(source * spread, spread)].reshape(2 * HALF, 2 * HALF)
+            w = serve[pl.ds(sources[k] * spread, spread)].reshape(2 * HALF, 2 * HALF)
             both = jnp.concatenate([left, right], axis=1)
             acc = acc + jnp.dot(both, w, preferred_element_type=F32)
             l32, r32 = left.astype(F32), right.astype(F32)
@@ -191,24 +190,12 @@
     return lax.ppermute(x, "tp", [(d, (d + shift) % n) for d in range(n)])
 
 
-def ring(x):
+def ring(x, end):
     r1, l1 = step(x, 1), step(x, -1)
     r2, l2 = step(r1, 1), step(l1, -1)
     r3, l3 = step(r2, 1), step(l2, -1)
-    return (x, r1, l1, r2, l2, r3, l3, step(r3, 1))
-
-
-def token_ring(x):
-    cut = x.shape[0] // 2
-    r1, l1 = step(x, 1), step(x, -1)
-    middle, late = [], []
-    for span, end in ((slice(0, cut), "r"), (slice(cut, None), "l")):
-        r2, l2 = step(r1[span], 1), step(l1[span], -1)
-        r3, l3 = step(r2, 1), step(l2, -1)
-        x4 = step(r3, 1) if end == "r" else step(l3, -1)
-        middle += [r2, l2]
-        late += [r3, l3, x4]
-    return (x, r1, l1), middle, late
+    x4 = step(r3, 1) if end == "r" else step(l3, -1)
+    return (x, r1, l1, r2, l2, r3, l3, x4)
 
 
 def mixture_of_experts(tokens, norm_gain, gate_weight, up_weight, down_weight, routes, route_weights):
@@ -253,20 +240,26 @@
     arrived_weights = all_to_all(weights_low)
     both_pieces = swapped(arrived_weights[:, : rows_in // count])
     down_pieces = swapped(arrived_weights[:, rows_in // count :])
-    whole, middle, late = token_ring(arrived)
+    cut = experts * SLAB // 2
+    chunks = ring(arrived[:cut], "r") + ring(arrived[cut:], "l")
+    fetched = [n % 8 in FETCHED for n in range(16)]
     hidden = pl.pallas_call(
         ffn_kernel,
-        in_specs=[smem] + [anywhere] * 7 + [vmem] * (6 + count),
+        in_specs=[smem] + [anywhere if f else vmem for f in fetched] + [vmem] * count,
         out_specs=vmem,
         out_shape=pltpu.VMEM((experts * CAP, cols), BF16),
         scratch_shapes=[
             pltpu.VMEM((experts, rows_in, 2 * cols), BF16),
-            pltpu.VMEM((4, 5, 8 * SLAB, HALF), BF16),
-            pltpu.SemaphoreType.DMA((4, 5)),
+            pltpu.VMEM((4, len(FETCHED), 8 * SLAB, HALF), BF16),
+            pltpu.SemaphoreType.DMA((4, len(FETCHED))),
         ],
         name="ffn",
         compiler_params=LIMIT,
-    )(me, *in_hbm(*whole, *middle), *in_vmem(*late, *both_pieces))
+    )(
+        me,
+        *[(in_hbm if f else in_vmem)(x)[0] for f, x in zip(fetched, chunks)],
+        *in_vmem(*both_pieces),
+    )
     expert_out = pl.pallas_call(
         down_kernel,
         in_specs=[smem] + [vmem] * (8 + count),
@@ -275,7 +268,7 @@
         scratch_shapes=[pltpu.VMEM((experts, rows_down, down_cols), BF16)],
         name="down",
         compiler_params=LIMIT,
-    )(me, *in_vmem(*ring(hidden), *down_pieces))
+    )(me, *in_vmem(*ring(hidden, "r"), *down_pieces))
     returned = all_to_all(expert_out).reshape(experts * SLAB, HALF)
     mixture = pl.pallas_call(
         combine_kernel,

time: 259 us -> 257 us (level)
  the two profiles are of different devices: /device:TPU:69 before, /device:TPU:65 now
where the time goes in v5:
time: 257 us; the launch traced here: 256 us
  starting transfers between devices  136 us (53%)
  waiting for transfers between devices  98.4 us (38%)
  Pallas kernels  11.1 us (4%)
  other arithmetic  6.5 us (3%)
    all_to_all x3, waiting for transfers between devices, all_to_all(): return lax.all_to_all(x, 'fs', split_axis=0, concat_axis=0, tiled=True)  76.1 us
    all_to_all x3, starting transfers between devices, all_to_all(): return lax.all_to_all(x, 'fs', split_axis=0, concat_axis=0, tiled=True)  64.7 us
    ppermute x21, starting transfers between devices, step(): return lax.ppermute(x, 'tp', [(d, (d + shift) % n) for d in range(n)])  64.6 us
    ppermute x21, waiting for transfers between devices, step(): return lax.ppermute(x, 'tp', [(d, (d + shift) % n) for d in range(n)])  17.8 us
    ppermute x2, starting transfers between devices, swapped(): return [x, lax.ppermute(x, 'grp', [(g, g ^ 1) for g in range(groups)])]  6.61 us
  transfers between devices with their start and end apart: 26, of which 12 were waited for; matrix products, arithmetic and copies ran while one was open for 4% of the time, Pallas kernels for 0%

profile of v5, /device:TPU:65, one launch (start us, length us, event | category | flops | bytes accessed | tf_op | source)
XLA Modules:
  0.0 255.6 jit_solution(6090230127558788572)
XLA Ops:
  0.7 2.4 route.1
  3.1 45.2 %all-to-all-start.1 = ((bf16[32,72,128]{2,1,0:T(8,128)(2,1)}), bf16[32,72,128]{2,1,0:T(8,128)(2,1)S(1)}, u32[]{:S(2)}, u32[]{:S(2)}) async-start(bf16[32,72,128]{2,1,0:T(8,128)(2,1)} %get-tuple-element.7), calls=%async_computation.1 | async-start | bytes 1179648 | tf_op jit(solution)/shard_map/all_to_all | solution.py:185
  48.5 1.4 multiply_convert_fusion.1
  49.8 1.0 pad_maximum_fusion
  50.8 33.7 %all-to-all-done.1 = bf16[32,72,128]{2,1,0:T(8,128)(2,1)S(1)} async-done(((bf16[32,72,128]{2,1,0:T(8,128)(2,1)}), bf16[32,72,128]{2,1,0:T(8,128)(2,1)S(1)}, u32[]{:S(2)}, u32[]{:S(2)}) %all-to-all-start.1) | async-done | bytes 589856 | tf_op jit(solution)/shard_map/all_to_all | solution.py:185
  84.5 5.2 %all-to-all-start = ((bf16[32,48,256]{2,1,0:T(8,128)(2,1)}), bf16[32,48,256]{2,1,0:T(8,128)(2,1)}, u32[]{:S(2)}, u32[]{:S(2)}) async-start(bf16[32,48,256]{2,1,0:T(8,128)(2,1)} %pad_maximum_fusion), calls=%async_computation | async-start | bytes 1572864 | tf_op jit(solution)/shard_map/all_to_all | solution.py:185
  89.8 5.0 %collective-permute-start.10 = (bf16[1152,128]{1,0:T(8,128)(2,1)S(1)}, bf16[1152,128]{1,0:T(8,128)(2,1)S(1)}, u32[]{:S(2)}, u32[]{:S(2)}) collective-permute-start(bf16[1152,128]{1,0:T(8,128)(2,1)S(1)} %bitcast.12), channel_id=1, source_target_pairs={{0,7},{1,0},{2,1},{3,2},{4,3},{5,4},{6,5},{7,6},{8,15},{9,8},{10,9... | collective-permute-start | bytes 884744 | tf_op jit(solution)/shard_map/ppermute | solution.py:190
  94.8 2.0 collective-permute-start.2
  96.8 2.0 collective-permute-start.9
  98.8 4.6 %collective-permute-start.3 = (bf16[1152,128]{1,0:T(8,128)(2,1)S(1)}, bf16[1152,128]{1,0:T(8,128)(2,1)S(1)}, u32[]{:S(2)}, u32[]{:S(2)}) collective-permute-start(bf16[1152,128]{1,0:T(8,128)(2,1)S(1)} %bitcast.16), channel_id=1, source_target_pairs={{0,7},{1,0},{2,1},{3,2},{4,3},{5,4},{6,5},{7,6},{8,15},{9,8},{10,9... | collective-permute-start | bytes 884744 | tf_op jit(solution)/shard_map/ppermute | solution.py:190
  103.4 3.4 %collective-permute-start.12 = (bf16[1152,128]{1,0:T(8,128)(2,1)S(1)}, bf16[1152,128]{1,0:T(8,128)(2,1)}, u32[]{:S(2)}, u32[]{:S(2)}) collective-permute-start(bf16[1152,128]{1,0:T(8,128)(2,1)S(1)} %collective-permute-done.10.refs_10_), channel_id=1, source_target_pairs={{0,7},{1,0},{2,1},{3,2},{4,3},{5,4},{6,5},{7,6},{8,15},{9,8},{10,9... | collective-permute-start | bytes 884744 | tf_op jit(solution)/shard_map/ppermute | solution.py:190
  106.8 2.0 collective-permute-start.4
  108.8 2.9 %collective-permute-done.9.refs_9_ = bf16[1152,128]{1,0:T(8,128)(2,1)S(1)} collective-permute-done((bf16[1152,128]{1,0:T(8,128)(2,1)S(1)}, bf16[1152,128]{1,0:T(8,128)(2,1)S(1)}, u32[]{:S(2)}, u32[]{:S(2)}) %collective-permute-start.9) | collective-permute-done | bytes 294944 | tf_op jit(solution)/shard_map/ppermute | solution.py:190
  111.7 1.9 collective-permute-start.11
  113.6 4.6 %collective-permute-start.5 = (bf16[1152,128]{1,0:T(8,128)(2,1)S(1)}, bf16[1152,128]{1,0:T(8,128)(2,1)}, u32[]{:S(2)}, u32[]{:S(2)}) collective-permute-start(bf16[1152,128]{1,0:T(8,128)(2,1)S(1)} %collective-permute-done.3.refs_2_), channel_id=1, source_target_pairs={{0,7},{1,0},{2,1},{3,2},{4,3},{5,4},{6,5},{7,6},{8,15},{9,8},{10,9... | collective-permute-start | bytes 884744 | tf_op jit(solution)/shard_map/ppermute | solution.py:190
  118.2 2.0 collective-permute-start.14
  120.2 3.4 %collective-permute-start.6 = (bf16[1152,128]{1,0:T(8,128)(2,1)}, bf16[1152,128]{1,0:T(8,128)(2,1)}, u32[]{:S(2)}, u32[]{:S(2)}) collective-permute-start(bf16[1152,128]{1,0:T(8,128)(2,1)} %collective-permute-done.4.refs_3_), channel_id=1, source_target_pairs={{0,1},{1,2},{2,3},{3,4},{4,5},{5,6},{6,7},{7,0},{8,9},{9,10},{10,1... | collective-permute-start | bytes 884744 | tf_op jit(solution)/shard_map/ppermute | solution.py:190
  123.6 10.7 %all-to-all-done = bf16[32,48,256]{2,1,0:T(8,128)(2,1)} async-done(((bf16[32,48,256]{2,1,0:T(8,128)(2,1)}), bf16[32,48,256]{2,1,0:T(8,128)(2,1)}, u32[]{:S(2)}, u32[]{:S(2)}) %all-to-all-start) | async-done | bytes 786464 | tf_op jit(solution)/shard_map/all_to_all | solution.py:185
  134.3 1.1 slice.43.refs_16_
  135.4 4.0 %collective-permute-start = (bf16[32,32,256]{2,1,0:T(8,128)(2,1)S(1)}, bf16[32,32,256]{2,1,0:T(8,128)(2,1)S(1)}, u32[]{:S(2)}, u32[]{:S(2)}) collective-permute-start(bf16[32,32,256]{2,1,0:T(8,128)(2,1)S(1)} %slice.43.refs_16_), channel_id=1, source_target_pairs={{0,256},{256,0},{1,257},{257,1},{2,258},{258,2},{3,259},{259,3},{4... | collective-permute-start | bytes 1572872 | tf_op jit(solution)/shard_map/ppermute | solution.py:235
  139.4 3.3 %collective-permute-start.13 = (bf16[1152,128]{1,0:T(8,128)(2,1)}, bf16[1152,128]{1,0:T(8,128)(2,1)}, u32[]{:S(2)}, u32[]{:S(2)}) collective-permute-start(bf16[1152,128]{1,0:T(8,128)(2,1)} %collective-permute-done.11.refs_11_), channel_id=1, source_target_pairs={{0,1},{1,2},{2,3},{3,4},{4,5},{5,6},{6,7},{7,0},{8,9},{9,10},{10,1... | collective-permute-start | bytes 884744 | tf_op jit(solution)/shard_map/ppermute | solution.py:190
  142.7 4.1 %collective-permute-start.7 = (bf16[1152,128]{1,0:T(8,128)(2,1)}, bf16[1152,128]{1,0:T(8,128)(2,1)}, u32[]{:S(2)}, u32[]{:S(2)}) collective-permute-start(bf16[1152,128]{1,0:T(8,128)(2,1)} %collective-permute-done.5.refs_4_), channel_id=1, source_target_pairs={{0,7},{1,0},{2,1},{3,2},{4,3},{5,4},{6,5},{7,6},{8,15},{9,8},{10,9... | collective-permute-start | bytes 884744 | tf_op jit(solution)/shard_map/ppermute | solution.py:190
  146.9 3.4 %collective-permute-start.15 = (bf16[1152,128]{1,0:T(8,128)(2,1)}, bf16[1152,128]{1,0:T(8,128)(2,1)}, u32[]{:S(2)}, u32[]{:S(2)}) collective-permute-start(bf16[1152,128]{1,0:T(8,128)(2,1)} %collective-permute-done.14.refs_14_), channel_id=1, source_target_pairs={{0,7},{1,0},{2,1},{3,2},{4,3},{5,4},{6,5},{7,6},{8,15},{9,8},{10,9... | collective-permute-start | bytes 884744 | tf_op jit(solution)/shard_map/ppermute | solution.py:190
  150.3 2.0 collective-permute-start.8
  152.4 6.3 %collective-permute-done.15.refs_15_ = bf16[1152,128]{1,0:T(8,128)(2,1)} collective-permute-done((bf16[1152,128]{1,0:T(8,128)(2,1)}, bf16[1152,128]{1,0:T(8,128)(2,1)}, u32[]{:S(2)}, u32[]{:S(2)}) %collective-permute-start.15) | collective-permute-done | bytes 294944 | tf_op jit(solution)/shard_map/ppermute | solution.py:190
  158.7 1.6 collective-permute-done.8.refs_7_
  160.3 4.8 %ffn.1.refs_0_ = bf16[1152,128]{1,0:T(8,128)(2,1)S(1)} custom-call(s32[2]{0:T(128)S(1)} %pad_add_fusion.me, bf16[1152,128]{1,0:T(8,128)(2,1)} %bitcast.17, bf16[1152,128]{1,0:T(8,128)(2,1)S(1)} %collective-permute-done.2.refs_1_, bf16[1152,128]{1,0:T(8,128)(2,1)S(1)} %collective-permute-done.3.refs_2_, bf16[1152,128]{1,0:T(8,128)(2,1)} %collective-permute-done.4.refs_3_, ...), custom_call_target="tpu_custom_call" | custom-call | tf_op jit(solution)/shard_map/ffn/pallas_call | solution.py:246
  165.1 2.0 collective-permute-start.16
  167.1 4.6 %collective-permute-start.17 = (bf16[1152,128]{1,0:T(8,128)(2,1)S(1)}, bf16[1152,128]{1,0:T(8,128)(2,1)S(1)}, u32[]{:S(2)}, u32[]{:S(2)}) collective-permute-start(bf16[1152,128]{1,0:T(8,128)(2,1)S(1)} %ffn.1.refs_0_), channel_id=1, source_target_pairs={{0,7},{1,0},{2,1},{3,2},{4,3},{5,4},{6,5},{7,6},{8,15},{9,8},{10,9... | collective-permute-start | bytes 884744 | tf_op jit(solution)/shard_map/ppermute | solution.py:190
  171.7 2.1 collective-permute-done.16.refs_1_
  173.8 1.9 collective-permute-start.18
  176.1 4.3 %collective-permute-start.19 = (bf16[1152,128]{1,0:T(8,128)(2,1)S(1)}, bf16[1152,128]{1,0:T(8,128)(2,1)S(1)}, u32[]{:S(2)}, u32[]{:S(2)}) collective-permute-start(bf16[1152,128]{1,0:T(8,128)(2,1)S(1)} %collective-permute-done.17.refs_2_), channel_id=1, source_target_pairs={{0,7},{1,0},{2,1},{3,2},{4,3},{5,4},{6,5},{7,6},{8,15},{9,8},{10,9... | collective-permute-start | bytes 884744 | tf_op jit(solution)/shard_map/ppermute | solution.py:190
  180.4 2.1 collective-permute-done.18.refs_3_
  182.5 1.9 collective-permute-start.20
  184.6 4.4 %collective-permute-start.21 = (bf16[1152,128]{1,0:T(8,128)(2,1)S(1)}, bf16[1152,128]{1,0:T(8,128)(2,1)S(1)}, u32[]{:S(2)}, u32[]{:S(2)}) collective-permute-start(bf16[1152,128]{1,0:T(8,128)(2,1)S(1)} %collective-permute-done.19.refs_4_), channel_id=1, source_target_pairs={{0,7},{1,0},{2,1},{3,2},{4,3},{5,4},{6,5},{7,6},{8,15},{9,8},{10,9... | collective-permute-start | bytes 884744 | tf_op jit(solution)/shard_map/ppermute | solution.py:190
  189.1 2.1 collective-permute-done.20.refs_5_
  191.2 1.9 collective-permute-start.22
  193.1 1.0 slice.47.refs_8_
  194.1 2.6 %collective-permute-start.1 = (bf16[32,16,256]{2,1,0:T(8,128)(2,1)S(1)}, bf16[32,16,256]{2,1,0:T(8,128)(2,1)S(1)}, u32[]{:S(2)}, u32[]{:S(2)}) collective-permute-start(bf16[32,16,256]{2,1,0:T(8,128)(2,1)S(1)} %slice.47.refs_8_), channel_id=1, source_target_pairs={{0,256},{256,0},{1,257},{257,1},{2,258},{258,2},{3,259},{259,3},{4... | collective-permute-start | bytes 786440 | tf_op jit(solution)/shard_map/ppermute | solution.py:235
  196.8 4.5 %collective-permute-done.1.refs_9_ = bf16[32,16,256]{2,1,0:T(8,128)(2,1)S(1)} collective-permute-done((bf16[32,16,256]{2,1,0:T(8,128)(2,1)S(1)}, bf16[32,16,256]{2,1,0:T(8,128)(2,1)S(1)}, u32[]{:S(2)}, u32[]{:S(2)}) %collective-permute-start.1) | collective-permute-done | bytes 262176 | tf_op jit(solution)/shard_map/ppermute | solution.py:235
  201.3 2.2 down.1
  203.5 14.3 %all-to-all-start.2 = ((bf16[32,72,128]{2,1,0:T(8,128)(2,1)}), bf16[32,72,128]{2,1,0:T(8,128)(2,1)S(1)}, u32[]{:S(2)}, u32[]{:S(2)}) async-start(bf16[32,72,128]{2,1,0:T(8,128)(2,1)} %down.1), calls=%async_computation.2 | async-start | bytes 1179648 | tf_op jit(solution)/shard_map/all_to_all | solution.py:185
  218.1 1.0 broadcast_select_fusion.1
  219.1 0.9 pad_maximum_fusion.3
  219.9 1.1 broadcast_select_fusion.3
  221.0 1.1 pad_maximum_fusion.1
  222.2 31.7 %all-to-all-done.2 = bf16[32,72,128]{2,1,0:T(8,128)(2,1)S(1)} async-done(((bf16[32,72,128]{2,1,0:T(8,128)(2,1)}), bf16[32,72,128]{2,1,0:T(8,128)(2,1)S(1)}, u32[]{:S(2)}, u32[]{:S(2)}) %all-to-all-start.2) | async-done | bytes 589856 | tf_op jit(solution)/shard_map/all_to_all | solution.py:185
  253.9 1.7 combine.1
  (32 shorter events, 1.1 us)
Async XLA Ops:
  0.6 47.8 %copy-start = (f32[32,32,256]{2,1,0:T(8,128)S(1)}, f32[32,32,256]{2,1,0:T(8,128)}, u32[]{:S(2)}) copy-start(f32[32,32,256]{2,1,0:T(8,128)} %param.11) | copy-start | bytes 3145732
  0.6 47.7 %copy-start.4 = (f32[64]{0:T(128)S(1)}, f32[64]{0:T(128)}, u32[]{:S(2)}) copy-start(f32[64]{0:T(128)} %param.8) | copy-start | bytes 772
  3.1 81.4 %all-to-all-start.1 = ((bf16[32,72,128]{2,1,0:T(8,128)(2,1)}), bf16[32,72,128]{2,1,0:T(8,128)(2,1)S(1)}, u32[]{:S(2)}, u32[]{:S(2)}) async-start(bf16[32,72,128]{2,1,0:T(8,128)(2,1)} %get-tuple-element.7), calls=%async_computation.1 | async-start | bytes 1179648 | tf_op jit(solution)/shard_map/all_to_all | solution.py:185
  84.5 49.8 %all-to-all-start = ((bf16[32,48,256]{2,1,0:T(8,128)(2,1)}), bf16[32,48,256]{2,1,0:T(8,128)(2,1)}, u32[]{:S(2)}, u32[]{:S(2)}) async-start(bf16[32,48,256]{2,1,0:T(8,128)(2,1)} %pad_maximum_fusion), calls=%async_computation | async-start | bytes 1572864 | tf_op jit(solution)/shard_map/all_to_all | solution.py:185
  89.8 30.4 %copy-start.2 = (bf16[16,72,128]{2,1,0:T(8,128)(2,1)}, bf16[16,72,128]{2,1,0:T(8,128)(2,1)S(1)}, u32[]{:S(2)}) copy-start(bf16[16,72,128]{2,1,0:T(8,128)(2,1)S(1)} %get-tuple-element.15) | copy-start | bytes 884740
  89.8 44.6 %copy-start.1 = (bf16[16,72,128]{2,1,0:T(8,128)(2,1)}, bf16[16,72,128]{2,1,0:T(8,128)(2,1)S(1)}, u32[]{:S(2)}) copy-start(bf16[16,72,128]{2,1,0:T(8,128)(2,1)S(1)} %get-tuple-element.14) | copy-start | bytes 884740
  89.8 13.6 %collective-permute-start.10 = (bf16[1152,128]{1,0:T(8,128)(2,1)S(1)}, bf16[1152,128]{1,0:T(8,128)(2,1)S(1)}, u32[]{:S(2)}, u32[]{:S(2)}) collective-permute-start(bf16[1152,128]{1,0:T(8,128)(2,1)S(1)} %bitcast.12), channel_id=1, source_target_pairs={{0,7},{1,0},{2,1},{3,2},{4,3},{5,4},{6,5},{7,6},{8,15},{9,8},{10,9... | collective-permute-start | bytes 884744 | tf_op jit(solution)/shard_map/ppermute | solution.py:190
  94.8 11.9 %collective-permute-start.2 = (bf16[1152,128]{1,0:T(8,128)(2,1)S(1)}, bf16[1152,128]{1,0:T(8,128)(2,1)S(1)}, u32[]{:S(2)}, u32[]{:S(2)}) collective-permute-start(bf16[1152,128]{1,0:T(8,128)(2,1)S(1)} %bitcast.15), channel_id=1, source_target_pairs={{0,1},{1,2},{2,3},{3,4},{4,5},{5,6},{6,7},{7,0},{8,9},{9,10},{10,1... | collective-permute-start | bytes 884744 | tf_op jit(solution)/shard_map/ppermute | solution.py:190
  96.8 14.9 %collective-permute-start.9 = (bf16[1152,128]{1,0:T(8,128)(2,1)S(1)}, bf16[1152,128]{1,0:T(8,128)(2,1)S(1)}, u32[]{:S(2)}, u32[]{:S(2)}) collective-permute-start(bf16[1152,128]{1,0:T(8,128)(2,1)S(1)} %bitcast.13), channel_id=1, source_target_pairs={{0,1},{1,2},{2,3},{3,4},{4,5},{5,6},{6,7},{7,0},{8,9},{9,10},{10,1... | collective-permute-start | bytes 884744 | tf_op jit(solution)/shard_map/ppermute | solution.py:190
  98.8 14.8 %collective-permute-start.3 = (bf16[1152,128]{1,0:T(8,128)(2,1)S(1)}, bf16[1152,128]{1,0:T(8,128)(2,1)S(1)}, u32[]{:S(2)}, u32[]{:S(2)}) collective-permute-start(bf16[1152,128]{1,0:T(8,128)(2,1)S(1)} %bitcast.16), channel_id=1, source_target_pairs={{0,7},{1,0},{2,1},{3,2},{4,3},{5,4},{6,5},{7,6},{8,15},{9,8},{10,9... | collective-permute-start | bytes 884744 | tf_op jit(solution)/shard_map/ppermute | solution.py:190
  103.4 14.9 %collective-permute-start.12 = (bf16[1152,128]{1,0:T(8,128)(2,1)S(1)}, bf16[1152,128]{1,0:T(8,128)(2,1)}, u32[]{:S(2)}, u32[]{:S(2)}) collective-permute-start(bf16[1152,128]{1,0:T(8,128)(2,1)S(1)} %collective-permute-done.10.refs_10_), channel_id=1, source_target_pairs={{0,7},{1,0},{2,1},{3,2},{4,3},{5,4},{6,5},{7,6},{8,15},{9,8},{10,9... | collective-permute-start | bytes 884744 | tf_op jit(solution)/shard_map/ppermute | solution.py:190
  106.8 13.4 %collective-permute-start.4 = (bf16[1152,128]{1,0:T(8,128)(2,1)S(1)}, bf16[1152,128]{1,0:T(8,128)(2,1)}, u32[]{:S(2)}, u32[]{:S(2)}) collective-permute-start(bf16[1152,128]{1,0:T(8,128)(2,1)S(1)} %collective-permute-done.2.refs_1_), channel_id=1, source_target_pairs={{0,1},{1,2},{2,3},{3,4},{4,5},{5,6},{6,7},{7,0},{8,9},{9,10},{10,1... | collective-permute-start | bytes 884744 | tf_op jit(solution)/shard_map/ppermute | solution.py:190
  111.7 27.8 %collective-permute-start.11 = (bf16[1152,128]{1,0:T(8,128)(2,1)S(1)}, bf16[1152,128]{1,0:T(8,128)(2,1)}, u32[]{:S(2)}, u32[]{:S(2)}) collective-permute-start(bf16[1152,128]{1,0:T(8,128)(2,1)S(1)} %collective-permute-done.9.refs_9_), channel_id=1, source_target_pairs={{0,1},{1,2},{2,3},{3,4},{4,5},{5,6},{6,7},{7,0},{8,9},{9,10},{10,1... | collective-permute-start | bytes 884744 | tf_op jit(solution)/shard_map/ppermute | solution.py:190
  113.6 29.1 %collective-permute-start.5 = (bf16[1152,128]{1,0:T(8,128)(2,1)S(1)}, bf16[1152,128]{1,0:T(8,128)(2,1)}, u32[]{:S(2)}, u32[]{:S(2)}) collective-permute-start(bf16[1152,128]{1,0:T(8,128)(2,1)S(1)} %collective-permute-done.3.refs_2_), channel_id=1, source_target_pairs={{0,7},{1,0},{2,1},{3,2},{4,3},{5,4},{6,5},{7,6},{8,15},{9,8},{10,9... | collective-permute-start | bytes 884744 | tf_op jit(solution)/shard_map/ppermute | solution.py:190
  118.2 28.7 %collective-permute-start.14 = (bf16[1152,128]{1,0:T(8,128)(2,1)}, bf16[1152,128]{1,0:T(8,128)(2,1)}, u32[]{:S(2)}, u32[]{:S(2)}) collective-permute-start(bf16[1152,128]{1,0:T(8,128)(2,1)} %collective-permute-done.12.refs_12_), channel_id=1, source_target_pairs={{0,7},{1,0},{2,1},{3,2},{4,3},{5,4},{6,5},{7,6},{8,15},{9,8},{10,9... | collective-permute-start | bytes 884744 | tf_op jit(solution)/shard_map/ppermute | solution.py:190
  120.2 30.1 %collective-permute-start.6 = (bf16[1152,128]{1,0:T(8,128)(2,1)}, bf16[1152,128]{1,0:T(8,128)(2,1)}, u32[]{:S(2)}, u32[]{:S(2)}) collective-permute-start(bf16[1152,128]{1,0:T(8,128)(2,1)} %collective-permute-done.4.refs_3_), channel_id=1, source_target_pairs={{0,1},{1,2},{2,3},{3,4},{4,5},{5,6},{6,7},{7,0},{8,9},{9,10},{10,1... | collective-permute-start | bytes 884744 | tf_op jit(solution)/shard_map/ppermute | solution.py:190
  135.4 24.9 %collective-permute-start = (bf16[32,32,256]{2,1,0:T(8,128)(2,1)S(1)}, bf16[32,32,256]{2,1,0:T(8,128)(2,1)S(1)}, u32[]{:S(2)}, u32[]{:S(2)}) collective-permute-start(bf16[32,32,256]{2,1,0:T(8,128)(2,1)S(1)} %slice.43.refs_16_), channel_id=1, source_target_pairs={{0,256},{256,0},{1,257},{257,1},{2,258},{258,2},{3,259},{259,3},{4... | collective-permute-start | bytes 1572872 | tf_op jit(solution)/shard_map/ppermute | solution.py:235
  139.4 12.9 %collective-permute-start.13 = (bf16[1152,128]{1,0:T(8,128)(2,1)}, bf16[1152,128]{1,0:T(8,128)(2,1)}, u32[]{:S(2)}, u32[]{:S(2)}) collective-permute-start(bf16[1152,128]{1,0:T(8,128)(2,1)} %collective-permute-done.11.refs_11_), channel_id=1, source_target_pairs={{0,1},{1,2},{2,3},{3,4},{4,5},{5,6},{6,7},{7,0},{8,9},{9,10},{10,1... | collective-permute-start | bytes 884744 | tf_op jit(solution)/shard_map/ppermute | solution.py:190
  142.7 9.6 %collective-permute-start.7 = (bf16[1152,128]{1,0:T(8,128)(2,1)}, bf16[1152,128]{1,0:T(8,128)(2,1)}, u32[]{:S(2)}, u32[]{:S(2)}) collective-permute-start(bf16[1152,128]{1,0:T(8,128)(2,1)} %collective-permute-done.5.refs_4_), channel_id=1, source_target_pairs={{0,7},{1,0},{2,1},{3,2},{4,3},{5,4},{6,5},{7,6},{8,15},{9,8},{10,9... | collective-permute-start | bytes 884744 | tf_op jit(solution)/shard_map/ppermute | solution.py:190
  146.9 11.8 %collective-permute-start.15 = (bf16[1152,128]{1,0:T(8,128)(2,1)}, bf16[1152,128]{1,0:T(8,128)(2,1)}, u32[]{:S(2)}, u32[]{:S(2)}) collective-permute-start(bf16[1152,128]{1,0:T(8,128)(2,1)} %collective-permute-done.14.refs_14_), channel_id=1, source_target_pairs={{0,7},{1,0},{2,1},{3,2},{4,3},{5,4},{6,5},{7,6},{8,15},{9,8},{10,9... | collective-permute-start | bytes 884744 | tf_op jit(solution)/shard_map/ppermute | solution.py:190
  150.3 10.0 %collective-permute-start.8 = (bf16[1152,128]{1,0:T(8,128)(2,1)}, bf16[1152,128]{1,0:T(8,128)(2,1)}, u32[]{:S(2)}, u32[]{:S(2)}) collective-permute-start(bf16[1152,128]{1,0:T(8,128)(2,1)} %collective-permute-done.6.refs_5_), channel_id=1, source_target_pairs={{0,1},{1,2},{2,3},{3,4},{4,5},{5,6},{6,7},{7,0},{8,9},{9,10},{10,1... | collective-permute-start | bytes 884744 | tf_op jit(solution)/shard_map/ppermute | solution.py:190
  165.1 8.7 %collective-permute-start.16 = (bf16[1152,128]{1,0:T(8,128)(2,1)S(1)}, bf16[1152,128]{1,0:T(8,128)(2,1)S(1)}, u32[]{:S(2)}, u32[]{:S(2)}) collective-permute-start(bf16[1152,128]{1,0:T(8,128)(2,1)S(1)} %ffn.1.refs_0_), channel_id=1, source_target_pairs={{0,1},{1,2},{2,3},{3,4},{4,5},{5,6},{6,7},{7,0},{8,9},{9,10},{10,1... | collective-permute-start | bytes 884744 | tf_op jit(solution)/shard_map/ppermute | solution.py:190
  167.1 9.0 %collective-permute-start.17 = (bf16[1152,128]{1,0:T(8,128)(2,1)S(1)}, bf16[1152,128]{1,0:T(8,128)(2,1)S(1)}, u32[]{:S(2)}, u32[]{:S(2)}) collective-permute-start(bf16[1152,128]{1,0:T(8,128)(2,1)S(1)} %ffn.1.refs_0_), channel_id=1, source_target_pairs={{0,7},{1,0},{2,1},{3,2},{4,3},{5,4},{6,5},{7,6},{8,15},{9,8},{10,9... | collective-permute-start | bytes 884744 | tf_op jit(solution)/shard_map/ppermute | solution.py:190
  173.8 8.7 %collective-permute-start.18 = (bf16[1152,128]{1,0:T(8,128)(2,1)S(1)}, bf16[1152,128]{1,0:T(8,128)(2,1)S(1)}, u32[]{:S(2)}, u32[]{:S(2)}) collective-permute-start(bf16[1152,128]{1,0:T(8,128)(2,1)S(1)} %collective-permute-done.16.refs_1_), channel_id=1, source_target_pairs={{0,1},{1,2},{2,3},{3,4},{4,5},{5,6},{6,7},{7,0},{8,9},{9,10},{10,1... | collective-permute-start | bytes 884744 | tf_op jit(solution)/shard_map/ppermute | solution.py:190
  176.1 8.6 %collective-permute-start.19 = (bf16[1152,128]{1,0:T(8,128)(2,1)S(1)}, bf16[1152,128]{1,0:T(8,128)(2,1)S(1)}, u32[]{:S(2)}, u32[]{:S(2)}) collective-permute-start(bf16[1152,128]{1,0:T(8,128)(2,1)S(1)} %collective-permute-done.17.refs_2_), channel_id=1, source_target_pairs={{0,7},{1,0},{2,1},{3,2},{4,3},{5,4},{6,5},{7,6},{8,15},{9,8},{10,9... | collective-permute-start | bytes 884744 | tf_op jit(solution)/shard_map/ppermute | solution.py:190
  182.5 8.7 %collective-permute-start.20 = (bf16[1152,128]{1,0:T(8,128)(2,1)S(1)}, bf16[1152,128]{1,0:T(8,128)(2,1)S(1)}, u32[]{:S(2)}, u32[]{:S(2)}) collective-permute-start(bf16[1152,128]{1,0:T(8,128)(2,1)S(1)} %collective-permute-done.18.refs_3_), channel_id=1, source_target_pairs={{0,1},{1,2},{2,3},{3,4},{4,5},{5,6},{6,7},{7,0},{8,9},{9,10},{10,1... | collective-permute-start | bytes 884744 | tf_op jit(solution)/shard_map/ppermute | solution.py:190
  184.6 16.6 %collective-permute-start.21 = (bf16[1152,128]{1,0:T(8,128)(2,1)S(1)}, bf16[1152,128]{1,0:T(8,128)(2,1)S(1)}, u32[]{:S(2)}, u32[]{:S(2)}) collective-permute-start(bf16[1152,128]{1,0:T(8,128)(2,1)S(1)} %collective-permute-done.19.refs_4_), channel_id=1, source_target_pairs={{0,7},{1,0},{2,1},{3,2},{4,3},{5,4},{6,5},{7,6},{8,15},{9,8},{10,9... | collective-permute-start | bytes 884744 | tf_op jit(solution)/shard_map/ppermute | solution.py:190
  191.2 10.1 %collective-permute-start.22 = (bf16[1152,128]{1,0:T(8,128)(2,1)S(1)}, bf16[1152,128]{1,0:T(8,128)(2,1)S(1)}, u32[]{:S(2)}, u32[]{:S(2)}) collective-permute-start(bf16[1152,128]{1,0:T(8,128)(2,1)S(1)} %collective-permute-done.20.refs_5_), channel_id=1, source_target_pairs={{0,1},{1,2},{2,3},{3,4},{4,5},{5,6},{6,7},{7,0},{8,9},{9,10},{10,1... | collective-permute-start | bytes 884744 | tf_op jit(solution)/shard_map/ppermute | solution.py:190
  194.1 7.1 %collective-permute-start.1 = (bf16[32,16,256]{2,1,0:T(8,128)(2,1)S(1)}, bf16[32,16,256]{2,1,0:T(8,128)(2,1)S(1)}, u32[]{:S(2)}, u32[]{:S(2)}) collective-permute-start(bf16[32,16,256]{2,1,0:T(8,128)(2,1)S(1)} %slice.47.refs_8_), channel_id=1, source_target_pairs={{0,256},{256,0},{1,257},{257,1},{2,258},{258,2},{3,259},{259,3},{4... | collective-permute-start | bytes 786440 | tf_op jit(solution)/shard_map/ppermute | solution.py:235
  203.5 14.4 %copy-start.3 = (f32[384,2]{0,1:T(2,128)S(1)}, f32[384,2]{0,1:T(2,128)}, u32[]{:S(2)}) copy-start(f32[384,2]{0,1:T(2,128)} %param.13) | copy-start | bytes 9220
  203.5 50.4 %all-to-all-start.2 = ((bf16[32,72,128]{2,1,0:T(8,128)(2,1)}), bf16[32,72,128]{2,1,0:T(8,128)(2,1)S(1)}, u32[]{:S(2)}, u32[]{:S(2)}) async-start(bf16[32,72,128]{2,1,0:T(8,128)(2,1)} %down.1), calls=%async_computation.2 | async-start | bytes 1179648 | tf_op jit(solution)/shard_map/all_to_all | solution.py:185

commit v6 on v5

--- a/solution.py
+++ b/solution.py
@@ -7,7 +7,8 @@
 
 
 CAP = 36
-FETCHED = (0,)
+SPREAD = 4
+FETCHED = (0, 1, 2)
 MAIN = 32
 SLAB = 72
 HALF = 128
@@ -97,11 +98,10 @@
 
 
 def ffn_kernel(me, *refs):
-    chunks, pieces = (refs[0:8], refs[8:16]), refs[16:-4]
-    hidden, serve, held, done = refs[-4:]
+    chunks, weights, hidden, held, done = (refs[0:8], refs[8:16]), *refs[16:]
     sources = offsets_of(me[0])
-    features = serve.shape[0] * serve.shape[1]
-    spread = 2 * HALF // serve.shape[1]
+    rows = 2 * HALF // SPREAD
+    features = weights.shape[0] * rows
     part, slabs = 8 * CAP, 8 * SLAB
 
     def fetch(g, n):
@@ -111,7 +111,6 @@
     for g in range(4):
         for n in range(len(FETCHED)):
             fetch(g, n).start()
-    join_pieces(me[1], pieces, serve)
     order = [k for k in range(8) if k not in FETCHED] + list(FETCHED)
     for g in range(4):
         acc = jnp.zeros((part, 2 * HALF), F32)
@@ -123,7 +122,7 @@
             else:
                 x = chunks[g // 2][k][(g % 2) * slabs : (g % 2 + 1) * slabs, :]
             left, right = from_slabs(x)
-            w = serve[pl.ds(sources[k] * spread, spread)].reshape(2 * HALF, 2 * HALF)
+            w = weights[pl.ds(sources[k] * SPREAD, SPREAD), :rows, :].reshape(2 * HALF, 2 * HALF)
             both = jnp.concatenate([left, right], axis=1)
             acc = acc + jnp.dot(both, w, preferred_element_type=F32)
             l32, r32 = left.astype(F32), right.astype(F32)
@@ -156,8 +155,10 @@
         to_slabs(acc, out, 8 * g)
 
 
-def combine_kernel(rows, gains, returned, mixture):
+def combine_kernel(rows, gains_in, returned, mixture, gains, done):
     n_tok = rows.shape[0]
+    fetch = pltpu.make_async_copy(gains_in, gains, done)
+    fetch.start()
     slabs, part = 8 * SLAB, 8 * CAP
     sums = [jnp.zeros((n_tok, 2 * HALF), F32) for _ in range(2)]
     for g in range(returned.shape[0] // slabs):
@@ -167,6 +168,7 @@
         for k in range(2):
             onehot = (ids == rows[:, k : k + 1]).astype(F32).astype(BF16)
             sums[k] = sums[k] + jnp.dot(onehot, both, preferred_element_type=F32)
+    fetch.wait()
     mixture[...] = (gains[:, 0:1] * sums[0] + gains[:, 1:2] * sums[1]).astype(BF16)
 
 
@@ -234,22 +236,20 @@
             return [x]
         return [x, lax.ppermute(x, "grp", [(g, g ^ 1) for g in range(groups)])]
 
-    gain = piece(norm_gain, 0)[None, :, None]
-    both_low = jnp.concatenate([gain * piece(gate_weight, 1), gain * piece(up_weight, 1)], axis=2)
+    gain = norm_gain[None, :, None]
+    both_low = jnp.concatenate([gain * gate_weight, gain * up_weight], axis=2)
     weights_low = jnp.concatenate([both_low, piece(down_weight, 1)], axis=1).astype(BF16)
     arrived_weights = all_to_all(weights_low)
-    both_pieces = swapped(arrived_weights[:, : rows_in // count])
-    down_pieces = swapped(arrived_weights[:, rows_in // count :])
+    down_pieces = swapped(arrived_weights[:, rows_in:])
     cut = experts * SLAB // 2
     chunks = ring(arrived[:cut], "r") + ring(arrived[cut:], "l")
     fetched = [n % 8 in FETCHED for n in range(16)]
     hidden = pl.pallas_call(
         ffn_kernel,
-        in_specs=[smem] + [anywhere if f else vmem for f in fetched] + [vmem] * count,
+        in_specs=[smem] + [anywhere if f else vmem for f in fetched] + [vmem],
         out_specs=vmem,
         out_shape=pltpu.VMEM((experts * CAP, cols), BF16),
         scratch_shapes=[
-            pltpu.VMEM((experts, rows_in, 2 * cols), BF16),
             pltpu.VMEM((4, len(FETCHED), 8 * SLAB, HALF), BF16),
             pltpu.SemaphoreType.DMA((4, len(FETCHED))),
         ],
@@ -258,7 +258,7 @@
     )(
         me,
         *[(in_hbm if f else in_vmem)(x)[0] for f, x in zip(fetched, chunks)],
-        *in_vmem(*both_pieces),
+        *in_vmem(arrived_weights),
     )
     expert_out = pl.pallas_call(
         down_kernel,
@@ -272,12 +272,13 @@
     returned = all_to_all(expert_out).reshape(experts * SLAB, HALF)
     mixture = pl.pallas_call(
         combine_kernel,
-        in_specs=[vmem] * 3,
+        in_specs=[vmem, anywhere, vmem],
         out_specs=vmem,
+        scratch_shapes=[pltpu.VMEM(route_weights.shape, F32), pltpu.SemaphoreType.DMA],
         out_shape=jax.ShapeDtypeStruct(tokens.shape, BF16),
         name="combine",
         compiler_params=LIMIT,
-    )(*in_vmem(rows.T, route_weights, returned))
+    )(*in_vmem(rows.T), *in_hbm(route_weights), *in_vmem(returned))
 
     def assembled(pieces):
         if count == 1:
@@ -286,8 +287,8 @@
         both = jnp.where(mine == 0, own, other), jnp.where(mine == 0, other, own)
         return jnp.concatenate(both, axis=1).reshape(1, -1, own.shape[2])
 
-    gate_serve = assembled([x[:, :, :cols] for x in both_pieces])
-    up_serve = assembled([x[:, :, cols:] for x in both_pieces])
+    both_serve = arrived_weights[:, :rows_in].reshape(1, -1, 2 * cols)
+    gate_serve, up_serve = both_serve[:, :, :cols], both_serve[:, :, cols:]
     return (gate_serve, up_serve, assembled(down_pieces), mixture)
 
 

time: 257 us -> 255 us (level)
  the two profiles are of different devices: /device:TPU:65 before, /device:TPU:71 now
where the time goes in v6:
time: 255 us; the launch traced here: 253 us
  starting transfers between devices  134 us (53%)
  waiting for transfers between devices  99.6 us (39%)
  Pallas kernels  12 us (5%)
  other arithmetic  4.09 us (2%)
    all_to_all x3, waiting for transfers between devices, all_to_all(): return lax.all_to_all(x, 'fs', split_axis=0, concat_axis=0, tiled=True)  82.1 us
    ppermute x21, starting transfers between devices, step(): return lax.ppermute(x, 'tp', [(d, (d + shift) % n) for d in range(n)])  69.6 us
    all_to_all x3, starting transfers between devices, all_to_all(): return lax.all_to_all(x, 'fs', split_axis=0, concat_axis=0, tiled=True)  60.3 us
    ppermute x21, waiting for transfers between devices, step(): return lax.ppermute(x, 'tp', [(d, (d + shift) % n) for d in range(n)])  13.8 us
  transfers between devices with their start and end apart: 25, of which 10 were waited for; matrix products, arithmetic and copies ran while one was open for 2% of the time, Pallas kernels for 0%

profile of v6, /device:TPU:71, one launch (start us, length us, event | category | flops | bytes accessed | tf_op | source)
XLA Modules:
  0.0 253.5 jit_solution(7728193256318212486)
XLA Ops:
  0.7 2.4 route.1
  3.1 44.4 %all-to-all-start.1 = ((bf16[32,72,128]{2,1,0:T(8,128)(2,1)}), bf16[32,72,128]{2,1,0:T(8,128)(2,1)S(1)}, u32[]{:S(2)}, u32[]{:S(2)}) async-start(bf16[32,72,128]{2,1,0:T(8,128)(2,1)} %get-tuple-element.7), calls=%async_computation.1 | async-start | bytes 1179648 | tf_op jit(solution)/shard_map/all_to_all | solution.py:187
  47.5 1.9 multiply_convert_fusion.1
  49.4 1.2 pad_maximum_fusion
  50.6 32.9 %all-to-all-done.1 = bf16[32,72,128]{2,1,0:T(8,128)(2,1)S(1)} async-done(((bf16[32,72,128]{2,1,0:T(8,128)(2,1)}), bf16[32,72,128]{2,1,0:T(8,128)(2,1)S(1)}, u32[]{:S(2)}, u32[]{:S(2)}) %all-to-all-start.1) | async-done | bytes 589856 | tf_op jit(solution)/shard_map/all_to_all | solution.py:187
  83.5 4.3 %all-to-all-start = ((bf16[32,80,256]{2,1,0:T(8,128)(2,1)}), bf16[32,80,256]{2,1,0:T(8,128)(2,1)S(1)}, u32[]{:S(2)}, u32[]{:S(2)}) async-start(bf16[32,80,256]{2,1,0:T(8,128)(2,1)} %pad_maximum_fusion), calls=%async_computation | async-start | bytes 2621440 | tf_op jit(solution)/shard_map/all_to_all | solution.py:187
  88.0 2.1 collective-permute-start.9
  90.0 4.5 %collective-permute-start.1 = (bf16[1152,128]{1,0:T(8,128)(2,1)S(1)}, bf16[1152,128]{1,0:T(8,128)(2,1)S(1)}, u32[]{:S(2)}, u32[]{:S(2)}) collective-permute-start(bf16[1152,128]{1,0:T(8,128)(2,1)S(1)} %bitcast.15), channel_id=1, source_target_pairs={{0,1},{1,2},{2,3},{3,4},{4,5},{5,6},{6,7},{7,0},{8,9},{9,10},{10,1... | collective-permute-start | bytes 884744 | tf_op jit(solution)/shard_map/ppermute | solution.py:192
  94.5 3.3 %collective-permute-start.8 = (bf16[1152,128]{1,0:T(8,128)(2,1)S(1)}, bf16[1152,128]{1,0:T(8,128)(2,1)S(1)}, u32[]{:S(2)}, u32[]{:S(2)}) collective-permute-start(bf16[1152,128]{1,0:T(8,128)(2,1)S(1)} %bitcast.13), channel_id=1, source_target_pairs={{0,1},{1,2},{2,3},{3,4},{4,5},{5,6},{6,7},{7,0},{8,9},{9,10},{10,1... | collective-permute-start | bytes 884744 | tf_op jit(solution)/shard_map/ppermute | solution.py:192
  97.8 2.1 collective-permute-start.2
  99.9 2.0 collective-permute-start.11
  101.9 4.6 %collective-permute-start.3 = (bf16[1152,128]{1,0:T(8,128)(2,1)S(1)}, bf16[1152,128]{1,0:T(8,128)(2,1)S(1)}, u32[]{:S(2)}, u32[]{:S(2)}) collective-permute-start(bf16[1152,128]{1,0:T(8,128)(2,1)S(1)} %collective-permute-done.1.refs_1_), channel_id=1, source_target_pairs={{0,1},{1,2},{2,3},{3,4},{4,5},{5,6},{6,7},{7,0},{8,9},{9,10},{10,1... | collective-permute-start | bytes 884744 | tf_op jit(solution)/shard_map/ppermute | solution.py:192
  106.5 4.7 %collective-permute-start.10 = (bf16[1152,128]{1,0:T(8,128)(2,1)S(1)}, bf16[1152,128]{1,0:T(8,128)(2,1)S(1)}, u32[]{:S(2)}, u32[]{:S(2)}) collective-permute-start(bf16[1152,128]{1,0:T(8,128)(2,1)S(1)} %collective-permute-done.8.refs_9_), channel_id=1, source_target_pairs={{0,1},{1,2},{2,3},{3,4},{4,5},{5,6},{6,7},{7,0},{8,9},{9,10},{10,1... | collective-permute-start | bytes 884744 | tf_op jit(solution)/shard_map/ppermute | solution.py:192
  111.3 2.0 collective-permute-start.4
  113.2 0.8 collective-permute-done.11.refs_12_
  114.0 1.9 collective-permute-start.13
  115.9 4.6 %collective-permute-start.5 = (bf16[1152,128]{1,0:T(8,128)(2,1)S(1)}, bf16[1152,128]{1,0:T(8,128)(2,1)}, u32[]{:S(2)}, u32[]{:S(2)}) collective-permute-start(bf16[1152,128]{1,0:T(8,128)(2,1)S(1)} %collective-permute-done.3.refs_3_), channel_id=1, source_target_pairs={{0,1},{1,2},{2,3},{3,4},{4,5},{5,6},{6,7},{7,0},{8,9},{9,10},{10,1... | collective-permute-start | bytes 884744 | tf_op jit(solution)/shard_map/ppermute | solution.py:192
  120.6 2.9 %collective-permute-start.12 = (bf16[1152,128]{1,0:T(8,128)(2,1)S(1)}, bf16[1152,128]{1,0:T(8,128)(2,1)}, u32[]{:S(2)}, u32[]{:S(2)}) collective-permute-start(bf16[1152,128]{1,0:T(8,128)(2,1)S(1)} %collective-permute-done.10.refs_11_), channel_id=1, source_target_pairs={{0,1},{1,2},{2,3},{3,4},{4,5},{5,6},{6,7},{7,0},{8,9},{9,10},{10,1... | collective-permute-start | bytes 884744 | tf_op jit(solution)/shard_map/ppermute | solution.py:192
  123.4 2.5 collective-permute-start.6
  125.9 0.2 collective-permute-done.13.refs_14_
  126.2 1.9 collective-permute-start.14
  128.2 4.6 %collective-permute-start.7 = (bf16[1152,128]{1,0:T(8,128)(2,1)}, bf16[1152,128]{1,0:T(8,128)(2,1)}, u32[]{:S(2)}, u32[]{:S(2)}) collective-permute-start(bf16[1152,128]{1,0:T(8,128)(2,1)} %collective-permute-done.5.refs_5_), channel_id=1, source_target_pairs={{0,1},{1,2},{2,3},{3,4},{4,5},{5,6},{6,7},{7,0},{8,9},{9,10},{10,1... | collective-permute-start | bytes 884744 | tf_op jit(solution)/shard_map/ppermute | solution.py:192
  132.8 0.1 pad_add_fusion.me
  132.9 0.0 collective-permute-done.6.refs_6_
  132.9 5.6 %collective-permute-done.14.refs_15_ = bf16[1152,128]{1,0:T(8,128)(2,1)} collective-permute-done((bf16[1152,128]{1,0:T(8,128)(2,1)}, bf16[1152,128]{1,0:T(8,128)(2,1)}, u32[]{:S(2)}, u32[]{:S(2)}) %collective-permute-start.14) | collective-permute-done | bytes 294944 | tf_op jit(solution)/shard_map/ppermute | solution.py:192
  138.5 16.2 %all-to-all-done.refs_16_ = bf16[32,80,256]{2,1,0:T(8,128)(2,1)S(1)} async-done(((bf16[32,80,256]{2,1,0:T(8,128)(2,1)}), bf16[32,80,256]{2,1,0:T(8,128)(2,1)S(1)}, u32[]{:S(2)}, u32[]{:S(2)}) %all-to-all-start) | async-done | bytes 1310752 | tf_op jit(solution)/shard_map/all_to_all | solution.py:187
  154.6 4.9 %ffn.1.refs_0_ = bf16[1152,128]{1,0:T(8,128)(2,1)S(1)} custom-call(s32[2]{0:T(128)S(1)} %pad_add_fusion.me, bf16[1152,128]{1,0:T(8,128)(2,1)} %bitcast.17, bf16[1152,128]{1,0:T(8,128)(2,1)} %copy-done.4, bf16[1152,128]{1,0:T(8,128)(2,1)} %copy-done.6, bf16[1152,128]{1,0:T(8,128)(2,1)S(1)} %collective-permute-done.3.refs_3_, ...), custom_call_target="tpu_custom_call" | custom-call | tf_op jit(solution)/shard_map/ffn/pallas_call | solution.py:247
  159.5 4.5 %collective-permute-start.15 = (bf16[1152,128]{1,0:T(8,128)(2,1)S(1)}, bf16[1152,128]{1,0:T(8,128)(2,1)S(1)}, u32[]{:S(2)}, u32[]{:S(2)}) collective-permute-start(bf16[1152,128]{1,0:T(8,128)(2,1)S(1)} %ffn.1.refs_0_), channel_id=1, source_target_pairs={{0,1},{1,2},{2,3},{3,4},{4,5},{5,6},{6,7},{7,0},{8,9},{9,10},{10,1... | collective-permute-start | bytes 884744 | tf_op jit(solution)/shard_map/ppermute | solution.py:192
  164.0 2.0 collective-permute-start.16
  166.0 3.2 %collective-permute-done.15.refs_1_ = bf16[1152,128]{1,0:T(8,128)(2,1)S(1)} collective-permute-done((bf16[1152,128]{1,0:T(8,128)(2,1)S(1)}, bf16[1152,128]{1,0:T(8,128)(2,1)S(1)}, u32[]{:S(2)}, u32[]{:S(2)}) %collective-permute-start.15) | collective-permute-done | bytes 294944 | tf_op jit(solution)/shard_map/ppermute | solution.py:192
  169.2 5.3 %collective-permute-start.17 = (bf16[1152,128]{1,0:T(8,128)(2,1)S(1)}, bf16[1152,128]{1,0:T(8,128)(2,1)S(1)}, u32[]{:S(2)}, u32[]{:S(2)}) collective-permute-start(bf16[1152,128]{1,0:T(8,128)(2,1)S(1)} %collective-permute-done.15.refs_1_), channel_id=1, source_target_pairs={{0,1},{1,2},{2,3},{3,4},{4,5},{5,6},{6,7},{7,0},{8,9},{9,10},{10,1... | collective-permute-start | bytes 884744 | tf_op jit(solution)/shard_map/ppermute | solution.py:192
  174.5 2.0 collective-permute-start.18
  176.5 2.3 collective-permute-done.17.refs_3_
  178.8 5.3 %collective-permute-start.19 = (bf16[1152,128]{1,0:T(8,128)(2,1)S(1)}, bf16[1152,128]{1,0:T(8,128)(2,1)S(1)}, u32[]{:S(2)}, u32[]{:S(2)}) collective-permute-start(bf16[1152,128]{1,0:T(8,128)(2,1)S(1)} %collective-permute-done.17.refs_3_), channel_id=1, source_target_pairs={{0,1},{1,2},{2,3},{3,4},{4,5},{5,6},{6,7},{7,0},{8,9},{9,10},{10,1... | collective-permute-start | bytes 884744 | tf_op jit(solution)/shard_map/ppermute | solution.py:192
  184.2 2.0 collective-permute-start.20
  186.1 1.7 collective-permute-done.19.refs_5_
  187.8 5.0 %collective-permute-start.21 = (bf16[1152,128]{1,0:T(8,128)(2,1)S(1)}, bf16[1152,128]{1,0:T(8,128)(2,1)S(1)}, u32[]{:S(2)}, u32[]{:S(2)}) collective-permute-start(bf16[1152,128]{1,0:T(8,128)(2,1)S(1)} %collective-permute-done.19.refs_5_), channel_id=1, source_target_pairs={{0,1},{1,2},{2,3},{3,4},{4,5},{5,6},{6,7},{7,0},{8,9},{9,10},{10,1... | collective-permute-start | bytes 884744 | tf_op jit(solution)/shard_map/ppermute | solution.py:192
  192.9 4.4 %collective-permute-start = (bf16[32,16,256]{2,1,0:T(8,128)(2,1)S(1)}, bf16[32,16,256]{2,1,0:T(8,128)(2,1)S(1)}, u32[]{:S(2)}, u32[]{:S(2)}) collective-permute-start(bf16[32,16,256]{2,1,0:T(8,128)(2,1)S(1)} %slice.35.refs_8_), channel_id=1, source_target_pairs={{0,256},{256,0},{1,257},{257,1},{2,258},{258,2},{3,259},{259,3},{4... | collective-permute-start | bytes 786440 | tf_op jit(solution)/shard_map/ppermute | solution.py:237
  197.3 3.7 %collective-permute-done.refs_9_ = bf16[32,16,256]{2,1,0:T(8,128)(2,1)S(1)} collective-permute-done((bf16[32,16,256]{2,1,0:T(8,128)(2,1)S(1)}, bf16[32,16,256]{2,1,0:T(8,128)(2,1)S(1)}, u32[]{:S(2)}, u32[]{:S(2)}) %collective-permute-start) | collective-permute-done | bytes 262176 | tf_op jit(solution)/shard_map/ppermute | solution.py:237
  201.1 2.2 down.1
  203.3 11.6 %all-to-all-start.2 = ((bf16[32,72,128]{2,1,0:T(8,128)(2,1)}), bf16[32,72,128]{2,1,0:T(8,128)(2,1)S(1)}, u32[]{:S(2)}, u32[]{:S(2)}) async-start(bf16[32,72,128]{2,1,0:T(8,128)(2,1)} %down.1), calls=%async_computation.2 | async-start | bytes 1179648 | tf_op jit(solution)/shard_map/all_to_all | solution.py:187
  214.9 0.1 copy.11
  215.0 0.8 copy.12.gains_in
  215.9 0.1 slice.32
  216.0 1.0 fusion
  217.1 0.9 pad_maximum_fusion.1
  218.0 33.0 %all-to-all-done.2 = bf16[32,72,128]{2,1,0:T(8,128)(2,1)S(1)} async-done(((bf16[32,72,128]{2,1,0:T(8,128)(2,1)}), bf16[32,72,128]{2,1,0:T(8,128)(2,1)S(1)}, u32[]{:S(2)}, u32[]{:S(2)}) %all-to-all-start.2) | async-done | bytes 589856 | tf_op jit(solution)/shard_map/all_to_all | solution.py:187
  251.0 2.5 combine.1
  (36 shorter events, 0.2 us)
Async XLA Ops:
  0.6 46.8 %copy-start = (f32[32,32,256]{2,1,0:T(8,128)S(1)}, f32[32,32,256]{2,1,0:T(8,128)}, u32[]{:S(2)}) copy-start(f32[32,32,256]{2,1,0:T(8,128)} %param.11) | copy-start | bytes 3145732
  0.6 46.9 %copy-start.8 = (f32[64]{0:T(128)S(1)}, f32[64]{0:T(128)}, u32[]{:S(2)}) copy-start(f32[64]{0:T(128)} %param.8) | copy-start | bytes 772
  3.1 80.5 %all-to-all-start.1 = ((bf16[32,72,128]{2,1,0:T(8,128)(2,1)}), bf16[32,72,128]{2,1,0:T(8,128)(2,1)S(1)}, u32[]{:S(2)}, u32[]{:S(2)}) async-start(bf16[32,72,128]{2,1,0:T(8,128)(2,1)} %get-tuple-element.7), calls=%async_computation.1 | async-start | bytes 1179648 | tf_op jit(solution)/shard_map/all_to_all | solution.py:187
  83.5 71.1 %all-to-all-start = ((bf16[32,80,256]{2,1,0:T(8,128)(2,1)}), bf16[32,80,256]{2,1,0:T(8,128)(2,1)S(1)}, u32[]{:S(2)}, u32[]{:S(2)}) async-start(bf16[32,80,256]{2,1,0:T(8,128)(2,1)} %pad_maximum_fusion), calls=%async_computation | async-start | bytes 2621440 | tf_op jit(solution)/shard_map/all_to_all | solution.py:187
  87.9 40.2 %copy-start.1 = (bf16[16,72,128]{2,1,0:T(8,128)(2,1)}, bf16[16,72,128]{2,1,0:T(8,128)(2,1)S(1)}, u32[]{:S(2)}) copy-start(bf16[16,72,128]{2,1,0:T(8,128)(2,1)S(1)} %get-tuple-element.12) | copy-start | bytes 884740
  87.9 40.2 %copy-start.2 = (bf16[16,72,128]{2,1,0:T(8,128)(2,1)}, bf16[16,72,128]{2,1,0:T(8,128)(2,1)S(1)}, u32[]{:S(2)}) copy-start(bf16[16,72,128]{2,1,0:T(8,128)(2,1)S(1)} %get-tuple-element.13) | copy-start | bytes 884740
  88.0 11.9 %collective-permute-start.9 = (bf16[1152,128]{1,0:T(8,128)(2,1)S(1)}, bf16[1152,128]{1,0:T(8,128)(2,1)S(1)}, u32[]{:S(2)}, u32[]{:S(2)}) collective-permute-start(bf16[1152,128]{1,0:T(8,128)(2,1)S(1)} %bitcast.12), channel_id=1, source_target_pairs={{0,7},{1,0},{2,1},{3,2},{4,3},{5,4},{6,5},{7,6},{8,15},{9,8},{10,9... | collective-permute-start | bytes 884744 | tf_op jit(solution)/shard_map/ppermute | solution.py:192
  90.0 11.8 %collective-permute-start.1 = (bf16[1152,128]{1,0:T(8,128)(2,1)S(1)}, bf16[1152,128]{1,0:T(8,128)(2,1)S(1)}, u32[]{:S(2)}, u32[]{:S(2)}) collective-permute-start(bf16[1152,128]{1,0:T(8,128)(2,1)S(1)} %bitcast.15), channel_id=1, source_target_pairs={{0,1},{1,2},{2,3},{3,4},{4,5},{5,6},{6,7},{7,0},{8,9},{9,10},{10,1... | collective-permute-start | bytes 884744 | tf_op jit(solution)/shard_map/ppermute | solution.py:192
  94.5 12.0 %collective-permute-start.8 = (bf16[1152,128]{1,0:T(8,128)(2,1)S(1)}, bf16[1152,128]{1,0:T(8,128)(2,1)S(1)}, u32[]{:S(2)}, u32[]{:S(2)}) collective-permute-start(bf16[1152,128]{1,0:T(8,128)(2,1)S(1)} %bitcast.13), channel_id=1, source_target_pairs={{0,1},{1,2},{2,3},{3,4},{4,5},{5,6},{6,7},{7,0},{8,9},{9,10},{10,1... | collective-permute-start | bytes 884744 | tf_op jit(solution)/shard_map/ppermute | solution.py:192
  97.8 13.4 %collective-permute-start.2 = (bf16[1152,128]{1,0:T(8,128)(2,1)S(1)}, bf16[1152,128]{1,0:T(8,128)(2,1)S(1)}, u32[]{:S(2)}, u32[]{:S(2)}) collective-permute-start(bf16[1152,128]{1,0:T(8,128)(2,1)S(1)} %bitcast.16), channel_id=1, source_target_pairs={{0,7},{1,0},{2,1},{3,2},{4,3},{5,4},{6,5},{7,6},{8,15},{9,8},{10,9... | collective-permute-start | bytes 884744 | tf_op jit(solution)/shard_map/ppermute | solution.py:192
  99.9 28.3 %copy-start.3 = (bf16[1152,128]{1,0:T(8,128)(2,1)}, bf16[1152,128]{1,0:T(8,128)(2,1)S(1)}, u32[]{:S(2)}) copy-start(bf16[1152,128]{1,0:T(8,128)(2,1)S(1)} %collective-permute-done.9.refs_10_) | copy-start | bytes 884740
  99.9 14.1 %collective-permute-start.11 = (bf16[1152,128]{1,0:T(8,128)(2,1)S(1)}, bf16[1152,128]{1,0:T(8,128)(2,1)S(1)}, u32[]{:S(2)}, u32[]{:S(2)}) collective-permute-start(bf16[1152,128]{1,0:T(8,128)(2,1)S(1)} %collective-permute-done.9.refs_10_), channel_id=1, source_target_pairs={{0,7},{1,0},{2,1},{3,2},{4,3},{5,4},{6,5},{7,6},{8,15},{9,8},{10,9... | collective-permute-start | bytes 884744 | tf_op jit(solution)/shard_map/ppermute | solution.py:192
  101.9 26.3 %copy-start.4 = (bf16[1152,128]{1,0:T(8,128)(2,1)}, bf16[1152,128]{1,0:T(8,128)(2,1)S(1)}, u32[]{:S(2)}) copy-start(bf16[1152,128]{1,0:T(8,128)(2,1)S(1)} %collective-permute-done.1.refs_1_) | copy-start | bytes 884740
  101.9 14.0 %collective-permute-start.3 = (bf16[1152,128]{1,0:T(8,128)(2,1)S(1)}, bf16[1152,128]{1,0:T(8,128)(2,1)S(1)}, u32[]{:S(2)}, u32[]{:S(2)}) collective-permute-start(bf16[1152,128]{1,0:T(8,128)(2,1)S(1)} %collective-permute-done.1.refs_1_), channel_id=1, source_target_pairs={{0,1},{1,2},{2,3},{3,4},{4,5},{5,6},{6,7},{7,0},{8,9},{9,10},{10,1... | collective-permute-start | bytes 884744 | tf_op jit(solution)/shard_map/ppermute | solution.py:192
  106.5 21.7 %copy-start.5 = (bf16[1152,128]{1,0:T(8,128)(2,1)}, bf16[1152,128]{1,0:T(8,128)(2,1)S(1)}, u32[]{:S(2)}) copy-start(bf16[1152,128]{1,0:T(8,128)(2,1)S(1)} %collective-permute-done.8.refs_9_) | copy-start | bytes 884740
  106.5 14.0 %collective-permute-start.10 = (bf16[1152,128]{1,0:T(8,128)(2,1)S(1)}, bf16[1152,128]{1,0:T(8,128)(2,1)S(1)}, u32[]{:S(2)}, u32[]{:S(2)}) collective-permute-start(bf16[1152,128]{1,0:T(8,128)(2,1)S(1)} %collective-permute-done.8.refs_9_), channel_id=1, source_target_pairs={{0,1},{1,2},{2,3},{3,4},{4,5},{5,6},{6,7},{7,0},{8,9},{9,10},{10,1... | collective-permute-start | bytes 884744 | tf_op jit(solution)/shard_map/ppermute | solution.py:192
  111.2 16.9 %copy-start.6 = (bf16[1152,128]{1,0:T(8,128)(2,1)}, bf16[1152,128]{1,0:T(8,128)(2,1)S(1)}, u32[]{:S(2)}) copy-start(bf16[1152,128]{1,0:T(8,128)(2,1)S(1)} %collective-permute-done.2.refs_2_) | copy-start | bytes 884740
  111.3 12.2 %collective-permute-start.4 = (bf16[1152,128]{1,0:T(8,128)(2,1)S(1)}, bf16[1152,128]{1,0:T(8,128)(2,1)S(1)}, u32[]{:S(2)}, u32[]{:S(2)}) collective-permute-start(bf16[1152,128]{1,0:T(8,128)(2,1)S(1)} %collective-permute-done.2.refs_2_), channel_id=1, source_target_pairs={{0,7},{1,0},{2,1},{3,2},{4,3},{5,4},{6,5},{7,6},{8,15},{9,8},{10,9... | collective-permute-start | bytes 884744 | tf_op jit(solution)/shard_map/ppermute | solution.py:192
  114.0 12.2 %collective-permute-start.13 = (bf16[1152,128]{1,0:T(8,128)(2,1)S(1)}, bf16[1152,128]{1,0:T(8,128)(2,1)}, u32[]{:S(2)}, u32[]{:S(2)}) collective-permute-start(bf16[1152,128]{1,0:T(8,128)(2,1)S(1)} %collective-permute-done.11.refs_12_), channel_id=1, source_target_pairs={{0,7},{1,0},{2,1},{3,2},{4,3},{5,4},{6,5},{7,6},{8,15},{9,8},{10,9... | collective-permute-start | bytes 884744 | tf_op jit(solution)/shard_map/ppermute | solution.py:192
  115.9 12.2 %collective-permute-start.5 = (bf16[1152,128]{1,0:T(8,128)(2,1)S(1)}, bf16[1152,128]{1,0:T(8,128)(2,1)}, u32[]{:S(2)}, u32[]{:S(2)}) collective-permute-start(bf16[1152,128]{1,0:T(8,128)(2,1)S(1)} %collective-permute-done.3.refs_3_), channel_id=1, source_target_pairs={{0,1},{1,2},{2,3},{3,4},{4,5},{5,6},{6,7},{7,0},{8,9},{9,10},{10,1... | collective-permute-start | bytes 884744 | tf_op jit(solution)/shard_map/ppermute | solution.py:192
  120.6 12.3 %collective-permute-start.12 = (bf16[1152,128]{1,0:T(8,128)(2,1)S(1)}, bf16[1152,128]{1,0:T(8,128)(2,1)}, u32[]{:S(2)}, u32[]{:S(2)}) collective-permute-start(bf16[1152,128]{1,0:T(8,128)(2,1)S(1)} %collective-permute-done.10.refs_11_), channel_id=1, source_target_pairs={{0,1},{1,2},{2,3},{3,4},{4,5},{5,6},{6,7},{7,0},{8,9},{9,10},{10,1... | collective-permute-start | bytes 884744 | tf_op jit(solution)/shard_map/ppermute | solution.py:192
  123.4 9.5 %collective-permute-start.6 = (bf16[1152,128]{1,0:T(8,128)(2,1)S(1)}, bf16[1152,128]{1,0:T(8,128)(2,1)}, u32[]{:S(2)}, u32[]{:S(2)}) collective-permute-start(bf16[1152,128]{1,0:T(8,128)(2,1)S(1)} %collective-permute-done.4.refs_4_), channel_id=1, source_target_pairs={{0,7},{1,0},{2,1},{3,2},{4,3},{5,4},{6,5},{7,6},{8,15},{9,8},{10,9... | collective-permute-start | bytes 884744 | tf_op jit(solution)/shard_map/ppermute | solution.py:192
  126.2 12.3 %collective-permute-start.14 = (bf16[1152,128]{1,0:T(8,128)(2,1)}, bf16[1152,128]{1,0:T(8,128)(2,1)}, u32[]{:S(2)}, u32[]{:S(2)}) collective-permute-start(bf16[1152,128]{1,0:T(8,128)(2,1)} %collective-permute-done.13.refs_14_), channel_id=1, source_target_pairs={{0,7},{1,0},{2,1},{3,2},{4,3},{5,4},{6,5},{7,6},{8,15},{9,8},{10,9... | collective-permute-start | bytes 884744 | tf_op jit(solution)/shard_map/ppermute | solution.py:192
  128.2 10.3 %collective-permute-start.7 = (bf16[1152,128]{1,0:T(8,128)(2,1)}, bf16[1152,128]{1,0:T(8,128)(2,1)}, u32[]{:S(2)}, u32[]{:S(2)}) collective-permute-start(bf16[1152,128]{1,0:T(8,128)(2,1)} %collective-permute-done.5.refs_5_), channel_id=1, source_target_pairs={{0,1},{1,2},{2,3},{3,4},{4,5},{5,6},{6,7},{7,0},{8,9},{9,10},{10,1... | collective-permute-start | bytes 884744 | tf_op jit(solution)/shard_map/ppermute | solution.py:192
  159.5 9.6 %collective-permute-start.15 = (bf16[1152,128]{1,0:T(8,128)(2,1)S(1)}, bf16[1152,128]{1,0:T(8,128)(2,1)S(1)}, u32[]{:S(2)}, u32[]{:S(2)}) collective-permute-start(bf16[1152,128]{1,0:T(8,128)(2,1)S(1)} %ffn.1.refs_0_), channel_id=1, source_target_pairs={{0,1},{1,2},{2,3},{3,4},{4,5},{5,6},{6,7},{7,0},{8,9},{9,10},{10,1... | collective-permute-start | bytes 884744 | tf_op jit(solution)/shard_map/ppermute | solution.py:192
  164.0 10.5 %collective-permute-start.16 = (bf16[1152,128]{1,0:T(8,128)(2,1)S(1)}, bf16[1152,128]{1,0:T(8,128)(2,1)S(1)}, u32[]{:S(2)}, u32[]{:S(2)}) collective-permute-start(bf16[1152,128]{1,0:T(8,128)(2,1)S(1)} %ffn.1.refs_0_), channel_id=1, source_target_pairs={{0,7},{1,0},{2,1},{3,2},{4,3},{5,4},{6,5},{7,6},{8,15},{9,8},{10,9... | collective-permute-start | bytes 884744 | tf_op jit(solution)/shard_map/ppermute | solution.py:192
  169.2 9.6 %collective-permute-start.17 = (bf16[1152,128]{1,0:T(8,128)(2,1)S(1)}, bf16[1152,128]{1,0:T(8,128)(2,1)S(1)}, u32[]{:S(2)}, u32[]{:S(2)}) collective-permute-start(bf16[1152,128]{1,0:T(8,128)(2,1)S(1)} %collective-permute-done.15.refs_1_), channel_id=1, source_target_pairs={{0,1},{1,2},{2,3},{3,4},{4,5},{5,6},{6,7},{7,0},{8,9},{9,10},{10,1... | collective-permute-start | bytes 884744 | tf_op jit(solution)/shard_map/ppermute | solution.py:192
  174.5 9.6 %collective-permute-start.18 = (bf16[1152,128]{1,0:T(8,128)(2,1)S(1)}, bf16[1152,128]{1,0:T(8,128)(2,1)S(1)}, u32[]{:S(2)}, u32[]{:S(2)}) collective-permute-start(bf16[1152,128]{1,0:T(8,128)(2,1)S(1)} %collective-permute-done.16.refs_2_), channel_id=1, source_target_pairs={{0,7},{1,0},{2,1},{3,2},{4,3},{5,4},{6,5},{7,6},{8,15},{9,8},{10,9... | collective-permute-start | bytes 884744 | tf_op jit(solution)/shard_map/ppermute | solution.py:192
  178.8 9.0 %collective-permute-start.19 = (bf16[1152,128]{1,0:T(8,128)(2,1)S(1)}, bf16[1152,128]{1,0:T(8,128)(2,1)S(1)}, u32[]{:S(2)}, u32[]{:S(2)}) collective-permute-start(bf16[1152,128]{1,0:T(8,128)(2,1)S(1)} %collective-permute-done.17.refs_3_), channel_id=1, source_target_pairs={{0,1},{1,2},{2,3},{3,4},{4,5},{5,6},{6,7},{7,0},{8,9},{9,10},{10,1... | collective-permute-start | bytes 884744 | tf_op jit(solution)/shard_map/ppermute | solution.py:192
  184.2 16.9 %collective-permute-start.20 = (bf16[1152,128]{1,0:T(8,128)(2,1)S(1)}, bf16[1152,128]{1,0:T(8,128)(2,1)S(1)}, u32[]{:S(2)}, u32[]{:S(2)}) collective-permute-start(bf16[1152,128]{1,0:T(8,128)(2,1)S(1)} %collective-permute-done.18.refs_4_), channel_id=1, source_target_pairs={{0,7},{1,0},{2,1},{3,2},{4,3},{5,4},{6,5},{7,6},{8,15},{9,8},{10,9... | collective-permute-start | bytes 884744 | tf_op jit(solution)/shard_map/ppermute | solution.py:192
  187.8 13.3 %collective-permute-start.21 = (bf16[1152,128]{1,0:T(8,128)(2,1)S(1)}, bf16[1152,128]{1,0:T(8,128)(2,1)S(1)}, u32[]{:S(2)}, u32[]{:S(2)}) collective-permute-start(bf16[1152,128]{1,0:T(8,128)(2,1)S(1)} %collective-permute-done.19.refs_5_), channel_id=1, source_target_pairs={{0,1},{1,2},{2,3},{3,4},{4,5},{5,6},{6,7},{7,0},{8,9},{9,10},{10,1... | collective-permute-start | bytes 884744 | tf_op jit(solution)/shard_map/ppermute | solution.py:192
  192.9 8.2 %collective-permute-start = (bf16[32,16,256]{2,1,0:T(8,128)(2,1)S(1)}, bf16[32,16,256]{2,1,0:T(8,128)(2,1)S(1)}, u32[]{:S(2)}, u32[]{:S(2)}) collective-permute-start(bf16[32,16,256]{2,1,0:T(8,128)(2,1)S(1)} %slice.35.refs_8_), channel_id=1, source_target_pairs={{0,256},{256,0},{1,257},{257,1},{2,258},{258,2},{3,259},{259,3},{4... | collective-permute-start | bytes 786440 | tf_op jit(solution)/shard_map/ppermute | solution.py:237
  203.3 11.8 %copy-start.7 = (f32[384,2]{0,1:T(2,128)S(1)}, f32[384,2]{0,1:T(2,128)}, u32[]{:S(2)}) copy-start(f32[384,2]{0,1:T(2,128)} %param.13) | copy-start | bytes 9220
  203.3 47.7 %all-to-all-start.2 = ((bf16[32,72,128]{2,1,0:T(8,128)(2,1)}), bf16[32,72,128]{2,1,0:T(8,128)(2,1)S(1)}, u32[]{:S(2)}, u32[]{:S(2)}) async-start(bf16[32,72,128]{2,1,0:T(8,128)(2,1)} %down.1), calls=%async_computation.2 | async-start | bytes 1179648 | tf_op jit(solution)/shard_map/all_to_all | solution.py:187

commit v7 on v2

--- a/solution.py
+++ b/solution.py
@@ -7,6 +7,7 @@
 
 
 CAP = 36
+FETCHED = (0, 1, 2)
 MAIN = 32
 SLAB = 72
 HALF = 128
@@ -44,9 +45,14 @@
     out[first : first + 8, 2 * MAIN :, :] = rest.astype(BF16)
 
 
-def route_kernel(routes, tokens, outbound, rows):
+def route_kernel(routes_in, tokens_in, outbound, rows, routes, tokens, done):
     experts = outbound.shape[0]
     n_tok = tokens.shape[0]
+    fetch_routes = pltpu.make_async_copy(routes_in, routes, done.at[0])
+    fetch_tokens = pltpu.make_async_copy(tokens_in, tokens, done.at[1])
+    fetch_routes.start()
+    fetch_tokens.start()
+    fetch_routes.wait()
     first, second = routes[0:1, :], routes[1:2, :]
     ids = lax.broadcasted_iota(jnp.int32, (experts, n_tok), 0)
     hit0 = (ids == first).astype(F32)
@@ -70,6 +76,7 @@
     row0, row1 = row_of(first, hit0, count0), row_of(second, hit1, count1)
     rows[...] = jnp.concatenate([row0, row1] * 4, axis=0)
     part = 8 * CAP
+    fetch_tokens.wait()
     for g in range(experts // 8):
         ids = lax.broadcasted_iota(jnp.int32, (part, n_tok), 0) + g * part
         select = jnp.logical_or(ids == row0, ids == row1).astype(F32).astype(BF16)
@@ -83,20 +90,39 @@
 
 
 def ffn_kernel(me, *refs):
-    halves, weights, hidden = (refs[0:8], refs[8:16]), refs[16], refs[17]
+    chunks, weights, hidden, held, partial, partial_square, done = (refs[0:8], refs[8:16]), *refs[16:]
     sources = offsets_of(me[0])
     features = weights.shape[0]
     part, slabs = 8 * CAP, 8 * SLAB
+
+    def fetch(g, n):
+        source = chunks[g // 2][FETCHED[n]].at[pl.ds((g % 2) * slabs, slabs), :]
+        return pltpu.make_async_copy(source, held.at[g, n], done.at[g, n])
+
+    def add(acc, square, k, x):
+        left, right = from_slabs(x)
+        w = weights[pl.ds(pl.multiple_of(sources[k] * 256, 256), 256), :]
+        both = jnp.concatenate([left, right], axis=1)
+        l32, r32 = left.astype(F32), right.astype(F32)
+        dot = jnp.dot(both, w, preferred_element_type=F32)
+        return acc + dot, square + (l32 * l32 + r32 * r32)
+
+    for g in range(4):
+        for n in range(len(FETCHED)):
+            fetch(g, n).start()
     for g in range(4):
         acc = jnp.zeros((part, 2 * HALF), F32)
         square = jnp.zeros((part, HALF), F32)
-        for source, chunk in zip(sources, halves[g // 2]):
-            left, right = from_slabs(chunk[(g % 2) * slabs : (g % 2 + 1) * slabs, :])
-            w = weights[pl.ds(pl.multiple_of(source * 256, 256), 256), :]
-            both = jnp.concatenate([left, right], axis=1)
-            acc = acc + jnp.dot(both, w, preferred_element_type=F32)
-            l32, r32 = left.astype(F32), right.astype(F32)
-            square = square + (l32 * l32 + r32 * r32)
+        for k in range(8):
+            if k not in FETCHED:
+                x = chunks[g // 2][k][(g % 2) * slabs : (g % 2 + 1) * slabs, :]
+                acc, square = add(acc, square, k, x)
+        partial[g], partial_square[g] = acc, square
+    for g in range(4):
+        acc, square = partial[g], partial_square[g]
+        for n, k in enumerate(FETCHED):
+            fetch(g, n).wait()
+            acc, square = add(acc, square, k, held[g, n])
         total = jnp.sum(square, axis=1, keepdims=True)
         scale = lax.rsqrt(total * (1.0 / features) + epsilon)
         gate = acc[:, :HALF] * scale
@@ -106,8 +132,10 @@
 
 
 def down_kernel(me, *refs):
-    chunks, weights, out = refs[0:8], refs[8], refs[9]
+    chunks, weights, out, serve, done = refs[0:8], *refs[8:]
     sources = offsets_of(me[0])
+    copy = pltpu.make_async_copy(weights, serve, done)
+    copy.start()
     part = 8 * CAP
     pairs = ((0, 7), (1, 2), (3, 4), (5, 6))
 
@@ -121,10 +149,13 @@
             w = jnp.concatenate([rows_of(sources[m]), rows_of(sources[n])], axis=0)
             acc = acc + jnp.dot(h, w, preferred_element_type=F32)
         to_slabs(acc, out, 8 * g)
-
-
-def combine_kernel(rows, gains, returned, mixture):
-    n_tok = rows.shape[0]
+    copy.wait()
+
+
+def combine_kernel(rows_in, gains_in, returned, mixture):
+    n_tok = rows_in.shape[1]
+    rows = rows_in[...].astype(F32).T.astype(jnp.int32)
+    gains = jnp.concatenate([gains_in[...]] * 4, axis=0).T
     slabs, part = 8 * SLAB, 8 * CAP
     sums = [jnp.zeros((n_tok, 2 * HALF), F32) for _ in range(2)]
     for g in range(returned.shape[0] // slabs):
@@ -144,21 +175,24 @@
     return [pltpu.with_memory_space_constraint(x, pltpu.VMEM) for x in arrays]
 
 
+def in_hbm(*arrays):
+    return [pltpu.with_memory_space_constraint(x, pltpu.HBM) for x in arrays]
+
+
 def all_to_all(x):
     return lax.all_to_all(x, "fs", split_axis=0, concat_axis=0, tiled=True)
 
 
-def ring(x, last):
+def step(x, shift):
     n = lax.axis_size("tp")
-
-    def step(v, side):
-        shift = 1 if side == "r" else -1
-        return lax.ppermute(v, "tp", [(d, (d + shift) % n) for d in range(n)])
-
-    r1, l1 = step(x, "r"), step(x, "l")
-    r2, l2 = step(r1, "r"), step(l1, "l")
-    r3, l3 = step(r2, "r"), step(l2, "l")
-    x4 = step(r3, "r") if last == "r" else step(l3, "l")
+    return lax.ppermute(x, "tp", [(d, (d + shift) % n) for d in range(n)])
+
+
+def ring(x, end):
+    r1, l1 = step(x, 1), step(x, -1)
+    r2, l2 = step(r1, 1), step(l1, -1)
+    r3, l3 = step(r2, 1), step(l2, -1)
+    x4 = step(r3, 1) if end == "r" else step(l3, -1)
     return (x, r1, l1, r2, l2, r3, l3, x4)
 
 
@@ -168,39 +202,57 @@
     me = lax.axis_index("tp").reshape(1).astype(jnp.int32)
     smem = pl.BlockSpec(memory_space=pltpu.SMEM)
     vmem = pl.BlockSpec(memory_space=pltpu.VMEM)
+    anywhere = pl.BlockSpec(memory_space=pl.ANY)
     slabs = (experts, SLAB, HALF)
     outbound, rows = pl.pallas_call(
         route_kernel,
-        in_specs=[vmem, vmem],
+        in_specs=[anywhere, anywhere],
         out_specs=(vmem, vmem),
+        scratch_shapes=[
+            pltpu.VMEM((2, n_tok), jnp.int32),
+            pltpu.VMEM(tokens.shape, BF16),
+            pltpu.SemaphoreType.DMA((2,)),
+        ],
         out_shape=(pltpu.VMEM(slabs, BF16), pltpu.VMEM((8, n_tok), jnp.int32)),
         name="route",
         compiler_params=LIMIT,
-    )(*in_vmem(routes.T, tokens))
+    )(*in_hbm(routes.T, tokens))
     arrived = all_to_all(outbound).reshape(experts * SLAB, HALF)
     gain = norm_gain[None, :, None]
     both_low = jnp.concatenate([gain * gate_weight, gain * up_weight], axis=2).astype(BF16)
+    both_low, down_low = lax.optimization_barrier((both_low, down_weight.astype(BF16)))
     both_serve = all_to_all(both_low).reshape(-1, 2 * cols)
+    down_rows = all_to_all(down_low).reshape(-1, down_low.shape[2])
     cut = experts * SLAB // 2
-    halves = ring(arrived[:cut], "r") + ring(arrived[cut:], "l")
+    chunks = ring(arrived[:cut], "r") + ring(arrived[cut:], "l")
+    fetched = [n % 8 in FETCHED for n in range(16)]
     hidden = pl.pallas_call(
         ffn_kernel,
-        in_specs=[smem] + [vmem] * 17,
+        in_specs=[smem] + [anywhere if f else vmem for f in fetched] + [vmem],
         out_specs=vmem,
         out_shape=pltpu.VMEM((experts * CAP, cols), BF16),
+        scratch_shapes=[
+            pltpu.VMEM((4, len(FETCHED), 8 * SLAB, HALF), BF16),
+            pltpu.VMEM((4, 8 * CAP, 2 * HALF), F32),
+            pltpu.VMEM((4, 8 * CAP, HALF), F32),
+            pltpu.SemaphoreType.DMA((4, len(FETCHED))),
+        ],
         name="ffn",
         compiler_params=LIMIT,
-    )(me, *in_vmem(*halves, both_serve))
-    down_low = down_weight.astype(BF16)
-    down_serve = all_to_all(down_low).reshape(-1, down_low.shape[2])
-    expert_out = pl.pallas_call(
+    )(
+        me,
+        *[(in_hbm if f else in_vmem)(x)[0] for f, x in zip(fetched, chunks)],
+        *in_vmem(both_serve),
+    )
+    expert_out, down_serve = pl.pallas_call(
         down_kernel,
         in_specs=[smem] + [vmem] * 9,
-        out_specs=vmem,
-        out_shape=pltpu.VMEM(slabs, BF16),
+        out_specs=(vmem, anywhere),
+        out_shape=(pltpu.VMEM(slabs, BF16), jax.ShapeDtypeStruct(down_rows.shape, BF16)),
+        scratch_shapes=[pltpu.SemaphoreType.DMA],
         name="down",
         compiler_params=LIMIT,
-    )(me, *in_vmem(*ring(hidden, "r"), down_serve))
+    )(me, *in_vmem(*ring(hidden, "r"), down_rows))
     returned = all_to_all(expert_out).reshape(experts * SLAB, HALF)
     mixture = pl.pallas_call(
         combine_kernel,
@@ -209,7 +261,7 @@
         out_shape=jax.ShapeDtypeStruct(tokens.shape, BF16),
         name="combine",
         compiler_params=LIMIT,
-    )(*in_vmem(rows.T, route_weights, returned))
+    )(*in_vmem(rows, route_weights.T, returned))
     gate_serve, up_serve = both_serve[None, :, :cols], both_serve[None, :, cols:]
     return (gate_serve, up_serve, down_serve[None], mixture)
 

time: 288 us -> 287 us (level)
  local copies, waits for them, and re-layouts: 7.11 us -> 3.31 us
    unnamed x20 -> x18, local copies, waits for them, and re-layouts: 5.9 us -> 2.22 us
  transfers between devices with their start and end apart: 25 -> 25, of which waited for: 10 -> 9; matrix products, arithmetic and copies ran while one was open for 2% -> 2% of each run, Pallas kernels for 1% -> 2%
where the time goes in v7:
time: 287 us; the launch traced here: 286 us
  starting transfers between devices  142 us (49%)
  waiting for transfers between devices  125 us (44%)
  Pallas kernels  11.8 us (4%)
  other arithmetic  3.57 us (1%)
  local copies, waits for them, and re-layouts  3.31 us (1%)
    all_to_all x4, waiting for transfers between devices, all_to_all(): return lax.all_to_all(x, 'fs', split_axis=0, concat_axis=0, tiled=True)  104 us
    all_to_all x4, starting transfers between devices, all_to_all(): return lax.all_to_all(x, 'fs', split_axis=0, concat_axis=0, tiled=True)  75.1 us
    ppermute x21, starting transfers between devices, step(): return lax.ppermute(x, 'tp', [(d, (d + shift) % n) for d in range(n)])  66.5 us
    ppermute x21, waiting for transfers between devices, step(): return lax.ppermute(x, 'tp', [(d, (d + shift) % n) for d in range(n)])  20.9 us
  transfers between devices with their start and end apart: 25, of which 9 were waited for; matrix products, arithmetic and copies ran while one was open for 2% of the time, Pallas kernels for 2%

profile of v7, /device:TPU:65, one launch (start us, length us, event | category | flops | bytes accessed | tf_op | source)
XLA Modules:
  0.0 285.9 jit_solution(11323339404824213743)
XLA Ops:
  0.6 2.4 route.1
  3.1 45.2 %all-to-all-start.1 = ((bf16[32,72,128]{2,1,0:T(8,128)(2,1)}), bf16[32,72,128]{2,1,0:T(8,128)(2,1)S(1)}, u32[]{:S(2)}, u32[]{:S(2)}) async-start(bf16[32,72,128]{2,1,0:T(8,128)(2,1)} %get-tuple-element.11), calls=%async_computation.1 | async-start | bytes 1179648 | tf_op jit(solution)/shard_map/all_to_all | solution.py:183
  48.3 0.0 copy-start.6
  48.3 0.0 copy-start.8
  48.3 0.9 convert_element_type.4
  49.2 0.5 copy-done.6
  49.7 1.6 multiply_convert_fusion.1
  51.3 1.1 pad_maximum_fusion
  52.4 32.1 %all-to-all-done.1 = bf16[32,72,128]{2,1,0:T(8,128)(2,1)S(1)} async-done(((bf16[32,72,128]{2,1,0:T(8,128)(2,1)}), bf16[32,72,128]{2,1,0:T(8,128)(2,1)S(1)}, u32[]{:S(2)}, u32[]{:S(2)}) %all-to-all-start.1) | async-done | bytes 589856 | tf_op jit(solution)/shard_map/all_to_all | solution.py:183
  84.5 4.6 %all-to-all-start = ((bf16[32,64,256]{2,1,0:T(8,128)(2,1)}), bf16[32,64,256]{2,1,0:T(8,128)(2,1)S(1)}, u32[]{:S(2)}, u32[]{:S(2)}) async-start(bf16[32,64,256]{2,1,0:T(8,128)(2,1)} %pad_maximum_fusion), calls=%async_computation | async-start | bytes 2097152 | tf_op jit(solution)/shard_map/all_to_all | solution.py:183
  89.2 0.0 copy-start.4
  89.2 5.0 %collective-permute-start.8 = (bf16[1152,128]{1,0:T(8,128)(2,1)S(1)}, bf16[1152,128]{1,0:T(8,128)(2,1)S(1)}, u32[]{:S(2)}, u32[]{:S(2)}) collective-permute-start(bf16[1152,128]{1,0:T(8,128)(2,1)S(1)} %bitcast.18), channel_id=1, source_target_pairs={{0,7},{1,0},{2,1},{3,2},{4,3},{5,4},{6,5},{7,6},{8,15},{9,8},{10,9... | collective-permute-start | bytes 884744 | tf_op jit(solution)/shard_map/ppermute | solution.py:188
  94.2 2.0 collective-permute-start
  96.2 2.0 collective-permute-start.7
  98.2 4.6 %collective-permute-start.1 = (bf16[1152,128]{1,0:T(8,128)(2,1)S(1)}, bf16[1152,128]{1,0:T(8,128)(2,1)}, u32[]{:S(2)}, u32[]{:S(2)}) collective-permute-start(bf16[1152,128]{1,0:T(8,128)(2,1)S(1)} %bitcast.22), channel_id=1, source_target_pairs={{0,7},{1,0},{2,1},{3,2},{4,3},{5,4},{6,5},{7,6},{8,15},{9,8},{10,9... | collective-permute-start | bytes 884744 | tf_op jit(solution)/shard_map/ppermute | solution.py:188
  102.8 3.4 %collective-permute-start.10 = (bf16[1152,128]{1,0:T(8,128)(2,1)S(1)}, bf16[1152,128]{1,0:T(8,128)(2,1)S(1)}, u32[]{:S(2)}, u32[]{:S(2)}) collective-permute-start(bf16[1152,128]{1,0:T(8,128)(2,1)S(1)} %collective-permute-done.8.refs_10_), channel_id=1, source_target_pairs={{0,7},{1,0},{2,1},{3,2},{4,3},{5,4},{6,5},{7,6},{8,15},{9,8},{10,9... | collective-permute-start | bytes 884744 | tf_op jit(solution)/shard_map/ppermute | solution.py:188
  106.2 2.0 collective-permute-start.2
  108.2 36.6 %all-to-all-done = bf16[32,64,256]{2,1,0:T(8,128)(2,1)S(1)} async-done(((bf16[32,64,256]{2,1,0:T(8,128)(2,1)}), bf16[32,64,256]{2,1,0:T(8,128)(2,1)S(1)}, u32[]{:S(2)}, u32[]{:S(2)}) %all-to-all-start) | async-done | bytes 1048608 | tf_op jit(solution)/shard_map/all_to_all | solution.py:183
  144.7 4.9 %all-to-all-start.2 = ((bf16[32,32,256]{2,1,0:T(8,128)(2,1)}), bf16[32,32,256]{2,1,0:T(8,128)(2,1)S(1)}, u32[]{:S(2)}, u32[]{:S(2)}) async-start(bf16[32,32,256]{2,1,0:T(8,128)(2,1)} %convert_element_type.4), calls=%async_computation.2 | async-start | bytes 1048576 | tf_op jit(solution)/shard_map/all_to_all | solution.py:183
  149.7 2.8 collective-permute-start.9
  152.5 4.1 %collective-permute-start.3 = (bf16[1152,128]{1,0:T(8,128)(2,1)}, bf16[1152,128]{1,0:T(8,128)(2,1)S(1)}, u32[]{:S(2)}, u32[]{:S(2)}) collective-permute-start(bf16[1152,128]{1,0:T(8,128)(2,1)} %collective-permute-done.1.refs_2_), channel_id=1, source_target_pairs={{0,7},{1,0},{2,1},{3,2},{4,3},{5,4},{6,5},{7,6},{8,15},{9,8},{10,9... | collective-permute-start | bytes 884744 | tf_op jit(solution)/shard_map/ppermute | solution.py:188
  156.7 3.4 %collective-permute-start.12 = (bf16[1152,128]{1,0:T(8,128)(2,1)S(1)}, bf16[1152,128]{1,0:T(8,128)(2,1)S(1)}, u32[]{:S(2)}, u32[]{:S(2)}) collective-permute-start(bf16[1152,128]{1,0:T(8,128)(2,1)S(1)} %collective-permute-done.10.refs_12_), channel_id=1, source_target_pairs={{0,7},{1,0},{2,1},{3,2},{4,3},{5,4},{6,5},{7,6},{8,15},{9,8},{10,9... | collective-permute-start | bytes 884744 | tf_op jit(solution)/shard_map/ppermute | solution.py:188
  160.1 2.0 collective-permute-start.4
  162.1 2.0 collective-permute-start.11
  164.1 4.6 %collective-permute-start.5 = (bf16[1152,128]{1,0:T(8,128)(2,1)S(1)}, bf16[1152,128]{1,0:T(8,128)(2,1)}, u32[]{:S(2)}, u32[]{:S(2)}) collective-permute-start(bf16[1152,128]{1,0:T(8,128)(2,1)S(1)} %collective-permute-done.3.refs_4_), channel_id=1, source_target_pairs={{0,7},{1,0},{2,1},{3,2},{4,3},{5,4},{6,5},{7,6},{8,15},{9,8},{10,9... | collective-permute-start | bytes 884744 | tf_op jit(solution)/shard_map/ppermute | solution.py:188
  168.7 5.2 %collective-permute-start.13 = (bf16[1152,128]{1,0:T(8,128)(2,1)S(1)}, bf16[1152,128]{1,0:T(8,128)(2,1)}, u32[]{:S(2)}, u32[]{:S(2)}) collective-permute-start(bf16[1152,128]{1,0:T(8,128)(2,1)S(1)} %collective-permute-done.12.refs_14_), channel_id=1, source_target_pairs={{0,7},{1,0},{2,1},{3,2},{4,3},{5,4},{6,5},{7,6},{8,15},{9,8},{10,9... | collective-permute-start | bytes 884744 | tf_op jit(solution)/shard_map/ppermute | solution.py:188
  173.9 2.0 collective-permute-start.6
  175.9 0.7 copy-done
  176.6 5.0 %collective-permute-done.13.refs_15_ = bf16[1152,128]{1,0:T(8,128)(2,1)} collective-permute-done((bf16[1152,128]{1,0:T(8,128)(2,1)S(1)}, bf16[1152,128]{1,0:T(8,128)(2,1)}, u32[]{:S(2)}, u32[]{:S(2)}) %collective-permute-start.13) | collective-permute-done | bytes 294944 | tf_op jit(solution)/shard_map/ppermute | solution.py:188
  181.6 1.3 collective-permute-done.6.refs_7_
  182.9 1.0 copy-done.1
  183.8 4.7 %ffn.1.refs_0_ = bf16[1152,128]{1,0:T(8,128)(2,1)S(1)} custom-call(s32[1]{0:T(128)} %bitcast.3.me, bf16[1152,128]{1,0:T(8,128)(2,1)} %bitcast.23, bf16[1152,128]{1,0:T(8,128)(2,1)} %collective-permute-done.refs_1_, bf16[1152,128]{1,0:T(8,128)(2,1)} %collective-permute-done.1.refs_2_, bf16[1152,128]{1,0:T(8,128)(2,1)S(1)} %collective-permute-done.2.refs_3_, ...), custom_call_target="tpu_custom_call" | custom-call | tf_op jit(solution)/shard_map/ffn/pallas_call | solution.py:229
  188.6 2.0 collective-permute-start.14
  190.6 4.6 %collective-permute-start.15 = (bf16[1152,128]{1,0:T(8,128)(2,1)S(1)}, bf16[1152,128]{1,0:T(8,128)(2,1)S(1)}, u32[]{:S(2)}, u32[]{:S(2)}) collective-permute-start(bf16[1152,128]{1,0:T(8,128)(2,1)S(1)} %ffn.1.refs_0_), channel_id=1, source_target_pairs={{0,7},{1,0},{2,1},{3,2},{4,3},{5,4},{6,5},{7,6},{8,15},{9,8},{10,9... | collective-permute-start | bytes 884744 | tf_op jit(solution)/shard_map/ppermute | solution.py:188
  195.2 2.1 collective-permute-done.14.refs_1_
  197.3 1.9 collective-permute-start.16
  199.3 4.6 %collective-permute-start.17 = (bf16[1152,128]{1,0:T(8,128)(2,1)S(1)}, bf16[1152,128]{1,0:T(8,128)(2,1)S(1)}, u32[]{:S(2)}, u32[]{:S(2)}) collective-permute-start(bf16[1152,128]{1,0:T(8,128)(2,1)S(1)} %collective-permute-done.15.refs_2_), channel_id=1, source_target_pairs={{0,7},{1,0},{2,1},{3,2},{4,3},{5,4},{6,5},{7,6},{8,15},{9,8},{10,9... | collective-permute-start | bytes 884744 | tf_op jit(solution)/shard_map/ppermute | solution.py:188
  203.9 2.1 collective-permute-done.16.refs_3_
  206.0 1.9 collective-permute-start.18
  208.0 4.6 %collective-permute-start.19 = (bf16[1152,128]{1,0:T(8,128)(2,1)S(1)}, bf16[1152,128]{1,0:T(8,128)(2,1)}, u32[]{:S(2)}, u32[]{:S(2)}) collective-permute-start(bf16[1152,128]{1,0:T(8,128)(2,1)S(1)} %collective-permute-done.17.refs_4_), channel_id=1, source_target_pairs={{0,7},{1,0},{2,1},{3,2},{4,3},{5,4},{6,5},{7,6},{8,15},{9,8},{10,9... | collective-permute-start | bytes 884744 | tf_op jit(solution)/shard_map/ppermute | solution.py:188
  212.6 2.2 collective-permute-done.18.refs_5_
  214.8 1.9 collective-permute-start.20
  216.7 8.1 %collective-permute-done.20.refs_7_ = bf16[1152,128]{1,0:T(8,128)(2,1)} collective-permute-done((bf16[1152,128]{1,0:T(8,128)(2,1)S(1)}, bf16[1152,128]{1,0:T(8,128)(2,1)}, u32[]{:S(2)}, u32[]{:S(2)}) %collective-permute-start.20) | collective-permute-done | bytes 294944 | tf_op jit(solution)/shard_map/ppermute | solution.py:188
  224.8 2.7 down.1
  227.5 20.4 %all-to-all-start.3 = ((bf16[32,72,128]{2,1,0:T(8,128)(2,1)}), bf16[32,72,128]{2,1,0:T(8,128)(2,1)S(1)}, u32[]{:S(2)}, u32[]{:S(2)}) async-start(bf16[32,72,128]{2,1,0:T(8,128)(2,1)} %get-tuple-element.15), calls=%async_computation.3 | async-start | bytes 1179648 | tf_op jit(solution)/shard_map/all_to_all | solution.py:183
  247.9 1.0 slice_bitcast_fusion
  248.9 35.0 %all-to-all-done.3 = bf16[32,72,128]{2,1,0:T(8,128)(2,1)S(1)} async-done(((bf16[32,72,128]{2,1,0:T(8,128)(2,1)}), bf16[32,72,128]{2,1,0:T(8,128)(2,1)S(1)}, u32[]{:S(2)}, u32[]{:S(2)}) %all-to-all-start.3) | async-done | bytes 589856 | tf_op jit(solution)/shard_map/all_to_all | solution.py:183
  284.0 1.9 combine.1
  (29 shorter events, 0.1 us)
Async XLA Ops:
  0.6 47.7 %copy-start.5 = (f32[32,32,256]{2,1,0:T(8,128)S(1)}, f32[32,32,256]{2,1,0:T(8,128)}, u32[]{:S(2)}) copy-start(f32[32,32,256]{2,1,0:T(8,128)} %param.11) | copy-start | bytes 3145732
  3.1 81.4 %all-to-all-start.1 = ((bf16[32,72,128]{2,1,0:T(8,128)(2,1)}), bf16[32,72,128]{2,1,0:T(8,128)(2,1)S(1)}, u32[]{:S(2)}, u32[]{:S(2)}) async-start(bf16[32,72,128]{2,1,0:T(8,128)(2,1)} %get-tuple-element.11), calls=%async_computation.1 | async-start | bytes 1179648 | tf_op jit(solution)/shard_map/all_to_all | solution.py:183
  48.3 1.4 copy-start.6
  48.3 1.4 copy-start.8
  84.5 60.3 %all-to-all-start = ((bf16[32,64,256]{2,1,0:T(8,128)(2,1)}), bf16[32,64,256]{2,1,0:T(8,128)(2,1)S(1)}, u32[]{:S(2)}, u32[]{:S(2)}) async-start(bf16[32,64,256]{2,1,0:T(8,128)(2,1)} %pad_maximum_fusion), calls=%async_computation | async-start | bytes 2097152 | tf_op jit(solution)/shard_map/all_to_all | solution.py:183
  89.2 60.5 %copy-start.3 = (bf16[16,72,128]{2,1,0:T(8,128)(2,1)}, bf16[16,72,128]{2,1,0:T(8,128)(2,1)S(1)}, u32[]{:S(2)}) copy-start(bf16[16,72,128]{2,1,0:T(8,128)(2,1)S(1)} %get-tuple-element.18) | copy-start | bytes 884740
  89.2 63.3 %copy-start.4 = (bf16[16,72,128]{2,1,0:T(8,128)(2,1)}, bf16[16,72,128]{2,1,0:T(8,128)(2,1)S(1)}, u32[]{:S(2)}) copy-start(bf16[16,72,128]{2,1,0:T(8,128)(2,1)S(1)} %get-tuple-element.19) | copy-start | bytes 884740
  89.2 13.6 %collective-permute-start.8 = (bf16[1152,128]{1,0:T(8,128)(2,1)S(1)}, bf16[1152,128]{1,0:T(8,128)(2,1)S(1)}, u32[]{:S(2)}, u32[]{:S(2)}) collective-permute-start(bf16[1152,128]{1,0:T(8,128)(2,1)S(1)} %bitcast.18), channel_id=1, source_target_pairs={{0,7},{1,0},{2,1},{3,2},{4,3},{5,4},{6,5},{7,6},{8,15},{9,8},{10,9... | collective-permute-start | bytes 884744 | tf_op jit(solution)/shard_map/ppermute | solution.py:188
  94.2 12.0 %collective-permute-start = (bf16[1152,128]{1,0:T(8,128)(2,1)S(1)}, bf16[1152,128]{1,0:T(8,128)(2,1)}, u32[]{:S(2)}, u32[]{:S(2)}) collective-permute-start(bf16[1152,128]{1,0:T(8,128)(2,1)S(1)} %bitcast.21), channel_id=1, source_target_pairs={{0,1},{1,2},{2,3},{3,4},{4,5},{5,6},{6,7},{7,0},{8,9},{9,10},{10,1... | collective-permute-start | bytes 884744 | tf_op jit(solution)/shard_map/ppermute | solution.py:188
  96.2 53.5 %collective-permute-start.7 = (bf16[1152,128]{1,0:T(8,128)(2,1)S(1)}, bf16[1152,128]{1,0:T(8,128)(2,1)}, u32[]{:S(2)}, u32[]{:S(2)}) collective-permute-start(bf16[1152,128]{1,0:T(8,128)(2,1)S(1)} %bitcast.19), channel_id=1, source_target_pairs={{0,1},{1,2},{2,3},{3,4},{4,5},{5,6},{6,7},{7,0},{8,9},{9,10},{10,1... | collective-permute-start | bytes 884744 | tf_op jit(solution)/shard_map/ppermute | solution.py:188
  98.2 54.4 %collective-permute-start.1 = (bf16[1152,128]{1,0:T(8,128)(2,1)S(1)}, bf16[1152,128]{1,0:T(8,128)(2,1)}, u32[]{:S(2)}, u32[]{:S(2)}) collective-permute-start(bf16[1152,128]{1,0:T(8,128)(2,1)S(1)} %bitcast.22), channel_id=1, source_target_pairs={{0,7},{1,0},{2,1},{3,2},{4,3},{5,4},{6,5},{7,6},{8,15},{9,8},{10,9... | collective-permute-start | bytes 884744 | tf_op jit(solution)/shard_map/ppermute | solution.py:188
  102.8 57.3 %copy-start.7 = (bf16[1152,128]{1,0:T(8,128)(2,1)}, bf16[1152,128]{1,0:T(8,128)(2,1)S(1)}, u32[]{:S(2)}) copy-start(bf16[1152,128]{1,0:T(8,128)(2,1)S(1)} %collective-permute-done.8.refs_10_) | copy-start | bytes 884740
  102.8 53.9 %collective-permute-start.10 = (bf16[1152,128]{1,0:T(8,128)(2,1)S(1)}, bf16[1152,128]{1,0:T(8,128)(2,1)S(1)}, u32[]{:S(2)}, u32[]{:S(2)}) collective-permute-start(bf16[1152,128]{1,0:T(8,128)(2,1)S(1)} %collective-permute-done.8.refs_10_), channel_id=1, source_target_pairs={{0,7},{1,0},{2,1},{3,2},{4,3},{5,4},{6,5},{7,6},{8,15},{9,8},{10,9... | collective-permute-start | bytes 884744 | tf_op jit(solution)/shard_map/ppermute | solution.py:188
  106.2 53.9 %collective-permute-start.2 = (bf16[1152,128]{1,0:T(8,128)(2,1)}, bf16[1152,128]{1,0:T(8,128)(2,1)S(1)}, u32[]{:S(2)}, u32[]{:S(2)}) collective-permute-start(bf16[1152,128]{1,0:T(8,128)(2,1)} %collective-permute-done.refs_1_), channel_id=1, source_target_pairs={{0,1},{1,2},{2,3},{3,4},{4,5},{5,6},{6,7},{7,0},{8,9},{9,10},{10,1... | collective-permute-start | bytes 884744 | tf_op jit(solution)/shard_map/ppermute | solution.py:188
  144.7 72.0 %all-to-all-start.2 = ((bf16[32,32,256]{2,1,0:T(8,128)(2,1)}), bf16[32,32,256]{2,1,0:T(8,128)(2,1)S(1)}, u32[]{:S(2)}, u32[]{:S(2)}) async-start(bf16[32,32,256]{2,1,0:T(8,128)(2,1)} %convert_element_type.4), calls=%async_computation.2 | async-start | bytes 1048576 | tf_op jit(solution)/shard_map/all_to_all | solution.py:183
  149.7 12.4 %collective-permute-start.9 = (bf16[1152,128]{1,0:T(8,128)(2,1)}, bf16[1152,128]{1,0:T(8,128)(2,1)S(1)}, u32[]{:S(2)}, u32[]{:S(2)}) collective-permute-start(bf16[1152,128]{1,0:T(8,128)(2,1)} %collective-permute-done.7.refs_9_), channel_id=1, source_target_pairs={{0,1},{1,2},{2,3},{3,4},{4,5},{5,6},{6,7},{7,0},{8,9},{9,10},{10,1... | collective-permute-start | bytes 884744 | tf_op jit(solution)/shard_map/ppermute | solution.py:188
  152.5 11.5 %collective-permute-start.3 = (bf16[1152,128]{1,0:T(8,128)(2,1)}, bf16[1152,128]{1,0:T(8,128)(2,1)S(1)}, u32[]{:S(2)}, u32[]{:S(2)}) collective-permute-start(bf16[1152,128]{1,0:T(8,128)(2,1)} %collective-permute-done.1.refs_2_), channel_id=1, source_target_pairs={{0,7},{1,0},{2,1},{3,2},{4,3},{5,4},{6,5},{7,6},{8,15},{9,8},{10,9... | collective-permute-start | bytes 884744 | tf_op jit(solution)/shard_map/ppermute | solution.py:188
  156.7 12.0 %collective-permute-start.12 = (bf16[1152,128]{1,0:T(8,128)(2,1)S(1)}, bf16[1152,128]{1,0:T(8,128)(2,1)S(1)}, u32[]{:S(2)}, u32[]{:S(2)}) collective-permute-start(bf16[1152,128]{1,0:T(8,128)(2,1)S(1)} %collective-permute-done.10.refs_12_), channel_id=1, source_target_pairs={{0,7},{1,0},{2,1},{3,2},{4,3},{5,4},{6,5},{7,6},{8,15},{9,8},{10,9... | collective-permute-start | bytes 884744 | tf_op jit(solution)/shard_map/ppermute | solution.py:188
  160.1 13.8 %collective-permute-start.4 = (bf16[1152,128]{1,0:T(8,128)(2,1)S(1)}, bf16[1152,128]{1,0:T(8,128)(2,1)S(1)}, u32[]{:S(2)}, u32[]{:S(2)}) collective-permute-start(bf16[1152,128]{1,0:T(8,128)(2,1)S(1)} %collective-permute-done.2.refs_3_), channel_id=1, source_target_pairs={{0,1},{1,2},{2,3},{3,4},{4,5},{5,6},{6,7},{7,0},{8,9},{9,10},{10,1... | collective-permute-start | bytes 884744 | tf_op jit(solution)/shard_map/ppermute | solution.py:188
  162.1 14.5 %collective-permute-start.11 = (bf16[1152,128]{1,0:T(8,128)(2,1)S(1)}, bf16[1152,128]{1,0:T(8,128)(2,1)}, u32[]{:S(2)}, u32[]{:S(2)}) collective-permute-start(bf16[1152,128]{1,0:T(8,128)(2,1)S(1)} %collective-permute-done.9.refs_11_), channel_id=1, source_target_pairs={{0,1},{1,2},{2,3},{3,4},{4,5},{5,6},{6,7},{7,0},{8,9},{9,10},{10,1... | collective-permute-start | bytes 884744 | tf_op jit(solution)/shard_map/ppermute | solution.py:188
  164.1 12.5 %collective-permute-start.5 = (bf16[1152,128]{1,0:T(8,128)(2,1)S(1)}, bf16[1152,128]{1,0:T(8,128)(2,1)}, u32[]{:S(2)}, u32[]{:S(2)}) collective-permute-start(bf16[1152,128]{1,0:T(8,128)(2,1)S(1)} %collective-permute-done.3.refs_4_), channel_id=1, source_target_pairs={{0,7},{1,0},{2,1},{3,2},{4,3},{5,4},{6,5},{7,6},{8,15},{9,8},{10,9... | collective-permute-start | bytes 884744 | tf_op jit(solution)/shard_map/ppermute | solution.py:188
  168.7 12.9 %collective-permute-start.13 = (bf16[1152,128]{1,0:T(8,128)(2,1)S(1)}, bf16[1152,128]{1,0:T(8,128)(2,1)}, u32[]{:S(2)}, u32[]{:S(2)}) collective-permute-start(bf16[1152,128]{1,0:T(8,128)(2,1)S(1)} %collective-permute-done.12.refs_14_), channel_id=1, source_target_pairs={{0,7},{1,0},{2,1},{3,2},{4,3},{5,4},{6,5},{7,6},{8,15},{9,8},{10,9... | collective-permute-start | bytes 884744 | tf_op jit(solution)/shard_map/ppermute | solution.py:188
  173.9 9.0 %collective-permute-start.6 = (bf16[1152,128]{1,0:T(8,128)(2,1)S(1)}, bf16[1152,128]{1,0:T(8,128)(2,1)}, u32[]{:S(2)}, u32[]{:S(2)}) collective-permute-start(bf16[1152,128]{1,0:T(8,128)(2,1)S(1)} %collective-permute-done.4.refs_5_), channel_id=1, source_target_pairs={{0,1},{1,2},{2,3},{3,4},{4,5},{5,6},{6,7},{7,0},{8,9},{9,10},{10,1... | collective-permute-start | bytes 884744 | tf_op jit(solution)/shard_map/ppermute | solution.py:188
  175.8 0.7 copy-start
  182.9 1.0 copy-start.1
  188.6 8.7 %collective-permute-start.14 = (bf16[1152,128]{1,0:T(8,128)(2,1)S(1)}, bf16[1152,128]{1,0:T(8,128)(2,1)S(1)}, u32[]{:S(2)}, u32[]{:S(2)}) collective-permute-start(bf16[1152,128]{1,0:T(8,128)(2,1)S(1)} %ffn.1.refs_0_), channel_id=1, source_target_pairs={{0,1},{1,2},{2,3},{3,4},{4,5},{5,6},{6,7},{7,0},{8,9},{9,10},{10,1... | collective-permute-start | bytes 884744 | tf_op jit(solution)/shard_map/ppermute | solution.py:188
  190.6 8.7 %collective-permute-start.15 = (bf16[1152,128]{1,0:T(8,128)(2,1)S(1)}, bf16[1152,128]{1,0:T(8,128)(2,1)S(1)}, u32[]{:S(2)}, u32[]{:S(2)}) collective-permute-start(bf16[1152,128]{1,0:T(8,128)(2,1)S(1)} %ffn.1.refs_0_), channel_id=1, source_target_pairs={{0,7},{1,0},{2,1},{3,2},{4,3},{5,4},{6,5},{7,6},{8,15},{9,8},{10,9... | collective-permute-start | bytes 884744 | tf_op jit(solution)/shard_map/ppermute | solution.py:188
  197.3 8.7 %collective-permute-start.16 = (bf16[1152,128]{1,0:T(8,128)(2,1)S(1)}, bf16[1152,128]{1,0:T(8,128)(2,1)S(1)}, u32[]{:S(2)}, u32[]{:S(2)}) collective-permute-start(bf16[1152,128]{1,0:T(8,128)(2,1)S(1)} %collective-permute-done.14.refs_1_), channel_id=1, source_target_pairs={{0,1},{1,2},{2,3},{3,4},{4,5},{5,6},{6,7},{7,0},{8,9},{9,10},{10,1... | collective-permute-start | bytes 884744 | tf_op jit(solution)/shard_map/ppermute | solution.py:188
  199.3 8.7 %collective-permute-start.17 = (bf16[1152,128]{1,0:T(8,128)(2,1)S(1)}, bf16[1152,128]{1,0:T(8,128)(2,1)S(1)}, u32[]{:S(2)}, u32[]{:S(2)}) collective-permute-start(bf16[1152,128]{1,0:T(8,128)(2,1)S(1)} %collective-permute-done.15.refs_2_), channel_id=1, source_target_pairs={{0,7},{1,0},{2,1},{3,2},{4,3},{5,4},{6,5},{7,6},{8,15},{9,8},{10,9... | collective-permute-start | bytes 884744 | tf_op jit(solution)/shard_map/ppermute | solution.py:188
  206.0 8.8 %collective-permute-start.18 = (bf16[1152,128]{1,0:T(8,128)(2,1)S(1)}, bf16[1152,128]{1,0:T(8,128)(2,1)S(1)}, u32[]{:S(2)}, u32[]{:S(2)}) collective-permute-start(bf16[1152,128]{1,0:T(8,128)(2,1)S(1)} %collective-permute-done.16.refs_3_), channel_id=1, source_target_pairs={{0,1},{1,2},{2,3},{3,4},{4,5},{5,6},{6,7},{7,0},{8,9},{9,10},{10,1... | collective-permute-start | bytes 884744 | tf_op jit(solution)/shard_map/ppermute | solution.py:188
  208.0 8.8 %collective-permute-start.19 = (bf16[1152,128]{1,0:T(8,128)(2,1)S(1)}, bf16[1152,128]{1,0:T(8,128)(2,1)}, u32[]{:S(2)}, u32[]{:S(2)}) collective-permute-start(bf16[1152,128]{1,0:T(8,128)(2,1)S(1)} %collective-permute-done.17.refs_4_), channel_id=1, source_target_pairs={{0,7},{1,0},{2,1},{3,2},{4,3},{5,4},{6,5},{7,6},{8,15},{9,8},{10,9... | collective-permute-start | bytes 884744 | tf_op jit(solution)/shard_map/ppermute | solution.py:188
  214.8 10.0 %collective-permute-start.20 = (bf16[1152,128]{1,0:T(8,128)(2,1)S(1)}, bf16[1152,128]{1,0:T(8,128)(2,1)}, u32[]{:S(2)}, u32[]{:S(2)}) collective-permute-start(bf16[1152,128]{1,0:T(8,128)(2,1)S(1)} %collective-permute-done.18.refs_5_), channel_id=1, source_target_pairs={{0,1},{1,2},{2,3},{3,4},{4,5},{5,6},{6,7},{7,0},{8,9},{9,10},{10,1... | collective-permute-start | bytes 884744 | tf_op jit(solution)/shard_map/ppermute | solution.py:188
  227.5 56.4 %all-to-all-start.3 = ((bf16[32,72,128]{2,1,0:T(8,128)(2,1)}), bf16[32,72,128]{2,1,0:T(8,128)(2,1)S(1)}, u32[]{:S(2)}, u32[]{:S(2)}) async-start(bf16[32,72,128]{2,1,0:T(8,128)(2,1)} %get-tuple-element.15), calls=%async_computation.3 | async-start | bytes 1179648 | tf_op jit(solution)/shard_map/all_to_all | solution.py:183
  247.9 36.1 %copy-start.2 = (f32[384,2]{0,1:T(2,128)S(1)}, f32[384,2]{0,1:T(2,128)}, u32[]{:S(2)}) copy-start(f32[384,2]{0,1:T(2,128)} %param.13) | copy-start | bytes 9220

commit v8 on v6

--- a/solution.py
+++ b/solution.py
@@ -8,7 +8,7 @@
 
 CAP = 36
 SPREAD = 4
-FETCHED = (0, 1, 2)
+WAITING = (0, 1, 2, 3, 4, 5, 6)
 MAIN = 32
 SLAB = 72
 HALF = 128
@@ -91,38 +91,27 @@
 
 
 def join_pieces(mine, pieces, serve):
-    count, rows = len(pieces), pieces[0].shape[1]
-    for n, piece in enumerate(pieces):
-        place = (mine + n) % count
-        serve[:, pl.ds(pl.multiple_of(place * rows, rows), rows), :] = piece[...]
+    rows = pieces[0].shape[1]
+    if len(pieces) == 1:
+        serve[...] = pieces[0][...]
+        return
+    own, other = pieces[0][...], pieces[1][...]
+    serve[:, :rows, :] = jnp.where(mine == 0, own, other)
+    serve[:, rows:, :] = jnp.where(mine == 0, other, own)
 
 
 def ffn_kernel(me, *refs):
-    chunks, weights, hidden, held, done = (refs[0:8], refs[8:16]), *refs[16:]
+    chunks, weights, hidden = (refs[0:8], refs[8:16]), *refs[16:]
     sources = offsets_of(me[0])
     rows = 2 * HALF // SPREAD
     features = weights.shape[0] * rows
     part, slabs = 8 * CAP, 8 * SLAB
-
-    def fetch(g, n):
-        source = chunks[g // 2][FETCHED[n]].at[pl.ds((g % 2) * slabs, slabs), :]
-        return pltpu.make_async_copy(source, held.at[g, n], done.at[g, n])
-
-    for g in range(4):
-        for n in range(len(FETCHED)):
-            fetch(g, n).start()
-    order = [k for k in range(8) if k not in FETCHED] + list(FETCHED)
     for g in range(4):
         acc = jnp.zeros((part, 2 * HALF), F32)
         square = jnp.zeros((part, HALF), F32)
-        for k in order:
-            if k in FETCHED:
-                fetch(g, FETCHED.index(k)).wait()
-                x = held[g, FETCHED.index(k)]
-            else:
-                x = chunks[g // 2][k][(g % 2) * slabs : (g % 2 + 1) * slabs, :]
-            left, right = from_slabs(x)
-            w = weights[pl.ds(sources[k] * SPREAD, SPREAD), :rows, :].reshape(2 * HALF, 2 * HALF)
+        for source, chunk in zip(sources, chunks[g // 2]):
+            left, right = from_slabs(chunk[(g % 2) * slabs : (g % 2 + 1) * slabs, :])
+            w = weights[pl.ds(source * SPREAD, SPREAD), :rows, :].reshape(2 * HALF, 2 * HALF)
             both = jnp.concatenate([left, right], axis=1)
             acc = acc + jnp.dot(both, w, preferred_element_type=F32)
             l32, r32 = left.astype(F32), right.astype(F32)
@@ -136,9 +125,11 @@
 
 
 def down_kernel(me, *refs):
-    chunks, pieces, out, serve = refs[0:8], refs[8:-2], *refs[-2:]
+    chunks, pieces, out, serve_out, serve, done = refs[0:8], refs[8:-4], *refs[-4:]
     sources = offsets_of(me[0])
     join_pieces(me[1], pieces, serve)
+    copy = pltpu.make_async_copy(serve, serve_out, done)
+    copy.start()
     spread = HALF // serve.shape[1]
     part = 8 * CAP
     pairs = ((0, 7), (1, 2), (3, 4), (5, 6))
@@ -153,12 +144,13 @@
             w = jnp.concatenate([rows_of(sources[m]), rows_of(sources[n])], axis=0)
             acc = acc + jnp.dot(h, w, preferred_element_type=F32)
         to_slabs(acc, out, 8 * g)
-
-
-def combine_kernel(rows, gains_in, returned, mixture, gains, done):
-    n_tok = rows.shape[0]
-    fetch = pltpu.make_async_copy(gains_in, gains, done)
-    fetch.start()
+    copy.wait()
+
+
+def combine_kernel(rows_in, gains_in, returned, mixture):
+    n_tok = rows_in.shape[1]
+    rows = rows_in[...].astype(F32).T.astype(jnp.int32)
+    gains = jnp.concatenate([gains_in[...]] * 4, axis=0).T
     slabs, part = 8 * SLAB, 8 * CAP
     sums = [jnp.zeros((n_tok, 2 * HALF), F32) for _ in range(2)]
     for g in range(returned.shape[0] // slabs):
@@ -168,7 +160,6 @@
         for k in range(2):
             onehot = (ids == rows[:, k : k + 1]).astype(F32).astype(BF16)
             sums[k] = sums[k] + jnp.dot(onehot, both, preferred_element_type=F32)
-    fetch.wait()
     mixture[...] = (gains[:, 0:1] * sums[0] + gains[:, 1:2] * sums[1]).astype(BF16)
 
 
@@ -190,13 +181,23 @@
 def step(x, shift):
     n = lax.axis_size("tp")
     return lax.ppermute(x, "tp", [(d, (d + shift) % n) for d in range(n)])
+
+
+def crossed_step(r3, l3):
+    n, devices = lax.axis_size("tp"), lax.axis_size("fs")
+    x = jnp.where(lax.axis_index("fs") % 2 == 0, r3, l3)
+    pairs = [(f * n + d, f * n + (d + 1 - 2 * (f % 2)) % n) for f in range(devices) for d in range(n)]
+    return lax.ppermute(x, ("fs", "tp"), pairs)
 
 
 def ring(x, end):
     r1, l1 = step(x, 1), step(x, -1)
     r2, l2 = step(r1, 1), step(l1, -1)
     r3, l3 = step(r2, 1), step(l2, -1)
-    x4 = step(r3, 1) if end == "r" else step(l3, -1)
+    if end == "both":
+        x4 = crossed_step(r3, l3)
+    else:
+        x4 = step(r3, 1) if end == "r" else step(l3, -1)
     return (x, r1, l1, r2, l2, r3, l3, x4)
 
 
@@ -243,16 +244,12 @@
     down_pieces = swapped(arrived_weights[:, rows_in:])
     cut = experts * SLAB // 2
     chunks = ring(arrived[:cut], "r") + ring(arrived[cut:], "l")
-    fetched = [n % 8 in FETCHED for n in range(16)]
+    fetched = [n % 8 in WAITING for n in range(16)]
     hidden = pl.pallas_call(
         ffn_kernel,
-        in_specs=[smem] + [anywhere if f else vmem for f in fetched] + [vmem],
+        in_specs=[smem] + [vmem] * 17,
         out_specs=vmem,
         out_shape=pltpu.VMEM((experts * CAP, cols), BF16),
-        scratch_shapes=[
-            pltpu.VMEM((4, len(FETCHED), 8 * SLAB, HALF), BF16),
-            pltpu.SemaphoreType.DMA((4, len(FETCHED))),
-        ],
         name="ffn",
         compiler_params=LIMIT,
     )(
@@ -260,36 +257,29 @@
         *[(in_hbm if f else in_vmem)(x)[0] for f, x in zip(fetched, chunks)],
         *in_vmem(arrived_weights),
     )
-    expert_out = pl.pallas_call(
+    down_shape = (experts, rows_down, down_cols)
+    expert_out, down_serve = pl.pallas_call(
         down_kernel,
         in_specs=[smem] + [vmem] * (8 + count),
-        out_specs=vmem,
-        out_shape=pltpu.VMEM(slabs, BF16),
-        scratch_shapes=[pltpu.VMEM((experts, rows_down, down_cols), BF16)],
+        out_specs=(vmem, anywhere),
+        out_shape=(pltpu.VMEM(slabs, BF16), jax.ShapeDtypeStruct(down_shape, BF16)),
+        scratch_shapes=[pltpu.VMEM(down_shape, BF16), pltpu.SemaphoreType.DMA],
         name="down",
         compiler_params=LIMIT,
-    )(me, *in_vmem(*ring(hidden, "r"), *down_pieces))
+    )(me, *in_vmem(*ring(hidden, "both"), *down_pieces))
     returned = all_to_all(expert_out).reshape(experts * SLAB, HALF)
     mixture = pl.pallas_call(
         combine_kernel,
-        in_specs=[vmem, anywhere, vmem],
+        in_specs=[vmem] * 3,
         out_specs=vmem,
-        scratch_shapes=[pltpu.VMEM(route_weights.shape, F32), pltpu.SemaphoreType.DMA],
         out_shape=jax.ShapeDtypeStruct(tokens.shape, BF16),
         name="combine",
         compiler_params=LIMIT,
-    )(*in_vmem(rows.T), *in_hbm(route_weights), *in_vmem(returned))
-
-    def assembled(pieces):
-        if count == 1:
-            return pieces[0].reshape(1, -1, pieces[0].shape[2])
-        own, other = pieces
-        both = jnp.where(mine == 0, own, other), jnp.where(mine == 0, other, own)
-        return jnp.concatenate(both, axis=1).reshape(1, -1, own.shape[2])
+    )(*in_vmem(rows, route_weights.T, returned))
 
     both_serve = arrived_weights[:, :rows_in].reshape(1, -1, 2 * cols)
     gate_serve, up_serve = both_serve[:, :, :cols], both_serve[:, :, cols:]
-    return (gate_serve, up_serve, assembled(down_pieces), mixture)
+    return (gate_serve, up_serve, down_serve.reshape(1, -1, down_cols), mixture)
 
 
 def solution(mesh):

time: 255 us -> 257 us (level)
  the two profiles are of different devices: /device:TPU:71 before, /device:TPU:65 now
where the time goes in v8:
time: 257 us; the launch traced here: 256 us
  starting transfers between devices  131 us (51%)
  waiting for transfers between devices  108 us (42%)
  Pallas kernels  10 us (4%)
  other arithmetic  3.25 us (1%)
  local copies, waits for them, and re-layouts  2.86 us (1%)
    all_to_all x3, waiting for transfers between devices, all_to_all(): return lax.all_to_all(x, 'fs', split_axis=0, concat_axis=0, tiled=True)  81.9 us
    ppermute x20, starting transfers between devices, step(): return lax.ppermute(x, 'tp', [(d, (d + shift) % n) for d in range(n)])  62.7 us
    all_to_all x3, starting transfers between devices, all_to_all(): return lax.all_to_all(x, 'fs', split_axis=0, concat_axis=0, tiled=True)  59.2 us
    ppermute x20, waiting for transfers between devices, step(): return lax.ppermute(x, 'tp', [(d, (d + shift) % n) for d in range(n)])  20.5 us
    ppermute x1, waiting for transfers between devices, swapped(): return [x, lax.ppermute(x, 'grp', [(g, g ^ 1) for g in range(groups)])]  5.37 us
  transfers between devices with their start and end apart: 25, of which 13 were waited for; matrix products, arithmetic and copies ran while one was open for 2% of the time, Pallas kernels for 0%

profile of v8, /device:TPU:65, one launch (start us, length us, event | category | flops | bytes accessed | tf_op | source)
XLA Modules:
  0.0 256.4 jit_solution(8368064374045903732)
XLA Ops:
  0.7 2.4 route.1
  3.1 45.2 %all-to-all-start.1 = ((bf16[32,72,128]{2,1,0:T(8,128)(2,1)}), bf16[32,72,128]{2,1,0:T(8,128)(2,1)S(1)}, u32[]{:S(2)}, u32[]{:S(2)}) async-start(bf16[32,72,128]{2,1,0:T(8,128)(2,1)} %get-tuple-element.8), calls=%async_computation.1 | async-start | bytes 1179648 | tf_op jit(solution)/shard_map/all_to_all | solution.py:178
  48.4 1.9 multiply_convert_fusion.1
  50.3 1.3 pad_maximum_fusion
  51.5 33.0 %all-to-all-done.1 = bf16[32,72,128]{2,1,0:T(8,128)(2,1)S(1)} async-done(((bf16[32,72,128]{2,1,0:T(8,128)(2,1)}), bf16[32,72,128]{2,1,0:T(8,128)(2,1)S(1)}, u32[]{:S(2)}, u32[]{:S(2)}) %all-to-all-start.1) | async-done | bytes 589856 | tf_op jit(solution)/shard_map/all_to_all | solution.py:178
  84.5 4.7 %all-to-all-start = ((bf16[32,80,256]{2,1,0:T(8,128)(2,1)}), bf16[32,80,256]{2,1,0:T(8,128)(2,1)S(1)}, u32[]{:S(2)}, u32[]{:S(2)}) async-start(bf16[32,80,256]{2,1,0:T(8,128)(2,1)} %pad_maximum_fusion), calls=%async_computation | async-start | bytes 2621440 | tf_op jit(solution)/shard_map/all_to_all | solution.py:178
  89.2 5.0 %collective-permute-start.8 = (bf16[1152,128]{1,0:T(8,128)(2,1)S(1)}, bf16[1152,128]{1,0:T(8,128)(2,1)S(1)}, u32[]{:S(2)}, u32[]{:S(2)}) collective-permute-start(bf16[1152,128]{1,0:T(8,128)(2,1)S(1)} %bitcast.12), channel_id=1, source_target_pairs={{0,7},{1,0},{2,1},{3,2},{4,3},{5,4},{6,5},{7,6},{8,15},{9,8},{10,9... | collective-permute-start | bytes 884744 | tf_op jit(solution)/shard_map/ppermute | solution.py:183
  94.3 2.0 collective-permute-start
  96.2 2.0 collective-permute-start.7
  98.2 4.6 %collective-permute-start.1 = (bf16[1152,128]{1,0:T(8,128)(2,1)S(1)}, bf16[1152,128]{1,0:T(8,128)(2,1)S(1)}, u32[]{:S(2)}, u32[]{:S(2)}) collective-permute-start(bf16[1152,128]{1,0:T(8,128)(2,1)S(1)} %bitcast.16), channel_id=1, source_target_pairs={{0,7},{1,0},{2,1},{3,2},{4,3},{5,4},{6,5},{7,6},{8,15},{9,8},{10,9... | collective-permute-start | bytes 884744 | tf_op jit(solution)/shard_map/ppermute | solution.py:183
  102.8 3.4 %collective-permute-start.10 = (bf16[1152,128]{1,0:T(8,128)(2,1)S(1)}, bf16[1152,128]{1,0:T(8,128)(2,1)S(1)}, u32[]{:S(2)}, u32[]{:S(2)}) collective-permute-start(bf16[1152,128]{1,0:T(8,128)(2,1)S(1)} %collective-permute-done.8.refs_10_), channel_id=1, source_target_pairs={{0,7},{1,0},{2,1},{3,2},{4,3},{5,4},{6,5},{7,6},{8,15},{9,8},{10,9... | collective-permute-start | bytes 884744 | tf_op jit(solution)/shard_map/ppermute | solution.py:183
  106.2 2.0 collective-permute-start.2
  108.2 2.8 %collective-permute-done.7.refs_9_ = bf16[1152,128]{1,0:T(8,128)(2,1)S(1)} collective-permute-done((bf16[1152,128]{1,0:T(8,128)(2,1)S(1)}, bf16[1152,128]{1,0:T(8,128)(2,1)S(1)}, u32[]{:S(2)}, u32[]{:S(2)}) %collective-permute-start.7) | collective-permute-done | bytes 294944 | tf_op jit(solution)/shard_map/ppermute | solution.py:183
  111.0 1.9 collective-permute-start.9
  112.9 4.6 %collective-permute-start.3 = (bf16[1152,128]{1,0:T(8,128)(2,1)S(1)}, bf16[1152,128]{1,0:T(8,128)(2,1)}, u32[]{:S(2)}, u32[]{:S(2)}) collective-permute-start(bf16[1152,128]{1,0:T(8,128)(2,1)S(1)} %collective-permute-done.1.refs_2_), channel_id=1, source_target_pairs={{0,7},{1,0},{2,1},{3,2},{4,3},{5,4},{6,5},{7,6},{8,15},{9,8},{10,9... | collective-permute-start | bytes 884744 | tf_op jit(solution)/shard_map/ppermute | solution.py:183
  117.6 2.0 collective-permute-start.12
  119.6 3.4 %collective-permute-start.4 = (bf16[1152,128]{1,0:T(8,128)(2,1)S(1)}, bf16[1152,128]{1,0:T(8,128)(2,1)}, u32[]{:S(2)}, u32[]{:S(2)}) collective-permute-start(bf16[1152,128]{1,0:T(8,128)(2,1)S(1)} %collective-permute-done.2.refs_3_), channel_id=1, source_target_pairs={{0,1},{1,2},{2,3},{3,4},{4,5},{5,6},{6,7},{7,0},{8,9},{9,10},{10,1... | collective-permute-start | bytes 884744 | tf_op jit(solution)/shard_map/ppermute | solution.py:183
  123.0 0.3 collective-permute-done.9.refs_11_
  123.3 1.9 collective-permute-start.11
  125.2 4.6 %collective-permute-start.5 = (bf16[1152,128]{1,0:T(8,128)(2,1)}, bf16[1152,128]{1,0:T(8,128)(2,1)}, u32[]{:S(2)}, u32[]{:S(2)}) collective-permute-start(bf16[1152,128]{1,0:T(8,128)(2,1)} %collective-permute-done.3.refs_4_), channel_id=1, source_target_pairs={{0,7},{1,0},{2,1},{3,2},{4,3},{5,4},{6,5},{7,6},{8,15},{9,8},{10,9... | collective-permute-start | bytes 884744 | tf_op jit(solution)/shard_map/ppermute | solution.py:183
  129.9 2.7 %collective-permute-start.13 = (bf16[1152,128]{1,0:T(8,128)(2,1)}, bf16[1152,128]{1,0:T(8,128)(2,1)S(1)}, u32[]{:S(2)}, u32[]{:S(2)}) collective-permute-start(bf16[1152,128]{1,0:T(8,128)(2,1)} %collective-permute-done.12.refs_14_), channel_id=1, source_target_pairs={{0,7},{1,0},{2,1},{3,2},{4,3},{5,4},{6,5},{7,6},{8,15},{9,8},{10,9... | collective-permute-start | bytes 884744 | tf_op jit(solution)/shard_map/ppermute | solution.py:183
  132.6 2.6 %collective-permute-start.6 = (bf16[1152,128]{1,0:T(8,128)(2,1)}, bf16[1152,128]{1,0:T(8,128)(2,1)S(1)}, u32[]{:S(2)}, u32[]{:S(2)}) collective-permute-start(bf16[1152,128]{1,0:T(8,128)(2,1)} %collective-permute-done.4.refs_5_), channel_id=1, source_target_pairs={{0,1},{1,2},{2,3},{3,4},{4,5},{5,6},{6,7},{7,0},{8,9},{9,10},{10,1... | collective-permute-start | bytes 884744 | tf_op jit(solution)/shard_map/ppermute | solution.py:183
  135.4 0.4 collective-permute-done.11.refs_13_
  135.7 5.3 %collective-permute-done.13.refs_15_ = bf16[1152,128]{1,0:T(8,128)(2,1)S(1)} collective-permute-done((bf16[1152,128]{1,0:T(8,128)(2,1)}, bf16[1152,128]{1,0:T(8,128)(2,1)S(1)}, u32[]{:S(2)}, u32[]{:S(2)}) %collective-permute-start.13) | collective-permute-done | bytes 294944 | tf_op jit(solution)/shard_map/ppermute | solution.py:183
  141.0 0.9 collective-permute-done.6.refs_7_
  141.9 14.0 %all-to-all-done.refs_16_ = bf16[32,80,256]{2,1,0:T(8,128)(2,1)S(1)} async-done(((bf16[32,80,256]{2,1,0:T(8,128)(2,1)}), bf16[32,80,256]{2,1,0:T(8,128)(2,1)S(1)}, u32[]{:S(2)}, u32[]{:S(2)}) %all-to-all-start) | async-done | bytes 1310752 | tf_op jit(solution)/shard_map/all_to_all | solution.py:178
  155.9 3.8 %ffn.1.refs_0_ = bf16[1152,128]{1,0:T(8,128)(2,1)S(1)} custom-call(s32[2]{0:T(128)S(1)} %pad_add_fusion.me, bf16[1152,128]{1,0:T(8,128)(2,1)} %bitcast.17, bf16[1152,128]{1,0:T(8,128)(2,1)} %copy-done.8, bf16[1152,128]{1,0:T(8,128)(2,1)} %copy-done.10, bf16[1152,128]{1,0:T(8,128)(2,1)} %copy-done.12, bf16[1152,128]{1,0:T(8,128)(2,1)} %collective-permute-done.3.refs_4_, ...), custom_call_target="tpu_custom_call" | custom-call | tf_op jit(solution)/shard_map/ffn/pallas_call | solution.py:248
  159.7 2.8 %collective-permute-start.14 = (bf16[1152,128]{1,0:T(8,128)(2,1)S(1)}, bf16[1152,128]{1,0:T(8,128)(2,1)S(1)}, u32[]{:S(2)}, u32[]{:S(2)}) collective-permute-start(bf16[1152,128]{1,0:T(8,128)(2,1)S(1)} %ffn.1.refs_0_), channel_id=1, source_target_pairs={{0,1},{1,2},{2,3},{3,4},{4,5},{5,6},{6,7},{7,0},{8,9},{9,10},{10,1... | collective-permute-start | bytes 884744 | tf_op jit(solution)/shard_map/ppermute | solution.py:183
  162.5 4.1 %collective-permute-start.15 = (bf16[1152,128]{1,0:T(8,128)(2,1)S(1)}, bf16[1152,128]{1,0:T(8,128)(2,1)S(1)}, u32[]{:S(2)}, u32[]{:S(2)}) collective-permute-start(bf16[1152,128]{1,0:T(8,128)(2,1)S(1)} %ffn.1.refs_0_), channel_id=1, source_target_pairs={{0,7},{1,0},{2,1},{3,2},{4,3},{5,4},{6,5},{7,6},{8,15},{9,8},{10,9... | collective-permute-start | bytes 884744 | tf_op jit(solution)/shard_map/ppermute | solution.py:183
  166.7 4.2 %collective-permute-done.14.refs_1_ = bf16[1152,128]{1,0:T(8,128)(2,1)S(1)} collective-permute-done((bf16[1152,128]{1,0:T(8,128)(2,1)S(1)}, bf16[1152,128]{1,0:T(8,128)(2,1)S(1)}, u32[]{:S(2)}, u32[]{:S(2)}) %collective-permute-start.14) | collective-permute-done | bytes 294944 | tf_op jit(solution)/shard_map/ppermute | solution.py:183
  170.9 1.9 collective-permute-start.16
  172.8 4.6 %collective-permute-start.17 = (bf16[1152,128]{1,0:T(8,128)(2,1)S(1)}, bf16[1152,128]{1,0:T(8,128)(2,1)}, u32[]{:S(2)}, u32[]{:S(2)}) collective-permute-start(bf16[1152,128]{1,0:T(8,128)(2,1)S(1)} %collective-permute-done.15.refs_2_), channel_id=1, source_target_pairs={{0,7},{1,0},{2,1},{3,2},{4,3},{5,4},{6,5},{7,6},{8,15},{9,8},{10,9... | collective-permute-start | bytes 884744 | tf_op jit(solution)/shard_map/ppermute | solution.py:183
  177.5 0.7 copy-done.2
  178.2 2.7 %collective-permute-done.16.refs_3_ = bf16[1152,128]{1,0:T(8,128)(2,1)} collective-permute-done((bf16[1152,128]{1,0:T(8,128)(2,1)S(1)}, bf16[1152,128]{1,0:T(8,128)(2,1)}, u32[]{:S(2)}, u32[]{:S(2)}) %collective-permute-start.16) | collective-permute-done | bytes 294944 | tf_op jit(solution)/shard_map/ppermute | solution.py:183
  180.9 1.9 collective-permute-start.18
  182.9 4.6 %collective-permute-start.19 = (bf16[1152,128]{1,0:T(8,128)(2,1)}, bf16[1152,128]{1,0:T(8,128)(2,1)S(1)}, u32[]{:S(2)}, u32[]{:S(2)}) collective-permute-start(bf16[1152,128]{1,0:T(8,128)(2,1)} %collective-permute-done.17.refs_4_), channel_id=1, source_target_pairs={{0,7},{1,0},{2,1},{3,2},{4,3},{5,4},{6,5},{7,6},{8,15},{9,8},{10,9... | collective-permute-start | bytes 884744 | tf_op jit(solution)/shard_map/ppermute | solution.py:183
  187.5 2.7 %collective-permute-done.18.refs_5_ = bf16[1152,128]{1,0:T(8,128)(2,1)S(1)} collective-permute-done((bf16[1152,128]{1,0:T(8,128)(2,1)}, bf16[1152,128]{1,0:T(8,128)(2,1)S(1)}, u32[]{:S(2)}, u32[]{:S(2)}) %collective-permute-start.18) | collective-permute-done | bytes 294944 | tf_op jit(solution)/shard_map/ppermute | solution.py:183
  190.2 1.3 collective-permute-done.19.refs_6_
  191.5 5.0 %collective-permute-start.20 = (bf16[1152,128]{1,0:T(8,128)(2,1)S(1)}, bf16[1152,128]{1,0:T(8,128)(2,1)S(1)}, u32[]{:S(2)}, u32[]{:S(2)}) collective-permute-start(bf16[1152,128]{1,0:T(8,128)(2,1)S(1)} %broadcast_select_fusion), channel_id=1, source_target_pairs={{0,1},{1,2},{2,3},{3,4},{4,5},{5,6},{6,7},{7,0},{8,15},{9,8},{10,9... | collective-permute-start | bytes 884744 | tf_op jit(solution)/shard_map/ppermute | solution.py:190
  196.4 4.4 %collective-permute-start.21 = (bf16[32,16,256]{2,1,0:T(8,128)(2,1)S(1)}, bf16[32,16,256]{2,1,0:T(8,128)(2,1)S(1)}, u32[]{:S(2)}, u32[]{:S(2)}) collective-permute-start(bf16[32,16,256]{2,1,0:T(8,128)(2,1)S(1)} %slice.37.refs_8_), channel_id=1, source_target_pairs={{0,256},{256,0},{1,257},{257,1},{2,258},{258,2},{3,259},{259,3},{4... | collective-permute-start | bytes 786440 | tf_op jit(solution)/shard_map/ppermute | solution.py:238
  200.9 5.4 %collective-permute-done.21.refs_9_ = bf16[32,16,256]{2,1,0:T(8,128)(2,1)S(1)} collective-permute-done((bf16[32,16,256]{2,1,0:T(8,128)(2,1)S(1)}, bf16[32,16,256]{2,1,0:T(8,128)(2,1)S(1)}, u32[]{:S(2)}, u32[]{:S(2)}) %collective-permute-start.21) | collective-permute-done | bytes 262176 | tf_op jit(solution)/shard_map/ppermute | solution.py:238
  206.3 1.9 down.1
  208.2 0.8 copy-done.1
  209.0 9.3 %all-to-all-start.2 = ((bf16[32,72,128]{2,1,0:T(8,128)(2,1)}), bf16[32,72,128]{2,1,0:T(8,128)(2,1)S(1)}, u32[]{:S(2)}, u32[]{:S(2)}) async-start(bf16[32,72,128]{2,1,0:T(8,128)(2,1)} %copy-done.1), calls=%async_computation.2 | async-start | bytes 1179648 | tf_op jit(solution)/shard_map/all_to_all | solution.py:178
  218.4 0.1 slice.32
  218.5 1.0 fusion
  219.6 34.9 %all-to-all-done.2 = bf16[32,72,128]{2,1,0:T(8,128)(2,1)S(1)} async-done(((bf16[32,72,128]{2,1,0:T(8,128)(2,1)}), bf16[32,72,128]{2,1,0:T(8,128)(2,1)S(1)}, u32[]{:S(2)}, u32[]{:S(2)}) %all-to-all-start.2) | async-done | bytes 589856 | tf_op jit(solution)/shard_map/all_to_all | solution.py:178
  254.5 1.9 combine.1
  (43 shorter events, 0.3 us)
Async XLA Ops:
  0.6 47.7 %copy-start = (f32[32,32,256]{2,1,0:T(8,128)S(1)}, f32[32,32,256]{2,1,0:T(8,128)}, u32[]{:S(2)}) copy-start(f32[32,32,256]{2,1,0:T(8,128)} %param.11) | copy-start | bytes 3145732
  0.6 47.7 %copy-start.13 = (f32[64]{0:T(128)S(1)}, f32[64]{0:T(128)}, u32[]{:S(2)}) copy-start(f32[64]{0:T(128)} %param.8) | copy-start | bytes 772
  3.1 81.4 %all-to-all-start.1 = ((bf16[32,72,128]{2,1,0:T(8,128)(2,1)}), bf16[32,72,128]{2,1,0:T(8,128)(2,1)S(1)}, u32[]{:S(2)}, u32[]{:S(2)}) async-start(bf16[32,72,128]{2,1,0:T(8,128)(2,1)} %get-tuple-element.8), calls=%async_computation.1 | async-start | bytes 1179648 | tf_op jit(solution)/shard_map/all_to_all | solution.py:178
  84.5 71.4 %all-to-all-start = ((bf16[32,80,256]{2,1,0:T(8,128)(2,1)}), bf16[32,80,256]{2,1,0:T(8,128)(2,1)S(1)}, u32[]{:S(2)}, u32[]{:S(2)}) async-start(bf16[32,80,256]{2,1,0:T(8,128)(2,1)} %pad_maximum_fusion), calls=%async_computation | async-start | bytes 2621440 | tf_op jit(solution)/shard_map/all_to_all | solution.py:178
  89.2 40.6 %copy-start.6 = (bf16[16,72,128]{2,1,0:T(8,128)(2,1)}, bf16[16,72,128]{2,1,0:T(8,128)(2,1)S(1)}, u32[]{:S(2)}) copy-start(bf16[16,72,128]{2,1,0:T(8,128)(2,1)S(1)} %get-tuple-element.15) | copy-start | bytes 884740
  89.2 66.7 %copy-start.5 = (bf16[16,72,128]{2,1,0:T(8,128)(2,1)}, bf16[16,72,128]{2,1,0:T(8,128)(2,1)S(1)}, u32[]{:S(2)}) copy-start(bf16[16,72,128]{2,1,0:T(8,128)(2,1)S(1)} %get-tuple-element.14) | copy-start | bytes 884740
  89.2 13.6 %collective-permute-start.8 = (bf16[1152,128]{1,0:T(8,128)(2,1)S(1)}, bf16[1152,128]{1,0:T(8,128)(2,1)S(1)}, u32[]{:S(2)}, u32[]{:S(2)}) collective-permute-start(bf16[1152,128]{1,0:T(8,128)(2,1)S(1)} %bitcast.12), channel_id=1, source_target_pairs={{0,7},{1,0},{2,1},{3,2},{4,3},{5,4},{6,5},{7,6},{8,15},{9,8},{10,9... | collective-permute-start | bytes 884744 | tf_op jit(solution)/shard_map/ppermute | solution.py:183
  94.3 12.0 %collective-permute-start = (bf16[1152,128]{1,0:T(8,128)(2,1)S(1)}, bf16[1152,128]{1,0:T(8,128)(2,1)S(1)}, u32[]{:S(2)}, u32[]{:S(2)}) collective-permute-start(bf16[1152,128]{1,0:T(8,128)(2,1)S(1)} %bitcast.15), channel_id=1, source_target_pairs={{0,1},{1,2},{2,3},{3,4},{4,5},{5,6},{6,7},{7,0},{8,9},{9,10},{10,1... | collective-permute-start | bytes 884744 | tf_op jit(solution)/shard_map/ppermute | solution.py:183
  96.2 14.8 %collective-permute-start.7 = (bf16[1152,128]{1,0:T(8,128)(2,1)S(1)}, bf16[1152,128]{1,0:T(8,128)(2,1)S(1)}, u32[]{:S(2)}, u32[]{:S(2)}) collective-permute-start(bf16[1152,128]{1,0:T(8,128)(2,1)S(1)} %bitcast.13), channel_id=1, source_target_pairs={{0,1},{1,2},{2,3},{3,4},{4,5},{5,6},{6,7},{7,0},{8,9},{9,10},{10,1... | collective-permute-start | bytes 884744 | tf_op jit(solution)/shard_map/ppermute | solution.py:183
  98.2 14.8 %collective-permute-start.1 = (bf16[1152,128]{1,0:T(8,128)(2,1)S(1)}, bf16[1152,128]{1,0:T(8,128)(2,1)S(1)}, u32[]{:S(2)}, u32[]{:S(2)}) collective-permute-start(bf16[1152,128]{1,0:T(8,128)(2,1)S(1)} %bitcast.16), channel_id=1, source_target_pairs={{0,7},{1,0},{2,1},{3,2},{4,3},{5,4},{6,5},{7,6},{8,15},{9,8},{10,9... | collective-permute-start | bytes 884744 | tf_op jit(solution)/shard_map/ppermute | solution.py:183
  102.8 29.8 %copy-start.7 = (bf16[1152,128]{1,0:T(8,128)(2,1)}, bf16[1152,128]{1,0:T(8,128)(2,1)S(1)}, u32[]{:S(2)}) copy-start(bf16[1152,128]{1,0:T(8,128)(2,1)S(1)} %collective-permute-done.8.refs_10_) | copy-start | bytes 884740
  102.8 14.8 %collective-permute-start.10 = (bf16[1152,128]{1,0:T(8,128)(2,1)S(1)}, bf16[1152,128]{1,0:T(8,128)(2,1)S(1)}, u32[]{:S(2)}, u32[]{:S(2)}) collective-permute-start(bf16[1152,128]{1,0:T(8,128)(2,1)S(1)} %collective-permute-done.8.refs_10_), channel_id=1, source_target_pairs={{0,7},{1,0},{2,1},{3,2},{4,3},{5,4},{6,5},{7,6},{8,15},{9,8},{10,9... | collective-permute-start | bytes 884744 | tf_op jit(solution)/shard_map/ppermute | solution.py:183
  106.2 26.4 %copy-start.8 = (bf16[1152,128]{1,0:T(8,128)(2,1)}, bf16[1152,128]{1,0:T(8,128)(2,1)S(1)}, u32[]{:S(2)}) copy-start(bf16[1152,128]{1,0:T(8,128)(2,1)S(1)} %collective-permute-done.refs_1_) | copy-start | bytes 884740
  106.2 13.3 %collective-permute-start.2 = (bf16[1152,128]{1,0:T(8,128)(2,1)S(1)}, bf16[1152,128]{1,0:T(8,128)(2,1)S(1)}, u32[]{:S(2)}, u32[]{:S(2)}) collective-permute-start(bf16[1152,128]{1,0:T(8,128)(2,1)S(1)} %collective-permute-done.refs_1_), channel_id=1, source_target_pairs={{0,1},{1,2},{2,3},{3,4},{4,5},{5,6},{6,7},{7,0},{8,9},{9,10},{10,1... | collective-permute-start | bytes 884744 | tf_op jit(solution)/shard_map/ppermute | solution.py:183
  111.0 21.6 %copy-start.9 = (bf16[1152,128]{1,0:T(8,128)(2,1)}, bf16[1152,128]{1,0:T(8,128)(2,1)S(1)}, u32[]{:S(2)}) copy-start(bf16[1152,128]{1,0:T(8,128)(2,1)S(1)} %collective-permute-done.7.refs_9_) | copy-start | bytes 884740
  111.0 12.3 %collective-permute-start.9 = (bf16[1152,128]{1,0:T(8,128)(2,1)S(1)}, bf16[1152,128]{1,0:T(8,128)(2,1)}, u32[]{:S(2)}, u32[]{:S(2)}) collective-permute-start(bf16[1152,128]{1,0:T(8,128)(2,1)S(1)} %collective-permute-done.7.refs_9_), channel_id=1, source_target_pairs={{0,1},{1,2},{2,3},{3,4},{4,5},{5,6},{6,7},{7,0},{8,9},{9,10},{10,1... | collective-permute-start | bytes 884744 | tf_op jit(solution)/shard_map/ppermute | solution.py:183
  112.9 19.7 %copy-start.10 = (bf16[1152,128]{1,0:T(8,128)(2,1)}, bf16[1152,128]{1,0:T(8,128)(2,1)S(1)}, u32[]{:S(2)}) copy-start(bf16[1152,128]{1,0:T(8,128)(2,1)S(1)} %collective-permute-done.1.refs_2_) | copy-start | bytes 884740
  112.9 12.3 %collective-permute-start.3 = (bf16[1152,128]{1,0:T(8,128)(2,1)S(1)}, bf16[1152,128]{1,0:T(8,128)(2,1)}, u32[]{:S(2)}, u32[]{:S(2)}) collective-permute-start(bf16[1152,128]{1,0:T(8,128)(2,1)S(1)} %collective-permute-done.1.refs_2_), channel_id=1, source_target_pairs={{0,7},{1,0},{2,1},{3,2},{4,3},{5,4},{6,5},{7,6},{8,15},{9,8},{10,9... | collective-permute-start | bytes 884744 | tf_op jit(solution)/shard_map/ppermute | solution.py:183
  117.6 15.1 %copy-start.11 = (bf16[1152,128]{1,0:T(8,128)(2,1)}, bf16[1152,128]{1,0:T(8,128)(2,1)S(1)}, u32[]{:S(2)}) copy-start(bf16[1152,128]{1,0:T(8,128)(2,1)S(1)} %collective-permute-done.10.refs_12_) | copy-start | bytes 884740
  117.6 12.3 %collective-permute-start.12 = (bf16[1152,128]{1,0:T(8,128)(2,1)S(1)}, bf16[1152,128]{1,0:T(8,128)(2,1)}, u32[]{:S(2)}, u32[]{:S(2)}) collective-permute-start(bf16[1152,128]{1,0:T(8,128)(2,1)S(1)} %collective-permute-done.10.refs_12_), channel_id=1, source_target_pairs={{0,7},{1,0},{2,1},{3,2},{4,3},{5,4},{6,5},{7,6},{8,15},{9,8},{10,9... | collective-permute-start | bytes 884744 | tf_op jit(solution)/shard_map/ppermute | solution.py:183
  119.6 22.3 %copy-start.12 = (bf16[1152,128]{1,0:T(8,128)(2,1)}, bf16[1152,128]{1,0:T(8,128)(2,1)S(1)}, u32[]{:S(2)}) copy-start(bf16[1152,128]{1,0:T(8,128)(2,1)S(1)} %collective-permute-done.2.refs_3_) | copy-start | bytes 884740
  119.6 13.0 %collective-permute-start.4 = (bf16[1152,128]{1,0:T(8,128)(2,1)S(1)}, bf16[1152,128]{1,0:T(8,128)(2,1)}, u32[]{:S(2)}, u32[]{:S(2)}) collective-permute-start(bf16[1152,128]{1,0:T(8,128)(2,1)S(1)} %collective-permute-done.2.refs_3_), channel_id=1, source_target_pairs={{0,1},{1,2},{2,3},{3,4},{4,5},{5,6},{6,7},{7,0},{8,9},{9,10},{10,1... | collective-permute-start | bytes 884744 | tf_op jit(solution)/shard_map/ppermute | solution.py:183
  123.3 12.5 %collective-permute-start.11 = (bf16[1152,128]{1,0:T(8,128)(2,1)}, bf16[1152,128]{1,0:T(8,128)(2,1)}, u32[]{:S(2)}, u32[]{:S(2)}) collective-permute-start(bf16[1152,128]{1,0:T(8,128)(2,1)} %collective-permute-done.9.refs_11_), channel_id=1, source_target_pairs={{0,1},{1,2},{2,3},{3,4},{4,5},{5,6},{6,7},{7,0},{8,9},{9,10},{10,1... | collective-permute-start | bytes 884744 | tf_op jit(solution)/shard_map/ppermute | solution.py:183
  125.2 10.5 %collective-permute-start.5 = (bf16[1152,128]{1,0:T(8,128)(2,1)}, bf16[1152,128]{1,0:T(8,128)(2,1)}, u32[]{:S(2)}, u32[]{:S(2)}) collective-permute-start(bf16[1152,128]{1,0:T(8,128)(2,1)} %collective-permute-done.3.refs_4_), channel_id=1, source_target_pairs={{0,7},{1,0},{2,1},{3,2},{4,3},{5,4},{6,5},{7,6},{8,15},{9,8},{10,9... | collective-permute-start | bytes 884744 | tf_op jit(solution)/shard_map/ppermute | solution.py:183
  129.9 11.2 %collective-permute-start.13 = (bf16[1152,128]{1,0:T(8,128)(2,1)}, bf16[1152,128]{1,0:T(8,128)(2,1)S(1)}, u32[]{:S(2)}, u32[]{:S(2)}) collective-permute-start(bf16[1152,128]{1,0:T(8,128)(2,1)} %collective-permute-done.12.refs_14_), channel_id=1, source_target_pairs={{0,7},{1,0},{2,1},{3,2},{4,3},{5,4},{6,5},{7,6},{8,15},{9,8},{10,9... | collective-permute-start | bytes 884744 | tf_op jit(solution)/shard_map/ppermute | solution.py:183
  132.6 9.3 %collective-permute-start.6 = (bf16[1152,128]{1,0:T(8,128)(2,1)}, bf16[1152,128]{1,0:T(8,128)(2,1)S(1)}, u32[]{:S(2)}, u32[]{:S(2)}) collective-permute-start(bf16[1152,128]{1,0:T(8,128)(2,1)} %collective-permute-done.4.refs_5_), channel_id=1, source_target_pairs={{0,1},{1,2},{2,3},{3,4},{4,5},{5,6},{6,7},{7,0},{8,9},{9,10},{10,1... | collective-permute-start | bytes 884744 | tf_op jit(solution)/shard_map/ppermute | solution.py:183
  159.7 11.2 %collective-permute-start.14 = (bf16[1152,128]{1,0:T(8,128)(2,1)S(1)}, bf16[1152,128]{1,0:T(8,128)(2,1)S(1)}, u32[]{:S(2)}, u32[]{:S(2)}) collective-permute-start(bf16[1152,128]{1,0:T(8,128)(2,1)S(1)} %ffn.1.refs_0_), channel_id=1, source_target_pairs={{0,1},{1,2},{2,3},{3,4},{4,5},{5,6},{6,7},{7,0},{8,9},{9,10},{10,1... | collective-permute-start | bytes 884744 | tf_op jit(solution)/shard_map/ppermute | solution.py:183
  162.5 10.3 %collective-permute-start.15 = (bf16[1152,128]{1,0:T(8,128)(2,1)S(1)}, bf16[1152,128]{1,0:T(8,128)(2,1)S(1)}, u32[]{:S(2)}, u32[]{:S(2)}) collective-permute-start(bf16[1152,128]{1,0:T(8,128)(2,1)S(1)} %ffn.1.refs_0_), channel_id=1, source_target_pairs={{0,7},{1,0},{2,1},{3,2},{4,3},{5,4},{6,5},{7,6},{8,15},{9,8},{10,9... | collective-permute-start | bytes 884744 | tf_op jit(solution)/shard_map/ppermute | solution.py:183
  170.9 10.0 %collective-permute-start.16 = (bf16[1152,128]{1,0:T(8,128)(2,1)S(1)}, bf16[1152,128]{1,0:T(8,128)(2,1)}, u32[]{:S(2)}, u32[]{:S(2)}) collective-permute-start(bf16[1152,128]{1,0:T(8,128)(2,1)S(1)} %collective-permute-done.14.refs_1_), channel_id=1, source_target_pairs={{0,1},{1,2},{2,3},{3,4},{4,5},{5,6},{6,7},{7,0},{8,9},{9,10},{10,1... | collective-permute-start | bytes 884744 | tf_op jit(solution)/shard_map/ppermute | solution.py:183
  172.8 10.0 %collective-permute-start.17 = (bf16[1152,128]{1,0:T(8,128)(2,1)S(1)}, bf16[1152,128]{1,0:T(8,128)(2,1)}, u32[]{:S(2)}, u32[]{:S(2)}) collective-permute-start(bf16[1152,128]{1,0:T(8,128)(2,1)S(1)} %collective-permute-done.15.refs_2_), channel_id=1, source_target_pairs={{0,7},{1,0},{2,1},{3,2},{4,3},{5,4},{6,5},{7,6},{8,15},{9,8},{10,9... | collective-permute-start | bytes 884744 | tf_op jit(solution)/shard_map/ppermute | solution.py:183
  177.5 0.7 copy-start.2
  180.9 9.3 %collective-permute-start.18 = (bf16[1152,128]{1,0:T(8,128)(2,1)}, bf16[1152,128]{1,0:T(8,128)(2,1)S(1)}, u32[]{:S(2)}, u32[]{:S(2)}) collective-permute-start(bf16[1152,128]{1,0:T(8,128)(2,1)} %collective-permute-done.16.refs_3_), channel_id=1, source_target_pairs={{0,1},{1,2},{2,3},{3,4},{4,5},{5,6},{6,7},{7,0},{8,9},{9,10},{10,1... | collective-permute-start | bytes 884744 | tf_op jit(solution)/shard_map/ppermute | solution.py:183
  182.9 8.6 %collective-permute-start.19 = (bf16[1152,128]{1,0:T(8,128)(2,1)}, bf16[1152,128]{1,0:T(8,128)(2,1)S(1)}, u32[]{:S(2)}, u32[]{:S(2)}) collective-permute-start(bf16[1152,128]{1,0:T(8,128)(2,1)} %collective-permute-done.17.refs_4_), channel_id=1, source_target_pairs={{0,7},{1,0},{2,1},{3,2},{4,3},{5,4},{6,5},{7,6},{8,15},{9,8},{10,9... | collective-permute-start | bytes 884744 | tf_op jit(solution)/shard_map/ppermute | solution.py:183
  187.5 18.8 %copy-start.3 = (bf16[1152,128]{1,0:T(8,128)(2,1)S(1)}, bf16[1152,128]{1,0:T(8,128)(2,1)}, u32[]{:S(2)}) copy-start(bf16[1152,128]{1,0:T(8,128)(2,1)} %copy-done.2) | copy-start | bytes 884740
  191.5 14.8 %collective-permute-start.20 = (bf16[1152,128]{1,0:T(8,128)(2,1)S(1)}, bf16[1152,128]{1,0:T(8,128)(2,1)S(1)}, u32[]{:S(2)}, u32[]{:S(2)}) collective-permute-start(bf16[1152,128]{1,0:T(8,128)(2,1)S(1)} %broadcast_select_fusion), channel_id=1, source_target_pairs={{0,1},{1,2},{2,3},{3,4},{4,5},{5,6},{6,7},{7,0},{8,15},{9,8},{10,9... | collective-permute-start | bytes 884744 | tf_op jit(solution)/shard_map/ppermute | solution.py:190
  196.4 9.8 %collective-permute-start.21 = (bf16[32,16,256]{2,1,0:T(8,128)(2,1)S(1)}, bf16[32,16,256]{2,1,0:T(8,128)(2,1)S(1)}, u32[]{:S(2)}, u32[]{:S(2)}) collective-permute-start(bf16[32,16,256]{2,1,0:T(8,128)(2,1)S(1)} %slice.37.refs_8_), channel_id=1, source_target_pairs={{0,256},{256,0},{1,257},{257,1},{2,258},{258,2},{3,259},{259,3},{4... | collective-permute-start | bytes 786440 | tf_op jit(solution)/shard_map/ppermute | solution.py:238
  208.2 0.8 copy-start.1
  209.0 45.4 %all-to-all-start.2 = ((bf16[32,72,128]{2,1,0:T(8,128)(2,1)}), bf16[32,72,128]{2,1,0:T(8,128)(2,1)S(1)}, u32[]{:S(2)}, u32[]{:S(2)}) async-start(bf16[32,72,128]{2,1,0:T(8,128)(2,1)} %copy-done.1), calls=%async_computation.2 | async-start | bytes 1179648 | tf_op jit(solution)/shard_map/all_to_all | solution.py:178
  218.5 36.0 %copy-start.4 = (f32[384,2]{0,1:T(2,128)S(1)}, f32[384,2]{0,1:T(2,128)}, u32[]{:S(2)}) copy-start(f32[384,2]{0,1:T(2,128)} %param.13) | copy-start | bytes 9220

commit v9 on v8

--- a/solution.py
+++ b/solution.py
@@ -8,7 +8,7 @@
 
 CAP = 36
 SPREAD = 4
-WAITING = (0, 1, 2, 3, 4, 5, 6)
+WAITING = (0, 1, 2)
 MAIN = 32
 SLAB = 72
 HALF = 128
@@ -183,21 +183,11 @@
     return lax.ppermute(x, "tp", [(d, (d + shift) % n) for d in range(n)])
 
 
-def crossed_step(r3, l3):
-    n, devices = lax.axis_size("tp"), lax.axis_size("fs")
-    x = jnp.where(lax.axis_index("fs") % 2 == 0, r3, l3)
-    pairs = [(f * n + d, f * n + (d + 1 - 2 * (f % 2)) % n) for f in range(devices) for d in range(n)]
-    return lax.ppermute(x, ("fs", "tp"), pairs)
-
-
 def ring(x, end):
     r1, l1 = step(x, 1), step(x, -1)
     r2, l2 = step(r1, 1), step(l1, -1)
     r3, l3 = step(r2, 1), step(l2, -1)
-    if end == "both":
-        x4 = crossed_step(r3, l3)
-    else:
-        x4 = step(r3, 1) if end == "r" else step(l3, -1)
+    x4 = step(r3, 1) if end == "r" else step(l3, -1)
     return (x, r1, l1, r2, l2, r3, l3, x4)
 
 
@@ -266,7 +256,7 @@
         scratch_shapes=[pltpu.VMEM(down_shape, BF16), pltpu.SemaphoreType.DMA],
         name="down",
         compiler_params=LIMIT,
-    )(me, *in_vmem(*ring(hidden, "both"), *down_pieces))
+    )(me, *in_vmem(*ring(hidden, "r"), *down_pieces))
     returned = all_to_all(expert_out).reshape(experts * SLAB, HALF)
     mixture = pl.pallas_call(
         combine_kernel,

time: 257 us -> 253 us (0.984)
  the two profiles are of different devices: /device:TPU:65 before, /device:TPU:71 now
where the time goes in v9:
time: 253 us; the launch traced here: 252 us
  starting transfers between devices  134 us (53%)
  waiting for transfers between devices  102 us (40%)
  Pallas kernels  10.7 us (4%)
  other arithmetic  3.19 us (1%)
    all_to_all x3, waiting for transfers between devices, all_to_all(): return lax.all_to_all(x, 'fs', split_axis=0, concat_axis=0, tiled=True)  84 us
    ppermute x21, starting transfers between devices, step(): return lax.ppermute(x, 'tp', [(d, (d + shift) % n) for d in range(n)])  69.6 us
    all_to_all x3, starting transfers between devices, all_to_all(): return lax.all_to_all(x, 'fs', split_axis=0, concat_axis=0, tiled=True)  60.2 us
    ppermute x21, waiting for transfers between devices, step(): return lax.ppermute(x, 'tp', [(d, (d + shift) % n) for d in range(n)])  13.8 us
  transfers between devices with their start and end apart: 25, of which 10 were waited for; matrix products, arithmetic and copies ran while one was open for 2% of the time, Pallas kernels for 0%

profile of v9, /device:TPU:71, one launch (start us, length us, event | category | flops | bytes accessed | tf_op | source)
XLA Modules:
  0.0 252.2 jit_solution(9207590484170276305)
XLA Ops:
  0.6 0.0 copy-start
  0.7 2.4 route.1
  3.1 44.4 %all-to-all-start.1 = ((bf16[32,72,128]{2,1,0:T(8,128)(2,1)}), bf16[32,72,128]{2,1,0:T(8,128)(2,1)S(1)}, u32[]{:S(2)}, u32[]{:S(2)}) async-start(bf16[32,72,128]{2,1,0:T(8,128)(2,1)} %get-tuple-element.8), calls=%async_computation.1 | async-start | bytes 1179648 | tf_op jit(solution)/shard_map/all_to_all | solution.py:178
  47.5 1.9 multiply_convert_fusion.1
  49.4 1.2 pad_maximum_fusion
  50.6 32.9 %all-to-all-done.1 = bf16[32,72,128]{2,1,0:T(8,128)(2,1)S(1)} async-done(((bf16[32,72,128]{2,1,0:T(8,128)(2,1)}), bf16[32,72,128]{2,1,0:T(8,128)(2,1)S(1)}, u32[]{:S(2)}, u32[]{:S(2)}) %all-to-all-start.1) | async-done | bytes 589856 | tf_op jit(solution)/shard_map/all_to_all | solution.py:178
  83.5 4.3 %all-to-all-start = ((bf16[32,80,256]{2,1,0:T(8,128)(2,1)}), bf16[32,80,256]{2,1,0:T(8,128)(2,1)S(1)}, u32[]{:S(2)}, u32[]{:S(2)}) async-start(bf16[32,80,256]{2,1,0:T(8,128)(2,1)} %pad_maximum_fusion), calls=%async_computation | async-start | bytes 2621440 | tf_op jit(solution)/shard_map/all_to_all | solution.py:178
  87.9 0.0 copy-start.3
  88.0 2.1 collective-permute-start.8
  90.0 4.5 %collective-permute-start = (bf16[1152,128]{1,0:T(8,128)(2,1)S(1)}, bf16[1152,128]{1,0:T(8,128)(2,1)S(1)}, u32[]{:S(2)}, u32[]{:S(2)}) collective-permute-start(bf16[1152,128]{1,0:T(8,128)(2,1)S(1)} %bitcast.15), channel_id=1, source_target_pairs={{0,1},{1,2},{2,3},{3,4},{4,5},{5,6},{6,7},{7,0},{8,9},{9,10},{10,1... | collective-permute-start | bytes 884744 | tf_op jit(solution)/shard_map/ppermute | solution.py:183
  94.5 3.3 %collective-permute-start.7 = (bf16[1152,128]{1,0:T(8,128)(2,1)S(1)}, bf16[1152,128]{1,0:T(8,128)(2,1)S(1)}, u32[]{:S(2)}, u32[]{:S(2)}) collective-permute-start(bf16[1152,128]{1,0:T(8,128)(2,1)S(1)} %bitcast.13), channel_id=1, source_target_pairs={{0,1},{1,2},{2,3},{3,4},{4,5},{5,6},{6,7},{7,0},{8,9},{9,10},{10,1... | collective-permute-start | bytes 884744 | tf_op jit(solution)/shard_map/ppermute | solution.py:183
  97.8 2.1 collective-permute-start.1
  99.9 2.0 collective-permute-start.10
  101.9 0.0 copy-start.5
  101.9 4.6 %collective-permute-start.2 = (bf16[1152,128]{1,0:T(8,128)(2,1)S(1)}, bf16[1152,128]{1,0:T(8,128)(2,1)S(1)}, u32[]{:S(2)}, u32[]{:S(2)}) collective-permute-start(bf16[1152,128]{1,0:T(8,128)(2,1)S(1)} %collective-permute-done.refs_1_), channel_id=1, source_target_pairs={{0,1},{1,2},{2,3},{3,4},{4,5},{5,6},{6,7},{7,0},{8,9},{9,10},{10,1... | collective-permute-start | bytes 884744 | tf_op jit(solution)/shard_map/ppermute | solution.py:183
  106.5 4.7 %collective-permute-start.9 = (bf16[1152,128]{1,0:T(8,128)(2,1)S(1)}, bf16[1152,128]{1,0:T(8,128)(2,1)S(1)}, u32[]{:S(2)}, u32[]{:S(2)}) collective-permute-start(bf16[1152,128]{1,0:T(8,128)(2,1)S(1)} %collective-permute-done.7.refs_9_), channel_id=1, source_target_pairs={{0,1},{1,2},{2,3},{3,4},{4,5},{5,6},{6,7},{7,0},{8,9},{9,10},{10,1... | collective-permute-start | bytes 884744 | tf_op jit(solution)/shard_map/ppermute | solution.py:183
  111.3 2.0 collective-permute-start.3
  113.2 0.8 collective-permute-done.10.refs_12_
  114.0 1.9 collective-permute-start.12
  115.9 4.6 %collective-permute-start.4 = (bf16[1152,128]{1,0:T(8,128)(2,1)S(1)}, bf16[1152,128]{1,0:T(8,128)(2,1)}, u32[]{:S(2)}, u32[]{:S(2)}) collective-permute-start(bf16[1152,128]{1,0:T(8,128)(2,1)S(1)} %collective-permute-done.2.refs_3_), channel_id=1, source_target_pairs={{0,1},{1,2},{2,3},{3,4},{4,5},{5,6},{6,7},{7,0},{8,9},{9,10},{10,1... | collective-permute-start | bytes 884744 | tf_op jit(solution)/shard_map/ppermute | solution.py:183
  120.6 2.9 %collective-permute-start.11 = (bf16[1152,128]{1,0:T(8,128)(2,1)S(1)}, bf16[1152,128]{1,0:T(8,128)(2,1)}, u32[]{:S(2)}, u32[]{:S(2)}) collective-permute-start(bf16[1152,128]{1,0:T(8,128)(2,1)S(1)} %collective-permute-done.9.refs_11_), channel_id=1, source_target_pairs={{0,1},{1,2},{2,3},{3,4},{4,5},{5,6},{6,7},{7,0},{8,9},{9,10},{10,1... | collective-permute-start | bytes 884744 | tf_op jit(solution)/shard_map/ppermute | solution.py:183
  123.4 2.5 collective-permute-start.5
  125.9 0.2 collective-permute-done.12.refs_14_
  126.2 1.9 collective-permute-start.13
  128.2 4.6 %collective-permute-start.6 = (bf16[1152,128]{1,0:T(8,128)(2,1)}, bf16[1152,128]{1,0:T(8,128)(2,1)}, u32[]{:S(2)}, u32[]{:S(2)}) collective-permute-start(bf16[1152,128]{1,0:T(8,128)(2,1)} %collective-permute-done.4.refs_5_), channel_id=1, source_target_pairs={{0,1},{1,2},{2,3},{3,4},{4,5},{5,6},{6,7},{7,0},{8,9},{9,10},{10,1... | collective-permute-start | bytes 884744 | tf_op jit(solution)/shard_map/ppermute | solution.py:183
  132.8 0.1 pad_add_fusion.me
  132.9 0.0 collective-permute-done.5.refs_6_
  132.9 5.6 %collective-permute-done.13.refs_15_ = bf16[1152,128]{1,0:T(8,128)(2,1)} collective-permute-done((bf16[1152,128]{1,0:T(8,128)(2,1)}, bf16[1152,128]{1,0:T(8,128)(2,1)}, u32[]{:S(2)}, u32[]{:S(2)}) %collective-permute-start.13) | collective-permute-done | bytes 294944 | tf_op jit(solution)/shard_map/ppermute | solution.py:183
  138.5 16.2 %all-to-all-done.refs_16_ = bf16[32,80,256]{2,1,0:T(8,128)(2,1)S(1)} async-done(((bf16[32,80,256]{2,1,0:T(8,128)(2,1)}), bf16[32,80,256]{2,1,0:T(8,128)(2,1)S(1)}, u32[]{:S(2)}, u32[]{:S(2)}) %all-to-all-start) | async-done | bytes 1310752 | tf_op jit(solution)/shard_map/all_to_all | solution.py:178
  154.6 3.6 %ffn.1.refs_0_ = bf16[1152,128]{1,0:T(8,128)(2,1)S(1)} custom-call(s32[2]{0:T(128)S(1)} %pad_add_fusion.me, bf16[1152,128]{1,0:T(8,128)(2,1)} %bitcast.17, bf16[1152,128]{1,0:T(8,128)(2,1)} %copy-done.5, bf16[1152,128]{1,0:T(8,128)(2,1)} %copy-done.7, bf16[1152,128]{1,0:T(8,128)(2,1)S(1)} %collective-permute-done.2.refs_3_, ...), custom_call_target="tpu_custom_call" | custom-call | tf_op jit(solution)/shard_map/ffn/pallas_call | solution.py:238
  158.3 4.5 %collective-permute-start.14 = (bf16[1152,128]{1,0:T(8,128)(2,1)S(1)}, bf16[1152,128]{1,0:T(8,128)(2,1)S(1)}, u32[]{:S(2)}, u32[]{:S(2)}) collective-permute-start(bf16[1152,128]{1,0:T(8,128)(2,1)S(1)} %ffn.1.refs_0_), channel_id=1, source_target_pairs={{0,1},{1,2},{2,3},{3,4},{4,5},{5,6},{6,7},{7,0},{8,9},{9,10},{10,1... | collective-permute-start | bytes 884744 | tf_op jit(solution)/shard_map/ppermute | solution.py:183
  162.8 2.0 collective-permute-start.15
  164.7 3.2 %collective-permute-done.14.refs_1_ = bf16[1152,128]{1,0:T(8,128)(2,1)S(1)} collective-permute-done((bf16[1152,128]{1,0:T(8,128)(2,1)S(1)}, bf16[1152,128]{1,0:T(8,128)(2,1)S(1)}, u32[]{:S(2)}, u32[]{:S(2)}) %collective-permute-start.14) | collective-permute-done | bytes 294944 | tf_op jit(solution)/shard_map/ppermute | solution.py:183
  167.9 5.3 %collective-permute-start.16 = (bf16[1152,128]{1,0:T(8,128)(2,1)S(1)}, bf16[1152,128]{1,0:T(8,128)(2,1)S(1)}, u32[]{:S(2)}, u32[]{:S(2)}) collective-permute-start(bf16[1152,128]{1,0:T(8,128)(2,1)S(1)} %collective-permute-done.14.refs_1_), channel_id=1, source_target_pairs={{0,1},{1,2},{2,3},{3,4},{4,5},{5,6},{6,7},{7,0},{8,9},{9,10},{10,1... | collective-permute-start | bytes 884744 | tf_op jit(solution)/shard_map/ppermute | solution.py:183
  173.3 2.0 collective-permute-start.17
  175.2 2.3 collective-permute-done.16.refs_3_
  177.6 5.3 %collective-permute-start.18 = (bf16[1152,128]{1,0:T(8,128)(2,1)S(1)}, bf16[1152,128]{1,0:T(8,128)(2,1)S(1)}, u32[]{:S(2)}, u32[]{:S(2)}) collective-permute-start(bf16[1152,128]{1,0:T(8,128)(2,1)S(1)} %collective-permute-done.16.refs_3_), channel_id=1, source_target_pairs={{0,1},{1,2},{2,3},{3,4},{4,5},{5,6},{6,7},{7,0},{8,9},{9,10},{10,1... | collective-permute-start | bytes 884744 | tf_op jit(solution)/shard_map/ppermute | solution.py:183
  182.9 2.0 collective-permute-start.19
  184.9 1.7 collective-permute-done.18.refs_5_
  186.5 5.0 %collective-permute-start.20 = (bf16[1152,128]{1,0:T(8,128)(2,1)S(1)}, bf16[1152,128]{1,0:T(8,128)(2,1)S(1)}, u32[]{:S(2)}, u32[]{:S(2)}) collective-permute-start(bf16[1152,128]{1,0:T(8,128)(2,1)S(1)} %collective-permute-done.18.refs_5_), channel_id=1, source_target_pairs={{0,1},{1,2},{2,3},{3,4},{4,5},{5,6},{6,7},{7,0},{8,9},{9,10},{10,1... | collective-permute-start | bytes 884744 | tf_op jit(solution)/shard_map/ppermute | solution.py:183
  191.6 4.4 %collective-permute-start.21 = (bf16[32,16,256]{2,1,0:T(8,128)(2,1)S(1)}, bf16[32,16,256]{2,1,0:T(8,128)(2,1)S(1)}, u32[]{:S(2)}, u32[]{:S(2)}) collective-permute-start(bf16[32,16,256]{2,1,0:T(8,128)(2,1)S(1)} %slice.37.refs_8_), channel_id=1, source_target_pairs={{0,256},{256,0},{1,257},{257,1},{2,258},{258,2},{3,259},{259,3},{4... | collective-permute-start | bytes 786440 | tf_op jit(solution)/shard_map/ppermute | solution.py:228
  196.0 3.7 %collective-permute-done.21.refs_9_ = bf16[32,16,256]{2,1,0:T(8,128)(2,1)S(1)} collective-permute-done((bf16[32,16,256]{2,1,0:T(8,128)(2,1)S(1)}, bf16[32,16,256]{2,1,0:T(8,128)(2,1)S(1)}, u32[]{:S(2)}, u32[]{:S(2)}) %collective-permute-start.21) | collective-permute-done | bytes 262176 | tf_op jit(solution)/shard_map/ppermute | solution.py:228
  199.8 2.8 %down.1 = (bf16[32,72,128]{2,1,0:T(8,128)(2,1)}, bf16[32,32,256]{2,1,0:T(8,128)(2,1)}) custom-call(s32[2]{0:T(128)S(1)} %pad_add_fusion.me, bf16[1152,128]{1,0:T(8,128)(2,1)S(1)} %ffn.1.refs_0_, bf16[1152,128]{1,0:T(8,128)(2,1)S(1)} %collective-permute-done.14.refs_1_, bf16[1152,128]{1,0:T(8,128)(2,1)S(1)} %collective-permute-done.15.refs_2_, ...), custom_call_target="tpu_custom_call" | custom-call | tf_op jit(solution)/shard_map/down/pallas_call | solution.py:251
  202.6 11.5 %all-to-all-start.2 = ((bf16[32,72,128]{2,1,0:T(8,128)(2,1)}), bf16[32,72,128]{2,1,0:T(8,128)(2,1)S(1)}, u32[]{:S(2)}, u32[]{:S(2)}) async-start(bf16[32,72,128]{2,1,0:T(8,128)(2,1)} %get-tuple-element.11), calls=%async_computation.2 | async-start | bytes 1179648 | tf_op jit(solution)/shard_map/all_to_all | solution.py:178
  214.1 0.1 slice.32
  214.3 1.0 fusion
  215.3 34.9 %all-to-all-done.2 = bf16[32,72,128]{2,1,0:T(8,128)(2,1)S(1)} async-done(((bf16[32,72,128]{2,1,0:T(8,128)(2,1)}), bf16[32,72,128]{2,1,0:T(8,128)(2,1)S(1)}, u32[]{:S(2)}, u32[]{:S(2)}) %all-to-all-start.2) | async-done | bytes 589856 | tf_op jit(solution)/shard_map/all_to_all | solution.py:178
  250.2 1.9 combine.1
  (32 shorter events, 0.2 us)
Async XLA Ops:
  0.6 46.8 %copy-start = (f32[32,32,256]{2,1,0:T(8,128)S(1)}, f32[32,32,256]{2,1,0:T(8,128)}, u32[]{:S(2)}) copy-start(f32[32,32,256]{2,1,0:T(8,128)} %param.11) | copy-start | bytes 3145732
  0.6 46.9 %copy-start.8 = (f32[64]{0:T(128)S(1)}, f32[64]{0:T(128)}, u32[]{:S(2)}) copy-start(f32[64]{0:T(128)} %param.8) | copy-start | bytes 772
  3.1 80.5 %all-to-all-start.1 = ((bf16[32,72,128]{2,1,0:T(8,128)(2,1)}), bf16[32,72,128]{2,1,0:T(8,128)(2,1)S(1)}, u32[]{:S(2)}, u32[]{:S(2)}) async-start(bf16[32,72,128]{2,1,0:T(8,128)(2,1)} %get-tuple-element.8), calls=%async_computation.1 | async-start | bytes 1179648 | tf_op jit(solution)/shard_map/all_to_all | solution.py:178
  83.5 71.1 %all-to-all-start = ((bf16[32,80,256]{2,1,0:T(8,128)(2,1)}), bf16[32,80,256]{2,1,0:T(8,128)(2,1)S(1)}, u32[]{:S(2)}, u32[]{:S(2)}) async-start(bf16[32,80,256]{2,1,0:T(8,128)(2,1)} %pad_maximum_fusion), calls=%async_computation | async-start | bytes 2621440 | tf_op jit(solution)/shard_map/all_to_all | solution.py:178
  87.9 40.2 %copy-start.2 = (bf16[16,72,128]{2,1,0:T(8,128)(2,1)}, bf16[16,72,128]{2,1,0:T(8,128)(2,1)S(1)}, u32[]{:S(2)}) copy-start(bf16[16,72,128]{2,1,0:T(8,128)(2,1)S(1)} %get-tuple-element.14) | copy-start | bytes 884740
  87.9 40.2 %copy-start.3 = (bf16[16,72,128]{2,1,0:T(8,128)(2,1)}, bf16[16,72,128]{2,1,0:T(8,128)(2,1)S(1)}, u32[]{:S(2)}) copy-start(bf16[16,72,128]{2,1,0:T(8,128)(2,1)S(1)} %get-tuple-element.15) | copy-start | bytes 884740
  88.0 11.9 %collective-permute-start.8 = (bf16[1152,128]{1,0:T(8,128)(2,1)S(1)}, bf16[1152,128]{1,0:T(8,128)(2,1)S(1)}, u32[]{:S(2)}, u32[]{:S(2)}) collective-permute-start(bf16[1152,128]{1,0:T(8,128)(2,1)S(1)} %bitcast.12), channel_id=1, source_target_pairs={{0,7},{1,0},{2,1},{3,2},{4,3},{5,4},{6,5},{7,6},{8,15},{9,8},{10,9... | collective-permute-start | bytes 884744 | tf_op jit(solution)/shard_map/ppermute | solution.py:183
  90.0 11.8 %collective-permute-start = (bf16[1152,128]{1,0:T(8,128)(2,1)S(1)}, bf16[1152,128]{1,0:T(8,128)(2,1)S(1)}, u32[]{:S(2)}, u32[]{:S(2)}) collective-permute-start(bf16[1152,128]{1,0:T(8,128)(2,1)S(1)} %bitcast.15), channel_id=1, source_target_pairs={{0,1},{1,2},{2,3},{3,4},{4,5},{5,6},{6,7},{7,0},{8,9},{9,10},{10,1... | collective-permute-start | bytes 884744 | tf_op jit(solution)/shard_map/ppermute | solution.py:183
  94.5 12.0 %collective-permute-start.7 = (bf16[1152,128]{1,0:T(8,128)(2,1)S(1)}, bf16[1152,128]{1,0:T(8,128)(2,1)S(1)}, u32[]{:S(2)}, u32[]{:S(2)}) collective-permute-start(bf16[1152,128]{1,0:T(8,128)(2,1)S(1)} %bitcast.13), channel_id=1, source_target_pairs={{0,1},{1,2},{2,3},{3,4},{4,5},{5,6},{6,7},{7,0},{8,9},{9,10},{10,1... | collective-permute-start | bytes 884744 | tf_op jit(solution)/shard_map/ppermute | solution.py:183
  97.8 13.4 %collective-permute-start.1 = (bf16[1152,128]{1,0:T(8,128)(2,1)S(1)}, bf16[1152,128]{1,0:T(8,128)(2,1)S(1)}, u32[]{:S(2)}, u32[]{:S(2)}) collective-permute-start(bf16[1152,128]{1,0:T(8,128)(2,1)S(1)} %bitcast.16), channel_id=1, source_target_pairs={{0,7},{1,0},{2,1},{3,2},{4,3},{5,4},{6,5},{7,6},{8,15},{9,8},{10,9... | collective-permute-start | bytes 884744 | tf_op jit(solution)/shard_map/ppermute | solution.py:183
  99.9 28.3 %copy-start.4 = (bf16[1152,128]{1,0:T(8,128)(2,1)}, bf16[1152,128]{1,0:T(8,128)(2,1)S(1)}, u32[]{:S(2)}) copy-start(bf16[1152,128]{1,0:T(8,128)(2,1)S(1)} %collective-permute-done.8.refs_10_) | copy-start | bytes 884740
  99.9 14.1 %collective-permute-start.10 = (bf16[1152,128]{1,0:T(8,128)(2,1)S(1)}, bf16[1152,128]{1,0:T(8,128)(2,1)S(1)}, u32[]{:S(2)}, u32[]{:S(2)}) collective-permute-start(bf16[1152,128]{1,0:T(8,128)(2,1)S(1)} %collective-permute-done.8.refs_10_), channel_id=1, source_target_pairs={{0,7},{1,0},{2,1},{3,2},{4,3},{5,4},{6,5},{7,6},{8,15},{9,8},{10,9... | collective-permute-start | bytes 884744 | tf_op jit(solution)/shard_map/ppermute | solution.py:183
  101.9 26.3 %copy-start.5 = (bf16[1152,128]{1,0:T(8,128)(2,1)}, bf16[1152,128]{1,0:T(8,128)(2,1)S(1)}, u32[]{:S(2)}) copy-start(bf16[1152,128]{1,0:T(8,128)(2,1)S(1)} %collective-permute-done.refs_1_) | copy-start | bytes 884740
  101.9 14.0 %collective-permute-start.2 = (bf16[1152,128]{1,0:T(8,128)(2,1)S(1)}, bf16[1152,128]{1,0:T(8,128)(2,1)S(1)}, u32[]{:S(2)}, u32[]{:S(2)}) collective-permute-start(bf16[1152,128]{1,0:T(8,128)(2,1)S(1)} %collective-permute-done.refs_1_), channel_id=1, source_target_pairs={{0,1},{1,2},{2,3},{3,4},{4,5},{5,6},{6,7},{7,0},{8,9},{9,10},{10,1... | collective-permute-start | bytes 884744 | tf_op jit(solution)/shard_map/ppermute | solution.py:183
  106.5 21.7 %copy-start.6 = (bf16[1152,128]{1,0:T(8,128)(2,1)}, bf16[1152,128]{1,0:T(8,128)(2,1)S(1)}, u32[]{:S(2)}) copy-start(bf16[1152,128]{1,0:T(8,128)(2,1)S(1)} %collective-permute-done.7.refs_9_) | copy-start | bytes 884740
  106.5 14.0 %collective-permute-start.9 = (bf16[1152,128]{1,0:T(8,128)(2,1)S(1)}, bf16[1152,128]{1,0:T(8,128)(2,1)S(1)}, u32[]{:S(2)}, u32[]{:S(2)}) collective-permute-start(bf16[1152,128]{1,0:T(8,128)(2,1)S(1)} %collective-permute-done.7.refs_9_), channel_id=1, source_target_pairs={{0,1},{1,2},{2,3},{3,4},{4,5},{5,6},{6,7},{7,0},{8,9},{9,10},{10,1... | collective-permute-start | bytes 884744 | tf_op jit(solution)/shard_map/ppermute | solution.py:183
  111.2 16.9 %copy-start.7 = (bf16[1152,128]{1,0:T(8,128)(2,1)}, bf16[1152,128]{1,0:T(8,128)(2,1)S(1)}, u32[]{:S(2)}) copy-start(bf16[1152,128]{1,0:T(8,128)(2,1)S(1)} %collective-permute-done.1.refs_2_) | copy-start | bytes 884740
  111.3 12.2 %collective-permute-start.3 = (bf16[1152,128]{1,0:T(8,128)(2,1)S(1)}, bf16[1152,128]{1,0:T(8,128)(2,1)S(1)}, u32[]{:S(2)}, u32[]{:S(2)}) collective-permute-start(bf16[1152,128]{1,0:T(8,128)(2,1)S(1)} %collective-permute-done.1.refs_2_), channel_id=1, source_target_pairs={{0,7},{1,0},{2,1},{3,2},{4,3},{5,4},{6,5},{7,6},{8,15},{9,8},{10,9... | collective-permute-start | bytes 884744 | tf_op jit(solution)/shard_map/ppermute | solution.py:183
  114.0 12.2 %collective-permute-start.12 = (bf16[1152,128]{1,0:T(8,128)(2,1)S(1)}, bf16[1152,128]{1,0:T(8,128)(2,1)}, u32[]{:S(2)}, u32[]{:S(2)}) collective-permute-start(bf16[1152,128]{1,0:T(8,128)(2,1)S(1)} %collective-permute-done.10.refs_12_), channel_id=1, source_target_pairs={{0,7},{1,0},{2,1},{3,2},{4,3},{5,4},{6,5},{7,6},{8,15},{9,8},{10,9... | collective-permute-start | bytes 884744 | tf_op jit(solution)/shard_map/ppermute | solution.py:183
  115.9 12.2 %collective-permute-start.4 = (bf16[1152,128]{1,0:T(8,128)(2,1)S(1)}, bf16[1152,128]{1,0:T(8,128)(2,1)}, u32[]{:S(2)}, u32[]{:S(2)}) collective-permute-start(bf16[1152,128]{1,0:T(8,128)(2,1)S(1)} %collective-permute-done.2.refs_3_), channel_id=1, source_target_pairs={{0,1},{1,2},{2,3},{3,4},{4,5},{5,6},{6,7},{7,0},{8,9},{9,10},{10,1... | collective-permute-start | bytes 884744 | tf_op jit(solution)/shard_map/ppermute | solution.py:183
  120.6 12.3 %collective-permute-start.11 = (bf16[1152,128]{1,0:T(8,128)(2,1)S(1)}, bf16[1152,128]{1,0:T(8,128)(2,1)}, u32[]{:S(2)}, u32[]{:S(2)}) collective-permute-start(bf16[1152,128]{1,0:T(8,128)(2,1)S(1)} %collective-permute-done.9.refs_11_), channel_id=1, source_target_pairs={{0,1},{1,2},{2,3},{3,4},{4,5},{5,6},{6,7},{7,0},{8,9},{9,10},{10,1... | collective-permute-start | bytes 884744 | tf_op jit(solution)/shard_map/ppermute | solution.py:183
  123.4 9.5 %collective-permute-start.5 = (bf16[1152,128]{1,0:T(8,128)(2,1)S(1)}, bf16[1152,128]{1,0:T(8,128)(2,1)}, u32[]{:S(2)}, u32[]{:S(2)}) collective-permute-start(bf16[1152,128]{1,0:T(8,128)(2,1)S(1)} %collective-permute-done.3.refs_4_), channel_id=1, source_target_pairs={{0,7},{1,0},{2,1},{3,2},{4,3},{5,4},{6,5},{7,6},{8,15},{9,8},{10,9... | collective-permute-start | bytes 884744 | tf_op jit(solution)/shard_map/ppermute | solution.py:183
  126.2 12.3 %collective-permute-start.13 = (bf16[1152,128]{1,0:T(8,128)(2,1)}, bf16[1152,128]{1,0:T(8,128)(2,1)}, u32[]{:S(2)}, u32[]{:S(2)}) collective-permute-start(bf16[1152,128]{1,0:T(8,128)(2,1)} %collective-permute-done.12.refs_14_), channel_id=1, source_target_pairs={{0,7},{1,0},{2,1},{3,2},{4,3},{5,4},{6,5},{7,6},{8,15},{9,8},{10,9... | collective-permute-start | bytes 884744 | tf_op jit(solution)/shard_map/ppermute | solution.py:183
  128.2 10.3 %collective-permute-start.6 = (bf16[1152,128]{1,0:T(8,128)(2,1)}, bf16[1152,128]{1,0:T(8,128)(2,1)}, u32[]{:S(2)}, u32[]{:S(2)}) collective-permute-start(bf16[1152,128]{1,0:T(8,128)(2,1)} %collective-permute-done.4.refs_5_), channel_id=1, source_target_pairs={{0,1},{1,2},{2,3},{3,4},{4,5},{5,6},{6,7},{7,0},{8,9},{9,10},{10,1... | collective-permute-start | bytes 884744 | tf_op jit(solution)/shard_map/ppermute | solution.py:183
  158.3 9.7 %collective-permute-start.14 = (bf16[1152,128]{1,0:T(8,128)(2,1)S(1)}, bf16[1152,128]{1,0:T(8,128)(2,1)S(1)}, u32[]{:S(2)}, u32[]{:S(2)}) collective-permute-start(bf16[1152,128]{1,0:T(8,128)(2,1)S(1)} %ffn.1.refs_0_), channel_id=1, source_target_pairs={{0,1},{1,2},{2,3},{3,4},{4,5},{5,6},{6,7},{7,0},{8,9},{9,10},{10,1... | collective-permute-start | bytes 884744 | tf_op jit(solution)/shard_map/ppermute | solution.py:183
  162.8 10.5 %collective-permute-start.15 = (bf16[1152,128]{1,0:T(8,128)(2,1)S(1)}, bf16[1152,128]{1,0:T(8,128)(2,1)S(1)}, u32[]{:S(2)}, u32[]{:S(2)}) collective-permute-start(bf16[1152,128]{1,0:T(8,128)(2,1)S(1)} %ffn.1.refs_0_), channel_id=1, source_target_pairs={{0,7},{1,0},{2,1},{3,2},{4,3},{5,4},{6,5},{7,6},{8,15},{9,8},{10,9... | collective-permute-start | bytes 884744 | tf_op jit(solution)/shard_map/ppermute | solution.py:183
  167.9 9.6 %collective-permute-start.16 = (bf16[1152,128]{1,0:T(8,128)(2,1)S(1)}, bf16[1152,128]{1,0:T(8,128)(2,1)S(1)}, u32[]{:S(2)}, u32[]{:S(2)}) collective-permute-start(bf16[1152,128]{1,0:T(8,128)(2,1)S(1)} %collective-permute-done.14.refs_1_), channel_id=1, source_target_pairs={{0,1},{1,2},{2,3},{3,4},{4,5},{5,6},{6,7},{7,0},{8,9},{9,10},{10,1... | collective-permute-start | bytes 884744 | tf_op jit(solution)/shard_map/ppermute | solution.py:183
  173.3 9.6 %collective-permute-start.17 = (bf16[1152,128]{1,0:T(8,128)(2,1)S(1)}, bf16[1152,128]{1,0:T(8,128)(2,1)S(1)}, u32[]{:S(2)}, u32[]{:S(2)}) collective-permute-start(bf16[1152,128]{1,0:T(8,128)(2,1)S(1)} %collective-permute-done.15.refs_2_), channel_id=1, source_target_pairs={{0,7},{1,0},{2,1},{3,2},{4,3},{5,4},{6,5},{7,6},{8,15},{9,8},{10,9... | collective-permute-start | bytes 884744 | tf_op jit(solution)/shard_map/ppermute | solution.py:183
  177.6 9.0 %collective-permute-start.18 = (bf16[1152,128]{1,0:T(8,128)(2,1)S(1)}, bf16[1152,128]{1,0:T(8,128)(2,1)S(1)}, u32[]{:S(2)}, u32[]{:S(2)}) collective-permute-start(bf16[1152,128]{1,0:T(8,128)(2,1)S(1)} %collective-permute-done.16.refs_3_), channel_id=1, source_target_pairs={{0,1},{1,2},{2,3},{3,4},{4,5},{5,6},{6,7},{7,0},{8,9},{9,10},{10,1... | collective-permute-start | bytes 884744 | tf_op jit(solution)/shard_map/ppermute | solution.py:183
  182.9 16.9 %collective-permute-start.19 = (bf16[1152,128]{1,0:T(8,128)(2,1)S(1)}, bf16[1152,128]{1,0:T(8,128)(2,1)S(1)}, u32[]{:S(2)}, u32[]{:S(2)}) collective-permute-start(bf16[1152,128]{1,0:T(8,128)(2,1)S(1)} %collective-permute-done.17.refs_4_), channel_id=1, source_target_pairs={{0,7},{1,0},{2,1},{3,2},{4,3},{5,4},{6,5},{7,6},{8,15},{9,8},{10,9... | collective-permute-start | bytes 884744 | tf_op jit(solution)/shard_map/ppermute | solution.py:183
  186.5 13.3 %collective-permute-start.20 = (bf16[1152,128]{1,0:T(8,128)(2,1)S(1)}, bf16[1152,128]{1,0:T(8,128)(2,1)S(1)}, u32[]{:S(2)}, u32[]{:S(2)}) collective-permute-start(bf16[1152,128]{1,0:T(8,128)(2,1)S(1)} %collective-permute-done.18.refs_5_), channel_id=1, source_target_pairs={{0,1},{1,2},{2,3},{3,4},{4,5},{5,6},{6,7},{7,0},{8,9},{9,10},{10,1... | collective-permute-start | bytes 884744 | tf_op jit(solution)/shard_map/ppermute | solution.py:183
  191.6 8.2 %collective-permute-start.21 = (bf16[32,16,256]{2,1,0:T(8,128)(2,1)S(1)}, bf16[32,16,256]{2,1,0:T(8,128)(2,1)S(1)}, u32[]{:S(2)}, u32[]{:S(2)}) collective-permute-start(bf16[32,16,256]{2,1,0:T(8,128)(2,1)S(1)} %slice.37.refs_8_), channel_id=1, source_target_pairs={{0,256},{256,0},{1,257},{257,1},{2,258},{258,2},{3,259},{259,3},{4... | collective-permute-start | bytes 786440 | tf_op jit(solution)/shard_map/ppermute | solution.py:228
  202.6 47.6 %all-to-all-start.2 = ((bf16[32,72,128]{2,1,0:T(8,128)(2,1)}), bf16[32,72,128]{2,1,0:T(8,128)(2,1)S(1)}, u32[]{:S(2)}, u32[]{:S(2)}) async-start(bf16[32,72,128]{2,1,0:T(8,128)(2,1)} %get-tuple-element.11), calls=%async_computation.2 | async-start | bytes 1179648 | tf_op jit(solution)/shard_map/all_to_all | solution.py:178
  214.3 36.0 %copy-start.1 = (f32[384,2]{0,1:T(2,128)S(1)}, f32[384,2]{0,1:T(2,128)}, u32[]{:S(2)}) copy-start(f32[384,2]{0,1:T(2,128)} %param.13) | copy-start | bytes 9220
